TPU v7x, 256 devices: a whole 4x4x8 slice. The times are simulated.
256 devices in a mesh: sp: 64 (over z, x, core), tp: 4 (over y).
Axes of the slice: x: 4, y: 4, z: 8, core: 2. Of those that a mesh axis runs over, the one named last changes fastest.
Arguments:
- residual: bfloat16 [32768, 2048], P(('sp', 'tp')), may hold values from -6 to 6
- conv_value: bfloat16 [32768, 1024], P('sp', 'tp'), may hold values from -6 to 6
- conv_gate: bfloat16 [32768, 1024], P('sp', 'tp'), may hold values from -9 to 9
- segments: int32 [32768], P('sp'), may hold values from 0 to 31, never falling along the last dimension, each value on 1 to 2048 neighbouring positions
- conv_weight: float32 [31, 1024], P(None, 'tp'), may hold values from -1 to 1
- norm_gain: float32 [1024], P('tp'), may hold values from 0.1 to 1.9
- norm_shift: float32 [1024], P('tp'), may hold values from -3 to 3
- out_weight: bfloat16 [1024, 2048], replicated, may hold values from -0.1875 to 0.1875
- ffn_gain: float32 [2048], replicated, may hold values from 0.1 to 1.9
- routes: int32 [32768, 2], P('sp'), may hold values from 0 to 63, all different within a row; in each aligned block of 128 rows (0 to 127, 128 to 255, ...) at most 8 rows name the same one
- route_weights: float32 [32768, 2], P('sp'), may hold values from 0.2 to 1
- w_gate: bfloat16 [64, 2048, 1024], P('sp', None, 'tp'), may hold values from -0.125 to 0.125
- w_up: bfloat16 [64, 2048, 1024], P('sp', None, 'tp'), may hold values from -0.125 to 0.125
- w_down: bfloat16 [64, 1024, 2048], P('sp', 'tp'), may hold values from -0.1875 to 0.1875
Outputs:
- layer_out: bfloat16 [32768, 2048], P(('sp', 'tp'))
Inputs may be any that keep to these rules, and one draw needn't show every extreme that they name: `routes`: within the rows of one device (aligned blocks of 512 / 4 rows), no expert is named more than 8 times; the two experts of a row differ. `segments`: document numbers never fall along the sequence.
All inputs are finite; a program needn't handle non-finite values.
Results may differ from a plain program's by a relative error of at most 0.007.
Values may be sent and summed in bfloat16 or wider, within the bound.
No kernel may reach another device: no remote copies, remote signals or barrier semaphores. Data moves between devices by JAX's collectives and lax.ppermute only.
A program may use at most 128 MiB of HBM per device.

v0:
```python
import jax
import jax.numpy as jnp
from jax import lax
from jax.sharding import PartitionSpec as P

DC = 1024
CONV_GROUPS = 8


def side_by_side(arrays, axis, dim, along):
    ends, at = ([], 0)
    for a in arrays[:-1]:
        at += a.shape[along]
        ends.append(at)
    both = jnp.concatenate(arrays, axis=along)
    return tuple(jnp.split(lax.all_gather(both, axis, axis=dim, tiled=True), ends, axis=along))


def passed_along(value, axis, steps):
    count = lax.axis_size(axis)
    initial, last = (max(0, -steps), min(count, count - steps))
    return lax.ppermute(value, axis, [(source, source + steps) for source in range(initial, last)])


def slot_numbers(block_routes, capacity, experts_n):
    route_pairs = block_routes.reshape(block_routes.shape[:-2] + (-1,))
    onehot = (route_pairs[..., None] == jnp.arange(experts_n, dtype=jnp.int32)).astype(jnp.int32)
    slot_rank = jnp.sum((jnp.cumsum(onehot, axis=-2) - onehot) * onehot, axis=-1)
    return (route_pairs * capacity + slot_rank).reshape(block_routes.shape)


def dispatch_matrix(slot_ids, slot_total):
    numbers = jnp.arange(slot_total, dtype=jnp.int32)[:, None, None]
    matches = jnp.any(numbers == slot_ids[..., None, :, :], axis=-1)
    return matches.astype(jnp.bfloat16)


def shards(
    residual,
    conv_value,
    conv_gate,
    segments,
    conv_weight,
    norm_gain,
    norm_shift,
    out_weight,
    ffn_gain,
    routes,
    route_weights,
    w_gate,
    w_up,
    w_down,
):
    tok_dev, local_channels = conv_value.shape
    reach = conv_weight.shape[0] - 1
    whole_gate, whole_up = side_by_side((w_gate[0], w_up[0]), "tp", 1, 0)
    whole_down = lax.all_gather(w_down[0], "tp", axis=0, tiled=True)
    gated = (conv_value.astype(jnp.float32) * jax.nn.sigmoid(conv_gate.astype(jnp.float32))).astype(
        jnp.bfloat16
    )
    rim_prev, seg_prev = passed_along(
        (gated[tok_dev - reach :], segments[tok_dev - reach :]), "sp", 1
    )
    extended = jnp.concatenate([rim_prev, gated], 0).astype(jnp.float32)
    seg_ext = jnp.concatenate([seg_prev, segments], 0)
    convolved = jnp.zeros((tok_dev, local_channels), jnp.float32)
    for offset in range(reach + 1):
        same_doc = (seg_ext[offset : offset + tok_dev] == segments)[:, None]
        convolved = convolved + jnp.where(
            same_doc, extended[offset : offset + tok_dev] * conv_weight[offset], 0.0
        )
    group_size = DC // CONV_GROUPS
    grouped = convolved.reshape(tok_dev, local_channels // group_size, group_size)
    group_mean = jnp.mean(grouped, axis=-1, keepdims=True)
    group_var = jnp.mean(jnp.square(grouped - group_mean), axis=-1, keepdims=True)
    scaled = ((grouped - group_mean) * lax.rsqrt(group_var + 1e-05)).reshape(
        tok_dev, local_channels
    ) * norm_gain + norm_shift
    conv_out = jax.nn.silu(scaled).astype(jnp.bfloat16)
    columns = lax.axis_size("tp")
    column = lax.axis_index("tp")
    rows_own = tok_dev // columns
    regrouped = lax.all_to_all(conv_out, "tp", split_axis=0, concat_axis=1, tiled=True)
    mixed = jnp.dot(regrouped, out_weight, preferred_element_type=jnp.float32)
    stream = residual.astype(jnp.float32) + lax.optimization_barrier(
        mixed.astype(jnp.bfloat16)
    ).astype(jnp.float32)
    normed = (
        stream * lax.rsqrt(jnp.mean(stream * stream, axis=-1, keepdims=True) + 1e-06) * ffn_gain
    ).astype(jnp.bfloat16)
    experts_n = lax.axis_size("sp")
    top_count = routes.shape[1]
    model_width = normed.shape[1]
    capacity = max(2, 2 * tok_dev * top_count // (columns * experts_n))
    slot_total = experts_n * capacity
    own_routes = lax.dynamic_slice_in_dim(routes, column * rows_own, rows_own, 0)
    own_weights = lax.dynamic_slice_in_dim(route_weights, column * rows_own, rows_own, 0)
    own_slots = slot_numbers(own_routes, capacity, experts_n)
    routing_table = dispatch_matrix(own_slots, slot_total)
    outgoing = jnp.dot(routing_table, normed, preferred_element_type=jnp.float32).astype(
        jnp.bfloat16
    )
    outgoing = outgoing.reshape(experts_n, capacity, model_width)
    arrived = lax.all_to_all(outgoing, "sp", split_axis=0, concat_axis=1, tiled=True).reshape(
        slot_total, model_width
    )
    gate_act = jnp.dot(arrived, whole_gate, preferred_element_type=jnp.float32)
    up_act = jnp.dot(arrived, whole_up, preferred_element_type=jnp.float32)
    hidden = (jax.nn.silu(gate_act) * up_act).astype(jnp.bfloat16)
    summed = jnp.dot(hidden, whole_down, preferred_element_type=jnp.float32)
    expert_out = summed.astype(jnp.bfloat16).reshape(experts_n, capacity, model_width)
    returned = lax.all_to_all(expert_out, "sp", split_axis=0, concat_axis=0, tiled=True).reshape(
        slot_total, model_width
    )
    combined = stream
    for member in range(top_count):
        chosen = jnp.take(returned, own_slots[:, member], axis=0).astype(jnp.float32)
        combined = combined + own_weights[:, member : member + 1] * chosen
    return combined.astype(jnp.bfloat16)


def solution(mesh):
    return jax.shard_map(
        shards,
        mesh=mesh,
        in_specs=(
            P(("sp", "tp"), None),
            P("sp", "tp"),
            P("sp", "tp"),
            P("sp"),
            P(None, "tp"),
            P("tp"),
            P("tp"),
            P(),
            P(),
            P("sp", None),
            P("sp", None),
            P("sp", None, "tp"),
            P("sp", None, "tp"),
            P("sp", "tp", None),
        ),
        out_specs=P(("sp", "tp"), None),
        check_vma=False,
    )
```

profile of v0, /device:TPU:2, one launch (start us, length us, event | category | flops | bytes accessed | tf_op | source)
XLA Modules:
  0.0 242.5 jit_solution(8489655379821655562)
XLA Ops:
  6.5 3.0 %pad_maximum_fusion = bf16[4096,256]{1,0:T(8,128)(2,1)} fusion(bf16[2048,256]{1,0:T(8,128)(2,1)} %bitcast.105, bf16[2048,256]{1,0:T(8,128)(2,1)} %bitcast.106), kind=kLoop, calls=%fused_computation.13 | loop fusion | flops 4194304 | bytes 4194304 | tf_op jit(solution)/shard_map/concatenate | solution.py:15
  9.7 0.6 copy-done.5
  10.3 1.9 collective-permute-start
  12.3 0.2 multiply_convert_fusion.4
  12.5 3.5 %collective-permute-start.1 = (bf16[30,256]{1,0:T(8,128)(2,1)S(1)}, bf16[30,256]{1,0:T(8,128)(2,1)S(1)}, u32[]{:S(2)}, u32[]{:S(2)}) collective-permute-start(bf16[30,256]{1,0:T(8,128)(2,1)S(1)} %slice.404), channel_id=1, source_target_pairs={{0,4},{4,8},{8,12},{12,16},{16,20},{20,24},{24,28},{28,32},{32,36}... | collective-permute-start | bytes 46088 | tf_op jit(solution)/shard_map/ppermute | solution.py:22
  16.5 0.6 reduce-window.6
  17.1 0.2 slice_reduce_fusion.2
  17.4 0.1 reduce_sum.41
  17.9 4.0 %fusion.26 = f32[512,256]{1,0:T(8,128)S(1)} fusion(f32[542,256]{1,0:T(8,128)S(1)} %maximum_convert_fusion, f32[256]{0:T(256)S(1)} %bitcast.127, f32[256]{0:T(256)S(1)} %bitcast.129, f32[256]{0:T(256)S(1)} %bitcast.133, f32[256]{0:T(256)S(1)} %bitcast.135, f32[256]{0:T(256)S(1)} %bitcast.137, f32[256]{0:T(256)S(1)} %bitcast.139, f32[256]{0:T(256)S(1)} %bitcast.141, ...), kind=kLoop, calls=%fused_computation.27 | loop fusion | flops 11927552 | bytes 16824320 | tf_op jit(solution)/shard_map/add | solution.py:69
  22.0 0.3 reshape.109
  22.3 0.6 reduce_sum.38
  22.9 1.6 multiply_reduce_fusion.1
  24.6 0.6 mul.492
  25.2 0.6 sub.20
  25.8 5.0 %multiply_convert_fusion.3 = bf16[512,256]{1,0:T(8,128)(2,1)} fusion(f32[64,8,2,128]{3,2,1,0:T(2,128)S(1)} %bitcast.101, f32[64,8,2,128]{3,2,1,0:T(2,128)S(1)} %bitcast.102, f32[256]{0:T(256)S(1)} %copy-done.7, f32[256]{0:T(256)S(1)} %copy-done.8, f32[256]{0:T(256)S(1)} %bitcast.128, f32[542,256]{1,0:T(8,128)S(1)} %maximum_convert_fusion, ...), kind=kLoop, calls=%fused_computation.120 | loop fusion | flops 13107200 | bytes 17612800 | tf_op jit(solution)/shard_map/convert_element_type | solution.py:79
  30.8 4.5 %all-to-all-start = ((bf16[4,128,256]{2,1,0:T(8,128)(2,1)}), bf16[4,128,256]{2,1,0:T(8,128)(2,1)S(1)}, u32[]{:S(2)}, u32[]{:S(2)}) async-start(bf16[4,128,256]{2,1,0:T(8,128)(2,1)} %bitcast.31), calls=%async_computation | async-start | bytes 524288 | tf_op jit(solution)/shard_map/all_to_all | solution.py:83
  35.4 10.4 %all-to-all-done = bf16[4,128,256]{2,1,0:T(8,128)(2,1)S(1)} async-done(((bf16[4,128,256]{2,1,0:T(8,128)(2,1)}), bf16[4,128,256]{2,1,0:T(8,128)(2,1)S(1)}, u32[]{:S(2)}, u32[]{:S(2)}) %all-to-all-start) | async-done | bytes 262176 | tf_op jit(solution)/shard_map/all_to_all | solution.py:83
  45.8 0.2 copy.21
  46.0 3.0 %convolution_convert_fusion.1 = bf16[128,2048]{1,0:T(8,128)(2,1)S(1)} fusion(bf16[128,1024]{0,1:T(8,128)(2,1)S(1)} %bitcast.103, bf16[1024,2048]{1,0:T(8,128)(2,1)} %param.23), kind=kOutput, calls=%fused_computation.12 | convolution fusion | flops 537133056 | bytes 4980736 | tf_op jit(solution)/shard_map/dot_general | solution.py:84
  49.0 0.3 multiply_reduce_fusion
  49.3 0.8 fusion.9
  50.0 62.8 %all_to_all.33 = bf16[64,8,2048]{2,1,0:T(8,128)(2,1)S(1)} all-to-all(bf16[64,8,2048]{2,1,0:T(8,128)(2,1)S(1)} %fusion.9), channel_id=1, replica_groups=mesh['sp'=64,'tp'=4] {'sp'}, dimensions={0} | all-to-all | bytes 4194304 | tf_op jit(solution)/shard_map/all_to_all | solution.py:104
  112.8 5.9 %fusion.2 = f32[512,1024]{1,0:T(8,128)} fusion(bf16[4096,1024]{1,0:T(8,128)(2,1)} %all-gather.4.cloned.1.call-done, bf16[64,8,2048]{2,1,0:T(8,128)(2,1)S(1)} %all_to_all.33), kind=kOutput, calls=%fused_computation.4 | convolution fusion | flops 2147483648 | bytes 8388608 | tf_op jit(solution)/shard_map/dot_general | solution.py:107
  118.7 39.2 %all-gather.6.cloned.1.call-done = bf16[1,1024,2048]{2,1,0:T(8,128)(2,1)} async-done(((bf16[1,256,2048]{2,1,0:T(8,128)(2,1)}), bf16[1,1024,2048]{2,1,0:T(8,128)(2,1)}) %all-gather.6.cloned.1.call-update) | async-done | bytes 4194320 | tf_op jit(solution)/shard_map/all_gather | solution.py:57
  157.9 10.0 %fusion.10 = bf16[64,8,2048]{2,1,0:T(8,128)(2,1)} fusion(bf16[1,1024,2048]{2,1,0:T(8,128)(2,1)} %all-gather.6.cloned.1.call-done, f32[512,1024]{1,0:T(8,128)} %fusion.2, bf16[4096,1024]{1,0:T(8,128)(2,1)} %all-gather.4.cloned.1.call-done, bf16[64,8,2048]{2,1,0:T(8,128)(2,1)S(1)} %all_to_all.33), kind=kOutput, calls=%fused_computation.11 | convolution fusion | flops 4299161600 | bytes 14680064 | tf_op jit(solution)/shard_map/dot_general | solution.py:110
  167.9 10.5 %all-to-all-start.2 = ((bf16[64,8,2048]{2,1,0:T(8,128)(2,1)}), bf16[64,8,2048]{2,1,0:T(8,128)(2,1)S(1)}, u32[]{:S(2)}, u32[]{:S(2)}) async-start(bf16[64,8,2048]{2,1,0:T(8,128)(2,1)} %fusion.10), calls=%async_computation.2 | async-start | bytes 4194304 | tf_op jit(solution)/shard_map/all_to_all | solution.py:112
  178.5 0.7 constant_dynamic-slice_fusion.1
  179.2 0.2 slice_reduce_fusion.1
  179.4 50.3 %all-to-all-done.2 = bf16[64,8,2048]{2,1,0:T(8,128)(2,1)S(1)} async-done(((bf16[64,8,2048]{2,1,0:T(8,128)(2,1)}), bf16[64,8,2048]{2,1,0:T(8,128)(2,1)S(1)}, u32[]{:S(2)}, u32[]{:S(2)}) %all-to-all-start.2) | async-done | bytes 2097184 | tf_op jit(solution)/shard_map/all_to_all | solution.py:112
  229.7 1.7 gather_fusion.1
  231.4 1.7 gather_fusion
  233.1 2.5 %add_convert_fusion = bf16[128,2048]{1,0:T(8,128)(2,1)} fusion(bf16[128,2048]{1,0:T(8,128)(2,1)S(1)} %convolution_convert_fusion.1, bf16[128,2048]{1,0:T(8,128)(2,1)S(1)} %copy-done.1, bf16[128,2048]{1,0:T(8,128)(2,1)} %gather_fusion.1, bf16[128,2048]{1,0:T(8,128)(2,1)} %gather_fusion, f32[128]{0:T(128)S(1)} %get-tuple-element.70, ...), kind=kLoop, calls=%fused_computation.17 | loop fusion | flops 3145728 | bytes 2622720 | tf_op jit(solution)/shard_map/convert_element_type | solution.py:119
  (51 shorter events, 1.4 us)
Async XLA Ops:
  6.5 9.5 %copy-start = (s32[512,2]{0,1:T(2,128)S(1)}, s32[512,2]{0,1:T(2,128)}, u32[]{:S(2)}) copy-start(s32[512,2]{0,1:T(2,128)} %param.25) | copy-start | bytes 12292
  6.5 106.3 %all-gather.4.cloned.1.call-start = ((), (), s32[]{:S(2)}) async-start(), calls=%async_computation.3 | async-start | bytes 10485760 | tf_op jit(solution)/shard_map/all_gather | solution.py:16
  9.6 0.7 copy-start.5
  9.6 2.7 %copy-start.2 = (bf16[512,256]{1,0:T(8,128)(2,1)S(1)}, bf16[512,256]{1,0:T(8,128)(2,1)}, u32[]{:S(2)}) copy-start(bf16[512,256]{1,0:T(8,128)(2,1)} %param.18) | copy-start | bytes 786436
  9.6 2.7 %copy-start.3 = (bf16[512,256]{1,0:T(8,128)(2,1)S(1)}, bf16[512,256]{1,0:T(8,128)(2,1)}, u32[]{:S(2)}) copy-start(bf16[512,256]{1,0:T(8,128)(2,1)} %param.17) | copy-start | bytes 786436
  9.6 6.4 %copy-start.4 = (f32[31,256]{1,0:T(8,128)S(1)}, f32[31,256]{1,0:T(8,128)}, u32[]{:S(2)}) copy-start(f32[31,256]{1,0:T(8,128)} %param.20) | copy-start | bytes 95236
  9.6 148.3 %all-gather.6.cloned.1.call-start = ((), (), s32[]{:S(2)}) async-start(), calls=%async_computation.4 | async-start | bytes 5242880 | tf_op jit(solution)/shard_map/all_gather | solution.py:57
  10.3 7.3 %collective-permute-start = (s32[30]{0:T(128)S(1)}, s32[30]{0:T(128)S(1)}, u32[]{:S(2)}, u32[]{:S(2)}) collective-permute-start(s32[30]{0:T(128)S(1)} %slice.300), channel_id=1, source_target_pairs={{0,4},{4,8},{8,12},{12,16},{16,20},{20,24},{24,28},{28,32},{32,36}... | collective-permute-start | bytes 368 | tf_op jit(solution)/shard_map/ppermute | solution.py:22
  12.5 5.4 %collective-permute-start.1 = (bf16[30,256]{1,0:T(8,128)(2,1)S(1)}, bf16[30,256]{1,0:T(8,128)(2,1)S(1)}, u32[]{:S(2)}, u32[]{:S(2)}) collective-permute-start(bf16[30,256]{1,0:T(8,128)(2,1)S(1)} %slice.404), channel_id=1, source_target_pairs={{0,4},{4,8},{8,12},{12,16},{16,20},{20,24},{24,28},{28,32},{32,36}... | collective-permute-start | bytes 46088 | tf_op jit(solution)/shard_map/ppermute | solution.py:22
  22.3 3.5 %copy-start.7 = (f32[256]{0:T(256)S(1)}, f32[256]{0:T(256)}, u32[]{:S(2)}) copy-start(f32[256]{0:T(256)} %param.22) | copy-start | bytes 3076
  22.3 3.5 %copy-start.8 = (f32[256]{0:T(256)S(1)}, f32[256]{0:T(256)}, u32[]{:S(2)}) copy-start(f32[256]{0:T(256)} %param.21) | copy-start | bytes 3076
  30.8 15.0 %all-to-all-start = ((bf16[4,128,256]{2,1,0:T(8,128)(2,1)}), bf16[4,128,256]{2,1,0:T(8,128)(2,1)S(1)}, u32[]{:S(2)}, u32[]{:S(2)}) async-start(bf16[4,128,256]{2,1,0:T(8,128)(2,1)} %bitcast.31), calls=%async_computation | async-start | bytes 524288 | tf_op jit(solution)/shard_map/all_to_all | solution.py:83
  46.0 3.0 %copy-start.1 = (bf16[128,2048]{1,0:T(8,128)(2,1)S(1)}, bf16[128,2048]{1,0:T(8,128)(2,1)}, u32[]{:S(2)}) copy-start(bf16[128,2048]{1,0:T(8,128)(2,1)} %param.16) | copy-start | bytes 1572868
  46.0 3.3 %copy-start.6 = (f32[2048]{0:T(1024)S(1)}, f32[2048]{0:T(1024)}, u32[]{:S(2)}) copy-start(f32[2048]{0:T(1024)} %param.24) | copy-start | bytes 24580
  167.9 61.8 %all-to-all-start.2 = ((bf16[64,8,2048]{2,1,0:T(8,128)(2,1)}), bf16[64,8,2048]{2,1,0:T(8,128)(2,1)S(1)}, u32[]{:S(2)}, u32[]{:S(2)}) async-start(bf16[64,8,2048]{2,1,0:T(8,128)(2,1)} %fusion.10), calls=%async_computation.2 | async-start | bytes 4194304 | tf_op jit(solution)/shard_map/all_to_all | solution.py:112
Sparse Core Ops, SparseCore 0:
  9.7 95.1 all-gather.3
  106.8 51.1 all-gather.5
where the time goes:
time: 243 us; the launch traced here: 242 us
  waiting for transfers between devices  99.9 us (41%)
  blocking collectives  62.8 us (26%)
  starting transfers between devices  20.5 us (8%)
  matrix products  19.7 us (8%)
  other arithmetic  18.4 us (8%)
  between operations  13.8 us (6%)
  local copies, waits for them, and re-layouts  7.49 us (3%)
    all_to_all x1, blocking collectives, shards(): lax.all_to_all(outgoing, 'sp', split_axis=0, concat_axis=1, tiled=True)  62.8 us
    all_to_all x1, waiting for transfers between devices, shards(): lax.all_to_all(expert_out, 'sp', split_axis=0, concat_axis=0, tiled=True)  50.3 us
    all_gather x1, waiting for transfers between devices, shards(): whole_down = lax.all_gather(w_down[0], 'tp', axis=0, tiled=True)  39.2 us
    all_to_all x1, starting transfers between devices, shards(): lax.all_to_all(expert_out, 'sp', split_axis=0, concat_axis=0, tiled=True)  10.5 us
    all_to_all x1, waiting for transfers between devices, shards(): lax.all_to_all(conv_out, 'tp', split_axis=0, concat_axis=1, tiled=True)  10.4 us
    dot_general x1, matrix products, shards(): summed = jnp.dot(hidden, whole_down, preferred_element_type=jnp.float32)  10 us
    dot_general x1, matrix products, shards(): gate_act = jnp.dot(arrived, whole_gate, preferred_element_type=jnp.float32)  5.92 us
    ppermute x2, starting transfers between devices, passed_along(): lax.ppermute(value, axis, [(source, source + steps) for source in range(i...  5.41 us
  transfers between devices with their start and end apart: 6, of which 3 were waited for; matrix products, arithmetic and copies ran while one was open for 11% of the time, Pallas kernels for 0%

commit v1 on v0

v1 whole, which is shorter than its diff:
```python
import jax
import jax.numpy as jnp
from jax import lax
from jax.experimental import pallas as pl
from jax.experimental.pallas import tpu as pltpu
from jax.sharding import PartitionSpec as P

TAPS = 31
RIM = 32
LANES = 128
BLOCK = 64


def passed_along(value, axis, steps):
    count = lax.axis_size(axis)
    initial, last = (max(0, -steps), min(count, count - steps))
    return lax.ppermute(value, axis, [(source, source + steps) for source in range(initial, last)])


def ring(value, axis, steps):
    count = lax.axis_size(axis)
    return lax.ppermute(value, axis, [(i, (i + steps) % count) for i in range(count)])


def slot_numbers(block_routes, capacity, experts_n):
    route_pairs = block_routes.reshape(block_routes.shape[:-2] + (-1,))
    onehot = (route_pairs[..., None] == jnp.arange(experts_n, dtype=jnp.int32)).astype(jnp.int32)
    slot_rank = jnp.sum((jnp.cumsum(onehot, axis=-2) - onehot) * onehot, axis=-1)
    return (route_pairs * capacity + slot_rank).reshape(block_routes.shape)


def dispatch_matrix(slot_ids, slot_total):
    numbers = jnp.arange(slot_total, dtype=jnp.int32)[:, None, None]
    matches = jnp.any(numbers == slot_ids[..., None, :, :], axis=-1)
    return matches.astype(jnp.bfloat16)


def conv_body(value_ref, gate_ref, rim_ref, seen_ref, taps_ref, gain_ref, shift_ref, out_ref, rows_ref):
    tok = value_ref.shape[0]
    gated = value_ref[...].astype(jnp.float32) * jax.nn.sigmoid(gate_ref[...].astype(jnp.float32))
    rows_ref[0, :RIM] = rim_ref[...].astype(jnp.float32)
    rows_ref[0, RIM:] = gated.astype(jnp.bfloat16).astype(jnp.float32)
    for r in range(1, 8):
        rows_ref[r, 8:] = rows_ref[0, 8 - r : RIM + tok - r]

    def block(i, carry):
        at = pl.multiple_of(i * BLOCK, BLOCK)
        seen = seen_ref[pl.ds(at, BLOCK), :]
        for lane in range(0, value_ref.shape[1], LANES):
            cols = slice(lane, lane + LANES)
            total = rows_ref[0, pl.ds(at + RIM, BLOCK), cols] * taps_ref[TAPS - 1 : TAPS, cols]
            for back in range(1, TAPS):
                tap = TAPS - 1 - back
                rows = rows_ref[back % 8, pl.ds(at + RIM - back // 8 * 8, BLOCK), cols]
                total = total + jnp.where(seen >= back, rows * taps_ref[tap : tap + 1, cols], 0.0)
            dev = total - jnp.mean(total, axis=1, keepdims=True)
            var = jnp.mean(dev * dev, axis=1, keepdims=True)
            v = dev * lax.rsqrt(var + 1e-05) * gain_ref[:, cols] + shift_ref[:, cols]
            out_ref[pl.ds(at, BLOCK), cols] = (v / (1.0 + jnp.exp(-v))).astype(jnp.bfloat16)
        return carry

    lax.fori_loop(0, tok // BLOCK, block, 0)


def conv_module(value, gate, rim, seen, taps, gain, shift):
    tok, width = value.shape
    return pl.pallas_call(
        conv_body,
        out_shape=jax.ShapeDtypeStruct((tok, width), jnp.bfloat16),
        scratch_shapes=[pltpu.VMEM((8, RIM + tok, width), jnp.float32)],
        name="conv_module",
    )(value, gate, rim, seen, taps, gain[None], shift[None])


def gathered(shard):
    half = shard.shape[0] // 2
    left, right, far = [], [], []
    for part in range(2):
        piece = shard[part * half : (part + 1) * half]
        left.append(ring(piece, "tp", 1))
        right.append(ring(piece, "tp", -1))
    far.append(ring(left[0], "tp", 1))
    far.append(ring(right[1], "tp", -1))
    return left, right, far


def dot(a, b):
    return jnp.dot(a, b, preferred_element_type=jnp.float32)


def shards(
    residual,
    conv_value,
    conv_gate,
    segments,
    conv_weight,
    norm_gain,
    norm_shift,
    out_weight,
    ffn_gain,
    routes,
    route_weights,
    w_gate,
    w_up,
    w_down,
):
    tok_dev, local_channels = conv_value.shape
    reach = conv_weight.shape[0] - 1
    gates = gathered(w_gate[0])
    ups = gathered(w_up[0])
    downs = gathered(w_down[0])
    tail = slice(tok_dev - reach, tok_dev)
    rim = (
        conv_value[tail].astype(jnp.float32) * jax.nn.sigmoid(conv_gate[tail].astype(jnp.float32))
    ).astype(jnp.bfloat16)
    named = jnp.pad(segments[tail].astype(jnp.bfloat16)[None], ((0, 1), (0, local_channels - reach)))
    rim = passed_along(jnp.concatenate([named, rim], 0), "sp", 1)
    seg_ext = jnp.concatenate([rim[0, :reach].astype(jnp.int32), segments], 0)
    seen = jnp.zeros((tok_dev,), jnp.int32)
    for offset in range(reach):
        seen = seen + (seg_ext[offset : offset + tok_dev] == segments).astype(jnp.int32)
    seen = jnp.broadcast_to(seen[:, None], (tok_dev, LANES))
    conv_out = conv_module(
        conv_value, conv_gate, rim, seen, conv_weight, norm_gain, norm_shift
    )
    columns = lax.axis_size("tp")
    column = lax.axis_index("tp")
    rows_own = tok_dev // columns
    regrouped = lax.all_to_all(conv_out, "tp", split_axis=0, concat_axis=1, tiled=True)
    mixed = dot(regrouped, out_weight)
    stream = residual.astype(jnp.float32) + lax.optimization_barrier(
        mixed.astype(jnp.bfloat16)
    ).astype(jnp.float32)
    normed = (
        stream * lax.rsqrt(jnp.mean(stream * stream, axis=-1, keepdims=True) + 1e-06) * ffn_gain
    ).astype(jnp.bfloat16)
    experts_n = lax.axis_size("sp")
    top_count = routes.shape[1]
    model_width = normed.shape[1]
    capacity = max(2, 2 * tok_dev * top_count // (columns * experts_n))
    slot_total = experts_n * capacity
    own_routes = lax.dynamic_slice_in_dim(routes, column * rows_own, rows_own, 0)
    own_weights = lax.dynamic_slice_in_dim(route_weights, column * rows_own, rows_own, 0)
    own_slots = slot_numbers(own_routes, capacity, experts_n)
    routing_table = dispatch_matrix(own_slots, slot_total)
    outgoing = dot(routing_table, normed).astype(jnp.bfloat16)
    outgoing = outgoing.reshape(experts_n, capacity, model_width)
    arrived = lax.all_to_all(outgoing, "sp", split_axis=0, concat_axis=1, tiled=True)
    arrived = arrived.reshape(slot_total, model_width)

    def quarter(gate, up, down):
        def rows(x, parts):
            half = x.shape[1] // 2
            return dot(x[:, :half], parts[0]) + dot(x[:, half:], parts[1])

        hidden = (jax.nn.silu(rows(arrived, gate)) * rows(arrived, up)).astype(jnp.bfloat16)
        return rows(hidden, down)

    hidden = (jax.nn.silu(dot(arrived, w_gate[0])) * dot(arrived, w_up[0])).astype(jnp.bfloat16)
    summed = dot(hidden, w_down[0])
    for side in range(3):
        summed = summed + quarter(gates[side], ups[side], downs[side])
    expert_out = summed.astype(jnp.bfloat16).reshape(experts_n, capacity, model_width)
    returned = lax.all_to_all(expert_out, "sp", split_axis=0, concat_axis=0, tiled=True)
    returned = returned.reshape(slot_total, model_width)
    combined = stream
    for member in range(top_count):
        chosen = jnp.take(returned, own_slots[:, member], axis=0).astype(jnp.float32)
        combined = combined + own_weights[:, member : member + 1] * chosen
    return combined.astype(jnp.bfloat16)


def solution(mesh):
    return jax.shard_map(
        shards,
        mesh=mesh,
        in_specs=(
            P(("sp", "tp"), None),
            P("sp", "tp"),
            P("sp", "tp"),
            P("sp"),
            P(None, "tp"),
            P("tp"),
            P("tp"),
            P(),
            P(),
            P("sp", None),
            P("sp", None),
            P("sp", None, "tp"),
            P("sp", None, "tp"),
            P("sp", "tp", None),
        ),
        out_specs=P(("sp", "tp"), None),
        check_vma=False,
    )
```

time: 243 us -> 280 us (1.15)
  blocking collectives: 62.8 us -> 0 us
  waiting for transfers between devices: 99.9 us -> 158 us
  matrix products: 19.7 us -> 49.8 us
  starting transfers between devices: 20.5 us -> 45.4 us
  between operations: 13.8 us -> 0.38 us
  other arithmetic: 18.4 us -> 6.64 us
  Pallas kernels: 0 us -> 6.12 us
  local copies, waits for them, and re-layouts: 7.49 us -> 13.2 us
    ppermute x0 -> x18, waiting for transfers between devices: none -> 78.9 us  [ring(): lax.ppermute(value, axis, [(i, (i + steps) % count) for i in range(count)])]
    all_to_all x1 -> x0, blocking collectives: 62.8 us -> none  [shards(): lax.all_to_all(outgoing, 'sp', split_axis=0, concat_axis=1, tiled=True)]
    all_gather x2 -> x0, waiting for transfers between devices: 39.2 us -> none  [the longest x1 39.2 us: shards(): whole_down = lax.all_gather(w_down[0], 'tp', axis=0, tiled=True)]
    dot_general x4 -> x22, matrix products: 19.7 us -> 49.8 us  [dot(): return jnp.dot(a, b, preferred_element_type=jnp.float32)]
    all_to_all x0 -> x1, waiting for transfers between devices: none -> 20.5 us  [shards(): lax.all_to_all(outgoing, 'sp', split_axis=0, concat_axis=1, tiled=True)]
    ppermute x0 -> x18, starting transfers between devices: none -> 17.6 us  [ring(): lax.ppermute(value, axis, [(i, (i + steps) % count) for i in range(count)])]
    all_to_all x0 -> x1, starting transfers between devices: none -> 12.7 us  [shards(): lax.all_to_all(outgoing, 'sp', split_axis=0, concat_axis=1, tiled=True)]
    pallas_call x0 -> x1, Pallas kernels: none -> 6.12 us  [conv_module(): pl.pallas_call(conv_body, out_shape=jax.ShapeDtypeStruct((tok, width), jn...]
  transfers between devices with their start and end apart: 6 -> 22, of which waited for: 3 -> 12; matrix products, arithmetic and copies ran while one was open for 11% -> 14% of each run, Pallas kernels for 0% -> 0%
where the time goes in v1:
time: 280 us; the launch traced here: 279 us
  waiting for transfers between devices  158 us (56%)
  matrix products  49.8 us (18%)
  starting transfers between devices  45.4 us (16%)
  local copies, waits for them, and re-layouts  13.2 us (5%)
  other arithmetic  6.64 us (2%)
  Pallas kernels  6.12 us (2%)
    ppermute x18, waiting for transfers between devices, ring(): lax.ppermute(value, axis, [(i, (i + steps) % count) for i in range(count)])  78.9 us
    all_to_all x1, waiting for transfers between devices, shards(): lax.all_to_all(expert_out, 'sp', split_axis=0, concat_axis=0, tiled=True)  50.3 us
    dot_general x22, matrix products, dot(): return jnp.dot(a, b, preferred_element_type=jnp.float32)  49.8 us
    all_to_all x1, waiting for transfers between devices, shards(): lax.all_to_all(outgoing, 'sp', split_axis=0, concat_axis=1, tiled=True)  20.5 us
    ppermute x18, starting transfers between devices, ring(): lax.ppermute(value, axis, [(i, (i + steps) % count) for i in range(count)])  17.6 us
    all_to_all x1, starting transfers between devices, shards(): lax.all_to_all(outgoing, 'sp', split_axis=0, concat_axis=1, tiled=True)  12.7 us
    all_to_all x1, starting transfers between devices, shards(): lax.all_to_all(expert_out, 'sp', split_axis=0, concat_axis=0, tiled=True)  8.63 us
    all_to_all x1, waiting for transfers between devices, shards(): lax.all_to_all(conv_out, 'tp', split_axis=0, concat_axis=1, tiled=True)  6.71 us
  transfers between devices with their start and end apart: 22, of which 12 were waited for; matrix products, arithmetic and copies ran while one was open for 14% of the time, Pallas kernels for 0%

profile of v1, /device:TPU:2, one launch (start us, length us, event | category | flops | bytes accessed | tf_op | source)
XLA Modules:
  0.0 279.4 jit_solution(3238281906677819888)
XLA Ops:
  1.6 1.9 collective-permute-start
  9.0 6.1 %conv_module.1 = bf16[512,256]{1,0:T(8,128)(2,1)} custom-call(bf16[512,256]{1,0:T(8,128)(2,1)} %value_ref.1, bf16[512,256]{1,0:T(8,128)(2,1)} %gate_ref.1, bf16[32,256]{1,0:T(8,128)(2,1)} %copy-done.7, s32[512,128]{1,0:T(8,128)} %broadcast_in_dim.29.seen_ref, f32[31,256]{1,0:T(8,128)} %taps_ref.1, f32[1,256]{1,0:T(1,128)} %bitcast.106, f32[1,256]{1,0:T(1,128)} %bitcast.107), custom_call_target="tpu_custom_call" | custom-call | tf_op jit(solution)/shard_map/conv_module/pallas_call | solution.py:67
  15.1 1.8 copy.22
  16.9 4.5 %all-to-all-start = ((bf16[4,128,256]{1,2,0:T(8,128)(2,1)}), bf16[4,128,256]{1,2,0:T(8,128)(2,1)S(1)}, u32[]{:S(2)}, u32[]{:S(2)}) async-start(bf16[4,128,256]{1,2,0:T(8,128)(2,1)} %copy.22), calls=%async_computation | async-start | bytes 524288 | tf_op jit(solution)/shard_map/all_to_all | solution.py:129
  21.5 6.7 %all-to-all-done = bf16[4,128,256]{1,2,0:T(8,128)(2,1)S(1)} async-done(((bf16[4,128,256]{1,2,0:T(8,128)(2,1)}), bf16[4,128,256]{1,2,0:T(8,128)(2,1)S(1)}, u32[]{:S(2)}, u32[]{:S(2)}) %all-to-all-start) | async-done | bytes 262176 | tf_op jit(solution)/shard_map/all_to_all | solution.py:129
  28.3 3.0 %convolution_convert_fusion.1 = bf16[128,2048]{1,0:T(8,128)(2,1)S(1)} fusion(bf16[128,1024]{0,1:T(8,128)(2,1)S(1)} %bitcast.104, bf16[1024,2048]{1,0:T(8,128)(2,1)} %param.23), kind=kOutput, calls=%fused_computation.6 | convolution fusion | flops 537133056 | bytes 4980736 | tf_op jit(solution)/shard_map/dot_general | solution.py:88
  31.5 2.1 fusion.1
  33.6 12.7 %all-to-all-start.1 = ((bf16[64,8,2048]{2,1,0:T(8,128)(2,1)}), bf16[64,8,2048]{2,1,0:T(8,128)(2,1)S(1)}, u32[]{:S(2)}, u32[]{:S(2)}) async-start(bf16[64,8,2048]{2,1,0:T(8,128)(2,1)} %fusion.1), calls=%async_computation.1 | async-start | bytes 4194304 | tf_op jit(solution)/shard_map/all_to_all | solution.py:148
  46.4 2.5 slice_bitcast_fusion.5
  50.9 2.4 collective-permute-start.8
  54.3 3.2 %collective-permute-start.9 = (bf16[1024,256]{1,0:T(8,128)(2,1)}, bf16[1024,256]{1,0:T(8,128)(2,1)}, u32[]{:S(2)}, u32[]{:S(2)}) collective-permute-start(bf16[1024,256]{1,0:T(8,128)(2,1)} %get-tuple-element.10), channel_id=1, source_target_pairs={{0,3},{1,0},{2,1},{3,2},{4,7},{5,4},{6,5},{7,6},{8,11},{9,8},{10,9... | collective-permute-start | bytes 1572872 | tf_op jit(solution)/shard_map/ppermute | solution.py:22
  58.6 17.8 %collective-permute-done.2 = bf16[1024,256]{1,0:T(8,128)(2,1)S(1)} collective-permute-done((bf16[1024,256]{1,0:T(8,128)(2,1)}, bf16[1024,256]{1,0:T(8,128)(2,1)S(1)}, u32[]{:S(2)}, u32[]{:S(2)}) %collective-permute-start.2) | collective-permute-done | bytes 524320 | tf_op jit(solution)/shard_map/ppermute | solution.py:22
  77.1 20.5 %all-to-all-done.1 = bf16[64,8,2048]{2,1,0:T(8,128)(2,1)S(1)} async-done(((bf16[64,8,2048]{2,1,0:T(8,128)(2,1)}), bf16[64,8,2048]{2,1,0:T(8,128)(2,1)S(1)}, u32[]{:S(2)}, u32[]{:S(2)}) %all-to-all-start.1) | async-done | bytes 2097184 | tf_op jit(solution)/shard_map/all_to_all | solution.py:148
  103.1 12.3 %collective-permute-done.3 = bf16[1024,256]{1,0:T(8,128)(2,1)S(1)} collective-permute-done((bf16[1024,256]{1,0:T(8,128)(2,1)}, bf16[1024,256]{1,0:T(8,128)(2,1)S(1)}, u32[]{:S(2)}, u32[]{:S(2)}) %collective-permute-start.3) | collective-permute-done | bytes 524320 | tf_op jit(solution)/shard_map/ppermute | solution.py:22
  115.9 10.8 %collective-permute-done.6 = bf16[128,2048]{1,0:T(8,128)(2,1)S(1)} collective-permute-done((bf16[128,2048]{1,0:T(8,128)(2,1)S(1)}, bf16[128,2048]{1,0:T(8,128)(2,1)S(1)}, u32[]{:S(2)}, u32[]{:S(2)}) %collective-permute-start.6) | collective-permute-done | bytes 524320 | tf_op jit(solution)/shard_map/ppermute | solution.py:22
  126.7 2.7 fusion.49
  129.4 6.0 %collective-permute-done.5 = bf16[128,2048]{1,0:T(8,128)(2,1)} collective-permute-done((bf16[128,2048]{1,0:T(8,128)(2,1)S(1)}, bf16[128,2048]{1,0:T(8,128)(2,1)}, u32[]{:S(2)}, u32[]{:S(2)}) %collective-permute-start.5) | collective-permute-done | bytes 524320 | tf_op jit(solution)/shard_map/ppermute | solution.py:22
  135.4 3.7 %fusion.51 = f32[512,2048]{1,0:T(8,128)} fusion(bf16[128,2048]{1,0:T(8,128)(2,1)} %collective-permute-done.5, bf16[512,256]{1,0:T(8,128)(2,1)S(1)} %multiply_convert_fusion.4), kind=kOutput, calls=%fused_computation.70 | convolution fusion | flops 268435456 | bytes 4849664 | tf_op jit(solution)/shard_map/dot_general | solution.py:88
  140.8 1.9 collective-permute-start.13
  148.3 13.1 %collective-permute-done.12 = bf16[128,2048]{1,0:T(8,128)(2,1)S(1)} collective-permute-done((bf16[128,2048]{1,0:T(8,128)(2,1)S(1)}, bf16[128,2048]{1,0:T(8,128)(2,1)S(1)}, u32[]{:S(2)}, u32[]{:S(2)}) %collective-permute-start.12) | collective-permute-done | bytes 524320 | tf_op jit(solution)/shard_map/ppermute | solution.py:22
  162.6 2.7 fusion.45
  165.3 7.4 %collective-permute-done.14 = bf16[1024,256]{1,0:T(8,128)(2,1)S(1)} collective-permute-done((bf16[1024,256]{1,0:T(8,128)(2,1)}, bf16[1024,256]{1,0:T(8,128)(2,1)S(1)}, u32[]{:S(2)}, u32[]{:S(2)}) %collective-permute-start.14) | collective-permute-done | bytes 524320 | tf_op jit(solution)/shard_map/ppermute | solution.py:22
  173.1 3.5 %collective-permute-start.18 = (bf16[128,2048]{1,0:T(8,128)(2,1)S(1)}, bf16[128,2048]{1,0:T(8,128)(2,1)S(1)}, u32[]{:S(2)}, u32[]{:S(2)}) collective-permute-start(bf16[128,2048]{1,0:T(8,128)(2,1)S(1)} %collective-permute-done.12), channel_id=1, source_target_pairs={{0,3},{1,0},{2,1},{3,2},{4,7},{5,4},{6,5},{7,6},{8,11},{9,8},{10,9... | collective-permute-start | bytes 1572872 | tf_op jit(solution)/shard_map/ppermute | solution.py:22
  177.1 6.8 %collective-permute-done.16 = bf16[1024,256]{1,0:T(8,128)(2,1)S(1)} collective-permute-done((bf16[1024,256]{1,0:T(8,128)(2,1)S(1)}, bf16[1024,256]{1,0:T(8,128)(2,1)S(1)}, u32[]{:S(2)}, u32[]{:S(2)}) %collective-permute-start.16) | collective-permute-done | bytes 524320 | tf_op jit(solution)/shard_map/ppermute | solution.py:22
  184.8 2.6 fusion.47
  187.5 4.8 %collective-permute-done.18 = bf16[128,2048]{1,0:T(8,128)(2,1)S(1)} collective-permute-done((bf16[128,2048]{1,0:T(8,128)(2,1)S(1)}, bf16[128,2048]{1,0:T(8,128)(2,1)S(1)}, u32[]{:S(2)}, u32[]{:S(2)}) %collective-permute-start.18) | collective-permute-done | bytes 524320 | tf_op jit(solution)/shard_map/ppermute | solution.py:22
  192.3 2.6 fusion.42
  196.4 6.0 %fusion.3 = f32[512,2048]{1,0:T(8,128)} fusion(bf16[1,256,2048]{2,1,0:T(8,128)(2,1)} %param.29, bf16[1,2048,256]{2,1,0:T(8,128)(2,1)} %param.28, f32[512,256]{1,0:T(8,128)} %fusion.7, bf16[64,8,2048]{2,1,0:T(8,128)(2,1)S(1)} %all-to-all-done.1), kind=kOutput, calls=%fused_computation.15 | convolution fusion | flops 1074528256 | bytes 8912896 | tf_op jit(solution)/shard_map/dot_general | solution.py:88
  202.4 11.2 %fusion = bf16[64,8,2048]{2,1,0:T(8,128)(2,1)} fusion(f32[512,2048]{1,0:T(8,128)} %fusion.42, bf16[128,2048]{1,0:T(8,128)(2,1)} %collective-permute-done.17, f32[512,2048]{1,0:T(8,128)} %fusion.47, f32[512,2048]{1,0:T(8,128)} %fusion.45, f32[512,2048]{1,0:T(8,128)} %fusion.3, f32[512,2048]{1,0:T(8,128)} %fusion.51, f32[512,2048]{1,0:T(8,128)} %fusion.49, ...), kind=kOutput, calls=%fused_computation.4 | convolution fusion | flops 275775488 | bytes 27918336 | tf_op jit(solution)/shard_map/dot_general | solution.py:88
  213.6 8.6 %all-to-all-start.2 = ((bf16[64,8,2048]{2,1,0:T(8,128)(2,1)}), bf16[64,8,2048]{2,1,0:T(8,128)(2,1)S(1)}, u32[]{:S(2)}, u32[]{:S(2)}) async-start(bf16[64,8,2048]{2,1,0:T(8,128)(2,1)} %fusion), calls=%async_computation.2 | async-start | bytes 4194304 | tf_op jit(solution)/shard_map/all_to_all | solution.py:164
  223.2 50.3 %all-to-all-done.2 = bf16[64,8,2048]{2,1,0:T(8,128)(2,1)S(1)} async-done(((bf16[64,8,2048]{2,1,0:T(8,128)(2,1)}), bf16[64,8,2048]{2,1,0:T(8,128)(2,1)S(1)}, u32[]{:S(2)}, u32[]{:S(2)}) %all-to-all-start.2) | async-done | bytes 2097184 | tf_op jit(solution)/shard_map/all_to_all | solution.py:164
  277.0 2.5 add_convert_fusion.1
  (93 shorter events, 34.5 us)
Async XLA Ops:
  0.0 3.5 %copy-start = (s32[512,2]{0,1:T(2,128)S(1)}, s32[512,2]{0,1:T(2,128)}, u32[]{:S(2)}) copy-start(s32[512,2]{0,1:T(2,128)} %param.25) | copy-start | bytes 12292
  1.6 5.1 %collective-permute-start = (bf16[32,256]{1,0:T(8,128)(2,1)S(1)}, bf16[32,256]{1,0:T(8,128)(2,1)S(1)}, u32[]{:S(2)}, u32[]{:S(2)}) collective-permute-start(bf16[32,256]{1,0:T(8,128)(2,1)S(1)} %fusion.58), channel_id=1, source_target_pairs={{0,4},{4,8},{8,12},{12,16},{16,20},{20,24},{24,28},{28,32},{32,36}... | collective-permute-start | bytes 49160 | tf_op jit(solution)/shard_map/ppermute | solution.py:17
  6.6 2.4 copy-start.7
  16.9 11.3 %all-to-all-start = ((bf16[4,128,256]{1,2,0:T(8,128)(2,1)}), bf16[4,128,256]{1,2,0:T(8,128)(2,1)S(1)}, u32[]{:S(2)}, u32[]{:S(2)}) async-start(bf16[4,128,256]{1,2,0:T(8,128)(2,1)} %copy.22), calls=%async_computation | async-start | bytes 524288 | tf_op jit(solution)/shard_map/all_to_all | solution.py:129
  28.2 3.0 %copy-start.1 = (bf16[128,2048]{1,0:T(8,128)(2,1)S(1)}, bf16[128,2048]{1,0:T(8,128)(2,1)}, u32[]{:S(2)}) copy-start(bf16[128,2048]{1,0:T(8,128)(2,1)} %param.16) | copy-start | bytes 1572868
  28.2 3.3 %copy-start.8 = (f32[2048]{0:T(1024)S(1)}, f32[2048]{0:T(1024)}, u32[]{:S(2)}) copy-start(f32[2048]{0:T(1024)} %param.24) | copy-start | bytes 24580
  33.6 63.9 %all-to-all-start.1 = ((bf16[64,8,2048]{2,1,0:T(8,128)(2,1)}), bf16[64,8,2048]{2,1,0:T(8,128)(2,1)S(1)}, u32[]{:S(2)}, u32[]{:S(2)}) async-start(bf16[64,8,2048]{2,1,0:T(8,128)(2,1)} %fusion.1), calls=%async_computation.1 | async-start | bytes 4194304 | tf_op jit(solution)/shard_map/all_to_all | solution.py:148
  46.4 6.9 %copy-start.3 = (bf16[1,2048,256]{2,1,0:T(8,128)(2,1)S(1)}, bf16[1,2048,256]{2,1,0:T(8,128)(2,1)}, u32[]{:S(2)}) copy-start(bf16[1,2048,256]{2,1,0:T(8,128)(2,1)} %param.28) | copy-start | bytes 3145732
  46.4 11.2 %copy-start.2 = (bf16[1,256,2048]{2,1,0:T(8,128)(2,1)S(1)}, bf16[1,256,2048]{2,1,0:T(8,128)(2,1)}, u32[]{:S(2)}) copy-start(bf16[1,256,2048]{2,1,0:T(8,128)(2,1)} %param.29) | copy-start | bytes 3145732
  48.8 92.0 %collective-permute-start.7 = (bf16[1024,256]{1,0:T(8,128)(2,1)}, bf16[1024,256]{1,0:T(8,128)(2,1)}, u32[]{:S(2)}, u32[]{:S(2)}) collective-permute-start(bf16[1024,256]{1,0:T(8,128)(2,1)} %get-tuple-element.12), channel_id=1, source_target_pairs={{0,3},{1,0},{2,1},{3,2},{4,7},{5,4},{6,5},{7,6},{8,11},{9,8},{10,9... | collective-permute-start | bytes 1572872 | tf_op jit(solution)/shard_map/ppermute | solution.py:22
  50.0 49.2 %collective-permute-start.1 = (bf16[1024,256]{1,0:T(8,128)(2,1)}, bf16[1024,256]{1,0:T(8,128)(2,1)}, u32[]{:S(2)}, u32[]{:S(2)}) collective-permute-start(bf16[1024,256]{1,0:T(8,128)(2,1)} %get-tuple-element.12), channel_id=1, source_target_pairs={{0,1},{1,2},{2,3},{3,0},{4,5},{5,6},{6,7},{7,4},{8,9},{9,10},{10,1... | collective-permute-start | bytes 1572872 | tf_op jit(solution)/shard_map/ppermute | solution.py:22
  50.9 88.2 %collective-permute-start.8 = (bf16[1024,256]{1,0:T(8,128)(2,1)}, bf16[1024,256]{1,0:T(8,128)(2,1)}, u32[]{:S(2)}, u32[]{:S(2)}) collective-permute-start(bf16[1024,256]{1,0:T(8,128)(2,1)} %get-tuple-element.13), channel_id=1, source_target_pairs={{0,3},{1,0},{2,1},{3,2},{4,7},{5,4},{6,5},{7,6},{8,11},{9,8},{10,9... | collective-permute-start | bytes 1572872 | tf_op jit(solution)/shard_map/ppermute | solution.py:22
  53.2 23.1 %collective-permute-start.2 = (bf16[1024,256]{1,0:T(8,128)(2,1)}, bf16[1024,256]{1,0:T(8,128)(2,1)S(1)}, u32[]{:S(2)}, u32[]{:S(2)}) collective-permute-start(bf16[1024,256]{1,0:T(8,128)(2,1)} %get-tuple-element.13), channel_id=1, source_target_pairs={{0,1},{1,2},{2,3},{3,0},{4,5},{5,6},{6,7},{7,4},{8,9},{9,10},{10,1... | collective-permute-start | bytes 1572872 | tf_op jit(solution)/shard_map/ppermute | solution.py:22
  54.3 91.9 %collective-permute-start.9 = (bf16[1024,256]{1,0:T(8,128)(2,1)}, bf16[1024,256]{1,0:T(8,128)(2,1)}, u32[]{:S(2)}, u32[]{:S(2)}) collective-permute-start(bf16[1024,256]{1,0:T(8,128)(2,1)} %get-tuple-element.10), channel_id=1, source_target_pairs={{0,3},{1,0},{2,1},{3,2},{4,7},{5,4},{6,5},{7,6},{8,11},{9,8},{10,9... | collective-permute-start | bytes 1572872 | tf_op jit(solution)/shard_map/ppermute | solution.py:22
  76.3 0.8 copy-start.9
  77.1 24.2 %collective-permute-start.4 = (bf16[1024,256]{1,0:T(8,128)(2,1)}, bf16[1024,256]{1,0:T(8,128)(2,1)}, u32[]{:S(2)}, u32[]{:S(2)}) collective-permute-start(bf16[1024,256]{1,0:T(8,128)(2,1)} %get-tuple-element.11), channel_id=1, source_target_pairs={{0,1},{1,2},{2,3},{3,0},{4,5},{5,6},{6,7},{7,4},{8,9},{9,10},{10,1... | collective-permute-start | bytes 1572872 | tf_op jit(solution)/shard_map/ppermute | solution.py:22
  97.6 3.7 %copy-start.6 = (bf16[128,2048]{1,0:T(8,128)(2,1)S(1)}, bf16[128,2048]{1,0:T(8,128)(2,1)}, u32[]{:S(2)}) copy-start(bf16[128,2048]{1,0:T(8,128)(2,1)} %get-tuple-element.9) | copy-start | bytes 1572868
  99.1 16.3 %copy-start.5 = (bf16[128,2048]{1,0:T(8,128)(2,1)S(1)}, bf16[128,2048]{1,0:T(8,128)(2,1)}, u32[]{:S(2)}) copy-start(bf16[128,2048]{1,0:T(8,128)(2,1)} %get-tuple-element.8) | copy-start | bytes 1572868
  99.2 16.3 %collective-permute-start.3 = (bf16[1024,256]{1,0:T(8,128)(2,1)}, bf16[1024,256]{1,0:T(8,128)(2,1)S(1)}, u32[]{:S(2)}, u32[]{:S(2)}) collective-permute-start(bf16[1024,256]{1,0:T(8,128)(2,1)} %get-tuple-element.10), channel_id=1, source_target_pairs={{0,1},{1,2},{2,3},{3,0},{4,5},{5,6},{6,7},{7,4},{8,9},{9,10},{10,1... | collective-permute-start | bytes 1572872 | tf_op jit(solution)/shard_map/ppermute | solution.py:22
  101.3 25.4 %collective-permute-start.6 = (bf16[128,2048]{1,0:T(8,128)(2,1)S(1)}, bf16[128,2048]{1,0:T(8,128)(2,1)S(1)}, u32[]{:S(2)}, u32[]{:S(2)}) collective-permute-start(bf16[128,2048]{1,0:T(8,128)(2,1)S(1)} %copy-done.6), channel_id=1, source_target_pairs={{0,1},{1,2},{2,3},{3,0},{4,5},{5,6},{6,7},{7,4},{8,9},{9,10},{10,1... | collective-permute-start | bytes 1572872 | tf_op jit(solution)/shard_map/ppermute | solution.py:22
  115.5 19.9 %collective-permute-start.5 = (bf16[128,2048]{1,0:T(8,128)(2,1)S(1)}, bf16[128,2048]{1,0:T(8,128)(2,1)}, u32[]{:S(2)}, u32[]{:S(2)}) collective-permute-start(bf16[128,2048]{1,0:T(8,128)(2,1)S(1)} %copy-done.5), channel_id=1, source_target_pairs={{0,1},{1,2},{2,3},{3,0},{4,5},{5,6},{6,7},{7,4},{8,9},{9,10},{10,1... | collective-permute-start | bytes 1572872 | tf_op jit(solution)/shard_map/ppermute | solution.py:22
  126.7 17.5 %collective-permute-start.10 = (bf16[1024,256]{1,0:T(8,128)(2,1)}, bf16[1024,256]{1,0:T(8,128)(2,1)S(1)}, u32[]{:S(2)}, u32[]{:S(2)}) collective-permute-start(bf16[1024,256]{1,0:T(8,128)(2,1)} %get-tuple-element.11), channel_id=1, source_target_pairs={{0,3},{1,0},{2,1},{3,2},{4,7},{5,4},{6,5},{7,6},{8,11},{9,8},{10,9... | collective-permute-start | bytes 1572872 | tf_op jit(solution)/shard_map/ppermute | solution.py:22
  135.4 49.4 %collective-permute-start.11 = (bf16[128,2048]{1,0:T(8,128)(2,1)S(1)}, bf16[128,2048]{1,0:T(8,128)(2,1)S(1)}, u32[]{:S(2)}, u32[]{:S(2)}) collective-permute-start(bf16[128,2048]{1,0:T(8,128)(2,1)S(1)} %copy-done.5), channel_id=1, source_target_pairs={{0,3},{1,0},{2,1},{3,2},{4,7},{5,4},{6,5},{7,6},{8,11},{9,8},{10,9... | collective-permute-start | bytes 1572872 | tf_op jit(solution)/shard_map/ppermute | solution.py:22
  139.1 22.3 %collective-permute-start.12 = (bf16[128,2048]{1,0:T(8,128)(2,1)S(1)}, bf16[128,2048]{1,0:T(8,128)(2,1)S(1)}, u32[]{:S(2)}, u32[]{:S(2)}) collective-permute-start(bf16[128,2048]{1,0:T(8,128)(2,1)S(1)} %copy-done.6), channel_id=1, source_target_pairs={{0,3},{1,0},{2,1},{3,2},{4,7},{5,4},{6,5},{7,6},{8,11},{9,8},{10,9... | collective-permute-start | bytes 1572872 | tf_op jit(solution)/shard_map/ppermute | solution.py:22
  140.8 32.3 %collective-permute-start.13 = (bf16[1024,256]{1,0:T(8,128)(2,1)}, bf16[1024,256]{1,0:T(8,128)(2,1)S(1)}, u32[]{:S(2)}, u32[]{:S(2)}) collective-permute-start(bf16[1024,256]{1,0:T(8,128)(2,1)} %collective-permute-done.1), channel_id=1, source_target_pairs={{0,1},{1,2},{2,3},{3,0},{4,5},{5,6},{6,7},{7,4},{8,9},{9,10},{10,1... | collective-permute-start | bytes 1572872 | tf_op jit(solution)/shard_map/ppermute | solution.py:22
  144.2 28.4 %collective-permute-start.14 = (bf16[1024,256]{1,0:T(8,128)(2,1)}, bf16[1024,256]{1,0:T(8,128)(2,1)S(1)}, u32[]{:S(2)}, u32[]{:S(2)}) collective-permute-start(bf16[1024,256]{1,0:T(8,128)(2,1)} %collective-permute-done.8), channel_id=1, source_target_pairs={{0,3},{1,0},{2,1},{3,2},{4,7},{5,4},{6,5},{7,6},{8,11},{9,8},{10,9... | collective-permute-start | bytes 1572872 | tf_op jit(solution)/shard_map/ppermute | solution.py:22
  146.2 38.1 %collective-permute-start.15 = (bf16[1024,256]{1,0:T(8,128)(2,1)S(1)}, bf16[1024,256]{1,0:T(8,128)(2,1)S(1)}, u32[]{:S(2)}, u32[]{:S(2)}) collective-permute-start(bf16[1024,256]{1,0:T(8,128)(2,1)S(1)} %collective-permute-done.3), channel_id=1, source_target_pairs={{0,1},{1,2},{2,3},{3,0},{4,5},{5,6},{6,7},{7,4},{8,9},{9,10},{10,1... | collective-permute-start | bytes 1572872 | tf_op jit(solution)/shard_map/ppermute | solution.py:22
  161.4 22.5 %collective-permute-start.16 = (bf16[1024,256]{1,0:T(8,128)(2,1)S(1)}, bf16[1024,256]{1,0:T(8,128)(2,1)S(1)}, u32[]{:S(2)}, u32[]{:S(2)}) collective-permute-start(bf16[1024,256]{1,0:T(8,128)(2,1)S(1)} %collective-permute-done.10), channel_id=1, source_target_pairs={{0,3},{1,0},{2,1},{3,2},{4,7},{5,4},{6,5},{7,6},{8,11},{9,8},{10,9... | collective-permute-start | bytes 1572872 | tf_op jit(solution)/shard_map/ppermute | solution.py:22
  172.7 29.7 %collective-permute-start.17 = (bf16[128,2048]{1,0:T(8,128)(2,1)}, bf16[128,2048]{1,0:T(8,128)(2,1)}, u32[]{:S(2)}, u32[]{:S(2)}) collective-permute-start(bf16[128,2048]{1,0:T(8,128)(2,1)} %collective-permute-done.5), channel_id=1, source_target_pairs={{0,1},{1,2},{2,3},{3,0},{4,5},{5,6},{6,7},{7,4},{8,9},{9,10},{10,1... | collective-permute-start | bytes 1572872 | tf_op jit(solution)/shard_map/ppermute | solution.py:22
  173.1 19.1 %collective-permute-start.18 = (bf16[128,2048]{1,0:T(8,128)(2,1)S(1)}, bf16[128,2048]{1,0:T(8,128)(2,1)S(1)}, u32[]{:S(2)}, u32[]{:S(2)}) collective-permute-start(bf16[128,2048]{1,0:T(8,128)(2,1)S(1)} %collective-permute-done.12), channel_id=1, source_target_pairs={{0,3},{1,0},{2,1},{3,2},{4,7},{5,4},{6,5},{7,6},{8,11},{9,8},{10,9... | collective-permute-start | bytes 1572872 | tf_op jit(solution)/shard_map/ppermute | solution.py:22
  187.5 7.4 %copy-start.4 = (bf16[1,2048,256]{2,1,0:T(8,128)(2,1)S(1)}, bf16[1,2048,256]{2,1,0:T(8,128)(2,1)}, u32[]{:S(2)}) copy-start(bf16[1,2048,256]{2,1,0:T(8,128)(2,1)} %param.27) | copy-start | bytes 3145732
  213.6 59.9 %all-to-all-start.2 = ((bf16[64,8,2048]{2,1,0:T(8,128)(2,1)}), bf16[64,8,2048]{2,1,0:T(8,128)(2,1)S(1)}, u32[]{:S(2)}, u32[]{:S(2)}) async-start(bf16[64,8,2048]{2,1,0:T(8,128)(2,1)} %fusion), calls=%async_computation.2 | async-start | bytes 4194304 | tf_op jit(solution)/shard_map/all_to_all | solution.py:164

commit v2 on v1

--- a/solution.py
+++ b/solution.py
@@ -1,3 +1,5 @@
+import functools
+
 import jax
 import jax.numpy as jnp
 from jax import lax
@@ -27,12 +29,6 @@
     onehot = (route_pairs[..., None] == jnp.arange(experts_n, dtype=jnp.int32)).astype(jnp.int32)
     slot_rank = jnp.sum((jnp.cumsum(onehot, axis=-2) - onehot) * onehot, axis=-1)
     return (route_pairs * capacity + slot_rank).reshape(block_routes.shape)
-
-
-def dispatch_matrix(slot_ids, slot_total):
-    numbers = jnp.arange(slot_total, dtype=jnp.int32)[:, None, None]
-    matches = jnp.any(numbers == slot_ids[..., None, :, :], axis=-1)
-    return matches.astype(jnp.bfloat16)
 
 
 def conv_body(value_ref, gate_ref, rim_ref, seen_ref, taps_ref, gain_ref, shift_ref, out_ref, rows_ref):
@@ -72,20 +68,170 @@
     )(value, gate, rim, seen, taps, gain[None], shift[None])
 
 
-def gathered(shard):
-    half = shard.shape[0] // 2
-    left, right, far = [], [], []
-    for part in range(2):
-        piece = shard[part * half : (part + 1) * half]
-        left.append(ring(piece, "tp", 1))
-        right.append(ring(piece, "tp", -1))
-    far.append(ring(left[0], "tp", 1))
-    far.append(ring(right[1], "tp", -1))
-    return left, right, far
-
-
 def dot(a, b):
     return jnp.dot(a, b, preferred_element_type=jnp.float32)
+
+
+def places(slots, total):
+    numbers = lax.broadcasted_iota(jnp.int32, (slots.shape[0], total), 1)
+    return [numbers == slots[:, m : m + 1] for m in range(slots.shape[1])]
+
+
+def route_body(parts_ref, out_weight_ref, residual_ref, gain_ref, slots_ref, stream_ref, *sent_refs):
+    width = parts_ref.shape[2]
+    mixed = dot(parts_ref[0], out_weight_ref[:width])
+    for j in range(1, parts_ref.shape[0]):
+        mixed = mixed + dot(parts_ref[j], out_weight_ref[j * width : (j + 1) * width])
+    stream = residual_ref[...].astype(jnp.float32) + mixed.astype(jnp.bfloat16).astype(jnp.float32)
+    stream_ref[...] = stream
+    scale = lax.rsqrt(jnp.mean(stream * stream, axis=1, keepdims=True) + 1e-06)
+    normed = (stream * scale * gain_ref[...]).astype(jnp.bfloat16)
+    table = functools.reduce(jnp.logical_or, places(slots_ref[...], sent_refs[0].shape[0]))
+    table = jnp.where(table, 1.0, 0.0).astype(jnp.bfloat16)
+    at = 0
+    for sent in sent_refs:
+        cols = normed[:, at : at + sent.shape[1]]
+        sent[...] = lax.dot_general(
+            table, cols, (((0,), (0,)), ((), ())), preferred_element_type=jnp.float32
+        ).astype(jnp.bfloat16)
+        at += sent.shape[1]
+
+
+def combine_body(stream_ref, slots_ref, weights_ref, *refs):
+    *back_refs, out_ref = refs
+    hits = places(slots_ref[...], back_refs[0].shape[0])
+    table = sum(
+        jnp.where(hit, weights_ref[:, m : m + 1], 0.0) for m, hit in enumerate(hits)
+    )
+    high = table.astype(jnp.bfloat16)
+    low = (table - high.astype(jnp.float32)).astype(jnp.bfloat16)
+    at = 0
+    for back in back_refs:
+        cols = slice(at, at + back.shape[1])
+        rows = back[...]
+        out_ref[:, cols] = (stream_ref[:, cols] + (dot(high, rows) + dot(low, rows))).astype(
+            jnp.bfloat16
+        )
+        at += back.shape[1]
+
+
+def fetch(copies, sems):
+    started = [pltpu.make_async_copy(src, dst, sems.at[i]) for i, (src, dst) in enumerate(copies)]
+    for c in started:
+        c.start()
+    return started
+
+
+def hidden_of(rows, weights):
+    act = dot(rows, weights)
+    half = act.shape[1] // 2
+    gate = act[:, :half]
+    return (gate / (1.0 + jnp.exp(-gate)) * act[:, half:]).astype(jnp.bfloat16)
+
+
+def near_body(n_rows, *refs):
+    rows_in, quarters, (out_ref, rows_ref, w_ref, sems) = refs[:n_rows], refs[n_rows:-4], refs[-4:]
+    width = quarters[0].shape[1]
+    copies, at = [], 0
+    for src in rows_in:
+        copies.append((src, rows_ref.at[:, at : at + src.shape[1]]))
+        at += src.shape[1]
+    ends, i = [], 0
+    for q in range(3):
+        for kind in range(2):
+            top = 0
+            while top < w_ref.shape[1]:
+                src = quarters[i]
+                copies.append(
+                    (src, w_ref.at[q, top : top + src.shape[0], kind * width : (kind + 1) * width])
+                )
+                top += src.shape[0]
+                i += 1
+        ends.append(len(copies))
+    copies = fetch(copies, sems)
+    done = 0
+    for q in range(3):
+        for c in copies[done : ends[q]]:
+            c.wait()
+        done = ends[q]
+        out_ref[:, q * width : (q + 1) * width] = hidden_of(rows_ref[...], w_ref[q])
+
+
+def near_hidden(rows, quarters):
+    n, width = rows[0].shape[0], quarters[0].shape[1]
+    d = sum(r.shape[1] for r in rows)
+    n_copies = len(rows) + len(quarters)
+    return pl.pallas_call(
+        functools.partial(near_body, len(rows)),
+        out_shape=jax.ShapeDtypeStruct((n, 3 * width), jnp.bfloat16),
+        in_specs=[pl.BlockSpec(memory_space=pl.ANY)] * n_copies,
+        out_specs=pl.BlockSpec(memory_space=pltpu.VMEM),
+        scratch_shapes=[
+            pltpu.VMEM((n, d), jnp.bfloat16),
+            pltpu.VMEM((3, d, 2 * width), jnp.bfloat16),
+            pltpu.SemaphoreType.DMA((n_copies,)),
+        ],
+        name="near_hidden",
+    )(*rows, *quarters)
+
+
+def far_body(n_rows, n_far, *refs):
+    rows_in, far_in = refs[:n_rows], refs[n_rows : n_rows + n_far]
+    near_ref, *downs = refs[n_rows + n_far : -6]
+    out_ref, rows_ref, w_ref, hidden_ref, down_ref, sems = refs[-6:]
+    width = far_in[0].shape[1]
+    copies, at = [], 0
+    for src in rows_in:
+        copies.append((src, rows_ref.at[:, at : at + src.shape[1]]))
+        at += src.shape[1]
+    i = 0
+    for kind in range(2):
+        top = 0
+        while top < w_ref.shape[0]:
+            src = far_in[i]
+            copies.append((src, w_ref.at[top : top + src.shape[0], kind * width : (kind + 1) * width]))
+            top += src.shape[0]
+            i += 1
+    first = len(copies)
+    copies.append((near_ref, hidden_ref.at[:, : 3 * width]))
+    top = 0
+    for src in downs:
+        copies.append((src, down_ref.at[top : top + src.shape[0]]))
+        top += src.shape[0]
+    copies = fetch(copies, sems)
+    for c in copies[:first]:
+        c.wait()
+    hidden_ref[:, 3 * width :] = hidden_of(rows_ref[...], w_ref[...])
+    for c in copies[first:]:
+        c.wait()
+    out_ref[...] = dot(hidden_ref[...], down_ref[...]).astype(jnp.bfloat16)
+
+
+def expert_rows(rows, far, near, downs):
+    n, width, cols = rows[0].shape[0], far[0].shape[1], downs[0].shape[1]
+    d = sum(r.shape[1] for r in rows)
+    n_copies = len(rows) + len(far) + 1 + len(downs)
+    return pl.pallas_call(
+        functools.partial(far_body, len(rows), len(far)),
+        out_shape=jax.ShapeDtypeStruct((n, cols), jnp.bfloat16),
+        in_specs=[pl.BlockSpec(memory_space=pl.ANY)] * n_copies,
+        out_specs=pl.BlockSpec(memory_space=pltpu.VMEM),
+        scratch_shapes=[
+            pltpu.VMEM((n, d), jnp.bfloat16),
+            pltpu.VMEM((d, 2 * width), jnp.bfloat16),
+            pltpu.VMEM((n, 4 * width), jnp.bfloat16),
+            pltpu.VMEM((4 * width, cols), jnp.bfloat16),
+            pltpu.SemaphoreType.DMA((n_copies,)),
+        ],
+        name="expert_rows",
+    )(*rows, *far, near, *downs)
+
+
+def gathered(shard):
+    left, right = ring(shard, "tp", 1), ring(shard, "tp", -1)
+    half = shard.shape[0] // 2
+    far = ring(left[:half], "tp", 1), ring(right[half:], "tp", -1)
+    return left, right, far
 
 
 def shards(
@@ -126,48 +272,42 @@
     columns = lax.axis_size("tp")
     column = lax.axis_index("tp")
     rows_own = tok_dev // columns
-    regrouped = lax.all_to_all(conv_out, "tp", split_axis=0, concat_axis=1, tiled=True)
-    mixed = dot(regrouped, out_weight)
-    stream = residual.astype(jnp.float32) + lax.optimization_barrier(
-        mixed.astype(jnp.bfloat16)
-    ).astype(jnp.float32)
-    normed = (
-        stream * lax.rsqrt(jnp.mean(stream * stream, axis=-1, keepdims=True) + 1e-06) * ffn_gain
-    ).astype(jnp.bfloat16)
+    regrouped = lax.all_to_all(
+        conv_out.reshape(columns, rows_own, local_channels), "tp", 0, 0, tiled=True
+    )
     experts_n = lax.axis_size("sp")
     top_count = routes.shape[1]
-    model_width = normed.shape[1]
+    model_width = residual.shape[1]
     capacity = max(2, 2 * tok_dev * top_count // (columns * experts_n))
     slot_total = experts_n * capacity
     own_routes = lax.dynamic_slice_in_dim(routes, column * rows_own, rows_own, 0)
     own_weights = lax.dynamic_slice_in_dim(route_weights, column * rows_own, rows_own, 0)
     own_slots = slot_numbers(own_routes, capacity, experts_n)
-    routing_table = dispatch_matrix(own_slots, slot_total)
-    outgoing = dot(routing_table, normed).astype(jnp.bfloat16)
-    outgoing = outgoing.reshape(experts_n, capacity, model_width)
-    arrived = lax.all_to_all(outgoing, "sp", split_axis=0, concat_axis=1, tiled=True)
-    arrived = arrived.reshape(slot_total, model_width)
-
-    def quarter(gate, up, down):
-        def rows(x, parts):
-            half = x.shape[1] // 2
-            return dot(x[:, :half], parts[0]) + dot(x[:, half:], parts[1])
-
-        hidden = (jax.nn.silu(rows(arrived, gate)) * rows(arrived, up)).astype(jnp.bfloat16)
-        return rows(hidden, down)
-
-    hidden = (jax.nn.silu(dot(arrived, w_gate[0])) * dot(arrived, w_up[0])).astype(jnp.bfloat16)
-    summed = dot(hidden, w_down[0])
-    for side in range(3):
-        summed = summed + quarter(gates[side], ups[side], downs[side])
-    expert_out = summed.astype(jnp.bfloat16).reshape(experts_n, capacity, model_width)
-    returned = lax.all_to_all(expert_out, "sp", split_axis=0, concat_axis=0, tiled=True)
-    returned = returned.reshape(slot_total, model_width)
-    combined = stream
-    for member in range(top_count):
-        chosen = jnp.take(returned, own_slots[:, member], axis=0).astype(jnp.float32)
-        combined = combined + own_weights[:, member : member + 1] * chosen
-    return combined.astype(jnp.bfloat16)
+    stream, outgoing = pl.pallas_call(
+        route_body,
+        out_shape=(
+            jax.ShapeDtypeStruct((rows_own, model_width), jnp.float32),
+            jax.ShapeDtypeStruct((slot_total, model_width), jnp.bfloat16),
+        ),
+        name="project",
+    )(regrouped, out_weight, residual, ffn_gain[None], own_slots)
+    arrived = lax.all_to_all(
+        outgoing.reshape(experts_n, capacity, model_width), "sp", 0, 0, tiled=True
+    ).reshape(slot_total, model_width)
+    near = near_hidden(
+        [arrived], [w_gate[0], w_up[0], gates[0], ups[0], gates[1], ups[1]]
+    )
+    out = expert_rows(
+        [arrived], [*gates[2], *ups[2]], near, [w_down[0], downs[0], downs[1], *downs[2]]
+    )
+    back = lax.all_to_all(
+        out.reshape(experts_n, capacity, model_width), "sp", 0, 0, tiled=True
+    ).reshape(slot_total, model_width)
+    return pl.pallas_call(
+        combine_body,
+        out_shape=jax.ShapeDtypeStruct((rows_own, model_width), jnp.bfloat16),
+        name="combine",
+    )(stream, own_slots, own_weights, back)
 
 
 def solution(mesh):

time: 280 us -> 225 us (0.80)
  matrix products: 49.8 us -> 0 us
  Pallas kernels: 6.12 us -> 29.3 us
  waiting for transfers between devices: 158 us -> 137 us
  starting transfers between devices: 45.4 us -> 42.3 us
    dot_general x22 -> x0, matrix products: 49.8 us -> none  [dot(): return jnp.dot(a, b, preferred_element_type=jnp.float32)]
    pallas_call x0 -> x4, Pallas kernels: none -> 23.1 us  [the longest x1 7.32 us: expert_rows(): pl.pallas_call(functools.partial(far_body, len(rows), len(far)), out_shap...]
    all_to_all x3, waiting for transfers between devices: 77.5 us -> 56 us  [the longest x1 49.8 us: shards(): lax.all_to_all(out.reshape(experts_n, capacity, model_width), 'sp', 0, 0,...]
    ppermute x18 -> x12, starting transfers between devices: 17.6 us -> 12.8 us  [ring(): lax.ppermute(value, axis, [(i, (i + steps) % count) for i in range(count)])]
    gather x2 -> x0, local copies, waits for them, and re-layouts: 3.46 us -> none  [shards(): jnp.take(returned, own_slots[:, member], axis=0).astype(jnp.float32)]
    unnamed x21 -> x30, local copies, waits for them, and re-layouts: 0.96 us -> 4.31 us
    ppermute x18 -> x12, waiting for transfers between devices: 78.9 us -> 79.7 us  [ring(): lax.ppermute(value, axis, [(i, (i + steps) % count) for i in range(count)])]
  transfers between devices with their start and end apart: 22 -> 16, of which waited for: 12 -> 9; matrix products, arithmetic and copies ran while one was open for 14% -> 4% of each run, Pallas kernels for 0% -> 3%
where the time goes in v2:
time: 225 us; the launch traced here: 224 us
  waiting for transfers between devices  137 us (61%)
  starting transfers between devices  42.3 us (19%)
  Pallas kernels  29.3 us (13%)
  local copies, waits for them, and re-layouts  10.8 us (5%)
  other arithmetic  4.41 us (2%)
    ppermute x12, waiting for transfers between devices, ring(): lax.ppermute(value, axis, [(i, (i + steps) % count) for i in range(count)])  79.7 us
    all_to_all x1, waiting for transfers between devices, shards(): lax.all_to_all(out.reshape(experts_n, capacity, model_width), 'sp', 0, 0,...  49.8 us
    all_to_all x1, starting transfers between devices, shards(): lax.all_to_all(outgoing.reshape(experts_n, capacity, model_width), 'sp',...  12.8 us
    ppermute x12, starting transfers between devices, ring(): lax.ppermute(value, axis, [(i, (i + steps) % count) for i in range(count)])  12.8 us
    all_to_all x1, starting transfers between devices, shards(): lax.all_to_all(out.reshape(experts_n, capacity, model_width), 'sp', 0, 0,...  10.3 us
    pallas_call x1, Pallas kernels, expert_rows(): pl.pallas_call(functools.partial(far_body, len(rows), len(far)), out_shap...  7.32 us
    pallas_call x1, Pallas kernels, near_hidden(): pl.pallas_call(functools.partial(near_body, len(rows)), out_shape=jax.Sha...  6.92 us
    all_to_all x1, waiting for transfers between devices, shards(): lax.all_to_all(conv_out.reshape(columns, rows_own, local_channels), 'tp',...  6.23 us
  transfers between devices with their start and end apart: 16, of which 9 were waited for; matrix products, arithmetic and copies ran while one was open for 4% of the time, Pallas kernels for 3%

profile of v2, /device:TPU:2, one launch (start us, length us, event | category | flops | bytes accessed | tf_op | source)
XLA Modules:
  0.0 224.4 jit_solution(190665673637031209)
XLA Ops:
  1.6 1.9 collective-permute-start
  5.0 1.6 collective-permute-done.rim_ref
  7.4 0.8 convert_add_fusion
  8.2 0.8 broadcast_in_dim.20.seen_ref
  9.0 6.1 %conv_module.1 = bf16[512,256]{1,0:T(8,128)(2,1)} custom-call(bf16[512,256]{1,0:T(8,128)(2,1)} %value_ref.1, bf16[512,256]{1,0:T(8,128)(2,1)} %gate_ref.1, bf16[32,256]{1,0:T(8,128)(2,1)} %copy-done.13, s32[512,128]{1,0:T(8,128)} %broadcast_in_dim.20.seen_ref, f32[31,256]{1,0:T(8,128)} %taps_ref.1, f32[1,256]{1,0:T(1,128)} %bitcast.53, f32[1,256]{1,0:T(1,128)} %bitcast.54), custom_call_target="tpu_custom_call" | custom-call | tf_op jit(solution)/shard_map/conv_module/pallas_call | solution.py:63
  15.1 4.5 %all-to-all-start = ((bf16[4,128,256]{2,1,0:T(8,128)(2,1)}), bf16[4,128,256]{2,1,0:T(8,128)(2,1)S(1)}, u32[]{:S(2)}, u32[]{:S(2)}) async-start(bf16[4,128,256]{2,1,0:T(8,128)(2,1)} %bitcast.48), calls=%async_computation | async-start | bytes 524288 | tf_op jit(solution)/shard_map/all_to_all | solution.py:275
  20.2 6.2 %all-to-all-done.parts_ref = bf16[4,128,256]{2,1,0:T(8,128)(2,1)S(1)} async-done(((bf16[4,128,256]{2,1,0:T(8,128)(2,1)}), bf16[4,128,256]{2,1,0:T(8,128)(2,1)S(1)}, u32[]{:S(2)}, u32[]{:S(2)}) %all-to-all-start) | async-done | bytes 262176 | tf_op jit(solution)/shard_map/all_to_all | solution.py:275
  27.2 5.3 %project.1 = (f32[128,2048]{1,0:T(8,128)}, bf16[512,2048]{1,0:T(8,128)(2,1)}) custom-call(bf16[4,128,256]{2,1,0:T(8,128)(2,1)} %copy-done.10, bf16[1024,2048]{1,0:T(8,128)(2,1)} %out_weight_ref.1, bf16[128,2048]{1,0:T(8,128)(2,1)} %residual_ref.1, f32[1,2048]{1,0:T(1,128)} %bitcast.52, s32[128,2]{1,0:T(8,128)} %multiply_add_fusion.slots_ref), custom_call_target="tpu_custom_call" | custom-call | tf_op jit(solution)/shard_map/project/pallas_call | solution.py:286
  32.5 12.8 %all-to-all-start.1 = ((bf16[64,8,2048]{2,1,0:T(8,128)(2,1)}), bf16[64,8,2048]{2,1,0:T(8,128)(2,1)S(1)}, u32[]{:S(2)}, u32[]{:S(2)}) async-start(bf16[64,8,2048]{2,1,0:T(8,128)(2,1)} %bitcast.41), calls=%async_computation.1 | async-start | bytes 4194304 | tf_op jit(solution)/shard_map/all_to_all | solution.py:294
  46.0 2.7 %collective-permute-start.3 = (bf16[2048,256]{1,0:T(8,128)(2,1)S(1)}, bf16[2048,256]{1,0:T(8,128)(2,1)S(1)}, u32[]{:S(2)}, u32[]{:S(2)}) collective-permute-start(bf16[2048,256]{1,0:T(8,128)(2,1)S(1)} %bitcast.44), channel_id=1, source_target_pairs={{0,3},{1,0},{2,1},{3,2},{4,7},{5,4},{6,5},{7,6},{8,11},{9,8},{10,9... | collective-permute-start | bytes 3145736 | tf_op jit(solution)/shard_map/ppermute | solution.py:24
  48.6 3.2 %collective-permute-start.7 = (bf16[2048,256]{1,0:T(8,128)(2,1)}, bf16[2048,256]{1,0:T(8,128)(2,1)S(1)}, u32[]{:S(2)}, u32[]{:S(2)}) collective-permute-start(bf16[2048,256]{1,0:T(8,128)(2,1)} %bitcast.46), channel_id=1, source_target_pairs={{0,3},{1,0},{2,1},{3,2},{4,7},{5,4},{6,5},{7,6},{8,11},{9,8},{10,9... | collective-permute-start | bytes 3145736 | tf_op jit(solution)/shard_map/ppermute | solution.py:24
  51.9 20.8 %collective-permute-done.1.refs_3_ = bf16[2048,256]{1,0:T(8,128)(2,1)S(1)} collective-permute-done((bf16[2048,256]{1,0:T(8,128)(2,1)S(1)}, bf16[2048,256]{1,0:T(8,128)(2,1)S(1)}, u32[]{:S(2)}, u32[]{:S(2)}) %collective-permute-start.1) | collective-permute-done | bytes 1048608 | tf_op jit(solution)/shard_map/ppermute | solution.py:24
  72.7 2.1 collective-permute-start.2
  74.8 0.8 slice.172
  75.6 19.5 %collective-permute-done.5.refs_4_ = bf16[2048,256]{1,0:T(8,128)(2,1)S(1)} collective-permute-done((bf16[2048,256]{1,0:T(8,128)(2,1)}, bf16[2048,256]{1,0:T(8,128)(2,1)S(1)}, u32[]{:S(2)}, u32[]{:S(2)}) %collective-permute-start.5) | collective-permute-done | bytes 1048608 | tf_op jit(solution)/shard_map/ppermute | solution.py:24
  95.1 0.9 slice.173
  96.0 2.0 collective-permute-start.6
  98.0 0.8 slice.174
  98.8 18.8 %collective-permute-done.9.refs_7_ = bf16[256,2048]{1,0:T(8,128)(2,1)S(1)} collective-permute-done((bf16[256,2048]{1,0:T(8,128)(2,1)}, bf16[256,2048]{1,0:T(8,128)(2,1)S(1)}, u32[]{:S(2)}, u32[]{:S(2)}) %collective-permute-start.9) | collective-permute-done | bytes 1048608 | tf_op jit(solution)/shard_map/ppermute | solution.py:24
  117.6 0.9 slice.175
  118.5 2.0 collective-permute-start.11
  120.5 0.8 slice.176
  121.3 7.5 %collective-permute-done.2.refs_1_ = bf16[1024,256]{1,0:T(8,128)(2,1)S(1)} collective-permute-done((bf16[1024,256]{1,0:T(8,128)(2,1)S(1)}, bf16[1024,256]{1,0:T(8,128)(2,1)S(1)}, u32[]{:S(2)}, u32[]{:S(2)}) %collective-permute-start.2) | collective-permute-done | bytes 524320 | tf_op jit(solution)/shard_map/ppermute | solution.py:24
  128.9 1.4 copy-done.1
  130.3 6.9 %near_hidden.1.refs_5_ = bf16[512,768]{1,0:T(8,128)(2,1)} custom-call(bf16[512,2048]{1,0:T(8,128)(2,1)} %bitcast.37, bf16[2048,256]{1,0:T(8,128)(2,1)} %bitcast.42, bf16[2048,256]{1,0:T(8,128)(2,1)} %bitcast.47, bf16[2048,256]{1,0:T(8,128)(2,1)} %copy-done.3, bf16[2048,256]{1,0:T(8,128)(2,1)} %copy-done.5, bf16[2048,256]{1,0:T(8,128)(2,1)} %copy-done.4, ...), custom_call_target="tpu_custom_call" | custom-call | tf_op jit(solution)/shard_map/near_hidden/pallas_call | solution.py:164
  137.3 2.9 %collective-permute-done.6.refs_3_ = bf16[1024,256]{1,0:T(8,128)(2,1)} collective-permute-done((bf16[1024,256]{1,0:T(8,128)(2,1)}, bf16[1024,256]{1,0:T(8,128)(2,1)}, u32[]{:S(2)}, u32[]{:S(2)}) %collective-permute-start.6) | collective-permute-done | bytes 524320 | tf_op jit(solution)/shard_map/ppermute | solution.py:24
  140.2 10.4 %collective-permute-done.11.refs_9_ = bf16[128,2048]{1,0:T(8,128)(2,1)} collective-permute-done((bf16[128,2048]{1,0:T(8,128)(2,1)}, bf16[128,2048]{1,0:T(8,128)(2,1)}, u32[]{:S(2)}, u32[]{:S(2)}) %collective-permute-start.11) | collective-permute-done | bytes 524320 | tf_op jit(solution)/shard_map/ppermute | solution.py:24
  150.5 7.3 %expert_rows.1 = bf16[512,2048]{1,0:T(8,128)(2,1)} custom-call(bf16[512,2048]{1,0:T(8,128)(2,1)} %bitcast.38, bf16[1024,256]{1,0:T(8,128)(2,1)} %copy-done.11, bf16[1024,256]{1,0:T(8,128)(2,1)} %copy-done.12, bf16[1024,256]{1,0:T(8,128)(2,1)} %collective-permute-done.6.refs_3_, bf16[1024,256]{1,0:T(8,128)(2,1)} %collective-permute-done.8.refs_4_, ...), custom_call_target="tpu_custom_call" | custom-call | tf_op jit(solution)/shard_map/expert_rows/pallas_call | solution.py:214
  157.9 10.3 %all-to-all-start.2 = ((bf16[64,8,2048]{2,1,0:T(8,128)(2,1)}), bf16[64,8,2048]{2,1,0:T(8,128)(2,1)S(1)}, u32[]{:S(2)}, u32[]{:S(2)}) async-start(bf16[64,8,2048]{2,1,0:T(8,128)(2,1)} %bitcast.40), calls=%async_computation.2 | async-start | bytes 4194304 | tf_op jit(solution)/shard_map/all_to_all | solution.py:303
  169.6 49.8 %all-to-all-done.2 = bf16[64,8,2048]{2,1,0:T(8,128)(2,1)S(1)} async-done(((bf16[64,8,2048]{2,1,0:T(8,128)(2,1)}), bf16[64,8,2048]{2,1,0:T(8,128)(2,1)S(1)}, u32[]{:S(2)}, u32[]{:S(2)}) %all-to-all-start.2) | async-done | bytes 2097184 | tf_op jit(solution)/shard_map/all_to_all | solution.py:303
  219.4 1.3 copy-done.2
  220.8 3.6 %combine.1 = bf16[128,2048]{1,0:T(8,128)(2,1)} custom-call(f32[128,2048]{1,0:T(8,128)} %get-tuple-element.7.stream_ref, s32[128,2]{1,0:T(8,128)} %multiply_add_fusion.slots_ref, f32[128,2]{1,0:T(8,128)} %copy.21.weights_ref, bf16[512,2048]{1,0:T(8,128)(2,1)} %bitcast.39), custom_call_target="tpu_custom_call" | custom-call | tf_op jit(solution)/shard_map/combine/pallas_call | solution.py:306
  (61 shorter events, 7.4 us)
Async XLA Ops:
  0.0 3.5 %copy-start = (s32[512,2]{0,1:T(2,128)S(1)}, s32[512,2]{0,1:T(2,128)}, u32[]{:S(2)}) copy-start(s32[512,2]{0,1:T(2,128)} %param.23) | copy-start | bytes 12292
  1.6 5.1 %collective-permute-start = (bf16[32,256]{1,0:T(8,128)(2,1)S(1)}, bf16[32,256]{1,0:T(8,128)(2,1)S(1)}, u32[]{:S(2)}, u32[]{:S(2)}) collective-permute-start(bf16[32,256]{1,0:T(8,128)(2,1)S(1)} %fusion.5), channel_id=1, source_target_pairs={{0,4},{4,8},{8,12},{12,16},{16,20},{20,24},{24,28},{28,32},{32,36}... | collective-permute-start | bytes 49160 | tf_op jit(solution)/shard_map/ppermute | solution.py:19
  6.6 2.4 %copy-start.13 = (bf16[32,256]{1,0:T(8,128)(2,1)}, bf16[32,256]{1,0:T(8,128)(2,1)S(1)}, u32[]{:S(2)}) copy-start(bf16[32,256]{1,0:T(8,128)(2,1)S(1)} %collective-permute-done.rim_ref) | copy-start | bytes 49156
  15.1 11.3 %all-to-all-start = ((bf16[4,128,256]{2,1,0:T(8,128)(2,1)}), bf16[4,128,256]{2,1,0:T(8,128)(2,1)S(1)}, u32[]{:S(2)}, u32[]{:S(2)}) async-start(bf16[4,128,256]{2,1,0:T(8,128)(2,1)} %bitcast.48), calls=%async_computation | async-start | bytes 524288 | tf_op jit(solution)/shard_map/all_to_all | solution.py:275
  26.4 0.7 copy-start.10
  32.5 12.8 %copy-start.9 = (bf16[1,2048,256]{2,1,0:T(8,128)(2,1)S(1)}, bf16[1,2048,256]{2,1,0:T(8,128)(2,1)}, u32[]{:S(2)}) copy-start(bf16[1,2048,256]{2,1,0:T(8,128)(2,1)} %param.25) | copy-start | bytes 3145732
  32.5 96.5 %all-to-all-start.1 = ((bf16[64,8,2048]{2,1,0:T(8,128)(2,1)}), bf16[64,8,2048]{2,1,0:T(8,128)(2,1)S(1)}, u32[]{:S(2)}, u32[]{:S(2)}) async-start(bf16[64,8,2048]{2,1,0:T(8,128)(2,1)} %bitcast.41), calls=%async_computation.1 | async-start | bytes 4194304 | tf_op jit(solution)/shard_map/all_to_all | solution.py:294
  45.3 27.3 %collective-permute-start.1 = (bf16[2048,256]{1,0:T(8,128)(2,1)S(1)}, bf16[2048,256]{1,0:T(8,128)(2,1)S(1)}, u32[]{:S(2)}, u32[]{:S(2)}) collective-permute-start(bf16[2048,256]{1,0:T(8,128)(2,1)S(1)} %bitcast.43), channel_id=1, source_target_pairs={{0,1},{1,2},{2,3},{3,0},{4,5},{5,6},{6,7},{7,4},{8,9},{9,10},{10,1... | collective-permute-start | bytes 3145736 | tf_op jit(solution)/shard_map/ppermute | solution.py:24
  46.0 26.7 %collective-permute-start.3 = (bf16[2048,256]{1,0:T(8,128)(2,1)S(1)}, bf16[2048,256]{1,0:T(8,128)(2,1)S(1)}, u32[]{:S(2)}, u32[]{:S(2)}) collective-permute-start(bf16[2048,256]{1,0:T(8,128)(2,1)S(1)} %bitcast.44), channel_id=1, source_target_pairs={{0,3},{1,0},{2,1},{3,2},{4,7},{5,4},{6,5},{7,6},{8,11},{9,8},{10,9... | collective-permute-start | bytes 3145736 | tf_op jit(solution)/shard_map/ppermute | solution.py:24
  48.6 46.5 %collective-permute-start.5 = (bf16[2048,256]{1,0:T(8,128)(2,1)}, bf16[2048,256]{1,0:T(8,128)(2,1)S(1)}, u32[]{:S(2)}, u32[]{:S(2)}) collective-permute-start(bf16[2048,256]{1,0:T(8,128)(2,1)} %bitcast.45), channel_id=1, source_target_pairs={{0,1},{1,2},{2,3},{3,0},{4,5},{5,6},{6,7},{7,4},{8,9},{9,10},{10,1... | collective-permute-start | bytes 3145736 | tf_op jit(solution)/shard_map/ppermute | solution.py:24
  48.6 47.4 %collective-permute-start.7 = (bf16[2048,256]{1,0:T(8,128)(2,1)}, bf16[2048,256]{1,0:T(8,128)(2,1)S(1)}, u32[]{:S(2)}, u32[]{:S(2)}) collective-permute-start(bf16[2048,256]{1,0:T(8,128)(2,1)} %bitcast.46), channel_id=1, source_target_pairs={{0,3},{1,0},{2,1},{3,2},{4,7},{5,4},{6,5},{7,6},{8,11},{9,8},{10,9... | collective-permute-start | bytes 3145736 | tf_op jit(solution)/shard_map/ppermute | solution.py:24
  51.9 65.7 %collective-permute-start.9 = (bf16[256,2048]{1,0:T(8,128)(2,1)}, bf16[256,2048]{1,0:T(8,128)(2,1)S(1)}, u32[]{:S(2)}, u32[]{:S(2)}) collective-permute-start(bf16[256,2048]{1,0:T(8,128)(2,1)} %bitcast.49), channel_id=1, source_target_pairs={{0,1},{1,2},{2,3},{3,0},{4,5},{5,6},{6,7},{7,4},{8,9},{9,10},{10,1... | collective-permute-start | bytes 3145736 | tf_op jit(solution)/shard_map/ppermute | solution.py:24
  72.6 26.2 %copy-start.3 = (bf16[2048,256]{1,0:T(8,128)(2,1)}, bf16[2048,256]{1,0:T(8,128)(2,1)S(1)}, u32[]{:S(2)}) copy-start(bf16[2048,256]{1,0:T(8,128)(2,1)S(1)} %collective-permute-done.1.refs_3_) | copy-start | bytes 3145732
  72.6 45.8 %collective-permute-start.10 = (bf16[256,2048]{1,0:T(8,128)(2,1)}, bf16[256,2048]{1,0:T(8,128)(2,1)S(1)}, u32[]{:S(2)}, u32[]{:S(2)}) collective-permute-start(bf16[256,2048]{1,0:T(8,128)(2,1)} %bitcast.50), channel_id=1, source_target_pairs={{0,3},{1,0},{2,1},{3,2},{4,7},{5,4},{6,5},{7,6},{8,11},{9,8},{10,9... | collective-permute-start | bytes 3145736 | tf_op jit(solution)/shard_map/ppermute | solution.py:24
  72.7 45.8 %copy-start.4 = (bf16[2048,256]{1,0:T(8,128)(2,1)}, bf16[2048,256]{1,0:T(8,128)(2,1)S(1)}, u32[]{:S(2)}) copy-start(bf16[2048,256]{1,0:T(8,128)(2,1)S(1)} %collective-permute-done.3.refs_5_) | copy-start | bytes 3145732
  72.7 56.1 %collective-permute-start.2 = (bf16[1024,256]{1,0:T(8,128)(2,1)S(1)}, bf16[1024,256]{1,0:T(8,128)(2,1)S(1)}, u32[]{:S(2)}, u32[]{:S(2)}) collective-permute-start(bf16[1024,256]{1,0:T(8,128)(2,1)S(1)} %slice.171), channel_id=1, source_target_pairs={{0,1},{1,2},{2,3},{3,0},{4,5},{5,6},{6,7},{7,4},{8,9},{9,10},{10,1... | collective-permute-start | bytes 1572872 | tf_op jit(solution)/shard_map/ppermute | solution.py:24
  95.1 26.2 %copy-start.5 = (bf16[2048,256]{1,0:T(8,128)(2,1)}, bf16[2048,256]{1,0:T(8,128)(2,1)S(1)}, u32[]{:S(2)}) copy-start(bf16[2048,256]{1,0:T(8,128)(2,1)S(1)} %collective-permute-done.5.refs_4_) | copy-start | bytes 3145732
  95.1 42.1 %collective-permute-start.4 = (bf16[1024,256]{1,0:T(8,128)(2,1)}, bf16[1024,256]{1,0:T(8,128)(2,1)S(1)}, u32[]{:S(2)}, u32[]{:S(2)}) collective-permute-start(bf16[1024,256]{1,0:T(8,128)(2,1)} %slice.172), channel_id=1, source_target_pairs={{0,3},{1,0},{2,1},{3,2},{4,7},{5,4},{6,5},{7,6},{8,11},{9,8},{10,9... | collective-permute-start | bytes 1572872 | tf_op jit(solution)/shard_map/ppermute | solution.py:24
  96.0 32.8 %copy-start.6 = (bf16[2048,256]{1,0:T(8,128)(2,1)}, bf16[2048,256]{1,0:T(8,128)(2,1)S(1)}, u32[]{:S(2)}) copy-start(bf16[2048,256]{1,0:T(8,128)(2,1)S(1)} %collective-permute-done.7.refs_6_) | copy-start | bytes 3145732
  96.0 44.1 %collective-permute-start.6 = (bf16[1024,256]{1,0:T(8,128)(2,1)}, bf16[1024,256]{1,0:T(8,128)(2,1)}, u32[]{:S(2)}, u32[]{:S(2)}) collective-permute-start(bf16[1024,256]{1,0:T(8,128)(2,1)} %slice.173), channel_id=1, source_target_pairs={{0,1},{1,2},{2,3},{3,0},{4,5},{5,6},{6,7},{7,4},{8,9},{9,10},{10,1... | collective-permute-start | bytes 1572872 | tf_op jit(solution)/shard_map/ppermute | solution.py:24
  117.6 11.2 %copy-start.7 = (bf16[256,2048]{1,0:T(8,128)(2,1)}, bf16[256,2048]{1,0:T(8,128)(2,1)S(1)}, u32[]{:S(2)}) copy-start(bf16[256,2048]{1,0:T(8,128)(2,1)S(1)} %collective-permute-done.9.refs_7_) | copy-start | bytes 3145732
  117.6 22.6 %collective-permute-start.8 = (bf16[1024,256]{1,0:T(8,128)(2,1)}, bf16[1024,256]{1,0:T(8,128)(2,1)}, u32[]{:S(2)}, u32[]{:S(2)}) collective-permute-start(bf16[1024,256]{1,0:T(8,128)(2,1)} %slice.174), channel_id=1, source_target_pairs={{0,3},{1,0},{2,1},{3,2},{4,7},{5,4},{6,5},{7,6},{8,11},{9,8},{10,9... | collective-permute-start | bytes 1572872 | tf_op jit(solution)/shard_map/ppermute | solution.py:24
  118.5 10.4 %copy-start.8 = (bf16[256,2048]{1,0:T(8,128)(2,1)}, bf16[256,2048]{1,0:T(8,128)(2,1)S(1)}, u32[]{:S(2)}) copy-start(bf16[256,2048]{1,0:T(8,128)(2,1)S(1)} %collective-permute-done.10.refs_8_) | copy-start | bytes 3145732
  118.5 32.1 %collective-permute-start.11 = (bf16[128,2048]{1,0:T(8,128)(2,1)}, bf16[128,2048]{1,0:T(8,128)(2,1)}, u32[]{:S(2)}, u32[]{:S(2)}) collective-permute-start(bf16[128,2048]{1,0:T(8,128)(2,1)} %slice.175), channel_id=1, source_target_pairs={{0,1},{1,2},{2,3},{3,0},{4,5},{5,6},{6,7},{7,4},{8,9},{9,10},{10,1... | collective-permute-start | bytes 1572872 | tf_op jit(solution)/shard_map/ppermute | solution.py:24
  128.8 21.7 %copy-start.11 = (bf16[1024,256]{1,0:T(8,128)(2,1)}, bf16[1024,256]{1,0:T(8,128)(2,1)S(1)}, u32[]{:S(2)}) copy-start(bf16[1024,256]{1,0:T(8,128)(2,1)S(1)} %collective-permute-done.2.refs_1_) | copy-start | bytes 1572868
  128.8 21.7 %collective-permute-start.12 = (bf16[128,2048]{1,0:T(8,128)(2,1)}, bf16[128,2048]{1,0:T(8,128)(2,1)}, u32[]{:S(2)}, u32[]{:S(2)}) collective-permute-start(bf16[128,2048]{1,0:T(8,128)(2,1)} %slice.176), channel_id=1, source_target_pairs={{0,3},{1,0},{2,1},{3,2},{4,7},{5,4},{6,5},{7,6},{8,11},{9,8},{10,9... | collective-permute-start | bytes 1572872 | tf_op jit(solution)/shard_map/ppermute | solution.py:24
  128.9 1.4 copy-start.1
  137.3 13.3 %copy-start.12 = (bf16[1024,256]{1,0:T(8,128)(2,1)}, bf16[1024,256]{1,0:T(8,128)(2,1)S(1)}, u32[]{:S(2)}) copy-start(bf16[1024,256]{1,0:T(8,128)(2,1)S(1)} %collective-permute-done.4.refs_2_) | copy-start | bytes 1572868
  157.9 61.6 %all-to-all-start.2 = ((bf16[64,8,2048]{2,1,0:T(8,128)(2,1)}), bf16[64,8,2048]{2,1,0:T(8,128)(2,1)S(1)}, u32[]{:S(2)}, u32[]{:S(2)}) async-start(bf16[64,8,2048]{2,1,0:T(8,128)(2,1)} %bitcast.40), calls=%async_computation.2 | async-start | bytes 4194304 | tf_op jit(solution)/shard_map/all_to_all | solution.py:303
  219.4 1.3 copy-start.2

commit v3 on v1

v3 whole, which is shorter than its diff:
```python
import functools

import jax
import jax.numpy as jnp
from jax import lax
from jax.experimental import pallas as pl
from jax.experimental.pallas import tpu as pltpu
from jax.sharding import PartitionSpec as P

TAPS = 31
RIM = 32
FIRST = 3
LANES = 128
BLOCK = 64


def passed_along(value, axis, steps):
    count = lax.axis_size(axis)
    initial, last = (max(0, -steps), min(count, count - steps))
    return lax.ppermute(value, axis, [(source, source + steps) for source in range(initial, last)])


def ring(value, axis, steps):
    count = lax.axis_size(axis)
    return lax.ppermute(value, axis, [(i, (i + steps) % count) for i in range(count)])


def slot_numbers(block_routes, capacity, experts_n):
    route_pairs = block_routes.reshape(block_routes.shape[:-2] + (-1,))
    onehot = (route_pairs[..., None] == jnp.arange(experts_n, dtype=jnp.int32)).astype(jnp.int32)
    slot_rank = jnp.sum((jnp.cumsum(onehot, axis=-2) - onehot) * onehot, axis=-1)
    return (route_pairs * capacity + slot_rank).reshape(block_routes.shape)


def kernel(body, out, args, scratch=(), limit=16, far_in=(), far_out=()):
    whole, far = pl.BlockSpec(memory_space=pltpu.VMEM), pl.BlockSpec(memory_space=pltpu.HBM)
    args = [
        pltpu.with_memory_space_constraint(a, pltpu.HBM if i in far_in else pltpu.VMEM)
        for i, a in enumerate(args)
    ]
    outs = out if isinstance(out, list) else [out]
    got = pl.pallas_call(
        body,
        out_shape=[
            pltpu.HBM(*o) if i in far_out else jax.ShapeDtypeStruct(*o) for i, o in enumerate(outs)
        ],
        in_specs=[far if i in far_in else whole for i in range(len(args))],
        out_specs=[far if i in far_out else whole for i in range(len(outs))],
        scratch_shapes=scratch,
        compiler_params=pltpu.CompilerParams(vmem_limit_bytes=limit << 20),
    )(*args)
    return got if isinstance(out, list) else got[0]


def fetch(copies, sems, first=0):
    started = [
        pltpu.make_async_copy(src, dst, sems.at[first + i]) for i, (src, dst) in enumerate(copies)
    ]
    for c in started:
        c.start()
    return started


def gated_rows(value, gate):
    return (value.astype(jnp.float32) * jax.nn.sigmoid(gate.astype(jnp.float32))).astype(jnp.bfloat16)


def rim_body(value_ref, gate_ref, segments_ref, out_ref):
    width = value_ref.shape[1]
    gated = gated_rows(value_ref[...], gate_ref[...]).astype(jnp.float32)
    last = segments_ref[segments_ref.shape[0] - 1 :, :].astype(jnp.float32)
    named = jnp.concatenate([last] + [jnp.zeros_like(last)] * (width // LANES - 1), axis=1)
    row = lax.broadcasted_iota(jnp.int32, gated.shape, 0)
    out_ref[...] = jnp.where(row == 0, named, gated).astype(jnp.bfloat16)


def rim_rows(value, gate, segments):
    tok, width = value.shape
    last = pl.BlockSpec((RIM, width), lambda i: (tok // RIM - 1, 0))
    return pl.pallas_call(
        rim_body,
        grid=(1,),
        in_specs=[last, last, pl.BlockSpec(segments.shape, lambda i: (0, 0))],
        out_specs=pl.BlockSpec((RIM, width), lambda i: (0, 0)),
        out_shape=jax.ShapeDtypeStruct((RIM, width), jnp.bfloat16),
        name="rim_rows",
    )(value, gate, segments)


def conv_body(value_ref, gate_ref, rim_ref, segments_ref, seen_ref, taps_ref, gain_ref, shift_ref, out_ref, rows_ref):
    tok = value_ref.shape[0]
    rows_ref[0, :RIM] = rim_ref[...].astype(jnp.float32)
    rows_ref[0, RIM:] = gated_rows(value_ref[...], gate_ref[...]).astype(jnp.float32)
    for r in range(1, 8):
        rows_ref[r, 8:] = rows_ref[0, 8 - r : RIM + tok - r]
    lane = lax.broadcasted_iota(jnp.int32, (1, LANES), 1)
    same = rim_ref[0:1, :LANES].astype(jnp.float32) == segments_ref[0:1, 0:1].astype(jnp.float32)
    same = jnp.where(same & (lane >= LANES - (TAPS - 1)), 1.0, 0.0)
    before = jnp.sum(same, axis=1, keepdims=True).astype(jnp.int32)

    def block(i, carry):
        at = pl.multiple_of(i * BLOCK, BLOCK)
        seen = seen_ref[pl.ds(at, BLOCK), :]
        row = at + lax.broadcasted_iota(jnp.int32, (BLOCK, LANES), 0)
        seen = jnp.where(seen == row, seen + before, seen)
        for lane in range(0, value_ref.shape[1], LANES):
            cols = slice(lane, lane + LANES)
            total = rows_ref[0, pl.ds(at + RIM, BLOCK), cols] * taps_ref[TAPS - 1 : TAPS, cols]
            for back in range(1, TAPS):
                tap = TAPS - 1 - back
                rows = rows_ref[back % 8, pl.ds(at + RIM - back // 8 * 8, BLOCK), cols]
                total = total + jnp.where(seen >= back, rows * taps_ref[tap : tap + 1, cols], 0.0)
            dev = total - jnp.mean(total, axis=1, keepdims=True)
            var = jnp.mean(dev * dev, axis=1, keepdims=True)
            v = dev * lax.rsqrt(var + 1e-05) * gain_ref[:, cols] + shift_ref[:, cols]
            out_ref[pl.ds(at, BLOCK), cols] = (v / (1.0 + jnp.exp(-v))).astype(jnp.bfloat16)
        return carry

    lax.fori_loop(0, tok // BLOCK, block, 0)


def conv_module(value, gate, rim, segments, seen, taps, gain, shift):
    tok, width = value.shape
    return kernel(
        conv_body,
        ((tok, width), jnp.bfloat16),
        (value, gate, rim, segments, seen, taps, gain[None], shift[None]),
        scratch=[pltpu.VMEM((8, RIM + tok, width), jnp.float32)],
    )


def dot(a, b):
    return jnp.dot(a, b, preferred_element_type=jnp.float32)


def places(slots, total):
    numbers = lax.broadcasted_iota(jnp.int32, (slots.shape[0], total), 1)
    return [numbers == slots[:, m : m + 1] for m in range(slots.shape[1])]


def route_body(
    parts_ref, residual_ref, gain_ref, slots_ref, weight_ref, stream_out, sent_out, w_ref, stream_ref, sent_ref, sems
):
    parts_n, _, width = parts_ref.shape
    spans = [slice(j * width, (j + 1) * width) for j in range(parts_n)]
    loads = fetch([(weight_ref.at[rows], w_ref.at[rows]) for rows in spans], sems)
    table = functools.reduce(jnp.logical_or, places(slots_ref[...], sent_ref.shape[0]))
    table = jnp.where(table, 1.0, 0.0).astype(jnp.bfloat16)
    for j, rows in enumerate(spans):
        loads[j].wait()
        part = dot(parts_ref[j], w_ref[rows])
        stream_ref[...] = part if j == 0 else stream_ref[...] + part
    mixed = stream_ref[...].astype(jnp.bfloat16).astype(jnp.float32)
    stream = residual_ref[...].astype(jnp.float32) + mixed
    stream_ref[...] = stream
    stores = fetch([(stream_ref, stream_out)], sems, parts_n)
    scale = lax.rsqrt(jnp.mean(stream * stream, axis=1, keepdims=True) + 1e-06)
    normed = (stream * scale * gain_ref[...]).astype(jnp.bfloat16)
    step = normed.shape[1] // 4
    for j in range(4):
        cols = slice(j * step, (j + 1) * step)
        sent_ref[:, cols] = lax.dot_general(
            table, normed[:, cols], (((0,), (0,)), ((), ())), preferred_element_type=jnp.float32
        ).astype(jnp.bfloat16)
        stores += fetch([(sent_ref.at[:, cols], sent_out.at[:, cols])], sems, parts_n + 1 + j)
    for c in stores:
        c.wait()


def combine_body(stream_in, slots_ref, weights_ref, *refs):
    *back_refs, out, stream_ref, out_ref, sems = refs
    (load,) = fetch([(stream_in, stream_ref)], sems)
    hits = places(slots_ref[...], back_refs[0].shape[0])
    table = sum(jnp.where(hit, weights_ref[:, m : m + 1], 0.0) for m, hit in enumerate(hits))
    high = table.astype(jnp.bfloat16)
    low = (table - high.astype(jnp.float32)).astype(jnp.bfloat16)
    load.wait()
    at, stores = 0, []
    for i, back in enumerate(back_refs):
        cols = slice(at, at + back.shape[1])
        rows = back[...]
        mixed = dot(high, rows) + dot(low, rows)
        out_ref[:, cols] = (stream_ref[:, cols] + mixed).astype(jnp.bfloat16)
        stores += fetch([(out_ref.at[:, cols], out.at[:, cols])], sems, 1 + i)
        at += back.shape[1]
    for c in stores:
        c.wait()


def hidden_body(counts, *refs):
    rows_in, *pieces, out_ref, rows_ref, w_ref, sems = refs
    width = pieces[0].shape[1]
    (load,) = fetch([(rows_in, rows_ref)], sems, len(pieces))
    loads = []
    for q, kinds in enumerate(counts):
        copies = []
        for kind, n in enumerate(kinds):
            top = 0
            for piece in pieces[:n]:
                end = top + piece.shape[0]
                copies.append((piece, w_ref.at[q, top:end, kind * width : (kind + 1) * width]))
                top = end
            pieces = pieces[n:]
        loads.append(fetch(copies, sems, sum(len(c) for c in loads)))
    load.wait()
    for q, copies in enumerate(loads):
        for c in copies:
            c.wait()
        act = dot(rows_ref[...], w_ref[q])
        gate = act[:, :width]
        hidden = gate / (1.0 + jnp.exp(-gate)) * act[:, width:]
        out_ref[:, q * width : (q + 1) * width] = hidden.astype(jnp.bfloat16)


def hidden_units(rows, quarters):
    counts = tuple((len(gates), len(ups)) for gates, ups in quarters)
    pieces = [p for gates, ups in quarters for p in (*gates, *ups)]
    (n, d), width = rows.shape, pieces[0].shape[1]
    return kernel(
        functools.partial(hidden_body, counts),
        ((n, width * len(counts)), jnp.bfloat16),
        (rows, *pieces),
        scratch=[
            pltpu.VMEM((n, d), jnp.bfloat16),
            pltpu.VMEM((len(counts), d, 2 * width), jnp.bfloat16),
            pltpu.SemaphoreType.DMA((len(pieces) + 1,)),
        ],
        limit=20,
        far_in=range(1 + len(pieces)),
    )


def down_body(cols, hidden_ref, own_ref, *refs):
    *pieces, out, down_ref, out_ref, sems = refs
    at = own_ref.shape[0]
    down_ref[:at] = own_ref[:, cols]
    for piece in pieces:
        down_ref[at : at + piece.shape[0]] = piece[...]
        at += piece.shape[0]
    half = out_ref.shape[1] // 2
    stores = []
    for i in range(2):
        span = slice(i * half, (i + 1) * half)
        out_ref[:, span] = dot(hidden_ref[...], down_ref[:, span]).astype(jnp.bfloat16)
        stores += fetch([(out_ref.at[:, span], out.at[:, span])], sems, i)
    for c in stores:
        c.wait()


def down_rows(hidden, own, pieces, cols):
    n, width = hidden.shape[0], cols.stop - cols.start
    return kernel(
        functools.partial(down_body, cols),
        ((n, width), jnp.bfloat16),
        (hidden, own, *pieces),
        scratch=[
            pltpu.VMEM((hidden.shape[1], width), jnp.bfloat16),
            pltpu.VMEM((n, width), jnp.bfloat16),
            pltpu.SemaphoreType.DMA((2,)),
        ],
        limit=16,
        far_out=(0,),
    )


def gathered(shard, parts):
    half = shard.shape[0] // 2
    pieces = [shard] if parts == 1 else [shard[:half], shard[half:]]
    left, right = [], []
    for piece in pieces:
        left.append(ring(piece, "tp", 1))
        right.append(ring(piece, "tp", -1))
    far = [ring(left[0][:half], "tp", 1), ring(right[-1][-half:], "tp", -1)]
    return left, right, far


def shards(
    residual,
    conv_value,
    conv_gate,
    segments,
    conv_weight,
    norm_gain,
    norm_shift,
    out_weight,
    ffn_gain,
    routes,
    route_weights,
    w_gate,
    w_up,
    w_down,
):
    tok_dev, local_channels = conv_value.shape
    reach = conv_weight.shape[0] - 1
    model_width = w_down.shape[2]
    gates = gathered(w_gate[0], 2)
    ups = gathered(w_up[0], 1)
    cut = model_width * FIRST // 8
    groups = slice(0, cut), slice(cut, model_width)
    downs = [gathered(w_down[0][:, cols], 1) for cols in groups]
    lines = segments.reshape(tok_dev // LANES, LANES)
    rim = passed_along(rim_rows(conv_value, conv_gate, lines), "sp", 1)
    padded = jnp.pad(segments, (reach, 0), constant_values=-1)
    seen = jnp.zeros((tok_dev,), jnp.int32)
    for offset in range(reach):
        seen = seen + (padded[offset : offset + tok_dev] == segments).astype(jnp.int32)
    seen = jnp.broadcast_to(seen[:, None], (tok_dev, LANES))
    conv_out = conv_module(
        conv_value, conv_gate, rim, lines, seen, conv_weight, norm_gain, norm_shift
    )
    columns = lax.axis_size("tp")
    column = lax.axis_index("tp")
    rows_own = tok_dev // columns
    regrouped = lax.all_to_all(
        conv_out.reshape(columns, rows_own, local_channels), "tp", 0, 0, tiled=True
    )
    experts_n = lax.axis_size("sp")
    top_count = routes.shape[1]
    capacity = max(2, 2 * tok_dev * top_count // (columns * experts_n))
    slot_total = experts_n * capacity
    own_routes = lax.dynamic_slice_in_dim(routes, column * rows_own, rows_own, 0)
    own_weights = lax.dynamic_slice_in_dim(route_weights, column * rows_own, rows_own, 0)
    own_slots = slot_numbers(own_routes, capacity, experts_n)
    stream, outgoing = kernel(
        route_body,
        [((rows_own, model_width), jnp.float32), ((slot_total, model_width), jnp.bfloat16)],
        (regrouped, residual, ffn_gain[None], own_slots, out_weight),
        scratch=[
            pltpu.VMEM(out_weight.shape, jnp.bfloat16),
            pltpu.VMEM((rows_own, model_width), jnp.float32),
            pltpu.VMEM((slot_total, model_width), jnp.bfloat16),
            pltpu.SemaphoreType.DMA((columns + 5,)),
        ],
        limit=24,
        far_in=(4,),
        far_out=(0, 1),
    )
    arrived = lax.all_to_all(
        outgoing.reshape(experts_n, capacity, model_width), "sp", 0, 0, tiled=True
    ).reshape(slot_total, model_width)
    hidden = hidden_units(
        arrived,
        [([w_gate[0]], [w_up[0]])] + [(gates[side], ups[side]) for side in range(3)],
    )
    back = []
    for cols, (left, right, far) in zip(groups, downs):
        out = down_rows(hidden, w_down[0], [*left, *right, *far], cols)
        back.append(
            lax.all_to_all(
                out.reshape(experts_n, capacity, -1), "sp", 0, 0, tiled=True
            ).reshape(slot_total, -1)
        )
    return kernel(
        combine_body,
        ((rows_own, model_width), jnp.bfloat16),
        (stream, own_slots, own_weights, *back),
        scratch=[
            pltpu.VMEM((rows_own, model_width), jnp.float32),
            pltpu.VMEM((rows_own, model_width), jnp.bfloat16),
            pltpu.SemaphoreType.DMA((1 + len(back),)),
        ],
        limit=24,
        far_in=(0,),
        far_out=(0,),
    )


def solution(mesh):
    return jax.shard_map(
        shards,
        mesh=mesh,
        in_specs=(
            P(("sp", "tp"), None),
            P("sp", "tp"),
            P("sp", "tp"),
            P("sp"),
            P(None, "tp"),
            P("tp"),
            P("tp"),
            P(),
            P(),
            P("sp", None),
            P("sp", None),
            P("sp", None, "tp"),
            P("sp", None, "tp"),
            P("sp", "tp", None),
        ),
        out_specs=P(("sp", "tp"), None),
        check_vma=False,
    )
```

time: 280 us -> 241 us (0.86)
  matrix products: 49.8 us -> 0 us
  waiting for transfers between devices: 158 us -> 138 us
  Pallas kernels: 6.12 us -> 25.9 us
  starting transfers between devices: 45.4 us -> 64.1 us
  local copies, waits for them, and re-layouts: 13.2 us -> 8.21 us
  other arithmetic: 6.64 us -> 2.68 us
    dot_general x22 -> x0, matrix products: 49.8 us -> none  [dot(): return jnp.dot(a, b, preferred_element_type=jnp.float32)]
    all_to_all x3 -> x4, waiting for transfers between devices: 77.5 us -> 41.3 us  [the longest x2 33.6 us: shards(): lax.all_to_all(out.reshape(experts_n, capacity, -1), 'sp', 0, 0, tiled=True)]
    pallas_call x1 -> x7, Pallas kernels: 6.12 us -> 25.9 us  [the longest x6 24.5 us: kernel(): pl.pallas_call(body, out_shape=[pltpu.HBM(*o) if i in far_out else jax.Sh...]
    ppermute x18, waiting for transfers between devices: 78.9 us -> 97 us  [ring(): lax.ppermute(value, axis, [(i, (i + steps) % count) for i in range(count)])]
    all_to_all x3 -> x4, starting transfers between devices: 25.8 us -> 37.6 us  [the longest x2 20.5 us: shards(): lax.all_to_all(out.reshape(experts_n, capacity, -1), 'sp', 0, 0, tiled=True)]
    ppermute x18, starting transfers between devices: 17.6 us -> 24.6 us  [ring(): lax.ppermute(value, axis, [(i, (i + steps) % count) for i in range(count)])]
    unnamed x21 -> x44, local copies, waits for them, and re-layouts: 0.96 us -> 5.78 us
    slice x5 -> x10, local copies, waits for them, and re-layouts: 4.89 us -> 1.19 us  [the longest x6 0.85 us: gathered(): far = [ring(left[0][:half], 'tp', 1), ring(right[-1][-half:], 'tp', -1)]]
  transfers between devices with their start and end apart: 22 -> 23, of which waited for: 12 -> 10; matrix products, arithmetic and copies ran while one was open for 14% -> 2% of each run, Pallas kernels for 0% -> 4%
where the time goes in v3:
time: 241 us; the launch traced here: 240 us
  waiting for transfers between devices  138 us (57%)
  starting transfers between devices  64.1 us (27%)
  Pallas kernels  25.9 us (11%)
  local copies, waits for them, and re-layouts  8.21 us (3%)
  other arithmetic  2.68 us (1%)
    ppermute x18, waiting for transfers between devices, ring(): lax.ppermute(value, axis, [(i, (i + steps) % count) for i in range(count)])  97 us
    all_to_all x2, waiting for transfers between devices, shards(): lax.all_to_all(out.reshape(experts_n, capacity, -1), 'sp', 0, 0, tiled=True)  33.6 us
    ppermute x18, starting transfers between devices, ring(): lax.ppermute(value, axis, [(i, (i + steps) % count) for i in range(count)])  24.6 us
    pallas_call x6, Pallas kernels, kernel(): pl.pallas_call(body, out_shape=[pltpu.HBM(*o) if i in far_out else jax.Sh...  24.5 us
    all_to_all x2, starting transfers between devices, shards(): lax.all_to_all(out.reshape(experts_n, capacity, -1), 'sp', 0, 0, tiled=True)  20.5 us
    all_to_all x1, starting transfers between devices, shards(): lax.all_to_all(outgoing.reshape(experts_n, capacity, model_width), 'sp',...  12.7 us
    all_to_all x1, waiting for transfers between devices, shards(): lax.all_to_all(conv_out.reshape(columns, rows_own, local_channels), 'tp',...  7.73 us
    unnamed x44, local copies, waits for them, and re-layouts  5.78 us
  transfers between devices with their start and end apart: 23, of which 10 were waited for; matrix products, arithmetic and copies ran while one was open for 2% of the time, Pallas kernels for 4%

profile of v3, /device:TPU:2, one launch (start us, length us, event | category | flops | bytes accessed | tf_op | source)
XLA Modules:
  0.0 239.8 jit_solution(4536170784185973806)
XLA Ops:
  0.0 1.4 rim_rows.1
  1.4 1.9 collective-permute-start
  3.8 1.9 convert_add_fusion
  7.9 0.9 copy-done.3
  11.7 5.1 %shard_map.136 = bf16[512,256]{1,0:T(8,128)(2,1)} custom-call(bf16[512,256]{1,0:T(8,128)(2,1)S(1)} %copy-done.2, bf16[512,256]{1,0:T(8,128)(2,1)S(1)} %copy-done.3, bf16[32,256]{1,0:T(8,128)(2,1)S(1)} %collective-permute-done.rim_ref, s32[4,128]{1,0:T(4,128)S(1)} %bitcast.44, s32[512,128]{1,0:T(8,128)S(1)} %broadcast_in_dim.16.seen_ref, ...), custom_call_target="tpu_custom_call" | custom-call | tf_op jit(solution)/shard_map/pallas_call | solution.py:42
  16.7 4.5 %all-to-all-start = ((bf16[4,128,256]{2,1,0:T(8,128)(2,1)}), bf16[4,128,256]{2,1,0:T(8,128)(2,1)S(1)}, u32[]{:S(2)}, u32[]{:S(2)}) async-start(bf16[4,128,256]{2,1,0:T(8,128)(2,1)} %bitcast.3), calls=%async_computation | async-start | bytes 524288 | tf_op jit(solution)/shard_map/all_to_all | solution.py:314
  21.2 7.7 %all-to-all-done.parts_ref = bf16[4,128,256]{2,1,0:T(8,128)(2,1)S(1)} async-done(((bf16[4,128,256]{2,1,0:T(8,128)(2,1)}), bf16[4,128,256]{2,1,0:T(8,128)(2,1)S(1)}, u32[]{:S(2)}, u32[]{:S(2)}) %all-to-all-start) | async-done | bytes 262176 | tf_op jit(solution)/shard_map/all_to_all | solution.py:314
  28.9 4.4 %shard_map.137 = (f32[128,2048]{1,0:T(8,128)}, bf16[512,2048]{1,0:T(8,128)(2,1)}) custom-call(bf16[4,128,256]{2,1,0:T(8,128)(2,1)S(1)} %all-to-all-done.parts_ref, bf16[128,2048]{1,0:T(8,128)(2,1)S(1)} %copy-done.4, f32[1,2048]{1,0:T(1,128)S(1)} %bitcast.45, s32[128,2]{1,0:T(8,128)S(1)} %multiply_add_fusion.slots_ref, bf16[1024,2048]{1,0:T(8,128)(2,1)} %weight_ref.1), custom_call_target="tpu_custom_call" | custom-call | tf_op jit(solution)/shard_map/pallas_call | solution.py:42
  33.3 12.7 %all-to-all-start.1 = ((bf16[64,8,2048]{2,1,0:T(8,128)(2,1)}), bf16[64,8,2048]{2,1,0:T(8,128)(2,1)}, u32[]{:S(2)}, u32[]{:S(2)}) async-start(bf16[64,8,2048]{2,1,0:T(8,128)(2,1)} %bitcast.51), calls=%async_computation.1 | async-start | bytes 4194304 | tf_op jit(solution)/shard_map/all_to_all | solution.py:338
  46.0 1.2 collective-permute-start.6
  49.0 3.1 %collective-permute-start.5 = (bf16[1024,256]{1,0:T(8,128)(2,1)S(1)}, bf16[1024,256]{1,0:T(8,128)(2,1)S(1)}, u32[]{:S(2)}, u32[]{:S(2)}) collective-permute-start(bf16[1024,256]{1,0:T(8,128)(2,1)S(1)} %get-tuple-element.9), channel_id=1, source_target_pairs={{0,3},{1,0},{2,1},{3,2},{4,7},{5,4},{6,5},{7,6},{8,11},{9,8},{10,9... | collective-permute-start | bytes 1572872 | tf_op jit(solution)/shard_map/ppermute | solution.py:25
  52.2 40.8 %collective-permute-done.11.refs_0_ = bf16[256,768]{1,0:T(8,128)(2,1)S(1)} collective-permute-done((bf16[256,768]{1,0:T(8,128)(2,1)S(1)}, bf16[256,768]{1,0:T(8,128)(2,1)S(1)}, u32[]{:S(2)}, u32[]{:S(2)}) %collective-permute-start.11) | collective-permute-done | bytes 393248 | tf_op jit(solution)/shard_map/ppermute | solution.py:25
  93.0 3.2 %collective-permute-start.12 = (bf16[256,768]{1,0:T(8,128)(2,1)S(1)}, bf16[256,768]{1,0:T(8,128)(2,1)S(1)}, u32[]{:S(2)}, u32[]{:S(2)}) collective-permute-start(bf16[256,768]{1,0:T(8,128)(2,1)S(1)} %slice.179), channel_id=1, source_target_pairs={{0,3},{1,0},{2,1},{3,2},{4,7},{5,4},{6,5},{7,6},{8,11},{9,8},{10,9... | collective-permute-start | bytes 1179656 | tf_op jit(solution)/shard_map/ppermute | solution.py:25
  96.3 1.9 collective-permute-start.7
  98.4 1.6 collective-permute-start.8
  99.9 5.8 %collective-permute-done.12.refs_1_ = bf16[256,768]{1,0:T(8,128)(2,1)S(1)} collective-permute-done((bf16[256,768]{1,0:T(8,128)(2,1)S(1)}, bf16[256,768]{1,0:T(8,128)(2,1)S(1)}, u32[]{:S(2)}, u32[]{:S(2)}) %collective-permute-start.12) | collective-permute-done | bytes 393248 | tf_op jit(solution)/shard_map/ppermute | solution.py:25
  105.7 3.7 %collective-permute-start.10 = (bf16[1024,256]{1,0:T(8,128)(2,1)S(1)}, bf16[1024,256]{1,0:T(8,128)(2,1)S(1)}, u32[]{:S(2)}, u32[]{:S(2)}) collective-permute-start(bf16[1024,256]{1,0:T(8,128)(2,1)S(1)} %slice.178), channel_id=1, source_target_pairs={{0,3},{1,0},{2,1},{3,2},{4,7},{5,4},{6,5},{7,6},{8,11},{9,8},{10,9... | collective-permute-start | bytes 1572872 | tf_op jit(solution)/shard_map/ppermute | solution.py:25
  110.2 6.8 %collective-permute-done.4.refs_6_ = bf16[1024,256]{1,0:T(8,128)(2,1)S(1)} collective-permute-done((bf16[1024,256]{1,0:T(8,128)(2,1)S(1)}, bf16[1024,256]{1,0:T(8,128)(2,1)S(1)}, u32[]{:S(2)}, u32[]{:S(2)}) %collective-permute-start.4) | collective-permute-done | bytes 524320 | tf_op jit(solution)/shard_map/ppermute | solution.py:25
  117.0 3.2 %collective-permute-done.7.refs_9_ = bf16[1024,256]{1,0:T(8,128)(2,1)S(1)} collective-permute-done((bf16[1024,256]{1,0:T(8,128)(2,1)S(1)}, bf16[1024,256]{1,0:T(8,128)(2,1)S(1)}, u32[]{:S(2)}, u32[]{:S(2)}) %collective-permute-start.7) | collective-permute-done | bytes 524320 | tf_op jit(solution)/shard_map/ppermute | solution.py:25
  120.8 7.4 %collective-permute-done.8.refs_10_ = bf16[1024,256]{1,0:T(8,128)(2,1)S(1)} collective-permute-done((bf16[1024,256]{1,0:T(8,128)(2,1)S(1)}, bf16[1024,256]{1,0:T(8,128)(2,1)S(1)}, u32[]{:S(2)}, u32[]{:S(2)}) %collective-permute-start.8) | collective-permute-done | bytes 524320 | tf_op jit(solution)/shard_map/ppermute | solution.py:25
  128.2 11.2 %collective-permute-done.10.refs_12_ = bf16[1024,256]{1,0:T(8,128)(2,1)S(1)} collective-permute-done((bf16[1024,256]{1,0:T(8,128)(2,1)S(1)}, bf16[1024,256]{1,0:T(8,128)(2,1)S(1)}, u32[]{:S(2)}, u32[]{:S(2)}) %collective-permute-start.10) | collective-permute-done | bytes 524320 | tf_op jit(solution)/shard_map/ppermute | solution.py:25
  140.2 7.4 %shard_map.138.hidden_ref = bf16[512,1024]{1,0:T(8,128)(2,1)S(1)} custom-call(bf16[512,2048]{1,0:T(8,128)(2,1)} %bitcast.7.refs_0_, bf16[2048,256]{1,0:T(8,128)(2,1)} %bitcast.49, bf16[2048,256]{1,0:T(8,128)(2,1)} %bitcast.52, bf16[1024,256]{1,0:T(8,128)(2,1)} %copy-done.14, bf16[1024,256]{1,0:T(8,128)(2,1)} %copy-done.16, bf16[2048,256]{1,0:T(8,128)(2,1)} %copy-done.12, ...), custom_call_target="tpu_custom_call" | custom-call | tf_op jit(solution)/shard_map/pallas_call | solution.py:42
  147.6 2.1 shard_map.139
  149.8 10.2 %all-to-all-start.2 = ((bf16[64,8,768]{2,1,0:T(8,128)(2,1)}), bf16[64,8,768]{2,1,0:T(8,128)(2,1)S(1)}, u32[]{:S(2)}, u32[]{:S(2)}) async-start(bf16[64,8,768]{2,1,0:T(8,128)(2,1)} %bitcast.50), calls=%async_computation.2 | async-start | bytes 1572864 | tf_op jit(solution)/shard_map/all_to_all | solution.py:349
  160.1 3.8 %collective-permute-start.16 = (bf16[256,1280]{1,0:T(8,128)(2,1)S(1)}, bf16[256,1280]{1,0:T(8,128)(2,1)S(1)}, u32[]{:S(2)}, u32[]{:S(2)}) collective-permute-start(bf16[256,1280]{1,0:T(8,128)(2,1)S(1)} %slice.182), channel_id=1, source_target_pairs={{0,3},{1,0},{2,1},{3,2},{4,7},{5,4},{6,5},{7,6},{8,11},{9,8},{10,9... | collective-permute-start | bytes 1966088 | tf_op jit(solution)/shard_map/ppermute | solution.py:25
  163.9 14.9 %collective-permute-done.15.refs_0_ = bf16[256,1280]{1,0:T(8,128)(2,1)S(1)} collective-permute-done((bf16[256,1280]{1,0:T(8,128)(2,1)S(1)}, bf16[256,1280]{1,0:T(8,128)(2,1)S(1)}, u32[]{:S(2)}, u32[]{:S(2)}) %collective-permute-start.15) | collective-permute-done | bytes 655392 | tf_op jit(solution)/shard_map/ppermute | solution.py:25
  179.0 3.5 %collective-permute-start.18 = (bf16[128,1280]{1,0:T(8,128)(2,1)S(1)}, bf16[128,1280]{1,0:T(8,128)(2,1)S(1)}, u32[]{:S(2)}, u32[]{:S(2)}) collective-permute-start(bf16[128,1280]{1,0:T(8,128)(2,1)S(1)} %slice.184), channel_id=1, source_target_pairs={{0,3},{1,0},{2,1},{3,2},{4,7},{5,4},{6,5},{7,6},{8,11},{9,8},{10,9... | collective-permute-start | bytes 983048 | tf_op jit(solution)/shard_map/ppermute | solution.py:25
  182.5 6.8 %collective-permute-done.17.refs_2_ = bf16[128,1280]{1,0:T(8,128)(2,1)S(1)} collective-permute-done((bf16[128,1280]{1,0:T(8,128)(2,1)S(1)}, bf16[128,1280]{1,0:T(8,128)(2,1)S(1)}, u32[]{:S(2)}, u32[]{:S(2)}) %collective-permute-start.17) | collective-permute-done | bytes 327712 | tf_op jit(solution)/shard_map/ppermute | solution.py:25
  189.3 2.8 %shard_map.140 = bf16[512,1280]{1,0:T(8,128)(2,1)} custom-call(bf16[512,1024]{1,0:T(8,128)(2,1)S(1)} %shard_map.138.hidden_ref, bf16[256,2048]{1,0:T(8,128)(2,1)S(1)} %bitcast.40, bf16[256,1280]{1,0:T(8,128)(2,1)S(1)} %collective-permute-done.15.refs_0_, bf16[256,1280]{1,0:T(8,128)(2,1)S(1)} %collective-permute-done.16.refs_1_, ...), custom_call_target="tpu_custom_call" | custom-call | tf_op jit(solution)/shard_map/pallas_call | solution.py:42
  192.2 10.3 %all-to-all-start.3 = ((bf16[64,8,1280]{2,1,0:T(8,128)(2,1)}), bf16[64,8,1280]{2,1,0:T(8,128)(2,1)S(1)}, u32[]{:S(2)}, u32[]{:S(2)}) async-start(bf16[64,8,1280]{2,1,0:T(8,128)(2,1)} %bitcast.48), calls=%async_computation.3 | async-start | bytes 2621440 | tf_op jit(solution)/shard_map/all_to_all | solution.py:349
  203.3 33.6 %all-to-all-done.3 = bf16[64,8,1280]{2,1,0:T(8,128)(2,1)S(1)} async-done(((bf16[64,8,1280]{2,1,0:T(8,128)(2,1)}), bf16[64,8,1280]{2,1,0:T(8,128)(2,1)S(1)}, u32[]{:S(2)}, u32[]{:S(2)}) %all-to-all-start.3) | async-done | bytes 1310752 | tf_op jit(solution)/shard_map/all_to_all | solution.py:349
  236.9 2.7 %shard_map.141 = bf16[128,2048]{1,0:T(8,128)(2,1)} custom-call(f32[128,2048]{1,0:T(8,128)} %get-tuple-element.7.stream_in, s32[128,2]{1,0:T(8,128)S(1)} %multiply_add_fusion.slots_ref, f32[128,2]{1,0:T(8,128)S(1)} %copy.21.weights_ref, bf16[512,768]{1,0:T(8,128)(2,1)S(1)} %bitcast.42, bf16[512,1280]{1,0:T(8,128)(2,1)S(1)} %bitcast.41), custom_call_target="tpu_custom_call" | custom-call | tf_op jit(solution)/shard_map/pallas_call | solution.py:42
  (88 shorter events, 10.6 us)
Async XLA Ops:
  0.0 28.9 %copy-start.7 = (f32[2048]{0:T(1024)S(1)}, f32[2048]{0:T(1024)}, u32[]{:S(2)}) copy-start(f32[2048]{0:T(1024)} %param.22) | copy-start | bytes 24580
  0.0 28.9 %copy-start.4 = (bf16[128,2048]{1,0:T(8,128)(2,1)S(1)}, bf16[128,2048]{1,0:T(8,128)(2,1)}, u32[]{:S(2)}) copy-start(bf16[128,2048]{1,0:T(8,128)(2,1)} %residual_ref.1) | copy-start | bytes 1572868
  1.4 5.4 %collective-permute-start = (bf16[32,256]{1,0:T(8,128)(2,1)}, bf16[32,256]{1,0:T(8,128)(2,1)S(1)}, u32[]{:S(2)}, u32[]{:S(2)}) collective-permute-start(bf16[32,256]{1,0:T(8,128)(2,1)} %rim_rows.1), channel_id=1, source_target_pairs={{0,4},{4,8},{8,12},{12,16},{16,20},{20,24},{24,28},{28,32},{32,36}... | collective-permute-start | bytes 49160 | tf_op jit(solution)/shard_map/ppermute | solution.py:20
  16.7 12.2 %all-to-all-start = ((bf16[4,128,256]{2,1,0:T(8,128)(2,1)}), bf16[4,128,256]{2,1,0:T(8,128)(2,1)S(1)}, u32[]{:S(2)}, u32[]{:S(2)}) async-start(bf16[4,128,256]{2,1,0:T(8,128)(2,1)} %bitcast.3), calls=%async_computation | async-start | bytes 524288 | tf_op jit(solution)/shard_map/all_to_all | solution.py:314
  33.3 106.9 %all-to-all-start.1 = ((bf16[64,8,2048]{2,1,0:T(8,128)(2,1)}), bf16[64,8,2048]{2,1,0:T(8,128)(2,1)}, u32[]{:S(2)}, u32[]{:S(2)}) async-start(bf16[64,8,2048]{2,1,0:T(8,128)(2,1)} %bitcast.51), calls=%async_computation.1 | async-start | bytes 4194304 | tf_op jit(solution)/shard_map/all_to_all | solution.py:338
  46.0 50.3 %collective-permute-start.6 = (bf16[2048,256]{1,0:T(8,128)(2,1)S(1)}, bf16[2048,256]{1,0:T(8,128)(2,1)S(1)}, u32[]{:S(2)}, u32[]{:S(2)}) collective-permute-start(bf16[2048,256]{1,0:T(8,128)(2,1)S(1)} %bitcast.53), channel_id=1, source_target_pairs={{0,3},{1,0},{2,1},{3,2},{4,7},{5,4},{6,5},{7,6},{8,11},{9,8},{10,9... | collective-permute-start | bytes 3145736 | tf_op jit(solution)/shard_map/ppermute | solution.py:25
  47.2 49.1 %collective-permute-start.3 = (bf16[2048,256]{1,0:T(8,128)(2,1)S(1)}, bf16[2048,256]{1,0:T(8,128)(2,1)S(1)}, u32[]{:S(2)}, u32[]{:S(2)}) collective-permute-start(bf16[2048,256]{1,0:T(8,128)(2,1)S(1)} %bitcast.54), channel_id=1, source_target_pairs={{0,1},{1,2},{2,3},{3,0},{4,5},{5,6},{6,7},{7,4},{8,9},{9,10},{10,1... | collective-permute-start | bytes 3145736 | tf_op jit(solution)/shard_map/ppermute | solution.py:25
  48.2 44.8 %collective-permute-start.1 = (bf16[1024,256]{1,0:T(8,128)(2,1)S(1)}, bf16[1024,256]{1,0:T(8,128)(2,1)S(1)}, u32[]{:S(2)}, u32[]{:S(2)}) collective-permute-start(bf16[1024,256]{1,0:T(8,128)(2,1)S(1)} %get-tuple-element.10), channel_id=1, source_target_pairs={{0,1},{1,2},{2,3},{3,0},{4,5},{5,6},{6,7},{7,4},{8,9},{9,10},{10,1... | collective-permute-start | bytes 1572872 | tf_op jit(solution)/shard_map/ppermute | solution.py:25
  48.8 44.2 %collective-permute-start.11 = (bf16[256,768]{1,0:T(8,128)(2,1)S(1)}, bf16[256,768]{1,0:T(8,128)(2,1)S(1)}, u32[]{:S(2)}, u32[]{:S(2)}) collective-permute-start(bf16[256,768]{1,0:T(8,128)(2,1)S(1)} %slice.179), channel_id=1, source_target_pairs={{0,1},{1,2},{2,3},{3,0},{4,5},{5,6},{6,7},{7,4},{8,9},{9,10},{10,1... | collective-permute-start | bytes 1179656 | tf_op jit(solution)/shard_map/ppermute | solution.py:25
  49.0 49.4 %collective-permute-start.5 = (bf16[1024,256]{1,0:T(8,128)(2,1)S(1)}, bf16[1024,256]{1,0:T(8,128)(2,1)S(1)}, u32[]{:S(2)}, u32[]{:S(2)}) collective-permute-start(bf16[1024,256]{1,0:T(8,128)(2,1)S(1)} %get-tuple-element.9), channel_id=1, source_target_pairs={{0,3},{1,0},{2,1},{3,2},{4,7},{5,4},{6,5},{7,6},{8,11},{9,8},{10,9... | collective-permute-start | bytes 1572872 | tf_op jit(solution)/shard_map/ppermute | solution.py:25
  93.0 16.4 %collective-permute-start.2 = (bf16[1024,256]{1,0:T(8,128)(2,1)S(1)}, bf16[1024,256]{1,0:T(8,128)(2,1)S(1)}, u32[]{:S(2)}, u32[]{:S(2)}) collective-permute-start(bf16[1024,256]{1,0:T(8,128)(2,1)S(1)} %get-tuple-element.9), channel_id=1, source_target_pairs={{0,1},{1,2},{2,3},{3,0},{4,5},{5,6},{6,7},{7,4},{8,9},{9,10},{10,1... | collective-permute-start | bytes 1572872 | tf_op jit(solution)/shard_map/ppermute | solution.py:25
  93.0 27.8 %copy-start.14 = (bf16[1024,256]{1,0:T(8,128)(2,1)}, bf16[1024,256]{1,0:T(8,128)(2,1)S(1)}, u32[]{:S(2)}) copy-start(bf16[1024,256]{1,0:T(8,128)(2,1)S(1)} %collective-permute-done.1.refs_3_) | copy-start | bytes 1572868
  93.0 12.7 %collective-permute-start.12 = (bf16[256,768]{1,0:T(8,128)(2,1)S(1)}, bf16[256,768]{1,0:T(8,128)(2,1)S(1)}, u32[]{:S(2)}, u32[]{:S(2)}) collective-permute-start(bf16[256,768]{1,0:T(8,128)(2,1)S(1)} %slice.179), channel_id=1, source_target_pairs={{0,3},{1,0},{2,1},{3,2},{4,7},{5,4},{6,5},{7,6},{8,11},{9,8},{10,9... | collective-permute-start | bytes 1179656 | tf_op jit(solution)/shard_map/ppermute | solution.py:25
  96.2 20.7 %copy-start.11 = (bf16[2048,256]{1,0:T(8,128)(2,1)}, bf16[2048,256]{1,0:T(8,128)(2,1)S(1)}, u32[]{:S(2)}) copy-start(bf16[2048,256]{1,0:T(8,128)(2,1)S(1)} %collective-permute-done.6.refs_8_) | copy-start | bytes 3145732
  96.2 20.7 %collective-permute-start.4 = (bf16[1024,256]{1,0:T(8,128)(2,1)S(1)}, bf16[1024,256]{1,0:T(8,128)(2,1)S(1)}, u32[]{:S(2)}, u32[]{:S(2)}) collective-permute-start(bf16[1024,256]{1,0:T(8,128)(2,1)S(1)} %get-tuple-element.10), channel_id=1, source_target_pairs={{0,3},{1,0},{2,1},{3,2},{4,7},{5,4},{6,5},{7,6},{8,11},{9,8},{10,9... | collective-permute-start | bytes 1572872 | tf_op jit(solution)/shard_map/ppermute | solution.py:25
  96.3 23.9 %copy-start.12 = (bf16[2048,256]{1,0:T(8,128)(2,1)}, bf16[2048,256]{1,0:T(8,128)(2,1)S(1)}, u32[]{:S(2)}) copy-start(bf16[2048,256]{1,0:T(8,128)(2,1)S(1)} %collective-permute-done.3.refs_5_) | copy-start | bytes 3145732
  96.3 23.9 %collective-permute-start.7 = (bf16[1024,256]{1,0:T(8,128)(2,1)S(1)}, bf16[1024,256]{1,0:T(8,128)(2,1)S(1)}, u32[]{:S(2)}, u32[]{:S(2)}) collective-permute-start(bf16[1024,256]{1,0:T(8,128)(2,1)S(1)} %collective-permute-done.1.refs_3_), channel_id=1, source_target_pairs={{0,1},{1,2},{2,3},{3,0},{4,5},{5,6},{6,7},{7,4},{8,9},{9,10},{10,1... | collective-permute-start | bytes 1572872 | tf_op jit(solution)/shard_map/ppermute | solution.py:25
  98.4 29.8 %copy-start.15 = (bf16[1024,256]{1,0:T(8,128)(2,1)}, bf16[1024,256]{1,0:T(8,128)(2,1)S(1)}, u32[]{:S(2)}) copy-start(bf16[1024,256]{1,0:T(8,128)(2,1)S(1)} %collective-permute-done.5.refs_7_) | copy-start | bytes 1572868
  98.4 29.8 %collective-permute-start.8 = (bf16[1024,256]{1,0:T(8,128)(2,1)S(1)}, bf16[1024,256]{1,0:T(8,128)(2,1)S(1)}, u32[]{:S(2)}, u32[]{:S(2)}) collective-permute-start(bf16[1024,256]{1,0:T(8,128)(2,1)S(1)} %collective-permute-done.5.refs_7_), channel_id=1, source_target_pairs={{0,3},{1,0},{2,1},{3,2},{4,7},{5,4},{6,5},{7,6},{8,11},{9,8},{10,9... | collective-permute-start | bytes 1572872 | tf_op jit(solution)/shard_map/ppermute | solution.py:25
  105.7 33.7 %collective-permute-start.10 = (bf16[1024,256]{1,0:T(8,128)(2,1)S(1)}, bf16[1024,256]{1,0:T(8,128)(2,1)S(1)}, u32[]{:S(2)}, u32[]{:S(2)}) collective-permute-start(bf16[1024,256]{1,0:T(8,128)(2,1)S(1)} %slice.178), channel_id=1, source_target_pairs={{0,3},{1,0},{2,1},{3,2},{4,7},{5,4},{6,5},{7,6},{8,11},{9,8},{10,9... | collective-permute-start | bytes 1572872 | tf_op jit(solution)/shard_map/ppermute | solution.py:25
  109.4 30.0 %copy-start.16 = (bf16[1024,256]{1,0:T(8,128)(2,1)}, bf16[1024,256]{1,0:T(8,128)(2,1)S(1)}, u32[]{:S(2)}) copy-start(bf16[1024,256]{1,0:T(8,128)(2,1)S(1)} %collective-permute-done.2.refs_4_) | copy-start | bytes 1572868
  109.4 30.8 %collective-permute-start.9 = (bf16[1024,256]{1,0:T(8,128)(2,1)S(1)}, bf16[1024,256]{1,0:T(8,128)(2,1)}, u32[]{:S(2)}, u32[]{:S(2)}) collective-permute-start(bf16[1024,256]{1,0:T(8,128)(2,1)S(1)} %slice.177), channel_id=1, source_target_pairs={{0,1},{1,2},{2,3},{3,0},{4,5},{5,6},{6,7},{7,4},{8,9},{9,10},{10,1... | collective-permute-start | bytes 1572872 | tf_op jit(solution)/shard_map/ppermute | solution.py:25
  117.0 22.4 %copy-start.17 = (bf16[1024,256]{1,0:T(8,128)(2,1)}, bf16[1024,256]{1,0:T(8,128)(2,1)S(1)}, u32[]{:S(2)}) copy-start(bf16[1024,256]{1,0:T(8,128)(2,1)S(1)} %collective-permute-done.4.refs_6_) | copy-start | bytes 1572868
  117.0 30.6 %collective-permute-start.13 = (bf16[128,768]{1,0:T(8,128)(2,1)}, bf16[128,768]{1,0:T(8,128)(2,1)S(1)}, u32[]{:S(2)}, u32[]{:S(2)}) collective-permute-start(bf16[128,768]{1,0:T(8,128)(2,1)} %slice.180), channel_id=1, source_target_pairs={{0,1},{1,2},{2,3},{3,0},{4,5},{5,6},{6,7},{7,4},{8,9},{9,10},{10,1... | collective-permute-start | bytes 589832 | tf_op jit(solution)/shard_map/ppermute | solution.py:25
  120.2 20.0 %copy-start.18 = (bf16[1024,256]{1,0:T(8,128)(2,1)}, bf16[1024,256]{1,0:T(8,128)(2,1)S(1)}, u32[]{:S(2)}) copy-start(bf16[1024,256]{1,0:T(8,128)(2,1)S(1)} %collective-permute-done.7.refs_9_) | copy-start | bytes 1572868
  120.2 27.4 %collective-permute-start.14 = (bf16[128,768]{1,0:T(8,128)(2,1)S(1)}, bf16[128,768]{1,0:T(8,128)(2,1)S(1)}, u32[]{:S(2)}, u32[]{:S(2)}) collective-permute-start(bf16[128,768]{1,0:T(8,128)(2,1)S(1)} %slice.181), channel_id=1, source_target_pairs={{0,3},{1,0},{2,1},{3,2},{4,7},{5,4},{6,5},{7,6},{8,11},{9,8},{10,9... | collective-permute-start | bytes 589832 | tf_op jit(solution)/shard_map/ppermute | solution.py:25
  149.8 42.4 %all-to-all-start.2 = ((bf16[64,8,768]{2,1,0:T(8,128)(2,1)}), bf16[64,8,768]{2,1,0:T(8,128)(2,1)S(1)}, u32[]{:S(2)}, u32[]{:S(2)}) async-start(bf16[64,8,768]{2,1,0:T(8,128)(2,1)} %bitcast.50), calls=%async_computation.2 | async-start | bytes 1572864 | tf_op jit(solution)/shard_map/all_to_all | solution.py:349
  160.1 18.8 %collective-permute-start.15 = (bf16[256,1280]{1,0:T(8,128)(2,1)S(1)}, bf16[256,1280]{1,0:T(8,128)(2,1)S(1)}, u32[]{:S(2)}, u32[]{:S(2)}) collective-permute-start(bf16[256,1280]{1,0:T(8,128)(2,1)S(1)} %slice.182), channel_id=1, source_target_pairs={{0,1},{1,2},{2,3},{3,0},{4,5},{5,6},{6,7},{7,4},{8,9},{9,10},{10,1... | collective-permute-start | bytes 1966088 | tf_op jit(solution)/shard_map/ppermute | solution.py:25
  160.1 18.8 %collective-permute-start.16 = (bf16[256,1280]{1,0:T(8,128)(2,1)S(1)}, bf16[256,1280]{1,0:T(8,128)(2,1)S(1)}, u32[]{:S(2)}, u32[]{:S(2)}) collective-permute-start(bf16[256,1280]{1,0:T(8,128)(2,1)S(1)} %slice.182), channel_id=1, source_target_pairs={{0,3},{1,0},{2,1},{3,2},{4,7},{5,4},{6,5},{7,6},{8,11},{9,8},{10,9... | collective-permute-start | bytes 1966088 | tf_op jit(solution)/shard_map/ppermute | solution.py:25
  178.9 10.4 %collective-permute-start.17 = (bf16[128,1280]{1,0:T(8,128)(2,1)S(1)}, bf16[128,1280]{1,0:T(8,128)(2,1)S(1)}, u32[]{:S(2)}, u32[]{:S(2)}) collective-permute-start(bf16[128,1280]{1,0:T(8,128)(2,1)S(1)} %slice.183), channel_id=1, source_target_pairs={{0,1},{1,2},{2,3},{3,0},{4,5},{5,6},{6,7},{7,4},{8,9},{9,10},{10,1... | collective-permute-start | bytes 983048 | tf_op jit(solution)/shard_map/ppermute | solution.py:25
  179.0 10.3 %collective-permute-start.18 = (bf16[128,1280]{1,0:T(8,128)(2,1)S(1)}, bf16[128,1280]{1,0:T(8,128)(2,1)S(1)}, u32[]{:S(2)}, u32[]{:S(2)}) collective-permute-start(bf16[128,1280]{1,0:T(8,128)(2,1)S(1)} %slice.184), channel_id=1, source_target_pairs={{0,3},{1,0},{2,1},{3,2},{4,7},{5,4},{6,5},{7,6},{8,11},{9,8},{10,9... | collective-permute-start | bytes 983048 | tf_op jit(solution)/shard_map/ppermute | solution.py:25
  192.2 44.7 %all-to-all-start.3 = ((bf16[64,8,1280]{2,1,0:T(8,128)(2,1)}), bf16[64,8,1280]{2,1,0:T(8,128)(2,1)S(1)}, u32[]{:S(2)}, u32[]{:S(2)}) async-start(bf16[64,8,1280]{2,1,0:T(8,128)(2,1)} %bitcast.48), calls=%async_computation.3 | async-start | bytes 2621440 | tf_op jit(solution)/shard_map/all_to_all | solution.py:349
  (12 other events, 51.2 us)

commit v4 on v3

--- a/solution.py
+++ b/solution.py
@@ -9,7 +9,7 @@
 
 TAPS = 31
 RIM = 32
-FIRST = 3
+FIRST = 2
 LANES = 128
 BLOCK = 64
 
@@ -23,13 +23,6 @@
 def ring(value, axis, steps):
     count = lax.axis_size(axis)
     return lax.ppermute(value, axis, [(i, (i + steps) % count) for i in range(count)])
-
-
-def slot_numbers(block_routes, capacity, experts_n):
-    route_pairs = block_routes.reshape(block_routes.shape[:-2] + (-1,))
-    onehot = (route_pairs[..., None] == jnp.arange(experts_n, dtype=jnp.int32)).astype(jnp.int32)
-    slot_rank = jnp.sum((jnp.cumsum(onehot, axis=-2) - onehot) * onehot, axis=-1)
-    return (route_pairs * capacity + slot_rank).reshape(block_routes.shape)
 
 
 def kernel(body, out, args, scratch=(), limit=16, far_in=(), far_out=()):
@@ -133,18 +126,31 @@
     return jnp.dot(a, b, preferred_element_type=jnp.float32)
 
 
-def places(slots, total):
-    numbers = lax.broadcasted_iota(jnp.int32, (slots.shape[0], total), 1)
-    return [numbers == slots[:, m : m + 1] for m in range(slots.shape[1])]
+def places(routes, experts_n, capacity):
+    rows, top_count = routes.shape
+    expert = lax.broadcasted_iota(jnp.int32, (rows, experts_n), 1)
+    named = [jnp.where(expert == routes[:, m : m + 1], 1.0, 0.0) for m in range(top_count)]
+    earlier = lax.broadcasted_iota(jnp.int32, (rows, rows), 0) > lax.broadcasted_iota(
+        jnp.int32, (rows, rows), 1
+    )
+    earlier = jnp.where(earlier, 1.0, 0.0).astype(jnp.bfloat16)
+    taken = dot(earlier, sum(named).astype(jnp.bfloat16))
+    number = lax.broadcasted_iota(jnp.int32, (rows, experts_n * capacity), 1)
+    found = []
+    for m in range(top_count):
+        rank = jnp.sum(named[m] * taken, axis=1, keepdims=True).astype(jnp.int32)
+        found.append(number == routes[:, m : m + 1] * capacity + rank)
+    return found
 
 
 def route_body(
-    parts_ref, residual_ref, gain_ref, slots_ref, weight_ref, stream_out, sent_out, w_ref, stream_ref, sent_ref, sems
+    experts_n, parts_ref, residual_ref, gain_ref, routes_ref, weight_ref, stream_out, sent_out, w_ref, stream_ref, sent_ref, sems
 ):
     parts_n, _, width = parts_ref.shape
     spans = [slice(j * width, (j + 1) * width) for j in range(parts_n)]
     loads = fetch([(weight_ref.at[rows], w_ref.at[rows]) for rows in spans], sems)
-    table = functools.reduce(jnp.logical_or, places(slots_ref[...], sent_ref.shape[0]))
+    found = places(routes_ref[...], experts_n, sent_ref.shape[0] // experts_n)
+    table = functools.reduce(jnp.logical_or, found)
     table = jnp.where(table, 1.0, 0.0).astype(jnp.bfloat16)
     for j, rows in enumerate(spans):
         loads[j].wait()
@@ -167,11 +173,11 @@
         c.wait()
 
 
-def combine_body(stream_in, slots_ref, weights_ref, *refs):
+def combine_body(experts_n, stream_in, routes_ref, weights_ref, *refs):
     *back_refs, out, stream_ref, out_ref, sems = refs
     (load,) = fetch([(stream_in, stream_ref)], sems)
-    hits = places(slots_ref[...], back_refs[0].shape[0])
-    table = sum(jnp.where(hit, weights_ref[:, m : m + 1], 0.0) for m, hit in enumerate(hits))
+    found = places(routes_ref[...], experts_n, back_refs[0].shape[0] // experts_n)
+    table = sum(jnp.where(hit, weights_ref[:, m : m + 1], 0.0) for m, hit in enumerate(found))
     high = table.astype(jnp.bfloat16)
     low = (table - high.astype(jnp.float32)).astype(jnp.bfloat16)
     load.wait()
@@ -187,11 +193,11 @@
         c.wait()
 
 
-def hidden_body(counts, *refs):
-    rows_in, *pieces, out_ref, rows_ref, w_ref, sems = refs
+def experts_body(counts, cols, *refs):
+    rows_in, *pieces, hidden_out, out, rows_ref, w_ref, hidden_ref, down_ref, out_ref, sems = refs
     width = pieces[0].shape[1]
-    (load,) = fetch([(rows_in, rows_ref)], sems, len(pieces))
-    loads = []
+    (load,) = fetch([(rows_in, rows_ref)], sems)
+    loads, at = [], 1
     for q, kinds in enumerate(counts):
         copies = []
         for kind, n in enumerate(kinds):
@@ -201,7 +207,14 @@
                 copies.append((piece, w_ref.at[q, top:end, kind * width : (kind + 1) * width]))
                 top = end
             pieces = pieces[n:]
-        loads.append(fetch(copies, sems, sum(len(c) for c in loads)))
+        loads.append(fetch(copies, sems, at))
+        at += len(copies)
+    copies, top = [], 0
+    for piece in pieces:
+        src = piece.at[:, cols] if top == 0 else piece
+        copies.append((src, down_ref.at[top : top + piece.shape[0]]))
+        top += piece.shape[0]
+    downs = fetch(copies, sems, at)
     load.wait()
     for q, copies in enumerate(loads):
         for c in copies:
@@ -209,24 +222,36 @@
         act = dot(rows_ref[...], w_ref[q])
         gate = act[:, :width]
         hidden = gate / (1.0 + jnp.exp(-gate)) * act[:, width:]
-        out_ref[:, q * width : (q + 1) * width] = hidden.astype(jnp.bfloat16)
-
-
-def hidden_units(rows, quarters):
+        hidden_ref[:, q * width : (q + 1) * width] = hidden.astype(jnp.bfloat16)
+    stores = fetch([(hidden_ref, hidden_out)], sems)
+    for c in downs:
+        c.wait()
+    out_ref[...] = dot(hidden_ref[...], down_ref[...]).astype(jnp.bfloat16)
+    stores += fetch([(out_ref, out)], sems, 1)
+    for c in stores:
+        c.wait()
+
+
+def expert_rows(rows, quarters, downs, cols):
     counts = tuple((len(gates), len(ups)) for gates, ups in quarters)
-    pieces = [p for gates, ups in quarters for p in (*gates, *ups)]
-    (n, d), width = rows.shape, pieces[0].shape[1]
+    pieces = [p for gates, ups in quarters for p in (*gates, *ups)] + downs
+    (n, d), width, out_width = rows.shape, pieces[0].shape[1], cols.stop - cols.start
+    units = width * len(counts)
     return kernel(
-        functools.partial(hidden_body, counts),
-        ((n, width * len(counts)), jnp.bfloat16),
+        functools.partial(experts_body, counts, cols),
+        [((n, units), jnp.bfloat16), ((n, out_width), jnp.bfloat16)],
         (rows, *pieces),
         scratch=[
             pltpu.VMEM((n, d), jnp.bfloat16),
             pltpu.VMEM((len(counts), d, 2 * width), jnp.bfloat16),
+            pltpu.VMEM((n, units), jnp.bfloat16),
+            pltpu.VMEM((units, out_width), jnp.bfloat16),
+            pltpu.VMEM((n, out_width), jnp.bfloat16),
             pltpu.SemaphoreType.DMA((len(pieces) + 1,)),
         ],
-        limit=20,
+        limit=22,
         far_in=range(1 + len(pieces)),
+        far_out=(0, 1),
     )
 
 
@@ -320,11 +345,10 @@
     slot_total = experts_n * capacity
     own_routes = lax.dynamic_slice_in_dim(routes, column * rows_own, rows_own, 0)
     own_weights = lax.dynamic_slice_in_dim(route_weights, column * rows_own, rows_own, 0)
-    own_slots = slot_numbers(own_routes, capacity, experts_n)
     stream, outgoing = kernel(
-        route_body,
+        functools.partial(route_body, experts_n),
         [((rows_own, model_width), jnp.float32), ((slot_total, model_width), jnp.bfloat16)],
-        (regrouped, residual, ffn_gain[None], own_slots, out_weight),
+        (regrouped, residual, ffn_gain[None], own_routes, out_weight),
         scratch=[
             pltpu.VMEM(out_weight.shape, jnp.bfloat16),
             pltpu.VMEM((rows_own, model_width), jnp.float32),
@@ -338,22 +362,22 @@
     arrived = lax.all_to_all(
         outgoing.reshape(experts_n, capacity, model_width), "sp", 0, 0, tiled=True
     ).reshape(slot_total, model_width)
-    hidden = hidden_units(
-        arrived,
-        [([w_gate[0]], [w_up[0]])] + [(gates[side], ups[side]) for side in range(3)],
-    )
-    back = []
-    for cols, (left, right, far) in zip(groups, downs):
-        out = down_rows(hidden, w_down[0], [*left, *right, *far], cols)
-        back.append(
-            lax.all_to_all(
-                out.reshape(experts_n, capacity, -1), "sp", 0, 0, tiled=True
-            ).reshape(slot_total, -1)
-        )
+
+    def returned(out):
+        return lax.all_to_all(
+            out.reshape(experts_n, capacity, -1), "sp", 0, 0, tiled=True
+        ).reshape(slot_total, -1)
+
+    first, second = ([w_down[0], *left, *right, *far] for left, right, far in downs)
+    quarters = [([w_gate[0]], [w_up[0]])] + [(gates[side], ups[side]) for side in range(3)]
+    hidden, out = expert_rows(arrived, quarters, first, groups[0])
+    back = [returned(out)]
+    out = down_rows(hidden, second[0], second[1:], groups[1])
+    back.append(returned(out))
     return kernel(
-        combine_body,
+        functools.partial(combine_body, experts_n),
         ((rows_own, model_width), jnp.bfloat16),
-        (stream, own_slots, own_weights, *back),
+        (stream, own_routes, own_weights, *back),
         scratch=[
             pltpu.VMEM((rows_own, model_width), jnp.float32),
             pltpu.VMEM((rows_own, model_width), jnp.bfloat16),

time: 241 us -> 227 us (0.942)
  waiting for transfers between devices: 138 us -> 124 us
    ppermute x18, waiting for transfers between devices: 97 us -> 76 us  [ring(): lax.ppermute(value, axis, [(i, (i + steps) % count) for i in range(count)])]
    all_to_all x2, waiting for transfers between devices: 33.6 us -> 39.2 us  [returned(): lax.all_to_all(out.reshape(experts_n, capacity, -1), 'sp', 0, 0, tiled=True)]
    pallas_call x6 -> x5, Pallas kernels: 24.5 us -> 25.4 us  [kernel(): pl.pallas_call(body, out_shape=[pltpu.HBM(*o) if i in far_out else jax.Sh...]
    unnamed x44 -> x52, local copies, waits for them, and re-layouts: 5.78 us -> 5.86 us
  transfers between devices with their start and end apart: 23 -> 23, of which waited for: 10 -> 11; matrix products, arithmetic and copies ran while one was open for 2% -> 2% of each run, Pallas kernels for 4% -> 6%
where the time goes in v4:
time: 227 us; the launch traced here: 225 us
  waiting for transfers between devices  124 us (55%)
  starting transfers between devices  63.2 us (28%)
  Pallas kernels  26.8 us (12%)
  local copies, waits for them, and re-layouts  8.98 us (4%)
    ppermute x18, waiting for transfers between devices, ring(): lax.ppermute(value, axis, [(i, (i + steps) % count) for i in range(count)])  76 us
    all_to_all x2, waiting for transfers between devices, returned(): lax.all_to_all(out.reshape(experts_n, capacity, -1), 'sp', 0, 0, tiled=True)  39.2 us
    pallas_call x5, Pallas kernels, kernel(): pl.pallas_call(body, out_shape=[pltpu.HBM(*o) if i in far_out else jax.Sh...  25.4 us
    ppermute x18, starting transfers between devices, ring(): lax.ppermute(value, axis, [(i, (i + steps) % count) for i in range(count)])  23.2 us
    all_to_all x2, starting transfers between devices, returned(): lax.all_to_all(out.reshape(experts_n, capacity, -1), 'sp', 0, 0, tiled=True)  20.8 us
    all_to_all x1, starting transfers between devices, shards(): lax.all_to_all(outgoing.reshape(experts_n, capacity, model_width), 'sp',...  12.9 us
    all_to_all x1, waiting for transfers between devices, shards(): lax.all_to_all(conv_out.reshape(columns, rows_own, local_channels), 'tp',...  6.89 us
    unnamed x52, local copies, waits for them, and re-layouts  5.86 us
  transfers between devices with their start and end apart: 23, of which 11 were waited for; matrix products, arithmetic and copies ran while one was open for 2% of the time, Pallas kernels for 6%

profile of v4, /device:TPU:2, one launch (start us, length us, event | category | flops | bytes accessed | tf_op | source)
XLA Modules:
  0.0 224.9 jit_solution(14931242571299085805)
XLA Ops:
  0.0 1.4 rim_rows.1
  1.4 1.9 collective-permute-start
  3.3 1.9 convert_add_fusion
  5.3 1.4 collective-permute-done.rim_ref
  7.8 0.9 copy-done.4
  11.5 5.1 %shard_map.136 = bf16[512,256]{1,0:T(8,128)(2,1)} custom-call(bf16[512,256]{1,0:T(8,128)(2,1)S(1)} %copy-done.3, bf16[512,256]{1,0:T(8,128)(2,1)S(1)} %copy-done.4, bf16[32,256]{1,0:T(8,128)(2,1)S(1)} %collective-permute-done.rim_ref, s32[4,128]{1,0:T(4,128)S(1)} %bitcast.25, s32[512,128]{1,0:T(8,128)S(1)} %broadcast_in_dim.15.seen_ref, ...), custom_call_target="tpu_custom_call" | custom-call | tf_op jit(solution)/shard_map/pallas_call | solution.py:35
  16.6 4.5 %all-to-all-start = ((bf16[4,128,256]{2,1,0:T(8,128)(2,1)}), bf16[4,128,256]{2,1,0:T(8,128)(2,1)S(1)}, u32[]{:S(2)}, u32[]{:S(2)}) async-start(bf16[4,128,256]{2,1,0:T(8,128)(2,1)} %bitcast.3), calls=%async_computation | async-start | bytes 524288 | tf_op jit(solution)/shard_map/all_to_all | solution.py:339
  21.2 6.9 %all-to-all-done.parts_ref = bf16[4,128,256]{2,1,0:T(8,128)(2,1)S(1)} async-done(((bf16[4,128,256]{2,1,0:T(8,128)(2,1)}), bf16[4,128,256]{2,1,0:T(8,128)(2,1)S(1)}, u32[]{:S(2)}, u32[]{:S(2)}) %all-to-all-start) | async-done | bytes 262176 | tf_op jit(solution)/shard_map/all_to_all | solution.py:339
  28.1 4.4 %shard_map.137 = (f32[128,2048]{1,0:T(8,128)}, bf16[512,2048]{1,0:T(8,128)(2,1)}) custom-call(bf16[4,128,256]{2,1,0:T(8,128)(2,1)S(1)} %all-to-all-done.parts_ref, bf16[128,2048]{1,0:T(8,128)(2,1)S(1)} %copy-done.6, f32[1,2048]{1,0:T(1,128)S(1)} %bitcast.26, s32[128,2]{1,0:T(8,128)S(1)} %copy.17.routes_ref, bf16[1024,2048]{1,0:T(8,128)(2,1)} %weight_ref.1), custom_call_target="tpu_custom_call" | custom-call | tf_op jit(solution)/shard_map/pallas_call | solution.py:35
  32.5 12.9 %all-to-all-start.1 = ((bf16[64,8,2048]{2,1,0:T(8,128)(2,1)}), bf16[64,8,2048]{2,1,0:T(8,128)(2,1)}, u32[]{:S(2)}, u32[]{:S(2)}) async-start(bf16[64,8,2048]{2,1,0:T(8,128)(2,1)} %bitcast.31), calls=%async_computation.1 | async-start | bytes 4194304 | tf_op jit(solution)/shard_map/all_to_all | solution.py:362
  45.3 1.2 collective-permute-start.6
  48.1 2.7 %collective-permute-start.12 = (bf16[256,512]{1,0:T(8,128)(2,1)S(1)}, bf16[256,512]{1,0:T(8,128)(2,1)S(1)}, u32[]{:S(2)}, u32[]{:S(2)}) collective-permute-start(bf16[256,512]{1,0:T(8,128)(2,1)S(1)} %slice.170), channel_id=1, source_target_pairs={{0,3},{1,0},{2,1},{3,2},{4,7},{5,4},{6,5},{7,6},{8,11},{9,8},{10,9... | collective-permute-start | bytes 786440 | tf_op jit(solution)/shard_map/ppermute | solution.py:25
  51.0 28.7 %collective-permute-done.11.refs_14_ = bf16[256,512]{1,0:T(8,128)(2,1)S(1)} collective-permute-done((bf16[256,512]{1,0:T(8,128)(2,1)S(1)}, bf16[256,512]{1,0:T(8,128)(2,1)S(1)}, u32[]{:S(2)}, u32[]{:S(2)}) %collective-permute-start.11) | collective-permute-done | bytes 262176 | tf_op jit(solution)/shard_map/ppermute | solution.py:25
  79.8 3.2 %collective-permute-start.5 = (bf16[1024,256]{1,0:T(8,128)(2,1)S(1)}, bf16[1024,256]{1,0:T(8,128)(2,1)S(1)}, u32[]{:S(2)}, u32[]{:S(2)}) collective-permute-start(bf16[1024,256]{1,0:T(8,128)(2,1)S(1)} %get-tuple-element.13), channel_id=1, source_target_pairs={{0,3},{1,0},{2,1},{3,2},{4,7},{5,4},{6,5},{7,6},{8,11},{9,8},{10,9... | collective-permute-start | bytes 1572872 | tf_op jit(solution)/shard_map/ppermute | solution.py:25
  83.0 9.6 %collective-permute-done.13.refs_16_ = bf16[128,512]{1,0:T(8,128)(2,1)S(1)} collective-permute-done((bf16[128,512]{1,0:T(8,128)(2,1)S(1)}, bf16[128,512]{1,0:T(8,128)(2,1)S(1)}, u32[]{:S(2)}, u32[]{:S(2)}) %collective-permute-start.13) | collective-permute-done | bytes 131104 | tf_op jit(solution)/shard_map/ppermute | solution.py:25
  92.6 3.2 %collective-permute-start.4 = (bf16[1024,256]{1,0:T(8,128)(2,1)S(1)}, bf16[1024,256]{1,0:T(8,128)(2,1)S(1)}, u32[]{:S(2)}, u32[]{:S(2)}) collective-permute-start(bf16[1024,256]{1,0:T(8,128)(2,1)S(1)} %get-tuple-element.14), channel_id=1, source_target_pairs={{0,3},{1,0},{2,1},{3,2},{4,7},{5,4},{6,5},{7,6},{8,11},{9,8},{10,9... | collective-permute-start | bytes 1572872 | tf_op jit(solution)/shard_map/ppermute | solution.py:25
  95.9 3.5 %collective-permute-start.14 = (bf16[128,512]{1,0:T(8,128)(2,1)S(1)}, bf16[128,512]{1,0:T(8,128)(2,1)S(1)}, u32[]{:S(2)}, u32[]{:S(2)}) collective-permute-start(bf16[128,512]{1,0:T(8,128)(2,1)S(1)} %slice.172), channel_id=1, source_target_pairs={{0,3},{1,0},{2,1},{3,2},{4,7},{5,4},{6,5},{7,6},{8,11},{9,8},{10,9... | collective-permute-start | bytes 393224 | tf_op jit(solution)/shard_map/ppermute | solution.py:25
  99.6 11.4 %collective-permute-done.14.refs_17_ = bf16[128,512]{1,0:T(8,128)(2,1)S(1)} collective-permute-done((bf16[128,512]{1,0:T(8,128)(2,1)S(1)}, bf16[128,512]{1,0:T(8,128)(2,1)S(1)}, u32[]{:S(2)}, u32[]{:S(2)}) %collective-permute-start.14) | collective-permute-done | bytes 131104 | tf_op jit(solution)/shard_map/ppermute | solution.py:25
  110.9 3.7 %collective-permute-start.10 = (bf16[1024,256]{1,0:T(8,128)(2,1)S(1)}, bf16[1024,256]{1,0:T(8,128)(2,1)S(1)}, u32[]{:S(2)}, u32[]{:S(2)}) collective-permute-start(bf16[1024,256]{1,0:T(8,128)(2,1)S(1)} %slice.169), channel_id=1, source_target_pairs={{0,3},{1,0},{2,1},{3,2},{4,7},{5,4},{6,5},{7,6},{8,11},{9,8},{10,9... | collective-permute-start | bytes 1572872 | tf_op jit(solution)/shard_map/ppermute | solution.py:25
  114.6 1.0 slice.173
  115.8 4.0 %collective-permute-done.7.refs_9_ = bf16[1024,256]{1,0:T(8,128)(2,1)S(1)} collective-permute-done((bf16[1024,256]{1,0:T(8,128)(2,1)S(1)}, bf16[1024,256]{1,0:T(8,128)(2,1)S(1)}, u32[]{:S(2)}, u32[]{:S(2)}) %collective-permute-start.7) | collective-permute-done | bytes 524320 | tf_op jit(solution)/shard_map/ppermute | solution.py:25
  119.8 2.4 %collective-permute-done.8.refs_10_ = bf16[1024,256]{1,0:T(8,128)(2,1)S(1)} collective-permute-done((bf16[1024,256]{1,0:T(8,128)(2,1)S(1)}, bf16[1024,256]{1,0:T(8,128)(2,1)S(1)}, u32[]{:S(2)}, u32[]{:S(2)}) %collective-permute-start.8) | collective-permute-done | bytes 524320 | tf_op jit(solution)/shard_map/ppermute | solution.py:25
  122.2 11.2 %collective-permute-done.10.refs_12_ = bf16[1024,256]{1,0:T(8,128)(2,1)S(1)} collective-permute-done((bf16[1024,256]{1,0:T(8,128)(2,1)S(1)}, bf16[1024,256]{1,0:T(8,128)(2,1)S(1)}, u32[]{:S(2)}, u32[]{:S(2)}) %collective-permute-start.10) | collective-permute-done | bytes 524320 | tf_op jit(solution)/shard_map/ppermute | solution.py:25
  134.3 8.9 %shard_map.138 = (bf16[512,1024]{1,0:T(8,128)(2,1)}, bf16[512,512]{1,0:T(8,128)(2,1)}) custom-call(bf16[512,2048]{1,0:T(8,128)(2,1)} %bitcast.6.refs_0_, bf16[2048,256]{1,0:T(8,128)(2,1)} %bitcast.30, bf16[2048,256]{1,0:T(8,128)(2,1)} %bitcast.34, bf16[1024,256]{1,0:T(8,128)(2,1)} %copy-done.17, bf16[1024,256]{1,0:T(8,128)(2,1)} %collective-permute-done.2.refs_4_, ...), custom_call_target="tpu_custom_call" | custom-call | tf_op jit(solution)/shard_map/pallas_call | solution.py:35
  143.3 10.4 %all-to-all-start.2 = ((bf16[64,8,512]{2,1,0:T(8,128)(2,1)}), bf16[64,8,512]{2,1,0:T(8,128)(2,1)S(1)}, u32[]{:S(2)}, u32[]{:S(2)}) async-start(bf16[64,8,512]{2,1,0:T(8,128)(2,1)} %bitcast.35), calls=%async_computation.2 | async-start | bytes 1048576 | tf_op jit(solution)/shard_map/all_to_all | solution.py:367
  153.9 1.1 slice.175
  155.0 3.8 %collective-permute-start.18 = (bf16[128,1536]{1,0:T(8,128)(2,1)S(1)}, bf16[128,1536]{1,0:T(8,128)(2,1)S(1)}, u32[]{:S(2)}, u32[]{:S(2)}) collective-permute-start(bf16[128,1536]{1,0:T(8,128)(2,1)S(1)} %slice.175), channel_id=1, source_target_pairs={{0,3},{1,0},{2,1},{3,2},{4,7},{5,4},{6,5},{7,6},{8,11},{9,8},{10,9... | collective-permute-start | bytes 1179656 | tf_op jit(solution)/shard_map/ppermute | solution.py:25
  158.8 8.2 %collective-permute-done.17.refs_2_ = bf16[128,1536]{1,0:T(8,128)(2,1)S(1)} collective-permute-done((bf16[128,1536]{1,0:T(8,128)(2,1)S(1)}, bf16[128,1536]{1,0:T(8,128)(2,1)S(1)}, u32[]{:S(2)}, u32[]{:S(2)}) %collective-permute-start.17) | collective-permute-done | bytes 393248 | tf_op jit(solution)/shard_map/ppermute | solution.py:25
  167.4 3.9 %shard_map.139 = bf16[512,1536]{1,0:T(8,128)(2,1)} custom-call(bf16[512,1024]{1,0:T(8,128)(2,1)S(1)} %copy-done.5, bf16[256,2048]{1,0:T(8,128)(2,1)S(1)} %bitcast.21, bf16[256,1536]{1,0:T(8,128)(2,1)S(1)} %collective-permute-done.15.refs_0_, bf16[256,1536]{1,0:T(8,128)(2,1)} %collective-permute-done.16.refs_1_, ...), custom_call_target="tpu_custom_call" | custom-call | tf_op jit(solution)/shard_map/pallas_call | solution.py:35
  171.4 10.3 %all-to-all-start.3 = ((bf16[64,8,1536]{2,1,0:T(8,128)(2,1)}), bf16[64,8,1536]{2,1,0:T(8,128)(2,1)S(1)}, u32[]{:S(2)}, u32[]{:S(2)}) async-start(bf16[64,8,1536]{2,1,0:T(8,128)(2,1)} %bitcast.29), calls=%async_computation.3 | async-start | bytes 3145728 | tf_op jit(solution)/shard_map/all_to_all | solution.py:367
  182.5 39.2 %all-to-all-done.3 = bf16[64,8,1536]{2,1,0:T(8,128)(2,1)S(1)} async-done(((bf16[64,8,1536]{2,1,0:T(8,128)(2,1)}), bf16[64,8,1536]{2,1,0:T(8,128)(2,1)S(1)}, u32[]{:S(2)}, u32[]{:S(2)}) %all-to-all-start.3) | async-done | bytes 1572896 | tf_op jit(solution)/shard_map/all_to_all | solution.py:367
  221.7 3.1 %shard_map.140 = bf16[128,2048]{1,0:T(8,128)(2,1)} custom-call(f32[128,2048]{1,0:T(8,128)} %get-tuple-element.9.stream_in, s32[128,2]{1,0:T(8,128)S(1)} %copy.17.routes_ref, f32[128,2]{1,0:T(8,128)S(1)} %copy.18.weights_ref, bf16[512,512]{1,0:T(8,128)(2,1)S(1)} %bitcast.23, bf16[512,1536]{1,0:T(8,128)(2,1)S(1)} %bitcast.22), custom_call_target="tpu_custom_call" | custom-call | tf_op jit(solution)/shard_map/pallas_call | solution.py:35
  (85 shorter events, 8.4 us)
Async XLA Ops:
  0.0 28.0 %copy-start.9 = (f32[2048]{0:T(1024)S(1)}, f32[2048]{0:T(1024)}, u32[]{:S(2)}) copy-start(f32[2048]{0:T(1024)} %param.22) | copy-start | bytes 24580
  0.0 28.0 %copy-start.6 = (bf16[128,2048]{1,0:T(8,128)(2,1)S(1)}, bf16[128,2048]{1,0:T(8,128)(2,1)}, u32[]{:S(2)}) copy-start(bf16[128,2048]{1,0:T(8,128)(2,1)} %residual_ref.1) | copy-start | bytes 1572868
  1.4 5.3 %collective-permute-start = (bf16[32,256]{1,0:T(8,128)(2,1)}, bf16[32,256]{1,0:T(8,128)(2,1)S(1)}, u32[]{:S(2)}, u32[]{:S(2)}) collective-permute-start(bf16[32,256]{1,0:T(8,128)(2,1)} %rim_rows.1), channel_id=1, source_target_pairs={{0,4},{4,8},{8,12},{12,16},{16,20},{20,24},{24,28},{28,32},{32,36}... | collective-permute-start | bytes 49160 | tf_op jit(solution)/shard_map/ppermute | solution.py:20
  16.6 11.5 %all-to-all-start = ((bf16[4,128,256]{2,1,0:T(8,128)(2,1)}), bf16[4,128,256]{2,1,0:T(8,128)(2,1)S(1)}, u32[]{:S(2)}, u32[]{:S(2)}) async-start(bf16[4,128,256]{2,1,0:T(8,128)(2,1)} %bitcast.3), calls=%async_computation | async-start | bytes 524288 | tf_op jit(solution)/shard_map/all_to_all | solution.py:339
  32.5 101.8 %all-to-all-start.1 = ((bf16[64,8,2048]{2,1,0:T(8,128)(2,1)}), bf16[64,8,2048]{2,1,0:T(8,128)(2,1)}, u32[]{:S(2)}, u32[]{:S(2)}) async-start(bf16[64,8,2048]{2,1,0:T(8,128)(2,1)} %bitcast.31), calls=%async_computation.1 | async-start | bytes 4194304 | tf_op jit(solution)/shard_map/all_to_all | solution.py:362
  45.3 50.5 %collective-permute-start.6 = (bf16[2048,256]{1,0:T(8,128)(2,1)}, bf16[2048,256]{1,0:T(8,128)(2,1)S(1)}, u32[]{:S(2)}, u32[]{:S(2)}) collective-permute-start(bf16[2048,256]{1,0:T(8,128)(2,1)} %bitcast.32), channel_id=1, source_target_pairs={{0,3},{1,0},{2,1},{3,2},{4,7},{5,4},{6,5},{7,6},{8,11},{9,8},{10,9... | collective-permute-start | bytes 3145736 | tf_op jit(solution)/shard_map/ppermute | solution.py:25
  46.6 49.3 %collective-permute-start.3 = (bf16[2048,256]{1,0:T(8,128)(2,1)}, bf16[2048,256]{1,0:T(8,128)(2,1)S(1)}, u32[]{:S(2)}, u32[]{:S(2)}) collective-permute-start(bf16[2048,256]{1,0:T(8,128)(2,1)} %bitcast.33), channel_id=1, source_target_pairs={{0,1},{1,2},{2,3},{3,0},{4,5},{5,6},{6,7},{7,4},{8,9},{9,10},{10,1... | collective-permute-start | bytes 3145736 | tf_op jit(solution)/shard_map/ppermute | solution.py:25
  47.5 32.2 %collective-permute-start.11 = (bf16[256,512]{1,0:T(8,128)(2,1)S(1)}, bf16[256,512]{1,0:T(8,128)(2,1)S(1)}, u32[]{:S(2)}, u32[]{:S(2)}) collective-permute-start(bf16[256,512]{1,0:T(8,128)(2,1)S(1)} %slice.170), channel_id=1, source_target_pairs={{0,1},{1,2},{2,3},{3,0},{4,5},{5,6},{6,7},{7,4},{8,9},{9,10},{10,1... | collective-permute-start | bytes 786440 | tf_op jit(solution)/shard_map/ppermute | solution.py:25
  48.1 31.7 %collective-permute-start.12 = (bf16[256,512]{1,0:T(8,128)(2,1)S(1)}, bf16[256,512]{1,0:T(8,128)(2,1)S(1)}, u32[]{:S(2)}, u32[]{:S(2)}) collective-permute-start(bf16[256,512]{1,0:T(8,128)(2,1)S(1)} %slice.170), channel_id=1, source_target_pairs={{0,3},{1,0},{2,1},{3,2},{4,7},{5,4},{6,5},{7,6},{8,11},{9,8},{10,9... | collective-permute-start | bytes 786440 | tf_op jit(solution)/shard_map/ppermute | solution.py:25
  50.9 41.7 %collective-permute-start.1 = (bf16[1024,256]{1,0:T(8,128)(2,1)S(1)}, bf16[1024,256]{1,0:T(8,128)(2,1)S(1)}, u32[]{:S(2)}, u32[]{:S(2)}) collective-permute-start(bf16[1024,256]{1,0:T(8,128)(2,1)S(1)} %get-tuple-element.14), channel_id=1, source_target_pairs={{0,1},{1,2},{2,3},{3,0},{4,5},{5,6},{6,7},{7,4},{8,9},{9,10},{10,1... | collective-permute-start | bytes 1572872 | tf_op jit(solution)/shard_map/ppermute | solution.py:25
  79.7 36.0 %copy-start.15 = (bf16[256,512]{1,0:T(8,128)(2,1)}, bf16[256,512]{1,0:T(8,128)(2,1)S(1)}, u32[]{:S(2)}) copy-start(bf16[256,512]{1,0:T(8,128)(2,1)S(1)} %collective-permute-done.11.refs_14_) | copy-start | bytes 786436
  79.7 12.9 %collective-permute-start.13 = (bf16[128,512]{1,0:T(8,128)(2,1)S(1)}, bf16[128,512]{1,0:T(8,128)(2,1)S(1)}, u32[]{:S(2)}, u32[]{:S(2)}) collective-permute-start(bf16[128,512]{1,0:T(8,128)(2,1)S(1)} %slice.171), channel_id=1, source_target_pairs={{0,1},{1,2},{2,3},{3,0},{4,5},{5,6},{6,7},{7,4},{8,9},{9,10},{10,1... | collective-permute-start | bytes 393224 | tf_op jit(solution)/shard_map/ppermute | solution.py:25
  79.8 35.9 %copy-start.16 = (bf16[256,512]{1,0:T(8,128)(2,1)}, bf16[256,512]{1,0:T(8,128)(2,1)S(1)}, u32[]{:S(2)}) copy-start(bf16[256,512]{1,0:T(8,128)(2,1)S(1)} %collective-permute-done.12.refs_15_) | copy-start | bytes 786436
  79.8 19.7 %collective-permute-start.5 = (bf16[1024,256]{1,0:T(8,128)(2,1)S(1)}, bf16[1024,256]{1,0:T(8,128)(2,1)S(1)}, u32[]{:S(2)}, u32[]{:S(2)}) collective-permute-start(bf16[1024,256]{1,0:T(8,128)(2,1)S(1)} %get-tuple-element.13), channel_id=1, source_target_pairs={{0,3},{1,0},{2,1},{3,2},{4,7},{5,4},{6,5},{7,6},{8,11},{9,8},{10,9... | collective-permute-start | bytes 1572872 | tf_op jit(solution)/shard_map/ppermute | solution.py:25
  92.6 41.7 %copy-start.23 = (bf16[128,512]{1,0:T(8,128)(2,1)}, bf16[128,512]{1,0:T(8,128)(2,1)S(1)}, u32[]{:S(2)}) copy-start(bf16[128,512]{1,0:T(8,128)(2,1)S(1)} %collective-permute-done.13.refs_16_) | copy-start | bytes 393220
  92.6 22.1 %collective-permute-start.2 = (bf16[1024,256]{1,0:T(8,128)(2,1)S(1)}, bf16[1024,256]{1,0:T(8,128)(2,1)}, u32[]{:S(2)}, u32[]{:S(2)}) collective-permute-start(bf16[1024,256]{1,0:T(8,128)(2,1)S(1)} %get-tuple-element.13), channel_id=1, source_target_pairs={{0,1},{1,2},{2,3},{3,0},{4,5},{5,6},{6,7},{7,4},{8,9},{9,10},{10,1... | collective-permute-start | bytes 1572872 | tf_op jit(solution)/shard_map/ppermute | solution.py:25
  92.6 41.7 %copy-start.17 = (bf16[1024,256]{1,0:T(8,128)(2,1)}, bf16[1024,256]{1,0:T(8,128)(2,1)S(1)}, u32[]{:S(2)}) copy-start(bf16[1024,256]{1,0:T(8,128)(2,1)S(1)} %collective-permute-done.1.refs_3_) | copy-start | bytes 1572868
  92.6 23.1 %collective-permute-start.4 = (bf16[1024,256]{1,0:T(8,128)(2,1)S(1)}, bf16[1024,256]{1,0:T(8,128)(2,1)S(1)}, u32[]{:S(2)}, u32[]{:S(2)}) collective-permute-start(bf16[1024,256]{1,0:T(8,128)(2,1)S(1)} %get-tuple-element.14), channel_id=1, source_target_pairs={{0,3},{1,0},{2,1},{3,2},{4,7},{5,4},{6,5},{7,6},{8,11},{9,8},{10,9... | collective-permute-start | bytes 1572872 | tf_op jit(solution)/shard_map/ppermute | solution.py:25
  95.8 38.5 %copy-start.13 = (bf16[2048,256]{1,0:T(8,128)(2,1)}, bf16[2048,256]{1,0:T(8,128)(2,1)S(1)}, u32[]{:S(2)}) copy-start(bf16[2048,256]{1,0:T(8,128)(2,1)S(1)} %collective-permute-done.6.refs_8_) | copy-start | bytes 3145732
  95.8 24.0 %collective-permute-start.7 = (bf16[1024,256]{1,0:T(8,128)(2,1)S(1)}, bf16[1024,256]{1,0:T(8,128)(2,1)S(1)}, u32[]{:S(2)}, u32[]{:S(2)}) collective-permute-start(bf16[1024,256]{1,0:T(8,128)(2,1)S(1)} %collective-permute-done.1.refs_3_), channel_id=1, source_target_pairs={{0,1},{1,2},{2,3},{3,0},{4,5},{5,6},{6,7},{7,4},{8,9},{9,10},{10,1... | collective-permute-start | bytes 1572872 | tf_op jit(solution)/shard_map/ppermute | solution.py:25
  95.9 15.1 %collective-permute-start.14 = (bf16[128,512]{1,0:T(8,128)(2,1)S(1)}, bf16[128,512]{1,0:T(8,128)(2,1)S(1)}, u32[]{:S(2)}, u32[]{:S(2)}) collective-permute-start(bf16[128,512]{1,0:T(8,128)(2,1)S(1)} %slice.172), channel_id=1, source_target_pairs={{0,3},{1,0},{2,1},{3,2},{4,7},{5,4},{6,5},{7,6},{8,11},{9,8},{10,9... | collective-permute-start | bytes 393224 | tf_op jit(solution)/shard_map/ppermute | solution.py:25
  99.4 34.9 %copy-start.18 = (bf16[1024,256]{1,0:T(8,128)(2,1)}, bf16[1024,256]{1,0:T(8,128)(2,1)S(1)}, u32[]{:S(2)}) copy-start(bf16[1024,256]{1,0:T(8,128)(2,1)S(1)} %collective-permute-done.5.refs_7_) | copy-start | bytes 1572868
  99.5 22.7 %collective-permute-start.8 = (bf16[1024,256]{1,0:T(8,128)(2,1)S(1)}, bf16[1024,256]{1,0:T(8,128)(2,1)S(1)}, u32[]{:S(2)}, u32[]{:S(2)}) collective-permute-start(bf16[1024,256]{1,0:T(8,128)(2,1)S(1)} %collective-permute-done.5.refs_7_), channel_id=1, source_target_pairs={{0,3},{1,0},{2,1},{3,2},{4,7},{5,4},{6,5},{7,6},{8,11},{9,8},{10,9... | collective-permute-start | bytes 1572872 | tf_op jit(solution)/shard_map/ppermute | solution.py:25
  110.9 22.5 %collective-permute-start.10 = (bf16[1024,256]{1,0:T(8,128)(2,1)S(1)}, bf16[1024,256]{1,0:T(8,128)(2,1)S(1)}, u32[]{:S(2)}, u32[]{:S(2)}) collective-permute-start(bf16[1024,256]{1,0:T(8,128)(2,1)S(1)} %slice.169), channel_id=1, source_target_pairs={{0,3},{1,0},{2,1},{3,2},{4,7},{5,4},{6,5},{7,6},{8,11},{9,8},{10,9... | collective-permute-start | bytes 1572872 | tf_op jit(solution)/shard_map/ppermute | solution.py:25
  114.6 19.6 %collective-permute-start.9 = (bf16[1024,256]{1,0:T(8,128)(2,1)S(1)}, bf16[1024,256]{1,0:T(8,128)(2,1)}, u32[]{:S(2)}, u32[]{:S(2)}) collective-permute-start(bf16[1024,256]{1,0:T(8,128)(2,1)S(1)} %slice.168), channel_id=1, source_target_pairs={{0,1},{1,2},{2,3},{3,0},{4,5},{5,6},{6,7},{7,4},{8,9},{9,10},{10,1... | collective-permute-start | bytes 1572872 | tf_op jit(solution)/shard_map/ppermute | solution.py:25
  115.7 38.1 %collective-permute-start.15 = (bf16[256,1536]{1,0:T(8,128)(2,1)}, bf16[256,1536]{1,0:T(8,128)(2,1)S(1)}, u32[]{:S(2)}, u32[]{:S(2)}) collective-permute-start(bf16[256,1536]{1,0:T(8,128)(2,1)} %slice.173), channel_id=1, source_target_pairs={{0,1},{1,2},{2,3},{3,0},{4,5},{5,6},{6,7},{7,4},{8,9},{9,10},{10,1... | collective-permute-start | bytes 2359304 | tf_op jit(solution)/shard_map/ppermute | solution.py:25
  119.8 34.1 %collective-permute-start.16 = (bf16[256,1536]{1,0:T(8,128)(2,1)}, bf16[256,1536]{1,0:T(8,128)(2,1)}, u32[]{:S(2)}, u32[]{:S(2)}) collective-permute-start(bf16[256,1536]{1,0:T(8,128)(2,1)} %slice.173), channel_id=1, source_target_pairs={{0,3},{1,0},{2,1},{3,2},{4,7},{5,4},{6,5},{7,6},{8,11},{9,8},{10,9... | collective-permute-start | bytes 2359304 | tf_op jit(solution)/shard_map/ppermute | solution.py:25
  143.3 24.2 %copy-start.2 = (bf16[1,256,2048]{2,1,0:T(8,128)(2,1)S(1)}, bf16[1,256,2048]{2,1,0:T(8,128)(2,1)}, u32[]{:S(2)}) copy-start(bf16[1,256,2048]{2,1,0:T(8,128)(2,1)} %param.27) | copy-start | bytes 3145732
  143.3 28.1 %all-to-all-start.2 = ((bf16[64,8,512]{2,1,0:T(8,128)(2,1)}), bf16[64,8,512]{2,1,0:T(8,128)(2,1)S(1)}, u32[]{:S(2)}, u32[]{:S(2)}) async-start(bf16[64,8,512]{2,1,0:T(8,128)(2,1)} %bitcast.35), calls=%async_computation.2 | async-start | bytes 1048576 | tf_op jit(solution)/shard_map/all_to_all | solution.py:367
  153.8 13.2 %collective-permute-start.17 = (bf16[128,1536]{1,0:T(8,128)(2,1)S(1)}, bf16[128,1536]{1,0:T(8,128)(2,1)S(1)}, u32[]{:S(2)}, u32[]{:S(2)}) collective-permute-start(bf16[128,1536]{1,0:T(8,128)(2,1)S(1)} %slice.174), channel_id=1, source_target_pairs={{0,1},{1,2},{2,3},{3,0},{4,5},{5,6},{6,7},{7,4},{8,9},{9,10},{10,1... | collective-permute-start | bytes 1179656 | tf_op jit(solution)/shard_map/ppermute | solution.py:25
  155.0 12.4 %collective-permute-start.18 = (bf16[128,1536]{1,0:T(8,128)(2,1)S(1)}, bf16[128,1536]{1,0:T(8,128)(2,1)S(1)}, u32[]{:S(2)}, u32[]{:S(2)}) collective-permute-start(bf16[128,1536]{1,0:T(8,128)(2,1)S(1)} %slice.175), channel_id=1, source_target_pairs={{0,3},{1,0},{2,1},{3,2},{4,7},{5,4},{6,5},{7,6},{8,11},{9,8},{10,9... | collective-permute-start | bytes 1179656 | tf_op jit(solution)/shard_map/ppermute | solution.py:25
  171.4 50.3 %all-to-all-start.3 = ((bf16[64,8,1536]{2,1,0:T(8,128)(2,1)}), bf16[64,8,1536]{2,1,0:T(8,128)(2,1)S(1)}, u32[]{:S(2)}, u32[]{:S(2)}) async-start(bf16[64,8,1536]{2,1,0:T(8,128)(2,1)} %bitcast.29), calls=%async_computation.3 | async-start | bytes 3145728 | tf_op jit(solution)/shard_map/all_to_all | solution.py:367
  (16 other events, 148.2 us)

commit v5 on v4

--- a/solution.py
+++ b/solution.py
@@ -9,7 +9,7 @@
 
 TAPS = 31
 RIM = 32
-FIRST = 2
+FIRST = 3
 LANES = 128
 BLOCK = 64
 
@@ -58,26 +58,52 @@
     return (value.astype(jnp.float32) * jax.nn.sigmoid(gate.astype(jnp.float32))).astype(jnp.bfloat16)
 
 
-def rim_body(value_ref, gate_ref, segments_ref, out_ref):
-    width = value_ref.shape[1]
+def rim_body(value_in, gate_in, segments_ref, w_gate_in, w_up_in, out_ref, head_out, tail_out, value_ref, gate_ref, sems):
+    tok, width = value_in.shape
+    deep, cut = w_gate_in.shape[0], head_out.shape[0]
+    loads = fetch(
+        [(value_in.at[tok - RIM :], value_ref), (gate_in.at[tok - RIM :], gate_ref)], sems
+    )
+    packs = fetch(
+        [
+            (w_gate_in.at[:cut], head_out),
+            (w_gate_in.at[cut:], tail_out.at[: deep - cut]),
+            (w_up_in, tail_out.at[deep - cut :]),
+        ],
+        sems,
+        2,
+    )
+    for c in loads:
+        c.wait()
     gated = gated_rows(value_ref[...], gate_ref[...]).astype(jnp.float32)
     last = segments_ref[segments_ref.shape[0] - 1 :, :].astype(jnp.float32)
     named = jnp.concatenate([last] + [jnp.zeros_like(last)] * (width // LANES - 1), axis=1)
     row = lax.broadcasted_iota(jnp.int32, gated.shape, 0)
     out_ref[...] = jnp.where(row == 0, named, gated).astype(jnp.bfloat16)
-
-
-def rim_rows(value, gate, segments):
-    tok, width = value.shape
-    last = pl.BlockSpec((RIM, width), lambda i: (tok // RIM - 1, 0))
-    return pl.pallas_call(
+    for c in packs:
+        c.wait()
+
+
+def rim_and_packs(value, gate, segments, w_gate, w_up):
+    width = value.shape[1]
+    deep, wide = w_gate.shape
+    return kernel(
         rim_body,
-        grid=(1,),
-        in_specs=[last, last, pl.BlockSpec(segments.shape, lambda i: (0, 0))],
-        out_specs=pl.BlockSpec((RIM, width), lambda i: (0, 0)),
-        out_shape=jax.ShapeDtypeStruct((RIM, width), jnp.bfloat16),
-        name="rim_rows",
-    )(value, gate, segments)
+        [
+            ((RIM, width), jnp.bfloat16),
+            ((deep // 2, wide), jnp.bfloat16),
+            ((deep - deep // 2 + w_up.shape[0], wide), jnp.bfloat16),
+        ],
+        (value, gate, segments, w_gate, w_up),
+        scratch=[
+            pltpu.VMEM((RIM, width), jnp.bfloat16),
+            pltpu.VMEM((RIM, width), jnp.bfloat16),
+            pltpu.SemaphoreType.DMA((5,)),
+        ],
+        limit=8,
+        far_in=(0, 1, 3, 4),
+        far_out=(1, 2),
+    )
 
 
 def conv_body(value_ref, gate_ref, rim_ref, segments_ref, seen_ref, taps_ref, gain_ref, shift_ref, out_ref, rows_ref):
@@ -193,24 +219,23 @@
         c.wait()
 
 
-def experts_body(counts, cols, *refs):
+def experts_body(layout, cols, *refs):
     rows_in, *pieces, hidden_out, out, rows_ref, w_ref, hidden_ref, down_ref, out_ref, sems = refs
     width = pieces[0].shape[1]
     (load,) = fetch([(rows_in, rows_ref)], sems)
     loads, at = [], 1
-    for q, kinds in enumerate(counts):
-        copies = []
-        for kind, n in enumerate(kinds):
-            top = 0
-            for piece in pieces[:n]:
-                end = top + piece.shape[0]
-                copies.append((piece, w_ref.at[q, top:end, kind * width : (kind + 1) * width]))
-                top = end
-            pieces = pieces[n:]
+    for q, spans in enumerate(layout):
+        copies = [
+            (
+                pieces[i].at[start:stop],
+                w_ref.at[q, top : top + stop - start, kind * width : (kind + 1) * width],
+            )
+            for i, start, stop, kind, top in spans
+        ]
         loads.append(fetch(copies, sems, at))
         at += len(copies)
     copies, top = [], 0
-    for piece in pieces:
+    for piece in pieces[1 + max(span[0] for spans in layout for span in spans) :]:
         src = piece.at[:, cols] if top == 0 else piece
         copies.append((src, down_ref.at[top : top + piece.shape[0]]))
         top += piece.shape[0]
@@ -232,25 +257,24 @@
         c.wait()
 
 
-def expert_rows(rows, quarters, downs, cols):
-    counts = tuple((len(gates), len(ups)) for gates, ups in quarters)
-    pieces = [p for gates, ups in quarters for p in (*gates, *ups)] + downs
+def expert_rows(rows, pieces, layout, downs, cols):
     (n, d), width, out_width = rows.shape, pieces[0].shape[1], cols.stop - cols.start
-    units = width * len(counts)
+    units = width * len(layout)
+    n_copies = 1 + sum(len(spans) for spans in layout) + len(downs)
     return kernel(
-        functools.partial(experts_body, counts, cols),
+        functools.partial(experts_body, layout, cols),
         [((n, units), jnp.bfloat16), ((n, out_width), jnp.bfloat16)],
-        (rows, *pieces),
+        (rows, *pieces, *downs),
         scratch=[
             pltpu.VMEM((n, d), jnp.bfloat16),
-            pltpu.VMEM((len(counts), d, 2 * width), jnp.bfloat16),
+            pltpu.VMEM((len(layout), d, 2 * width), jnp.bfloat16),
             pltpu.VMEM((n, units), jnp.bfloat16),
             pltpu.VMEM((units, out_width), jnp.bfloat16),
             pltpu.VMEM((n, out_width), jnp.bfloat16),
-            pltpu.SemaphoreType.DMA((len(pieces) + 1,)),
+            pltpu.SemaphoreType.DMA((n_copies,)),
         ],
         limit=22,
-        far_in=range(1 + len(pieces)),
+        far_in=range(1 + len(pieces) + len(downs)),
         far_out=(0, 1),
     )
 
@@ -288,15 +312,20 @@
     )
 
 
-def gathered(shard, parts):
+def gathered_down(shard):
     half = shard.shape[0] // 2
-    pieces = [shard] if parts == 1 else [shard[:half], shard[half:]]
-    left, right = [], []
-    for piece in pieces:
-        left.append(ring(piece, "tp", 1))
-        right.append(ring(piece, "tp", -1))
-    far = [ring(left[0][:half], "tp", 1), ring(right[-1][-half:], "tp", -1)]
-    return left, right, far
+    left, right = ring(shard, "tp", 1), ring(shard, "tp", -1)
+    far = [ring(left[:half], "tp", 1), ring(right[half:], "tp", -1)]
+    return [left], [right], far
+
+
+def gathered_down_halves(shard):
+    half = shard.shape[0] // 2
+    top, low = shard[:half], shard[half:]
+    left_top, right_low = ring(top, "tp", 1), ring(low, "tp", -1)
+    left_low, right_top = ring(low, "tp", 1), ring(top, "tp", -1)
+    far = [ring(left_top, "tp", 1), ring(right_low, "tp", -1)]
+    return [left_top, left_low], [right_top, right_low], far
 
 
 def shards(
@@ -318,13 +347,20 @@
     tok_dev, local_channels = conv_value.shape
     reach = conv_weight.shape[0] - 1
     model_width = w_down.shape[2]
-    gates = gathered(w_gate[0], 2)
-    ups = gathered(w_up[0], 1)
     cut = model_width * FIRST // 8
     groups = slice(0, cut), slice(cut, model_width)
-    downs = [gathered(w_down[0][:, cols], 1) for cols in groups]
     lines = segments.reshape(tok_dev // LANES, LANES)
-    rim = passed_along(rim_rows(conv_value, conv_gate, lines), "sp", 1)
+    rim, head, tail = rim_and_packs(conv_value, conv_gate, lines, w_gate[0], w_up[0])
+    rim = passed_along(rim, "sp", 1)
+    deep, split = w_gate.shape[1], head.shape[0]
+    head_left, head_right = ring(head, "tp", 1), ring(head, "tp", -1)
+    tail_left, tail_right = ring(tail, "tp", 1), ring(tail, "tp", -1)
+    last = deep
+    far_head = ring(head_left, "tp", 1)
+    far_first = ring(tail_right[:last], "tp", -1)
+    far_last = ring(tail_left[last:], "tp", 1)
+    first = gathered_down(w_down[0][:, groups[0]])
+    second = gathered_down_halves(w_down[0][:, groups[1]])
     padded = jnp.pad(segments, (reach, 0), constant_values=-1)
     seen = jnp.zeros((tok_dev,), jnp.int32)
     for offset in range(reach):
@@ -368,11 +404,24 @@
             out.reshape(experts_n, capacity, -1), "sp", 0, 0, tiled=True
         ).reshape(slot_total, -1)
 
-    first, second = ([w_down[0], *left, *right, *far] for left, right, far in downs)
-    quarters = [([w_gate[0]], [w_up[0]])] + [(gates[side], ups[side]) for side in range(3)]
-    hidden, out = expert_rows(arrived, quarters, first, groups[0])
+    pieces = [w_gate[0], w_up[0], head_left, tail_left, head_right, tail_right, far_head, far_first, far_last]
+    own = ((0, 0, deep, 0, 0), (1, 0, deep, 1, 0))
+    near = [
+        ((i, 0, split, 0, 0), (i + 1, 0, deep - split, 0, split), (i + 1, deep - split, 2 * deep - split, 1, 0))
+        for i in (2, 4)
+    ]
+    met = last - (deep - split)
+    far = (
+        (6, 0, split, 0, 0),
+        (7, 0, deep - split, 0, split),
+        (7, deep - split, last, 1, 0),
+        (8, 0, deep - met, 1, met),
+    )
+    hidden, out = expert_rows(
+        arrived, pieces, (own, *near, far), [w_down[0]] + [p for side in first for p in side], groups[0]
+    )
     back = [returned(out)]
-    out = down_rows(hidden, second[0], second[1:], groups[1])
+    out = down_rows(hidden, w_down[0], [p for side in second for p in side], groups[1])
     back.append(returned(out))
     return kernel(
         functools.partial(combine_body, experts_n),

time: 227 us -> 293 us (1.29)
  Pallas kernels: 26.8 us -> 89.8 us
  waiting for transfers between devices: 124 us -> 131 us
    pallas_call x5 -> x6, Pallas kernels: 25.4 us -> 89.8 us  [kernel(): pl.pallas_call(body, out_shape=[pltpu.HBM(*o) if i in far_out else jax.Sh...]
    ppermute x18 -> x17, waiting for transfers between devices: 76 us -> 87.9 us  [ring(): lax.ppermute(value, axis, [(i, (i + steps) % count) for i in range(count)])]
    all_to_all x2, waiting for transfers between devices: 39.2 us -> 33.6 us  [returned(): lax.all_to_all(out.reshape(experts_n, capacity, -1), 'sp', 0, 0, tiled=True)]
    ppermute x18 -> x17, starting transfers between devices: 23.2 us -> 24.5 us  [ring(): lax.ppermute(value, axis, [(i, (i + steps) % count) for i in range(count)])]
  transfers between devices with their start and end apart: 23 -> 22, of which waited for: 11 -> 12; matrix products, arithmetic and copies ran while one was open for 2% -> 1% of each run, Pallas kernels for 6% -> 1%
where the time goes in v5:
time: 293 us
  waiting for transfers between devices  131 us (45%)
  Pallas kernels  89.8 us (31%)
  starting transfers between devices  64.7 us (22%)
  local copies, waits for them, and re-layouts  6.35 us (2%)
    pallas_call x6, Pallas kernels, kernel(): pl.pallas_call(body, out_shape=[pltpu.HBM(*o) if i in far_out else jax.Sh...  89.8 us
    ppermute x17, waiting for transfers between devices, ring(): lax.ppermute(value, axis, [(i, (i + steps) % count) for i in range(count)])  87.9 us
    all_to_all x2, waiting for transfers between devices, returned(): lax.all_to_all(out.reshape(experts_n, capacity, -1), 'sp', 0, 0, tiled=True)  33.6 us
    ppermute x17, starting transfers between devices, ring(): lax.ppermute(value, axis, [(i, (i + steps) % count) for i in range(count)])  24.5 us
    all_to_all x2, starting transfers between devices, returned(): lax.all_to_all(out.reshape(experts_n, capacity, -1), 'sp', 0, 0, tiled=True)  20.8 us
    all_to_all x1, starting transfers between devices, shards(): lax.all_to_all(outgoing.reshape(experts_n, capacity, model_width), 'sp',...  12.9 us
    all_to_all x1, waiting for transfers between devices, shards(): lax.all_to_all(conv_out.reshape(columns, rows_own, local_channels), 'tp',...  6.56 us
  transfers between devices with their start and end apart: 22, of which 12 were waited for; matrix products, arithmetic and copies ran while one was open for 1% of the time, Pallas kernels for 1%

profile of v5, /device:TPU:2, one launch (start us, length us, event | category | flops | bytes accessed | tf_op | source)
XLA Modules:
  0.0 292.5 jit_solution(483933421597856659)
XLA Ops:
  0.8 64.7 %shard_map.136 = (bf16[32,256]{1,0:T(8,128)(2,1)S(1)}, bf16[1024,256]{1,0:T(8,128)(2,1)}, bf16[3072,256]{1,0:T(8,128)(2,1)}) custom-call(bf16[512,256]{1,0:T(8,128)(2,1)} %value_ref.1, bf16[512,256]{1,0:T(8,128)(2,1)} %gate_ref.1, s32[4,128]{1,0:T(4,128)S(1)} %bitcast.20, bf16[2048,256]{1,0:T(8,128)(2,1)} %bitcast.27, bf16[2048,256]{1,0:T(8,128)(2,1)} %bitcast.29), custom_call_target="tpu_custom_call" | custom-call | tf_op jit(solution)/shard_map/pallas_call | solution.py:35
  65.5 2.1 collective-permute-start
  67.7 3.0 %collective-permute-done.rim_ref = bf16[32,256]{1,0:T(8,128)(2,1)S(1)} collective-permute-done((bf16[32,256]{1,0:T(8,128)(2,1)S(1)}, bf16[32,256]{1,0:T(8,128)(2,1)S(1)}, u32[]{:S(2)}, u32[]{:S(2)}) %collective-permute-start) | collective-permute-done | bytes 16416 | tf_op jit(solution)/shard_map/ppermute | solution.py:20
  70.8 5.1 %shard_map.137 = bf16[512,256]{1,0:T(8,128)(2,1)} custom-call(bf16[512,256]{1,0:T(8,128)(2,1)S(1)} %copy-done.2, bf16[512,256]{1,0:T(8,128)(2,1)S(1)} %copy-done.3, bf16[32,256]{1,0:T(8,128)(2,1)S(1)} %collective-permute-done.rim_ref, s32[4,128]{1,0:T(4,128)S(1)} %bitcast.21, s32[512,128]{1,0:T(8,128)S(1)} %broadcast_in_dim.15.seen_ref, ...), custom_call_target="tpu_custom_call" | custom-call | tf_op jit(solution)/shard_map/pallas_call | solution.py:35
  75.9 4.5 %all-to-all-start = ((bf16[4,128,256]{2,1,0:T(8,128)(2,1)}), bf16[4,128,256]{2,1,0:T(8,128)(2,1)S(1)}, u32[]{:S(2)}, u32[]{:S(2)}) async-start(bf16[4,128,256]{2,1,0:T(8,128)(2,1)} %bitcast.5), calls=%async_computation | async-start | bytes 524288 | tf_op jit(solution)/shard_map/all_to_all | solution.py:375
  80.5 6.6 %all-to-all-done.parts_ref = bf16[4,128,256]{2,1,0:T(8,128)(2,1)S(1)} async-done(((bf16[4,128,256]{2,1,0:T(8,128)(2,1)}), bf16[4,128,256]{2,1,0:T(8,128)(2,1)S(1)}, u32[]{:S(2)}, u32[]{:S(2)}) %all-to-all-start) | async-done | bytes 262176 | tf_op jit(solution)/shard_map/all_to_all | solution.py:375
  87.1 4.4 %shard_map.138 = (f32[128,2048]{1,0:T(8,128)}, bf16[512,2048]{1,0:T(8,128)(2,1)}) custom-call(bf16[4,128,256]{2,1,0:T(8,128)(2,1)S(1)} %all-to-all-done.parts_ref, bf16[128,2048]{1,0:T(8,128)(2,1)S(1)} %copy-done.5, f32[1,2048]{1,0:T(1,128)S(1)} %bitcast.22, s32[128,2]{1,0:T(8,128)S(1)} %copy.17.routes_ref, bf16[1024,2048]{1,0:T(8,128)(2,1)} %weight_ref.1), custom_call_target="tpu_custom_call" | custom-call | tf_op jit(solution)/shard_map/pallas_call | solution.py:35
  91.4 12.9 %all-to-all-start.1 = ((bf16[64,8,2048]{2,1,0:T(8,128)(2,1)}), bf16[64,8,2048]{2,1,0:T(8,128)(2,1)S(1)}, u32[]{:S(2)}, u32[]{:S(2)}) async-start(bf16[64,8,2048]{2,1,0:T(8,128)(2,1)} %bitcast.31), calls=%async_computation.1 | async-start | bytes 4194304 | tf_op jit(solution)/shard_map/all_to_all | solution.py:398
  104.3 1.3 collective-permute-start.4
  107.0 34.0 %collective-permute-done.4.refs_6_ = bf16[3072,256]{1,0:T(8,128)(2,1)S(1)} collective-permute-done((bf16[3072,256]{1,0:T(8,128)(2,1)}, bf16[3072,256]{1,0:T(8,128)(2,1)S(1)}, u32[]{:S(2)}, u32[]{:S(2)}) %collective-permute-start.4) | collective-permute-done | bytes 1572896 | tf_op jit(solution)/shard_map/ppermute | solution.py:25
  141.1 2.5 collective-permute-start.6
  143.6 1.0 slice.153
  144.7 3.2 %collective-permute-start.3 = (bf16[1024,256]{1,0:T(8,128)(2,1)}, bf16[1024,256]{1,0:T(8,128)(2,1)S(1)}, u32[]{:S(2)}, u32[]{:S(2)}) collective-permute-start(bf16[1024,256]{1,0:T(8,128)(2,1)} %get-tuple-element.15), channel_id=1, source_target_pairs={{0,3},{1,0},{2,1},{3,2},{4,7},{5,4},{6,5},{7,6},{8,11},{9,8},{10,9... | collective-permute-start | bytes 1572872 | tf_op jit(solution)/shard_map/ppermute | solution.py:25
  147.9 7.6 %collective-permute-done.1.refs_3_ = bf16[1024,256]{1,0:T(8,128)(2,1)S(1)} collective-permute-done((bf16[1024,256]{1,0:T(8,128)(2,1)}, bf16[1024,256]{1,0:T(8,128)(2,1)S(1)}, u32[]{:S(2)}, u32[]{:S(2)}) %collective-permute-start.1) | collective-permute-done | bytes 524320 | tf_op jit(solution)/shard_map/ppermute | solution.py:25
  155.5 2.0 collective-permute-start.5
  157.6 6.3 %collective-permute-done.8.refs_11_ = bf16[256,768]{1,0:T(8,128)(2,1)S(1)} collective-permute-done((bf16[256,768]{1,0:T(8,128)(2,1)S(1)}, bf16[256,768]{1,0:T(8,128)(2,1)S(1)}, u32[]{:S(2)}, u32[]{:S(2)}) %collective-permute-start.8) | collective-permute-done | bytes 393248 | tf_op jit(solution)/shard_map/ppermute | solution.py:25
  163.9 21.2 %collective-permute-done.9.refs_12_ = bf16[256,768]{1,0:T(8,128)(2,1)S(1)} collective-permute-done((bf16[256,768]{1,0:T(8,128)(2,1)S(1)}, bf16[256,768]{1,0:T(8,128)(2,1)S(1)}, u32[]{:S(2)}, u32[]{:S(2)}) %collective-permute-start.9) | collective-permute-done | bytes 393248 | tf_op jit(solution)/shard_map/ppermute | solution.py:25
  185.8 3.3 %collective-permute-start.11 = (bf16[128,768]{1,0:T(8,128)(2,1)S(1)}, bf16[128,768]{1,0:T(8,128)(2,1)S(1)}, u32[]{:S(2)}, u32[]{:S(2)}) collective-permute-start(bf16[128,768]{1,0:T(8,128)(2,1)S(1)} %slice.155), channel_id=1, source_target_pairs={{0,3},{1,0},{2,1},{3,2},{4,7},{5,4},{6,5},{7,6},{8,11},{9,8},{10,9... | collective-permute-start | bytes 589832 | tf_op jit(solution)/shard_map/ppermute | solution.py:25
  189.1 3.3 %collective-permute-done.10.refs_13_ = bf16[128,768]{1,0:T(8,128)(2,1)S(1)} collective-permute-done((bf16[128,768]{1,0:T(8,128)(2,1)S(1)}, bf16[128,768]{1,0:T(8,128)(2,1)S(1)}, u32[]{:S(2)}, u32[]{:S(2)}) %collective-permute-start.10) | collective-permute-done | bytes 196640 | tf_op jit(solution)/shard_map/ppermute | solution.py:25
  195.8 9.8 %shard_map.139 = (bf16[512,1024]{1,0:T(8,128)(2,1)}, bf16[512,768]{1,0:T(8,128)(2,1)}) custom-call(bf16[512,2048]{1,0:T(8,128)(2,1)} %bitcast.25, bf16[2048,256]{1,0:T(8,128)(2,1)} %bitcast.28, bf16[2048,256]{1,0:T(8,128)(2,1)} %bitcast.30, bf16[1024,256]{1,0:T(8,128)(2,1)} %copy-done.18, bf16[3072,256]{1,0:T(8,128)(2,1)} %copy-done.14, ...), custom_call_target="tpu_custom_call" | custom-call | tf_op jit(solution)/shard_map/pallas_call | solution.py:35
  205.6 10.4 %all-to-all-start.2 = ((bf16[64,8,768]{2,1,0:T(8,128)(2,1)}), bf16[64,8,768]{2,1,0:T(8,128)(2,1)S(1)}, u32[]{:S(2)}, u32[]{:S(2)}) async-start(bf16[64,8,768]{2,1,0:T(8,128)(2,1)} %bitcast.32), calls=%async_computation.2 | async-start | bytes 1572864 | tf_op jit(solution)/shard_map/all_to_all | solution.py:403
  216.2 1.8 collective-permute-start.12
  217.9 1.9 collective-permute-start.15
  220.0 3.1 %collective-permute-start.14 = (bf16[128,1280]{1,0:T(8,128)(2,1)S(1)}, bf16[128,1280]{1,0:T(8,128)(2,1)S(1)}, u32[]{:S(2)}, u32[]{:S(2)}) collective-permute-start(bf16[128,1280]{1,0:T(8,128)(2,1)S(1)} %get-tuple-element.20), channel_id=1, source_target_pairs={{0,3},{1,0},{2,1},{3,2},{4,7},{5,4},{6,5},{7,6},{8,11},{9,8},{10,9... | collective-permute-start | bytes 983048 | tf_op jit(solution)/shard_map/ppermute | solution.py:25
  223.1 5.2 %collective-permute-done.12.refs_0_ = bf16[128,1280]{1,0:T(8,128)(2,1)S(1)} collective-permute-done((bf16[128,1280]{1,0:T(8,128)(2,1)S(1)}, bf16[128,1280]{1,0:T(8,128)(2,1)S(1)}, u32[]{:S(2)}, u32[]{:S(2)}) %collective-permute-start.12) | collective-permute-done | bytes 327712 | tf_op jit(solution)/shard_map/ppermute | solution.py:25
  228.5 3.1 %collective-permute-start.17 = (bf16[128,1280]{1,0:T(8,128)(2,1)S(1)}, bf16[128,1280]{1,0:T(8,128)(2,1)S(1)}, u32[]{:S(2)}, u32[]{:S(2)}) collective-permute-start(bf16[128,1280]{1,0:T(8,128)(2,1)S(1)} %collective-permute-done.15.refs_3_), channel_id=1, source_target_pairs={{0,3},{1,0},{2,1},{3,2},{4,7},{5,4},{6,5},{7,6},{8,11},{9,8},{10,9... | collective-permute-start | bytes 983048 | tf_op jit(solution)/shard_map/ppermute | solution.py:25
  231.6 3.7 %collective-permute-done.13.refs_1_ = bf16[128,1280]{1,0:T(8,128)(2,1)S(1)} collective-permute-done((bf16[128,1280]{1,0:T(8,128)(2,1)S(1)}, bf16[128,1280]{1,0:T(8,128)(2,1)S(1)}, u32[]{:S(2)}, u32[]{:S(2)}) %collective-permute-start.13) | collective-permute-done | bytes 327712 | tf_op jit(solution)/shard_map/ppermute | solution.py:25
  235.5 6.2 %collective-permute-done.16.refs_4_ = bf16[128,1280]{1,0:T(8,128)(2,1)S(1)} collective-permute-done((bf16[128,1280]{1,0:T(8,128)(2,1)S(1)}, bf16[128,1280]{1,0:T(8,128)(2,1)S(1)}, u32[]{:S(2)}, u32[]{:S(2)}) %collective-permute-start.16) | collective-permute-done | bytes 327712 | tf_op jit(solution)/shard_map/ppermute | solution.py:25
  241.8 2.8 shard_map.140
  244.6 10.3 %all-to-all-start.3 = ((bf16[64,8,1280]{2,1,0:T(8,128)(2,1)}), bf16[64,8,1280]{2,1,0:T(8,128)(2,1)S(1)}, u32[]{:S(2)}, u32[]{:S(2)}) async-start(bf16[64,8,1280]{2,1,0:T(8,128)(2,1)} %bitcast.26), calls=%async_computation.3 | async-start | bytes 2621440 | tf_op jit(solution)/shard_map/all_to_all | solution.py:403
  255.8 33.6 %all-to-all-done.3 = bf16[64,8,1280]{2,1,0:T(8,128)(2,1)S(1)} async-done(((bf16[64,8,1280]{2,1,0:T(8,128)(2,1)}), bf16[64,8,1280]{2,1,0:T(8,128)(2,1)S(1)}, u32[]{:S(2)}, u32[]{:S(2)}) %all-to-all-start.3) | async-done | bytes 1310752 | tf_op jit(solution)/shard_map/all_to_all | solution.py:403
  289.3 3.1 %shard_map.141 = bf16[128,2048]{1,0:T(8,128)(2,1)} custom-call(f32[128,2048]{1,0:T(8,128)} %get-tuple-element.13.stream_in, s32[128,2]{1,0:T(8,128)S(1)} %copy.17.routes_ref, f32[128,2]{1,0:T(8,128)S(1)} %copy.18.weights_ref, bf16[512,768]{1,0:T(8,128)(2,1)S(1)} %bitcast.19, bf16[512,1280]{1,0:T(8,128)(2,1)S(1)} %bitcast.18), custom_call_target="tpu_custom_call" | custom-call | tf_op jit(solution)/shard_map/pallas_call | solution.py:35
  (78 shorter events, 8.1 us)
Async XLA Ops:
  0.0 80.4 %copy-start = (s32[512,2]{0,1:T(2,128)S(1)}, s32[512,2]{0,1:T(2,128)}, u32[]{:S(2)}) copy-start(s32[512,2]{0,1:T(2,128)} %param.23) | copy-start | bytes 12292
  0.0 70.8 %copy-start.2 = (bf16[512,256]{1,0:T(8,128)(2,1)S(1)}, bf16[512,256]{1,0:T(8,128)(2,1)}, u32[]{:S(2)}) copy-start(bf16[512,256]{1,0:T(8,128)(2,1)} %value_ref.1) | copy-start | bytes 786436
  0.0 70.8 %copy-start.3 = (bf16[512,256]{1,0:T(8,128)(2,1)S(1)}, bf16[512,256]{1,0:T(8,128)(2,1)}, u32[]{:S(2)}) copy-start(bf16[512,256]{1,0:T(8,128)(2,1)} %gate_ref.1) | copy-start | bytes 786436
  0.0 70.8 %copy-start.6 = (f32[31,256]{1,0:T(8,128)S(1)}, f32[31,256]{1,0:T(8,128)}, u32[]{:S(2)}) copy-start(f32[31,256]{1,0:T(8,128)} %taps_ref.1) | copy-start | bytes 95236
  0.8 66.8 %copy-start.8 = (s32[512]{0:T(512)S(1)}, s32[512]{0:T(512)}, u32[]{:S(2)}) copy-start(s32[512]{0:T(512)} %param.17) | copy-start | bytes 6148
  0.8 70.1 %copy-start.10 = (f32[256]{0:T(256)S(1)}, f32[256]{0:T(256)}, u32[]{:S(2)}) copy-start(f32[256]{0:T(256)} %param.19) | copy-start | bytes 3076
  0.8 70.1 %copy-start.11 = (f32[256]{0:T(256)S(1)}, f32[256]{0:T(256)}, u32[]{:S(2)}) copy-start(f32[256]{0:T(256)} %param.20) | copy-start | bytes 3076
  65.5 5.2 %collective-permute-start = (bf16[32,256]{1,0:T(8,128)(2,1)S(1)}, bf16[32,256]{1,0:T(8,128)(2,1)S(1)}, u32[]{:S(2)}, u32[]{:S(2)}) collective-permute-start(bf16[32,256]{1,0:T(8,128)(2,1)S(1)} %get-tuple-element.12), channel_id=1, source_target_pairs={{0,4},{4,8},{8,12},{12,16},{16,20},{20,24},{24,28},{28,32},{32,36}... | collective-permute-start | bytes 49160 | tf_op jit(solution)/shard_map/ppermute | solution.py:20
  75.9 11.1 %all-to-all-start = ((bf16[4,128,256]{2,1,0:T(8,128)(2,1)}), bf16[4,128,256]{2,1,0:T(8,128)(2,1)S(1)}, u32[]{:S(2)}, u32[]{:S(2)}) async-start(bf16[4,128,256]{2,1,0:T(8,128)(2,1)} %bitcast.5), calls=%async_computation | async-start | bytes 524288 | tf_op jit(solution)/shard_map/all_to_all | solution.py:375
  91.4 102.7 %all-to-all-start.1 = ((bf16[64,8,2048]{2,1,0:T(8,128)(2,1)}), bf16[64,8,2048]{2,1,0:T(8,128)(2,1)S(1)}, u32[]{:S(2)}, u32[]{:S(2)}) async-start(bf16[64,8,2048]{2,1,0:T(8,128)(2,1)} %bitcast.31), calls=%async_computation.1 | async-start | bytes 4194304 | tf_op jit(solution)/shard_map/all_to_all | solution.py:398
  104.3 36.7 %collective-permute-start.4 = (bf16[3072,256]{1,0:T(8,128)(2,1)}, bf16[3072,256]{1,0:T(8,128)(2,1)S(1)}, u32[]{:S(2)}, u32[]{:S(2)}) collective-permute-start(bf16[3072,256]{1,0:T(8,128)(2,1)} %get-tuple-element.16), channel_id=1, source_target_pairs={{0,3},{1,0},{2,1},{3,2},{4,7},{5,4},{6,5},{7,6},{8,11},{9,8},{10,9... | collective-permute-start | bytes 4718600 | tf_op jit(solution)/shard_map/ppermute | solution.py:25
  105.6 49.9 %collective-permute-start.2 = (bf16[3072,256]{1,0:T(8,128)(2,1)}, bf16[3072,256]{1,0:T(8,128)(2,1)S(1)}, u32[]{:S(2)}, u32[]{:S(2)}) collective-permute-start(bf16[3072,256]{1,0:T(8,128)(2,1)} %get-tuple-element.16), channel_id=1, source_target_pairs={{0,1},{1,2},{2,3},{3,0},{4,5},{5,6},{6,7},{7,4},{8,9},{9,10},{10,1... | collective-permute-start | bytes 4718600 | tf_op jit(solution)/shard_map/ppermute | solution.py:25
  106.4 49.1 %collective-permute-start.1 = (bf16[1024,256]{1,0:T(8,128)(2,1)}, bf16[1024,256]{1,0:T(8,128)(2,1)S(1)}, u32[]{:S(2)}, u32[]{:S(2)}) collective-permute-start(bf16[1024,256]{1,0:T(8,128)(2,1)} %get-tuple-element.15), channel_id=1, source_target_pairs={{0,1},{1,2},{2,3},{3,0},{4,5},{5,6},{6,7},{7,4},{8,9},{9,10},{10,1... | collective-permute-start | bytes 1572872 | tf_op jit(solution)/shard_map/ppermute | solution.py:25
  141.1 53.0 %collective-permute-start.6 = (bf16[2048,256]{1,0:T(8,128)(2,1)S(1)}, bf16[2048,256]{1,0:T(8,128)(2,1)S(1)}, u32[]{:S(2)}, u32[]{:S(2)}) collective-permute-start(bf16[2048,256]{1,0:T(8,128)(2,1)S(1)} %slice.151), channel_id=1, source_target_pairs={{0,3},{1,0},{2,1},{3,2},{4,7},{5,4},{6,5},{7,6},{8,11},{9,8},{10,9... | collective-permute-start | bytes 3145736 | tf_op jit(solution)/shard_map/ppermute | solution.py:25
  144.6 19.3 %collective-permute-start.8 = (bf16[256,768]{1,0:T(8,128)(2,1)S(1)}, bf16[256,768]{1,0:T(8,128)(2,1)S(1)}, u32[]{:S(2)}, u32[]{:S(2)}) collective-permute-start(bf16[256,768]{1,0:T(8,128)(2,1)S(1)} %slice.153), channel_id=1, source_target_pairs={{0,1},{1,2},{2,3},{3,0},{4,5},{5,6},{6,7},{7,4},{8,9},{9,10},{10,1... | collective-permute-start | bytes 1179656 | tf_op jit(solution)/shard_map/ppermute | solution.py:25
  144.7 41.1 %collective-permute-start.3 = (bf16[1024,256]{1,0:T(8,128)(2,1)}, bf16[1024,256]{1,0:T(8,128)(2,1)S(1)}, u32[]{:S(2)}, u32[]{:S(2)}) collective-permute-start(bf16[1024,256]{1,0:T(8,128)(2,1)} %get-tuple-element.15), channel_id=1, source_target_pairs={{0,3},{1,0},{2,1},{3,2},{4,7},{5,4},{6,5},{7,6},{8,11},{9,8},{10,9... | collective-permute-start | bytes 1572872 | tf_op jit(solution)/shard_map/ppermute | solution.py:25
  155.5 36.9 %copy-start.18 = (bf16[1024,256]{1,0:T(8,128)(2,1)}, bf16[1024,256]{1,0:T(8,128)(2,1)S(1)}, u32[]{:S(2)}) copy-start(bf16[1024,256]{1,0:T(8,128)(2,1)S(1)} %collective-permute-done.1.refs_3_) | copy-start | bytes 1572868
  155.5 29.7 %collective-permute-start.9 = (bf16[256,768]{1,0:T(8,128)(2,1)S(1)}, bf16[256,768]{1,0:T(8,128)(2,1)S(1)}, u32[]{:S(2)}, u32[]{:S(2)}) collective-permute-start(bf16[256,768]{1,0:T(8,128)(2,1)S(1)} %slice.153), channel_id=1, source_target_pairs={{0,3},{1,0},{2,1},{3,2},{4,7},{5,4},{6,5},{7,6},{8,11},{9,8},{10,9... | collective-permute-start | bytes 1179656 | tf_op jit(solution)/shard_map/ppermute | solution.py:25
  155.5 36.9 %copy-start.14 = (bf16[3072,256]{1,0:T(8,128)(2,1)}, bf16[3072,256]{1,0:T(8,128)(2,1)S(1)}, u32[]{:S(2)}) copy-start(bf16[3072,256]{1,0:T(8,128)(2,1)S(1)} %collective-permute-done.2.refs_4_) | copy-start | bytes 4718596
  155.5 36.9 %collective-permute-start.5 = (bf16[1024,256]{1,0:T(8,128)(2,1)S(1)}, bf16[1024,256]{1,0:T(8,128)(2,1)S(1)}, u32[]{:S(2)}, u32[]{:S(2)}) collective-permute-start(bf16[1024,256]{1,0:T(8,128)(2,1)S(1)} %collective-permute-done.1.refs_3_), channel_id=1, source_target_pairs={{0,1},{1,2},{2,3},{3,0},{4,5},{5,6},{6,7},{7,4},{8,9},{9,10},{10,1... | collective-permute-start | bytes 1572872 | tf_op jit(solution)/shard_map/ppermute | solution.py:25
  163.9 28.5 %collective-permute-start.7 = (bf16[1024,256]{1,0:T(8,128)(2,1)S(1)}, bf16[1024,256]{1,0:T(8,128)(2,1)S(1)}, u32[]{:S(2)}, u32[]{:S(2)}) collective-permute-start(bf16[1024,256]{1,0:T(8,128)(2,1)S(1)} %slice.152), channel_id=1, source_target_pairs={{0,1},{1,2},{2,3},{3,0},{4,5},{5,6},{6,7},{7,4},{8,9},{9,10},{10,1... | collective-permute-start | bytes 1572872 | tf_op jit(solution)/shard_map/ppermute | solution.py:25
  185.2 7.2 %collective-permute-start.10 = (bf16[128,768]{1,0:T(8,128)(2,1)S(1)}, bf16[128,768]{1,0:T(8,128)(2,1)S(1)}, u32[]{:S(2)}, u32[]{:S(2)}) collective-permute-start(bf16[128,768]{1,0:T(8,128)(2,1)S(1)} %slice.154), channel_id=1, source_target_pairs={{0,1},{1,2},{2,3},{3,0},{4,5},{5,6},{6,7},{7,4},{8,9},{9,10},{10,1... | collective-permute-start | bytes 589832 | tf_op jit(solution)/shard_map/ppermute | solution.py:25
  185.8 6.6 %collective-permute-start.11 = (bf16[128,768]{1,0:T(8,128)(2,1)S(1)}, bf16[128,768]{1,0:T(8,128)(2,1)S(1)}, u32[]{:S(2)}, u32[]{:S(2)}) collective-permute-start(bf16[128,768]{1,0:T(8,128)(2,1)S(1)} %slice.155), channel_id=1, source_target_pairs={{0,3},{1,0},{2,1},{3,2},{4,7},{5,4},{6,5},{7,6},{8,11},{9,8},{10,9... | collective-permute-start | bytes 589832 | tf_op jit(solution)/shard_map/ppermute | solution.py:25
  205.6 36.2 %copy-start.4 = (bf16[512,1024]{1,0:T(8,128)(2,1)S(1)}, bf16[512,1024]{1,0:T(8,128)(2,1)}, u32[]{:S(2)}) copy-start(bf16[512,1024]{1,0:T(8,128)(2,1)} %get-tuple-element.18.hidden_ref) | copy-start | bytes 3145732
  205.6 39.0 %all-to-all-start.2 = ((bf16[64,8,768]{2,1,0:T(8,128)(2,1)}), bf16[64,8,768]{2,1,0:T(8,128)(2,1)S(1)}, u32[]{:S(2)}, u32[]{:S(2)}) async-start(bf16[64,8,768]{2,1,0:T(8,128)(2,1)} %bitcast.32), calls=%async_computation.2 | async-start | bytes 1572864 | tf_op jit(solution)/shard_map/all_to_all | solution.py:403
  216.2 12.1 %collective-permute-start.12 = (bf16[128,1280]{1,0:T(8,128)(2,1)S(1)}, bf16[128,1280]{1,0:T(8,128)(2,1)S(1)}, u32[]{:S(2)}, u32[]{:S(2)}) collective-permute-start(bf16[128,1280]{1,0:T(8,128)(2,1)S(1)} %get-tuple-element.20), channel_id=1, source_target_pairs={{0,1},{1,2},{2,3},{3,0},{4,5},{5,6},{6,7},{7,4},{8,9},{9,10},{10,1... | collective-permute-start | bytes 983048 | tf_op jit(solution)/shard_map/ppermute | solution.py:25
  217.9 10.6 %collective-permute-start.15 = (bf16[128,1280]{1,0:T(8,128)(2,1)S(1)}, bf16[128,1280]{1,0:T(8,128)(2,1)S(1)}, u32[]{:S(2)}, u32[]{:S(2)}) collective-permute-start(bf16[128,1280]{1,0:T(8,128)(2,1)S(1)} %get-tuple-element.19), channel_id=1, source_target_pairs={{0,3},{1,0},{2,1},{3,2},{4,7},{5,4},{6,5},{7,6},{8,11},{9,8},{10,9... | collective-permute-start | bytes 983048 | tf_op jit(solution)/shard_map/ppermute | solution.py:25
  219.8 15.5 %collective-permute-start.13 = (bf16[128,1280]{1,0:T(8,128)(2,1)S(1)}, bf16[128,1280]{1,0:T(8,128)(2,1)S(1)}, u32[]{:S(2)}, u32[]{:S(2)}) collective-permute-start(bf16[128,1280]{1,0:T(8,128)(2,1)S(1)} %get-tuple-element.19), channel_id=1, source_target_pairs={{0,1},{1,2},{2,3},{3,0},{4,5},{5,6},{6,7},{7,4},{8,9},{9,10},{10,1... | collective-permute-start | bytes 983048 | tf_op jit(solution)/shard_map/ppermute | solution.py:25
  220.0 15.6 %collective-permute-start.14 = (bf16[128,1280]{1,0:T(8,128)(2,1)S(1)}, bf16[128,1280]{1,0:T(8,128)(2,1)S(1)}, u32[]{:S(2)}, u32[]{:S(2)}) collective-permute-start(bf16[128,1280]{1,0:T(8,128)(2,1)S(1)} %get-tuple-element.20), channel_id=1, source_target_pairs={{0,3},{1,0},{2,1},{3,2},{4,7},{5,4},{6,5},{7,6},{8,11},{9,8},{10,9... | collective-permute-start | bytes 983048 | tf_op jit(solution)/shard_map/ppermute | solution.py:25
  228.3 13.5 %collective-permute-start.16 = (bf16[128,1280]{1,0:T(8,128)(2,1)S(1)}, bf16[128,1280]{1,0:T(8,128)(2,1)S(1)}, u32[]{:S(2)}, u32[]{:S(2)}) collective-permute-start(bf16[128,1280]{1,0:T(8,128)(2,1)S(1)} %collective-permute-done.12.refs_0_), channel_id=1, source_target_pairs={{0,1},{1,2},{2,3},{3,0},{4,5},{5,6},{6,7},{7,4},{8,9},{9,10},{10,1... | collective-permute-start | bytes 983048 | tf_op jit(solution)/shard_map/ppermute | solution.py:25
  228.5 13.3 %collective-permute-start.17 = (bf16[128,1280]{1,0:T(8,128)(2,1)S(1)}, bf16[128,1280]{1,0:T(8,128)(2,1)S(1)}, u32[]{:S(2)}, u32[]{:S(2)}) collective-permute-start(bf16[128,1280]{1,0:T(8,128)(2,1)S(1)} %collective-permute-done.15.refs_3_), channel_id=1, source_target_pairs={{0,3},{1,0},{2,1},{3,2},{4,7},{5,4},{6,5},{7,6},{8,11},{9,8},{10,9... | collective-permute-start | bytes 983048 | tf_op jit(solution)/shard_map/ppermute | solution.py:25
  244.6 44.7 %all-to-all-start.3 = ((bf16[64,8,1280]{2,1,0:T(8,128)(2,1)}), bf16[64,8,1280]{2,1,0:T(8,128)(2,1)S(1)}, u32[]{:S(2)}, u32[]{:S(2)}) async-start(bf16[64,8,1280]{2,1,0:T(8,128)(2,1)} %bitcast.26), calls=%async_computation.3 | async-start | bytes 2621440 | tf_op jit(solution)/shard_map/all_to_all | solution.py:403
  (14 other events, 120.4 us)

commit v6 on v3

--- a/solution.py
+++ b/solution.py
@@ -9,7 +9,6 @@
 
 TAPS = 31
 RIM = 32
-FIRST = 3
 LANES = 128
 BLOCK = 64
 
@@ -25,17 +24,12 @@
     return lax.ppermute(value, axis, [(i, (i + steps) % count) for i in range(count)])
 
 
-def slot_numbers(block_routes, capacity, experts_n):
-    route_pairs = block_routes.reshape(block_routes.shape[:-2] + (-1,))
-    onehot = (route_pairs[..., None] == jnp.arange(experts_n, dtype=jnp.int32)).astype(jnp.int32)
-    slot_rank = jnp.sum((jnp.cumsum(onehot, axis=-2) - onehot) * onehot, axis=-1)
-    return (route_pairs * capacity + slot_rank).reshape(block_routes.shape)
-
-
-def kernel(body, out, args, scratch=(), limit=16, far_in=(), far_out=()):
+def kernel(body, out, args, scratch=(), limit=16, far_in=(), far_out=(), own_in=()):
     whole, far = pl.BlockSpec(memory_space=pltpu.VMEM), pl.BlockSpec(memory_space=pltpu.HBM)
     args = [
-        pltpu.with_memory_space_constraint(a, pltpu.HBM if i in far_in else pltpu.VMEM)
+        a
+        if i in own_in
+        else pltpu.with_memory_space_constraint(a, pltpu.HBM if i in far_in else pltpu.VMEM)
         for i, a in enumerate(args)
     ]
     outs = out if isinstance(out, list) else [out]
@@ -126,6 +120,7 @@
         ((tok, width), jnp.bfloat16),
         (value, gate, rim, segments, seen, taps, gain[None], shift[None]),
         scratch=[pltpu.VMEM((8, RIM + tok, width), jnp.float32)],
+        own_in=(0, 1, 3, 5, 6, 7),
     )
 
 
@@ -133,18 +128,31 @@
     return jnp.dot(a, b, preferred_element_type=jnp.float32)
 
 
-def places(slots, total):
-    numbers = lax.broadcasted_iota(jnp.int32, (slots.shape[0], total), 1)
-    return [numbers == slots[:, m : m + 1] for m in range(slots.shape[1])]
+def places(routes, experts_n, capacity):
+    rows, top_count = routes.shape
+    expert = lax.broadcasted_iota(jnp.int32, (rows, experts_n), 1)
+    named = [jnp.where(expert == routes[:, m : m + 1], 1.0, 0.0) for m in range(top_count)]
+    earlier = lax.broadcasted_iota(jnp.int32, (rows, rows), 0) > lax.broadcasted_iota(
+        jnp.int32, (rows, rows), 1
+    )
+    earlier = jnp.where(earlier, 1.0, 0.0).astype(jnp.bfloat16)
+    taken = dot(earlier, sum(named).astype(jnp.bfloat16))
+    number = lax.broadcasted_iota(jnp.int32, (rows, experts_n * capacity), 1)
+    found = []
+    for m in range(top_count):
+        rank = jnp.sum(named[m] * taken, axis=1, keepdims=True).astype(jnp.int32)
+        found.append(number == routes[:, m : m + 1] * capacity + rank)
+    return found
 
 
 def route_body(
-    parts_ref, residual_ref, gain_ref, slots_ref, weight_ref, stream_out, sent_out, w_ref, stream_ref, sent_ref, sems
+    experts_n, parts_ref, residual_ref, gain_ref, routes_ref, weight_ref, stream_out, sent_out, w_ref, stream_ref, sent_ref, sems
 ):
     parts_n, _, width = parts_ref.shape
     spans = [slice(j * width, (j + 1) * width) for j in range(parts_n)]
     loads = fetch([(weight_ref.at[rows], w_ref.at[rows]) for rows in spans], sems)
-    table = functools.reduce(jnp.logical_or, places(slots_ref[...], sent_ref.shape[0]))
+    found = places(routes_ref[...], experts_n, sent_ref.shape[0] // experts_n)
+    table = functools.reduce(jnp.logical_or, found)
     table = jnp.where(table, 1.0, 0.0).astype(jnp.bfloat16)
     for j, rows in enumerate(spans):
         loads[j].wait()
@@ -167,22 +175,22 @@
         c.wait()
 
 
-def combine_body(stream_in, slots_ref, weights_ref, *refs):
-    *back_refs, out, stream_ref, out_ref, sems = refs
+def combine_body(
+    experts_n, stream_in, routes_ref, weights_ref, back_ref, out, stream_ref, out_ref, sems
+):
     (load,) = fetch([(stream_in, stream_ref)], sems)
-    hits = places(slots_ref[...], back_refs[0].shape[0])
-    table = sum(jnp.where(hit, weights_ref[:, m : m + 1], 0.0) for m, hit in enumerate(hits))
+    found = places(routes_ref[...], experts_n, back_ref.shape[0] // experts_n)
+    table = sum(jnp.where(hit, weights_ref[:, m : m + 1], 0.0) for m, hit in enumerate(found))
     high = table.astype(jnp.bfloat16)
     low = (table - high.astype(jnp.float32)).astype(jnp.bfloat16)
     load.wait()
-    at, stores = 0, []
-    for i, back in enumerate(back_refs):
-        cols = slice(at, at + back.shape[1])
-        rows = back[...]
+    stores, step = [], out_ref.shape[1] // 4
+    for i in range(4):
+        cols = slice(i * step, (i + 1) * step)
+        rows = back_ref[:, cols]
         mixed = dot(high, rows) + dot(low, rows)
         out_ref[:, cols] = (stream_ref[:, cols] + mixed).astype(jnp.bfloat16)
         stores += fetch([(out_ref.at[:, cols], out.at[:, cols])], sems, 1 + i)
-        at += back.shape[1]
     for c in stores:
         c.wait()
 
@@ -230,48 +238,45 @@
     )
 
 
-def down_body(cols, hidden_ref, own_ref, *refs):
+def down_body(hidden_ref, own_ref, *refs):
     *pieces, out, down_ref, out_ref, sems = refs
     at = own_ref.shape[0]
-    down_ref[:at] = own_ref[:, cols]
+    (load,) = fetch([(own_ref, down_ref.at[:at])], sems)
     for piece in pieces:
         down_ref[at : at + piece.shape[0]] = piece[...]
         at += piece.shape[0]
-    half = out_ref.shape[1] // 2
-    stores = []
-    for i in range(2):
-        span = slice(i * half, (i + 1) * half)
+    load.wait()
+    stores, step = [], out_ref.shape[1] // 4
+    for i in range(4):
+        span = slice(i * step, (i + 1) * step)
         out_ref[:, span] = dot(hidden_ref[...], down_ref[:, span]).astype(jnp.bfloat16)
         stores += fetch([(out_ref.at[:, span], out.at[:, span])], sems, i)
     for c in stores:
         c.wait()
 
 
-def down_rows(hidden, own, pieces, cols):
-    n, width = hidden.shape[0], cols.stop - cols.start
+def down_rows(hidden, own, pieces):
+    n, width = hidden.shape[0], own.shape[1]
     return kernel(
-        functools.partial(down_body, cols),
+        down_body,
         ((n, width), jnp.bfloat16),
         (hidden, own, *pieces),
         scratch=[
             pltpu.VMEM((hidden.shape[1], width), jnp.bfloat16),
             pltpu.VMEM((n, width), jnp.bfloat16),
-            pltpu.SemaphoreType.DMA((2,)),
+            pltpu.SemaphoreType.DMA((4,)),
         ],
         limit=16,
+        far_in=(1,),
         far_out=(0,),
     )
 
 
-def gathered(shard, parts):
+def gathered(shard):
+    left, right = ring(shard, "tp", 1), ring(shard, "tp", -1)
     half = shard.shape[0] // 2
-    pieces = [shard] if parts == 1 else [shard[:half], shard[half:]]
-    left, right = [], []
-    for piece in pieces:
-        left.append(ring(piece, "tp", 1))
-        right.append(ring(piece, "tp", -1))
-    far = [ring(left[0][:half], "tp", 1), ring(right[-1][-half:], "tp", -1)]
-    return left, right, far
+    far = [ring(left[:half], "tp", 1), ring(right[half:], "tp", -1)]
+    return [left], [right], far
 
 
 def shards(
@@ -293,11 +298,9 @@
     tok_dev, local_channels = conv_value.shape
     reach = conv_weight.shape[0] - 1
     model_width = w_down.shape[2]
-    gates = gathered(w_gate[0], 2)
-    ups = gathered(w_up[0], 1)
-    cut = model_width * FIRST // 8
-    groups = slice(0, cut), slice(cut, model_width)
-    downs = [gathered(w_down[0][:, cols], 1) for cols in groups]
+    gates = gathered(w_gate[0])
+    ups = gathered(w_up[0])
+    downs = gathered(w_down[0])
     lines = segments.reshape(tok_dev // LANES, LANES)
     rim = passed_along(rim_rows(conv_value, conv_gate, lines), "sp", 1)
     padded = jnp.pad(segments, (reach, 0), constant_values=-1)
@@ -320,11 +323,10 @@
     slot_total = experts_n * capacity
     own_routes = lax.dynamic_slice_in_dim(routes, column * rows_own, rows_own, 0)
     own_weights = lax.dynamic_slice_in_dim(route_weights, column * rows_own, rows_own, 0)
-    own_slots = slot_numbers(own_routes, capacity, experts_n)
     stream, outgoing = kernel(
-        route_body,
+        functools.partial(route_body, experts_n),
         [((rows_own, model_width), jnp.float32), ((slot_total, model_width), jnp.bfloat16)],
-        (regrouped, residual, ffn_gain[None], own_slots, out_weight),
+        (regrouped, residual, ffn_gain[None], own_routes, out_weight),
         scratch=[
             pltpu.VMEM(out_weight.shape, jnp.bfloat16),
             pltpu.VMEM((rows_own, model_width), jnp.float32),
@@ -342,22 +344,18 @@
         arrived,
         [([w_gate[0]], [w_up[0]])] + [(gates[side], ups[side]) for side in range(3)],
     )
-    back = []
-    for cols, (left, right, far) in zip(groups, downs):
-        out = down_rows(hidden, w_down[0], [*left, *right, *far], cols)
-        back.append(
-            lax.all_to_all(
-                out.reshape(experts_n, capacity, -1), "sp", 0, 0, tiled=True
-            ).reshape(slot_total, -1)
-        )
+    out = down_rows(hidden, w_down[0], [p for side in downs for p in side])
+    back = lax.all_to_all(
+        out.reshape(experts_n, capacity, model_width), "sp", 0, 0, tiled=True
+    ).reshape(slot_total, model_width)
     return kernel(
-        combine_body,
+        functools.partial(combine_body, experts_n),
         ((rows_own, model_width), jnp.bfloat16),
-        (stream, own_slots, own_weights, *back),
+        (stream, own_routes, own_weights, back),
         scratch=[
             pltpu.VMEM((rows_own, model_width), jnp.float32),
             pltpu.VMEM((rows_own, model_width), jnp.bfloat16),
-            pltpu.SemaphoreType.DMA((1 + len(back),)),
+            pltpu.SemaphoreType.DMA((5,)),
         ],
         limit=24,
         far_in=(0,),

time: 241 us -> 221 us (0.917)
  starting transfers between devices: 64.1 us -> 42.3 us
    all_to_all x2 -> x1, waiting for transfers between devices: 33.6 us -> 50.4 us  [shards(): lax.all_to_all(out.reshape(experts_n, capacity, model_width), 'sp', 0, 0,...]
    ppermute x18 -> x12, waiting for transfers between devices: 97 us -> 80.9 us  [ring(): lax.ppermute(value, axis, [(i, (i + steps) % count) for i in range(count)])]
    ppermute x18 -> x12, starting transfers between devices: 24.6 us -> 12.8 us  [ring(): lax.ppermute(value, axis, [(i, (i + steps) % count) for i in range(count)])]
    all_to_all x2 -> x1, starting transfers between devices: 20.5 us -> 10.3 us  [shards(): lax.all_to_all(out.reshape(experts_n, capacity, model_width), 'sp', 0, 0,...]
    unnamed x44 -> x36, local copies, waits for them, and re-layouts: 5.78 us -> 7.32 us
    pallas_call x6 -> x5, Pallas kernels: 24.5 us -> 24.3 us  [kernel(): pl.pallas_call(body, out_shape=[pltpu.HBM(*o) if i in far_out else jax.Sh...]
  transfers between devices with their start and end apart: 23 -> 16, of which waited for: 10 -> 9; matrix products, arithmetic and copies ran while one was open for 2% -> 2% of each run, Pallas kernels for 4% -> 3%
where the time goes in v6:
time: 221 us; the launch traced here: 220 us
  waiting for transfers between devices  140 us (63%)
  starting transfers between devices  42.3 us (19%)
  Pallas kernels  25.7 us (12%)
  local copies, waits for them, and re-layouts  9.92 us (4%)
    ppermute x12, waiting for transfers between devices, ring(): lax.ppermute(value, axis, [(i, (i + steps) % count) for i in range(count)])  80.9 us
    all_to_all x1, waiting for transfers between devices, shards(): lax.all_to_all(out.reshape(experts_n, capacity, model_width), 'sp', 0, 0,...  50.4 us
    pallas_call x5, Pallas kernels, kernel(): pl.pallas_call(body, out_shape=[pltpu.HBM(*o) if i in far_out else jax.Sh...  24.3 us
    all_to_all x1, starting transfers between devices, shards(): lax.all_to_all(outgoing.reshape(experts_n, capacity, model_width), 'sp',...  12.9 us
    ppermute x12, starting transfers between devices, ring(): lax.ppermute(value, axis, [(i, (i + steps) % count) for i in range(count)])  12.8 us
    all_to_all x1, starting transfers between devices, shards(): lax.all_to_all(out.reshape(experts_n, capacity, model_width), 'sp', 0, 0,...  10.3 us
    unnamed x36, local copies, waits for them, and re-layouts  7.32 us
    all_to_all x1, waiting for transfers between devices, shards(): lax.all_to_all(conv_out.reshape(columns, rows_own, local_channels), 'tp',...  6.89 us
  transfers between devices with their start and end apart: 16, of which 9 were waited for; matrix products, arithmetic and copies ran while one was open for 2% of the time, Pallas kernels for 3%

profile of v6, /device:TPU:2, one launch (start us, length us, event | category | flops | bytes accessed | tf_op | source)
XLA Modules:
  0.0 219.9 jit_solution(124676117214314241)
XLA Ops:
  0.0 1.4 rim_rows.1
  1.4 1.9 collective-permute-start
  3.3 1.9 convert_add_fusion
  5.3 1.4 collective-permute-done.rim_ref
  6.8 0.9 copy-done.1
  7.8 0.9 copy-done.2
  11.5 5.1 %shard_map.136 = bf16[512,256]{1,0:T(8,128)(2,1)} custom-call(bf16[512,256]{1,0:T(8,128)(2,1)S(1)} %copy-done.1, bf16[512,256]{1,0:T(8,128)(2,1)S(1)} %copy-done.2, bf16[32,256]{1,0:T(8,128)(2,1)S(1)} %collective-permute-done.rim_ref, s32[4,128]{1,0:T(4,128)S(1)} %bitcast.14, s32[512,128]{1,0:T(8,128)S(1)} %broadcast_in_dim.15.seen_ref, ...), custom_call_target="tpu_custom_call" | custom-call | tf_op jit(solution)/shard_map/pallas_call | solution.py:36
  16.6 4.5 %all-to-all-start = ((bf16[4,128,256]{2,1,0:T(8,128)(2,1)}), bf16[4,128,256]{2,1,0:T(8,128)(2,1)S(1)}, u32[]{:S(2)}, u32[]{:S(2)}) async-start(bf16[4,128,256]{2,1,0:T(8,128)(2,1)} %bitcast.3), calls=%async_computation | async-start | bytes 524288 | tf_op jit(solution)/shard_map/all_to_all | solution.py:317
  21.2 6.9 %all-to-all-done.parts_ref = bf16[4,128,256]{2,1,0:T(8,128)(2,1)S(1)} async-done(((bf16[4,128,256]{2,1,0:T(8,128)(2,1)}), bf16[4,128,256]{2,1,0:T(8,128)(2,1)S(1)}, u32[]{:S(2)}, u32[]{:S(2)}) %all-to-all-start) | async-done | bytes 262176 | tf_op jit(solution)/shard_map/all_to_all | solution.py:317
  28.1 4.4 %shard_map.137 = (f32[128,2048]{1,0:T(8,128)}, bf16[512,2048]{1,0:T(8,128)(2,1)}) custom-call(bf16[4,128,256]{2,1,0:T(8,128)(2,1)S(1)} %all-to-all-done.parts_ref, bf16[128,2048]{1,0:T(8,128)(2,1)S(1)} %copy-done.3, f32[1,2048]{1,0:T(1,128)S(1)} %bitcast.15, s32[128,2]{1,0:T(8,128)S(1)} %copy.17.routes_ref, bf16[1024,2048]{1,0:T(8,128)(2,1)} %weight_ref.1), custom_call_target="tpu_custom_call" | custom-call | tf_op jit(solution)/shard_map/pallas_call | solution.py:36
  32.4 12.9 %all-to-all-start.1 = ((bf16[64,8,2048]{2,1,0:T(8,128)(2,1)}), bf16[64,8,2048]{2,1,0:T(8,128)(2,1)}, u32[]{:S(2)}, u32[]{:S(2)}) async-start(bf16[64,8,2048]{2,1,0:T(8,128)(2,1)} %bitcast.19), calls=%async_computation.1 | async-start | bytes 4194304 | tf_op jit(solution)/shard_map/all_to_all | solution.py:340
  46.0 2.7 %collective-permute-start.3 = (bf16[2048,256]{1,0:T(8,128)(2,1)}, bf16[2048,256]{1,0:T(8,128)(2,1)S(1)}, u32[]{:S(2)}, u32[]{:S(2)}) collective-permute-start(bf16[2048,256]{1,0:T(8,128)(2,1)} %bitcast.7.refs_1_), channel_id=1, source_target_pairs={{0,3},{1,0},{2,1},{3,2},{4,7},{5,4},{6,5},{7,6},{8,11},{9,8},{10,9... | collective-permute-start | bytes 3145736 | tf_op jit(solution)/shard_map/ppermute | solution.py:24
  48.6 3.2 %collective-permute-start.4 = (bf16[2048,256]{1,0:T(8,128)(2,1)}, bf16[2048,256]{1,0:T(8,128)(2,1)S(1)}, u32[]{:S(2)}, u32[]{:S(2)}) collective-permute-start(bf16[2048,256]{1,0:T(8,128)(2,1)} %bitcast.8.refs_2_), channel_id=1, source_target_pairs={{0,3},{1,0},{2,1},{3,2},{4,7},{5,4},{6,5},{7,6},{8,11},{9,8},{10,9... | collective-permute-start | bytes 3145736 | tf_op jit(solution)/shard_map/ppermute | solution.py:24
  51.9 21.0 %collective-permute-done.1.refs_3_ = bf16[2048,256]{1,0:T(8,128)(2,1)S(1)} collective-permute-done((bf16[2048,256]{1,0:T(8,128)(2,1)}, bf16[2048,256]{1,0:T(8,128)(2,1)S(1)}, u32[]{:S(2)}, u32[]{:S(2)}) %collective-permute-start.1) | collective-permute-done | bytes 1048608 | tf_op jit(solution)/shard_map/ppermute | solution.py:24
  72.9 2.1 collective-permute-start.5
  75.0 20.3 %collective-permute-done.2.refs_4_ = bf16[2048,256]{1,0:T(8,128)(2,1)S(1)} collective-permute-done((bf16[2048,256]{1,0:T(8,128)(2,1)}, bf16[2048,256]{1,0:T(8,128)(2,1)S(1)}, u32[]{:S(2)}, u32[]{:S(2)}) %collective-permute-start.2) | collective-permute-done | bytes 1048608 | tf_op jit(solution)/shard_map/ppermute | solution.py:24
  95.4 2.1 collective-permute-start.7
  97.5 20.3 %collective-permute-done.9.refs_0_ = bf16[256,2048]{1,0:T(8,128)(2,1)S(1)} collective-permute-done((bf16[256,2048]{1,0:T(8,128)(2,1)S(1)}, bf16[256,2048]{1,0:T(8,128)(2,1)S(1)}, u32[]{:S(2)}, u32[]{:S(2)}) %collective-permute-start.9) | collective-permute-done | bytes 1048608 | tf_op jit(solution)/shard_map/ppermute | solution.py:24
  117.8 0.8 slice.148
  118.6 2.0 collective-permute-start.11
  120.6 0.8 slice.149
  121.5 7.5 %collective-permute-done.5.refs_7_ = bf16[1024,256]{1,0:T(8,128)(2,1)S(1)} collective-permute-done((bf16[1024,256]{1,0:T(8,128)(2,1)S(1)}, bf16[1024,256]{1,0:T(8,128)(2,1)S(1)}, u32[]{:S(2)}, u32[]{:S(2)}) %collective-permute-start.5) | collective-permute-done | bytes 524320 | tf_op jit(solution)/shard_map/ppermute | solution.py:24
  129.0 0.8 copy-done.14
  129.8 0.8 copy-done.15
  130.6 9.7 %collective-permute-done.7.refs_9_ = bf16[1024,256]{1,0:T(8,128)(2,1)S(1)} collective-permute-done((bf16[1024,256]{1,0:T(8,128)(2,1)S(1)}, bf16[1024,256]{1,0:T(8,128)(2,1)S(1)}, u32[]{:S(2)}, u32[]{:S(2)}) %collective-permute-start.7) | collective-permute-done | bytes 524320 | tf_op jit(solution)/shard_map/ppermute | solution.py:24
  140.3 0.8 copy-done.16
  141.0 7.4 %shard_map.138.hidden_ref = bf16[512,1024]{1,0:T(8,128)(2,1)S(1)} custom-call(bf16[512,2048]{1,0:T(8,128)(2,1)} %bitcast.6.refs_0_, bf16[2048,256]{1,0:T(8,128)(2,1)} %bitcast.7.refs_1_, bf16[2048,256]{1,0:T(8,128)(2,1)} %bitcast.8.refs_2_, bf16[2048,256]{1,0:T(8,128)(2,1)} %copy-done.9, bf16[2048,256]{1,0:T(8,128)(2,1)} %copy-done.11, ...), custom_call_target="tpu_custom_call" | custom-call | tf_op jit(solution)/shard_map/pallas_call | solution.py:36
  148.4 2.2 %collective-permute-done.11.refs_2_ = bf16[128,2048]{1,0:T(8,128)(2,1)S(1)} collective-permute-done((bf16[128,2048]{1,0:T(8,128)(2,1)}, bf16[128,2048]{1,0:T(8,128)(2,1)S(1)}, u32[]{:S(2)}, u32[]{:S(2)}) %collective-permute-start.11) | collective-permute-done | bytes 524320 | tf_op jit(solution)/shard_map/ppermute | solution.py:24
  150.6 4.5 %shard_map.139 = bf16[512,2048]{1,0:T(8,128)(2,1)} custom-call(bf16[512,1024]{1,0:T(8,128)(2,1)S(1)} %shard_map.138.hidden_ref, bf16[256,2048]{1,0:T(8,128)(2,1)} %bitcast.20, bf16[256,2048]{1,0:T(8,128)(2,1)S(1)} %collective-permute-done.9.refs_0_, bf16[256,2048]{1,0:T(8,128)(2,1)S(1)} %collective-permute-done.10.refs_1_, ...), custom_call_target="tpu_custom_call" | custom-call | tf_op jit(solution)/shard_map/pallas_call | solution.py:36
  155.2 10.3 %all-to-all-start.2 = ((bf16[64,8,2048]{2,1,0:T(8,128)(2,1)}), bf16[64,8,2048]{2,1,0:T(8,128)(2,1)S(1)}, u32[]{:S(2)}, u32[]{:S(2)}) async-start(bf16[64,8,2048]{2,1,0:T(8,128)(2,1)} %bitcast.18), calls=%async_computation.2 | async-start | bytes 4194304 | tf_op jit(solution)/shard_map/all_to_all | solution.py:348
  166.3 50.4 %all-to-all-done.2 = bf16[64,8,2048]{2,1,0:T(8,128)(2,1)S(1)} async-done(((bf16[64,8,2048]{2,1,0:T(8,128)(2,1)}), bf16[64,8,2048]{2,1,0:T(8,128)(2,1)S(1)}, u32[]{:S(2)}, u32[]{:S(2)}) %all-to-all-start.2) | async-done | bytes 2097184 | tf_op jit(solution)/shard_map/all_to_all | solution.py:348
  216.7 3.0 %shard_map.140 = bf16[128,2048]{1,0:T(8,128)(2,1)} custom-call(f32[128,2048]{1,0:T(8,128)} %get-tuple-element.7.stream_in, s32[128,2]{1,0:T(8,128)S(1)} %copy.17.routes_ref, f32[128,2]{1,0:T(8,128)S(1)} %copy.18.weights_ref, bf16[512,2048]{1,0:T(8,128)(2,1)S(1)} %bitcast.12), custom_call_target="tpu_custom_call" | custom-call | tf_op jit(solution)/shard_map/pallas_call | solution.py:36
  (52 shorter events, 4.7 us)
Async XLA Ops:
  0.0 21.0 %copy-start = (s32[512,2]{0,1:T(2,128)S(1)}, s32[512,2]{0,1:T(2,128)}, u32[]{:S(2)}) copy-start(s32[512,2]{0,1:T(2,128)} %param.23) | copy-start | bytes 12292
  0.0 28.0 %copy-start.6 = (f32[2048]{0:T(1024)S(1)}, f32[2048]{0:T(1024)}, u32[]{:S(2)}) copy-start(f32[2048]{0:T(1024)} %param.22) | copy-start | bytes 24580
  0.0 28.0 %copy-start.3 = (bf16[128,2048]{1,0:T(8,128)(2,1)S(1)}, bf16[128,2048]{1,0:T(8,128)(2,1)}, u32[]{:S(2)}) copy-start(bf16[128,2048]{1,0:T(8,128)(2,1)} %residual_ref.1) | copy-start | bytes 1572868
  1.4 5.3 %collective-permute-start = (bf16[32,256]{1,0:T(8,128)(2,1)}, bf16[32,256]{1,0:T(8,128)(2,1)S(1)}, u32[]{:S(2)}, u32[]{:S(2)}) collective-permute-start(bf16[32,256]{1,0:T(8,128)(2,1)} %rim_rows.1), channel_id=1, source_target_pairs={{0,4},{4,8},{8,12},{12,16},{16,20},{20,24},{24,28},{28,32},{32,36}... | collective-permute-start | bytes 49160 | tf_op jit(solution)/shard_map/ppermute | solution.py:19
  6.8 1.0 copy-start.1
  7.8 0.9 copy-start.2
  8.7 0.8 copy-start.4
  9.5 0.7 copy-start.5
  10.2 0.7 copy-start.7
  16.6 11.5 %all-to-all-start = ((bf16[4,128,256]{2,1,0:T(8,128)(2,1)}), bf16[4,128,256]{2,1,0:T(8,128)(2,1)S(1)}, u32[]{:S(2)}, u32[]{:S(2)}) async-start(bf16[4,128,256]{2,1,0:T(8,128)(2,1)} %bitcast.3), calls=%async_computation | async-start | bytes 524288 | tf_op jit(solution)/shard_map/all_to_all | solution.py:317
  32.4 19.5 %copy-start.13 = (bf16[1,256,2048]{2,1,0:T(8,128)(2,1)S(1)}, bf16[1,256,2048]{2,1,0:T(8,128)(2,1)}, u32[]{:S(2)}) copy-start(bf16[1,256,2048]{2,1,0:T(8,128)(2,1)} %param.27) | copy-start | bytes 3145732
  32.4 108.6 %all-to-all-start.1 = ((bf16[64,8,2048]{2,1,0:T(8,128)(2,1)}), bf16[64,8,2048]{2,1,0:T(8,128)(2,1)}, u32[]{:S(2)}, u32[]{:S(2)}) async-start(bf16[64,8,2048]{2,1,0:T(8,128)(2,1)} %bitcast.19), calls=%async_computation.1 | async-start | bytes 4194304 | tf_op jit(solution)/shard_map/all_to_all | solution.py:340
  45.3 27.5 %collective-permute-start.1 = (bf16[2048,256]{1,0:T(8,128)(2,1)}, bf16[2048,256]{1,0:T(8,128)(2,1)S(1)}, u32[]{:S(2)}, u32[]{:S(2)}) collective-permute-start(bf16[2048,256]{1,0:T(8,128)(2,1)} %bitcast.7.refs_1_), channel_id=1, source_target_pairs={{0,1},{1,2},{2,3},{3,0},{4,5},{5,6},{6,7},{7,4},{8,9},{9,10},{10,1... | collective-permute-start | bytes 3145736 | tf_op jit(solution)/shard_map/ppermute | solution.py:24
  46.0 26.9 %collective-permute-start.3 = (bf16[2048,256]{1,0:T(8,128)(2,1)}, bf16[2048,256]{1,0:T(8,128)(2,1)S(1)}, u32[]{:S(2)}, u32[]{:S(2)}) collective-permute-start(bf16[2048,256]{1,0:T(8,128)(2,1)} %bitcast.7.refs_1_), channel_id=1, source_target_pairs={{0,3},{1,0},{2,1},{3,2},{4,7},{5,4},{6,5},{7,6},{8,11},{9,8},{10,9... | collective-permute-start | bytes 3145736 | tf_op jit(solution)/shard_map/ppermute | solution.py:24
  48.6 46.7 %collective-permute-start.2 = (bf16[2048,256]{1,0:T(8,128)(2,1)}, bf16[2048,256]{1,0:T(8,128)(2,1)S(1)}, u32[]{:S(2)}, u32[]{:S(2)}) collective-permute-start(bf16[2048,256]{1,0:T(8,128)(2,1)} %bitcast.8.refs_2_), channel_id=1, source_target_pairs={{0,1},{1,2},{2,3},{3,0},{4,5},{5,6},{6,7},{7,4},{8,9},{9,10},{10,1... | collective-permute-start | bytes 3145736 | tf_op jit(solution)/shard_map/ppermute | solution.py:24
  48.6 46.7 %collective-permute-start.4 = (bf16[2048,256]{1,0:T(8,128)(2,1)}, bf16[2048,256]{1,0:T(8,128)(2,1)S(1)}, u32[]{:S(2)}, u32[]{:S(2)}) collective-permute-start(bf16[2048,256]{1,0:T(8,128)(2,1)} %bitcast.8.refs_2_), channel_id=1, source_target_pairs={{0,3},{1,0},{2,1},{3,2},{4,7},{5,4},{6,5},{7,6},{8,11},{9,8},{10,9... | collective-permute-start | bytes 3145736 | tf_op jit(solution)/shard_map/ppermute | solution.py:24
  51.9 65.9 %collective-permute-start.9 = (bf16[256,2048]{1,0:T(8,128)(2,1)S(1)}, bf16[256,2048]{1,0:T(8,128)(2,1)S(1)}, u32[]{:S(2)}, u32[]{:S(2)}) collective-permute-start(bf16[256,2048]{1,0:T(8,128)(2,1)S(1)} %bitcast.21), channel_id=1, source_target_pairs={{0,1},{1,2},{2,3},{3,0},{4,5},{5,6},{6,7},{7,4},{8,9},{9,10},{10,1... | collective-permute-start | bytes 3145736 | tf_op jit(solution)/shard_map/ppermute | solution.py:24
  72.8 24.7 %copy-start.9 = (bf16[2048,256]{1,0:T(8,128)(2,1)}, bf16[2048,256]{1,0:T(8,128)(2,1)S(1)}, u32[]{:S(2)}) copy-start(bf16[2048,256]{1,0:T(8,128)(2,1)S(1)} %collective-permute-done.1.refs_3_) | copy-start | bytes 3145732
  72.8 45.8 %collective-permute-start.10 = (bf16[256,2048]{1,0:T(8,128)(2,1)S(1)}, bf16[256,2048]{1,0:T(8,128)(2,1)S(1)}, u32[]{:S(2)}, u32[]{:S(2)}) collective-permute-start(bf16[256,2048]{1,0:T(8,128)(2,1)S(1)} %bitcast.22), channel_id=1, source_target_pairs={{0,3},{1,0},{2,1},{3,2},{4,7},{5,4},{6,5},{7,6},{8,11},{9,8},{10,9... | collective-permute-start | bytes 3145736 | tf_op jit(solution)/shard_map/ppermute | solution.py:24
  72.9 45.7 %copy-start.10 = (bf16[2048,256]{1,0:T(8,128)(2,1)}, bf16[2048,256]{1,0:T(8,128)(2,1)S(1)}, u32[]{:S(2)}) copy-start(bf16[2048,256]{1,0:T(8,128)(2,1)S(1)} %collective-permute-done.3.refs_5_) | copy-start | bytes 3145732
  72.9 56.1 %collective-permute-start.5 = (bf16[1024,256]{1,0:T(8,128)(2,1)S(1)}, bf16[1024,256]{1,0:T(8,128)(2,1)S(1)}, u32[]{:S(2)}, u32[]{:S(2)}) collective-permute-start(bf16[1024,256]{1,0:T(8,128)(2,1)S(1)} %slice.144), channel_id=1, source_target_pairs={{0,1},{1,2},{2,3},{3,0},{4,5},{5,6},{6,7},{7,4},{8,9},{9,10},{10,1... | collective-permute-start | bytes 1572872 | tf_op jit(solution)/shard_map/ppermute | solution.py:24
  95.3 26.2 %copy-start.11 = (bf16[2048,256]{1,0:T(8,128)(2,1)}, bf16[2048,256]{1,0:T(8,128)(2,1)S(1)}, u32[]{:S(2)}) copy-start(bf16[2048,256]{1,0:T(8,128)(2,1)S(1)} %collective-permute-done.2.refs_4_) | copy-start | bytes 3145732
  95.3 34.5 %collective-permute-start.6 = (bf16[1024,256]{1,0:T(8,128)(2,1)S(1)}, bf16[1024,256]{1,0:T(8,128)(2,1)S(1)}, u32[]{:S(2)}, u32[]{:S(2)}) collective-permute-start(bf16[1024,256]{1,0:T(8,128)(2,1)S(1)} %slice.145), channel_id=1, source_target_pairs={{0,3},{1,0},{2,1},{3,2},{4,7},{5,4},{6,5},{7,6},{8,11},{9,8},{10,9... | collective-permute-start | bytes 1572872 | tf_op jit(solution)/shard_map/ppermute | solution.py:24
  95.4 33.7 %copy-start.12 = (bf16[2048,256]{1,0:T(8,128)(2,1)}, bf16[2048,256]{1,0:T(8,128)(2,1)S(1)}, u32[]{:S(2)}) copy-start(bf16[2048,256]{1,0:T(8,128)(2,1)S(1)} %collective-permute-done.4.refs_6_) | copy-start | bytes 3145732
  95.4 44.9 %collective-permute-start.7 = (bf16[1024,256]{1,0:T(8,128)(2,1)S(1)}, bf16[1024,256]{1,0:T(8,128)(2,1)S(1)}, u32[]{:S(2)}, u32[]{:S(2)}) collective-permute-start(bf16[1024,256]{1,0:T(8,128)(2,1)S(1)} %slice.146), channel_id=1, source_target_pairs={{0,1},{1,2},{2,3},{3,0},{4,5},{5,6},{6,7},{7,4},{8,9},{9,10},{10,1... | collective-permute-start | bytes 1572872 | tf_op jit(solution)/shard_map/ppermute | solution.py:24
  117.8 23.3 %collective-permute-start.8 = (bf16[1024,256]{1,0:T(8,128)(2,1)S(1)}, bf16[1024,256]{1,0:T(8,128)(2,1)}, u32[]{:S(2)}, u32[]{:S(2)}) collective-permute-start(bf16[1024,256]{1,0:T(8,128)(2,1)S(1)} %slice.147), channel_id=1, source_target_pairs={{0,3},{1,0},{2,1},{3,2},{4,7},{5,4},{6,5},{7,6},{8,11},{9,8},{10,9... | collective-permute-start | bytes 1572872 | tf_op jit(solution)/shard_map/ppermute | solution.py:24
  118.6 32.0 %collective-permute-start.11 = (bf16[128,2048]{1,0:T(8,128)(2,1)}, bf16[128,2048]{1,0:T(8,128)(2,1)S(1)}, u32[]{:S(2)}, u32[]{:S(2)}) collective-permute-start(bf16[128,2048]{1,0:T(8,128)(2,1)} %slice.148), channel_id=1, source_target_pairs={{0,1},{1,2},{2,3},{3,0},{4,5},{5,6},{6,7},{7,4},{8,9},{9,10},{10,1... | collective-permute-start | bytes 1572872 | tf_op jit(solution)/shard_map/ppermute | solution.py:24
  129.0 0.8 copy-start.14
  129.0 21.6 %collective-permute-start.12 = (bf16[128,2048]{1,0:T(8,128)(2,1)}, bf16[128,2048]{1,0:T(8,128)(2,1)S(1)}, u32[]{:S(2)}, u32[]{:S(2)}) collective-permute-start(bf16[128,2048]{1,0:T(8,128)(2,1)} %slice.149), channel_id=1, source_target_pairs={{0,3},{1,0},{2,1},{3,2},{4,7},{5,4},{6,5},{7,6},{8,11},{9,8},{10,9... | collective-permute-start | bytes 1572872 | tf_op jit(solution)/shard_map/ppermute | solution.py:24
  129.8 0.8 copy-start.15
  140.3 0.8 copy-start.16
  155.2 61.6 %all-to-all-start.2 = ((bf16[64,8,2048]{2,1,0:T(8,128)(2,1)}), bf16[64,8,2048]{2,1,0:T(8,128)(2,1)S(1)}, u32[]{:S(2)}, u32[]{:S(2)}) async-start(bf16[64,8,2048]{2,1,0:T(8,128)(2,1)} %bitcast.18), calls=%async_computation.2 | async-start | bytes 4194304 | tf_op jit(solution)/shard_map/all_to_all | solution.py:348
  (1 other events, 0.7 us)

commit v7 on v6

--- a/solution.py
+++ b/solution.py
@@ -24,12 +24,10 @@
     return lax.ppermute(value, axis, [(i, (i + steps) % count) for i in range(count)])
 
 
-def kernel(body, out, args, scratch=(), limit=16, far_in=(), far_out=(), own_in=()):
+def kernel(body, out, args, scratch=(), limit=16, far_in=(), far_out=()):
     whole, far = pl.BlockSpec(memory_space=pltpu.VMEM), pl.BlockSpec(memory_space=pltpu.HBM)
     args = [
-        a
-        if i in own_in
-        else pltpu.with_memory_space_constraint(a, pltpu.HBM if i in far_in else pltpu.VMEM)
+        pltpu.with_memory_space_constraint(a, pltpu.HBM if i in far_in else pltpu.VMEM)
         for i, a in enumerate(args)
     ]
     outs = out if isinstance(out, list) else [out]
@@ -81,7 +79,11 @@
     )(value, gate, segments)
 
 
-def conv_body(value_ref, gate_ref, rim_ref, segments_ref, seen_ref, taps_ref, gain_ref, shift_ref, out_ref, rows_ref):
+def conv_body(rim_ref, seen_ref, *refs):
+    sources, (out_ref, rows_ref, *held, sems) = refs[:6], refs[6:]
+    for c in fetch(list(zip(sources, held)), sems):
+        c.wait()
+    value_ref, gate_ref, segments_ref, taps_ref, gain_ref, shift_ref = held
     tok = value_ref.shape[0]
     rows_ref[0, :RIM] = rim_ref[...].astype(jnp.float32)
     rows_ref[0, RIM:] = gated_rows(value_ref[...], gate_ref[...]).astype(jnp.float32)
@@ -115,12 +117,15 @@
 
 def conv_module(value, gate, rim, segments, seen, taps, gain, shift):
     tok, width = value.shape
+    fetched = (value, gate, segments, taps, gain[None], shift[None])
     return kernel(
         conv_body,
         ((tok, width), jnp.bfloat16),
-        (value, gate, rim, segments, seen, taps, gain[None], shift[None]),
-        scratch=[pltpu.VMEM((8, RIM + tok, width), jnp.float32)],
-        own_in=(0, 1, 3, 5, 6, 7),
+        (rim, seen, *fetched),
+        scratch=[pltpu.VMEM((8, RIM + tok, width), jnp.float32)]
+        + [pltpu.VMEM(a.shape, a.dtype) for a in fetched]
+        + [pltpu.SemaphoreType.DMA((len(fetched),))],
+        far_in=range(2, 2 + len(fetched)),
     )
 
 
@@ -175,31 +180,31 @@
         c.wait()
 
 
-def combine_body(
-    experts_n, stream_in, routes_ref, weights_ref, back_ref, out, stream_ref, out_ref, sems
-):
-    (load,) = fetch([(stream_in, stream_ref)], sems)
-    found = places(routes_ref[...], experts_n, back_ref.shape[0] // experts_n)
+def table_body(experts_n, routes_ref, weights_ref, high_ref, low_ref):
+    found = places(routes_ref[...], experts_n, high_ref.shape[1] // experts_n)
     table = sum(jnp.where(hit, weights_ref[:, m : m + 1], 0.0) for m, hit in enumerate(found))
     high = table.astype(jnp.bfloat16)
-    low = (table - high.astype(jnp.float32)).astype(jnp.bfloat16)
-    load.wait()
+    high_ref[...] = high
+    low_ref[...] = (table - high.astype(jnp.float32)).astype(jnp.bfloat16)
+
+
+def combine_body(stream_ref, high_ref, low_ref, back_ref, out, out_ref, sems):
     stores, step = [], out_ref.shape[1] // 4
     for i in range(4):
         cols = slice(i * step, (i + 1) * step)
         rows = back_ref[:, cols]
-        mixed = dot(high, rows) + dot(low, rows)
+        mixed = dot(high_ref[...], rows) + dot(low_ref[...], rows)
         out_ref[:, cols] = (stream_ref[:, cols] + mixed).astype(jnp.bfloat16)
-        stores += fetch([(out_ref.at[:, cols], out.at[:, cols])], sems, 1 + i)
+        stores += fetch([(out_ref.at[:, cols], out.at[:, cols])], sems, i)
     for c in stores:
         c.wait()
 
 
 def hidden_body(counts, *refs):
-    rows_in, *pieces, out_ref, rows_ref, w_ref, sems = refs
+    rows_in, *pieces, far_ref, sum_ref, rows_ref, w_ref, hidden_ref, down_ref, sems = refs
     width = pieces[0].shape[1]
-    (load,) = fetch([(rows_in, rows_ref)], sems, len(pieces))
-    loads = []
+    (load,) = fetch([(rows_in, rows_ref)], sems)
+    loads, at = [], 1
     for q, kinds in enumerate(counts):
         copies = []
         for kind, n in enumerate(kinds):
@@ -209,65 +214,72 @@
                 copies.append((piece, w_ref.at[q, top:end, kind * width : (kind + 1) * width]))
                 top = end
             pieces = pieces[n:]
-        loads.append(fetch(copies, sems, sum(len(c) for c in loads)))
+        loads.append(fetch(copies, sems, at))
+        at += len(copies)
+    spans = [slice(q * width, (q + 1) * width) for q in range(len(pieces))]
+    downs = fetch([(piece, down_ref.at[rows]) for piece, rows in zip(pieces, spans)], sems, at)
     load.wait()
     for q, copies in enumerate(loads):
         for c in copies:
             c.wait()
         act = dot(rows_ref[...], w_ref[q])
         gate = act[:, :width]
-        hidden = gate / (1.0 + jnp.exp(-gate)) * act[:, width:]
-        out_ref[:, q * width : (q + 1) * width] = hidden.astype(jnp.bfloat16)
-
-
-def hidden_units(rows, quarters):
+        hidden = (gate / (1.0 + jnp.exp(-gate)) * act[:, width:]).astype(jnp.bfloat16)
+        if q < len(spans):
+            hidden_ref[:, spans[q]] = hidden
+        else:
+            far_ref[...] = hidden
+    for c in downs:
+        c.wait()
+    step = sum_ref.shape[1] // 4
+    for i in range(4):
+        cols = slice(i * step, (i + 1) * step)
+        sum_ref[:, cols] = dot(hidden_ref[...], down_ref[:, cols])
+
+
+def hidden_units(rows, quarters, downs):
     counts = tuple((len(gates), len(ups)) for gates, ups in quarters)
-    pieces = [p for gates, ups in quarters for p in (*gates, *ups)]
-    (n, d), width = rows.shape, pieces[0].shape[1]
+    pieces = [p for gates, ups in quarters for p in (*gates, *ups)] + downs
+    (n, d), width, out_width = rows.shape, pieces[0].shape[1], downs[0].shape[1]
     return kernel(
         functools.partial(hidden_body, counts),
-        ((n, width * len(counts)), jnp.bfloat16),
+        [((n, width), jnp.bfloat16), ((n, out_width), jnp.float32)],
         (rows, *pieces),
         scratch=[
             pltpu.VMEM((n, d), jnp.bfloat16),
             pltpu.VMEM((len(counts), d, 2 * width), jnp.bfloat16),
+            pltpu.VMEM((n, len(downs) * width), jnp.bfloat16),
+            pltpu.VMEM((len(downs) * width, out_width), jnp.bfloat16),
             pltpu.SemaphoreType.DMA((len(pieces) + 1,)),
         ],
-        limit=20,
+        limit=26,
         far_in=range(1 + len(pieces)),
     )
 
 
-def down_body(hidden_ref, own_ref, *refs):
-    *pieces, out, down_ref, out_ref, sems = refs
-    at = own_ref.shape[0]
-    (load,) = fetch([(own_ref, down_ref.at[:at])], sems)
-    for piece in pieces:
-        down_ref[at : at + piece.shape[0]] = piece[...]
-        at += piece.shape[0]
-    load.wait()
+def down_body(hidden_ref, sum_ref, *refs):
+    *pieces, out, out_ref, sems = refs
     stores, step = [], out_ref.shape[1] // 4
     for i in range(4):
-        span = slice(i * step, (i + 1) * step)
-        out_ref[:, span] = dot(hidden_ref[...], down_ref[:, span]).astype(jnp.bfloat16)
-        stores += fetch([(out_ref.at[:, span], out.at[:, span])], sems, i)
+        cols = slice(i * step, (i + 1) * step)
+        total, at = sum_ref[:, cols], 0
+        for piece in pieces:
+            total = total + dot(hidden_ref[:, at : at + piece.shape[0]], piece[:, cols])
+            at += piece.shape[0]
+        out_ref[:, cols] = total.astype(jnp.bfloat16)
+        stores += fetch([(out_ref.at[:, cols], out.at[:, cols])], sems, i)
     for c in stores:
         c.wait()
 
 
-def down_rows(hidden, own, pieces):
-    n, width = hidden.shape[0], own.shape[1]
+def down_rows(hidden, total, pieces):
+    n, width = total.shape
     return kernel(
         down_body,
         ((n, width), jnp.bfloat16),
-        (hidden, own, *pieces),
-        scratch=[
-            pltpu.VMEM((hidden.shape[1], width), jnp.bfloat16),
-            pltpu.VMEM((n, width), jnp.bfloat16),
-            pltpu.SemaphoreType.DMA((4,)),
-        ],
+        (hidden, total, *pieces),
+        scratch=[pltpu.VMEM((n, width), jnp.bfloat16), pltpu.SemaphoreType.DMA((4,))],
         limit=16,
-        far_in=(1,),
         far_out=(0,),
     )
 
@@ -340,25 +352,26 @@
     arrived = lax.all_to_all(
         outgoing.reshape(experts_n, capacity, model_width), "sp", 0, 0, tiled=True
     ).reshape(slot_total, model_width)
-    hidden = hidden_units(
+    hidden, total = hidden_units(
         arrived,
         [([w_gate[0]], [w_up[0]])] + [(gates[side], ups[side]) for side in range(3)],
-    )
-    out = down_rows(hidden, w_down[0], [p for side in downs for p in side])
+        [w_down[0], *downs[0], *downs[1]],
+    )
+    out = down_rows(hidden, total, downs[2])
     back = lax.all_to_all(
         out.reshape(experts_n, capacity, model_width), "sp", 0, 0, tiled=True
     ).reshape(slot_total, model_width)
+    high, low = kernel(
+        functools.partial(table_body, experts_n),
+        [((rows_own, slot_total), jnp.bfloat16)] * 2,
+        (own_routes, own_weights),
+    )
     return kernel(
-        functools.partial(combine_body, experts_n),
+        combine_body,
         ((rows_own, model_width), jnp.bfloat16),
-        (stream, own_routes, own_weights, back),
-        scratch=[
-            pltpu.VMEM((rows_own, model_width), jnp.float32),
-            pltpu.VMEM((rows_own, model_width), jnp.bfloat16),
-            pltpu.SemaphoreType.DMA((5,)),
-        ],
+        (stream, high, low, back),
+        scratch=[pltpu.VMEM((rows_own, model_width), jnp.bfloat16), pltpu.SemaphoreType.DMA((4,))],
         limit=24,
-        far_in=(0,),
         far_out=(0,),
     )
 

time: 221 us -> 214 us (0.968)
  local copies, waits for them, and re-layouts: 9.92 us -> 5.08 us
    unnamed x36 -> x32, local copies, waits for them, and re-layouts: 7.32 us -> 2.41 us
    pallas_call x5 -> x6, Pallas kernels: 24.3 us -> 23.8 us  [kernel(): pl.pallas_call(body, out_shape=[pltpu.HBM(*o) if i in far_out else jax.Sh...]
  transfers between devices with their start and end apart: 16 -> 16, of which waited for: 9 -> 8; matrix products, arithmetic and copies ran while one was open for 2% -> 2% of each run, Pallas kernels for 3% -> 5%
where the time goes in v7:
time: 214 us; the launch traced here: 213 us
  waiting for transfers between devices  138 us (64%)
  starting transfers between devices  42.5 us (20%)
  Pallas kernels  25.2 us (12%)
  local copies, waits for them, and re-layouts  5.08 us (2%)
    ppermute x12, waiting for transfers between devices, ring(): lax.ppermute(value, axis, [(i, (i + steps) % count) for i in range(count)])  79.8 us
    all_to_all x1, waiting for transfers between devices, shards(): lax.all_to_all(out.reshape(experts_n, capacity, model_width), 'sp', 0, 0,...  50 us
    pallas_call x6, Pallas kernels, kernel(): pl.pallas_call(body, out_shape=[pltpu.HBM(*o) if i in far_out else jax.Sh...  23.8 us
    ppermute x12, starting transfers between devices, ring(): lax.ppermute(value, axis, [(i, (i + steps) % count) for i in range(count)])  13 us
    all_to_all x1, starting transfers between devices, shards(): lax.all_to_all(outgoing.reshape(experts_n, capacity, model_width), 'sp',...  12.7 us
    all_to_all x1, starting transfers between devices, shards(): lax.all_to_all(out.reshape(experts_n, capacity, model_width), 'sp', 0, 0,...  10.4 us
    all_to_all x1, waiting for transfers between devices, shards(): lax.all_to_all(conv_out.reshape(columns, rows_own, local_channels), 'tp',...  6.89 us
    all_to_all x1, starting transfers between devices, shards(): lax.all_to_all(conv_out.reshape(columns, rows_own, local_channels), 'tp',...  4.48 us
  transfers between devices with their start and end apart: 16, of which 8 were waited for; matrix products, arithmetic and copies ran while one was open for 2% of the time, Pallas kernels for 5%

profile of v7, /device:TPU:2, one launch (start us, length us, event | category | flops | bytes accessed | tf_op | source)
XLA Modules:
  0.0 213.2 jit_solution(1770990678632674573)
XLA Ops:
  0.0 1.4 rim_rows.1
  1.4 1.9 collective-permute-start
  3.3 1.9 convert_add_fusion
  5.3 1.4 collective-permute-done.rim_ref
  6.7 0.1 broadcast_in_dim.15.seen_ref
  6.8 6.3 %shard_map.136 = bf16[512,256]{1,0:T(8,128)(2,1)} custom-call(bf16[32,256]{1,0:T(8,128)(2,1)S(1)} %collective-permute-done.rim_ref, s32[512,128]{1,0:T(8,128)S(1)} %broadcast_in_dim.15.seen_ref, bf16[512,256]{1,0:T(8,128)(2,1)} %refs_0_.1, bf16[512,256]{1,0:T(8,128)(2,1)} %refs_1_.1, s32[4,128]{1,0:T(4,128)} %bitcast.27, f32[31,256]{1,0:T(8,128)} %refs_3_.1, ...), custom_call_target="tpu_custom_call" | custom-call | tf_op jit(solution)/shard_map/pallas_call | solution.py:34
  13.1 4.5 %all-to-all-start = ((bf16[4,128,256]{2,1,0:T(8,128)(2,1)}), bf16[4,128,256]{2,1,0:T(8,128)(2,1)S(1)}, u32[]{:S(2)}, u32[]{:S(2)}) async-start(bf16[4,128,256]{2,1,0:T(8,128)(2,1)} %bitcast.3), calls=%async_computation | async-start | bytes 524288 | tf_op jit(solution)/shard_map/all_to_all | solution.py:329
  17.7 6.9 %all-to-all-done.parts_ref = bf16[4,128,256]{2,1,0:T(8,128)(2,1)S(1)} async-done(((bf16[4,128,256]{2,1,0:T(8,128)(2,1)}), bf16[4,128,256]{2,1,0:T(8,128)(2,1)S(1)}, u32[]{:S(2)}, u32[]{:S(2)}) %all-to-all-start) | async-done | bytes 262176 | tf_op jit(solution)/shard_map/all_to_all | solution.py:329
  24.6 4.4 %shard_map.137 = (f32[128,2048]{1,0:T(8,128)}, bf16[512,2048]{1,0:T(8,128)(2,1)}) custom-call(bf16[4,128,256]{2,1,0:T(8,128)(2,1)S(1)} %all-to-all-done.parts_ref, bf16[128,2048]{1,0:T(8,128)(2,1)S(1)} %copy-done.2, f32[1,2048]{1,0:T(1,128)S(1)} %bitcast.13, s32[128,2]{1,0:T(8,128)S(1)} %copy.17.routes_ref, bf16[1024,2048]{1,0:T(8,128)(2,1)} %weight_ref.1), custom_call_target="tpu_custom_call" | custom-call | tf_op jit(solution)/shard_map/pallas_call | solution.py:34
  29.0 12.7 %all-to-all-start.1 = ((bf16[64,8,2048]{2,1,0:T(8,128)(2,1)}), bf16[64,8,2048]{2,1,0:T(8,128)(2,1)S(1)}, u32[]{:S(2)}, u32[]{:S(2)}) async-start(bf16[64,8,2048]{2,1,0:T(8,128)(2,1)} %bitcast.16), calls=%async_computation.1 | async-start | bytes 4194304 | tf_op jit(solution)/shard_map/all_to_all | solution.py:352
  41.7 0.6 collective-permute-start.1
  42.3 2.7 %collective-permute-start.3 = (bf16[2048,256]{1,0:T(8,128)(2,1)S(1)}, bf16[2048,256]{1,0:T(8,128)(2,1)S(1)}, u32[]{:S(2)}, u32[]{:S(2)}) collective-permute-start(bf16[2048,256]{1,0:T(8,128)(2,1)S(1)} %bitcast.19), channel_id=1, source_target_pairs={{0,3},{1,0},{2,1},{3,2},{4,7},{5,4},{6,5},{7,6},{8,11},{9,8},{10,9... | collective-permute-start | bytes 3145736 | tf_op jit(solution)/shard_map/ppermute | solution.py:24
  45.0 3.2 %collective-permute-start.4 = (bf16[2048,256]{1,0:T(8,128)(2,1)}, bf16[2048,256]{1,0:T(8,128)(2,1)S(1)}, u32[]{:S(2)}, u32[]{:S(2)}) collective-permute-start(bf16[2048,256]{1,0:T(8,128)(2,1)} %bitcast.21), channel_id=1, source_target_pairs={{0,3},{1,0},{2,1},{3,2},{4,7},{5,4},{6,5},{7,6},{8,11},{9,8},{10,9... | collective-permute-start | bytes 3145736 | tf_op jit(solution)/shard_map/ppermute | solution.py:24
  48.2 20.8 %collective-permute-done.1.refs_3_ = bf16[2048,256]{1,0:T(8,128)(2,1)S(1)} collective-permute-done((bf16[2048,256]{1,0:T(8,128)(2,1)S(1)}, bf16[2048,256]{1,0:T(8,128)(2,1)S(1)}, u32[]{:S(2)}, u32[]{:S(2)}) %collective-permute-start.1) | collective-permute-done | bytes 1048608 | tf_op jit(solution)/shard_map/ppermute | solution.py:24
  69.0 2.1 collective-permute-start.5
  71.2 20.3 %collective-permute-done.2.refs_4_ = bf16[2048,256]{1,0:T(8,128)(2,1)S(1)} collective-permute-done((bf16[2048,256]{1,0:T(8,128)(2,1)}, bf16[2048,256]{1,0:T(8,128)(2,1)S(1)}, u32[]{:S(2)}, u32[]{:S(2)}) %collective-permute-start.2) | collective-permute-done | bytes 1048608 | tf_op jit(solution)/shard_map/ppermute | solution.py:24
  91.5 2.1 collective-permute-start.7
  93.7 20.3 %collective-permute-done.9.refs_12_ = bf16[256,2048]{1,0:T(8,128)(2,1)S(1)} collective-permute-done((bf16[256,2048]{1,0:T(8,128)(2,1)}, bf16[256,2048]{1,0:T(8,128)(2,1)S(1)}, u32[]{:S(2)}, u32[]{:S(2)}) %collective-permute-start.9) | collective-permute-done | bytes 1048608 | tf_op jit(solution)/shard_map/ppermute | solution.py:24
  113.9 0.9 slice.148
  114.8 2.2 %collective-permute-start.11 = (bf16[128,2048]{1,0:T(8,128)(2,1)}, bf16[128,2048]{1,0:T(8,128)(2,1)S(1)}, u32[]{:S(2)}, u32[]{:S(2)}) collective-permute-start(bf16[128,2048]{1,0:T(8,128)(2,1)} %slice.148), channel_id=1, source_target_pairs={{0,1},{1,2},{2,3},{3,0},{4,5},{5,6},{6,7},{7,4},{8,9},{9,10},{10,1... | collective-permute-start | bytes 1572872 | tf_op jit(solution)/shard_map/ppermute | solution.py:24
  117.0 0.8 slice.149
  117.9 7.3 %collective-permute-done.5.refs_7_ = bf16[1024,256]{1,0:T(8,128)(2,1)S(1)} collective-permute-done((bf16[1024,256]{1,0:T(8,128)(2,1)S(1)}, bf16[1024,256]{1,0:T(8,128)(2,1)S(1)}, u32[]{:S(2)}, u32[]{:S(2)}) %collective-permute-start.5) | collective-permute-done | bytes 524320 | tf_op jit(solution)/shard_map/ppermute | solution.py:24
  125.2 11.2 %collective-permute-done.7.refs_9_ = bf16[1024,256]{1,0:T(8,128)(2,1)S(1)} collective-permute-done((bf16[1024,256]{1,0:T(8,128)(2,1)S(1)}, bf16[1024,256]{1,0:T(8,128)(2,1)S(1)}, u32[]{:S(2)}, u32[]{:S(2)}) %collective-permute-start.7) | collective-permute-done | bytes 524320 | tf_op jit(solution)/shard_map/ppermute | solution.py:24
  136.4 0.8 copy-done.14
  137.2 1.3 copy-done.4
  138.6 9.2 %shard_map.139 = (bf16[512,256]{1,0:T(8,128)(2,1)S(1)}, f32[512,2048]{1,0:T(8,128)S(1)}) custom-call(bf16[512,2048]{1,0:T(8,128)(2,1)} %bitcast.14, bf16[2048,256]{1,0:T(8,128)(2,1)} %bitcast.17, bf16[2048,256]{1,0:T(8,128)(2,1)} %bitcast.22, bf16[2048,256]{1,0:T(8,128)(2,1)} %copy-done.5, bf16[2048,256]{1,0:T(8,128)(2,1)} %copy-done.7, ...), custom_call_target="tpu_custom_call" | custom-call | tf_op jit(solution)/shard_map/pallas_call | solution.py:34
  147.8 2.1 shard_map.140
  149.9 10.4 %all-to-all-start.2 = ((bf16[64,8,2048]{2,1,0:T(8,128)(2,1)}), bf16[64,8,2048]{2,1,0:T(8,128)(2,1)S(1)}, u32[]{:S(2)}, u32[]{:S(2)}) async-start(bf16[64,8,2048]{2,1,0:T(8,128)(2,1)} %bitcast.15), calls=%async_computation.2 | async-start | bytes 4194304 | tf_op jit(solution)/shard_map/all_to_all | solution.py:361
  160.4 0.7 constant_dynamic-slice_fusion
  161.2 0.5 shard_map.138
  161.6 50.0 %all-to-all-done.2 = bf16[64,8,2048]{2,1,0:T(8,128)(2,1)S(1)} async-done(((bf16[64,8,2048]{2,1,0:T(8,128)(2,1)}), bf16[64,8,2048]{2,1,0:T(8,128)(2,1)S(1)}, u32[]{:S(2)}, u32[]{:S(2)}) %all-to-all-start.2) | async-done | bytes 2097184 | tf_op jit(solution)/shard_map/all_to_all | solution.py:361
  211.6 1.4 shard_map.141
  (49 shorter events, 0.5 us)
Async XLA Ops:
  0.0 17.6 %copy-start = (s32[512,2]{0,1:T(2,128)S(1)}, s32[512,2]{0,1:T(2,128)}, u32[]{:S(2)}) copy-start(s32[512,2]{0,1:T(2,128)} %param.23) | copy-start | bytes 12292
  0.0 24.6 %copy-start.3 = (f32[2048]{0:T(1024)S(1)}, f32[2048]{0:T(1024)}, u32[]{:S(2)}) copy-start(f32[2048]{0:T(1024)} %param.22) | copy-start | bytes 24580
  0.0 24.6 %copy-start.2 = (bf16[128,2048]{1,0:T(8,128)(2,1)S(1)}, bf16[128,2048]{1,0:T(8,128)(2,1)}, u32[]{:S(2)}) copy-start(bf16[128,2048]{1,0:T(8,128)(2,1)} %residual_ref.1) | copy-start | bytes 1572868
  1.4 5.3 %collective-permute-start = (bf16[32,256]{1,0:T(8,128)(2,1)}, bf16[32,256]{1,0:T(8,128)(2,1)S(1)}, u32[]{:S(2)}, u32[]{:S(2)}) collective-permute-start(bf16[32,256]{1,0:T(8,128)(2,1)} %rim_rows.1), channel_id=1, source_target_pairs={{0,4},{4,8},{8,12},{12,16},{16,20},{20,24},{24,28},{28,32},{32,36}... | collective-permute-start | bytes 49160 | tf_op jit(solution)/shard_map/ppermute | solution.py:19
  13.1 11.5 %all-to-all-start = ((bf16[4,128,256]{2,1,0:T(8,128)(2,1)}), bf16[4,128,256]{2,1,0:T(8,128)(2,1)S(1)}, u32[]{:S(2)}, u32[]{:S(2)}) async-start(bf16[4,128,256]{2,1,0:T(8,128)(2,1)} %bitcast.3), calls=%async_computation | async-start | bytes 524288 | tf_op jit(solution)/shard_map/all_to_all | solution.py:329
  28.9 12.7 %copy-start.11 = (bf16[1,2048,256]{2,1,0:T(8,128)(2,1)S(1)}, bf16[1,2048,256]{2,1,0:T(8,128)(2,1)}, u32[]{:S(2)}) copy-start(bf16[1,2048,256]{2,1,0:T(8,128)(2,1)} %param.25) | copy-start | bytes 3145732
  29.0 108.3 %all-to-all-start.1 = ((bf16[64,8,2048]{2,1,0:T(8,128)(2,1)}), bf16[64,8,2048]{2,1,0:T(8,128)(2,1)S(1)}, u32[]{:S(2)}, u32[]{:S(2)}) async-start(bf16[64,8,2048]{2,1,0:T(8,128)(2,1)} %bitcast.16), calls=%async_computation.1 | async-start | bytes 4194304 | tf_op jit(solution)/shard_map/all_to_all | solution.py:352
  41.7 27.3 %collective-permute-start.1 = (bf16[2048,256]{1,0:T(8,128)(2,1)S(1)}, bf16[2048,256]{1,0:T(8,128)(2,1)S(1)}, u32[]{:S(2)}, u32[]{:S(2)}) collective-permute-start(bf16[2048,256]{1,0:T(8,128)(2,1)S(1)} %bitcast.18), channel_id=1, source_target_pairs={{0,1},{1,2},{2,3},{3,0},{4,5},{5,6},{6,7},{7,4},{8,9},{9,10},{10,1... | collective-permute-start | bytes 3145736 | tf_op jit(solution)/shard_map/ppermute | solution.py:24
  42.3 26.7 %collective-permute-start.3 = (bf16[2048,256]{1,0:T(8,128)(2,1)S(1)}, bf16[2048,256]{1,0:T(8,128)(2,1)S(1)}, u32[]{:S(2)}, u32[]{:S(2)}) collective-permute-start(bf16[2048,256]{1,0:T(8,128)(2,1)S(1)} %bitcast.19), channel_id=1, source_target_pairs={{0,3},{1,0},{2,1},{3,2},{4,7},{5,4},{6,5},{7,6},{8,11},{9,8},{10,9... | collective-permute-start | bytes 3145736 | tf_op jit(solution)/shard_map/ppermute | solution.py:24
  45.0 46.5 %collective-permute-start.2 = (bf16[2048,256]{1,0:T(8,128)(2,1)}, bf16[2048,256]{1,0:T(8,128)(2,1)S(1)}, u32[]{:S(2)}, u32[]{:S(2)}) collective-permute-start(bf16[2048,256]{1,0:T(8,128)(2,1)} %bitcast.20), channel_id=1, source_target_pairs={{0,1},{1,2},{2,3},{3,0},{4,5},{5,6},{6,7},{7,4},{8,9},{9,10},{10,1... | collective-permute-start | bytes 3145736 | tf_op jit(solution)/shard_map/ppermute | solution.py:24
  45.0 46.5 %collective-permute-start.4 = (bf16[2048,256]{1,0:T(8,128)(2,1)}, bf16[2048,256]{1,0:T(8,128)(2,1)S(1)}, u32[]{:S(2)}, u32[]{:S(2)}) collective-permute-start(bf16[2048,256]{1,0:T(8,128)(2,1)} %bitcast.21), channel_id=1, source_target_pairs={{0,3},{1,0},{2,1},{3,2},{4,7},{5,4},{6,5},{7,6},{8,11},{9,8},{10,9... | collective-permute-start | bytes 3145736 | tf_op jit(solution)/shard_map/ppermute | solution.py:24
  48.2 65.7 %collective-permute-start.9 = (bf16[256,2048]{1,0:T(8,128)(2,1)}, bf16[256,2048]{1,0:T(8,128)(2,1)S(1)}, u32[]{:S(2)}, u32[]{:S(2)}) collective-permute-start(bf16[256,2048]{1,0:T(8,128)(2,1)} %bitcast.23), channel_id=1, source_target_pairs={{0,1},{1,2},{2,3},{3,0},{4,5},{5,6},{6,7},{7,4},{8,9},{9,10},{10,1... | collective-permute-start | bytes 3145736 | tf_op jit(solution)/shard_map/ppermute | solution.py:24
  69.0 24.7 %copy-start.5 = (bf16[2048,256]{1,0:T(8,128)(2,1)}, bf16[2048,256]{1,0:T(8,128)(2,1)S(1)}, u32[]{:S(2)}) copy-start(bf16[2048,256]{1,0:T(8,128)(2,1)S(1)} %collective-permute-done.1.refs_3_) | copy-start | bytes 3145732
  69.0 45.8 %collective-permute-start.10 = (bf16[256,2048]{1,0:T(8,128)(2,1)}, bf16[256,2048]{1,0:T(8,128)(2,1)S(1)}, u32[]{:S(2)}, u32[]{:S(2)}) collective-permute-start(bf16[256,2048]{1,0:T(8,128)(2,1)} %bitcast.24), channel_id=1, source_target_pairs={{0,3},{1,0},{2,1},{3,2},{4,7},{5,4},{6,5},{7,6},{8,11},{9,8},{10,9... | collective-permute-start | bytes 3145736 | tf_op jit(solution)/shard_map/ppermute | solution.py:24
  69.0 45.8 %copy-start.6 = (bf16[2048,256]{1,0:T(8,128)(2,1)}, bf16[2048,256]{1,0:T(8,128)(2,1)S(1)}, u32[]{:S(2)}) copy-start(bf16[2048,256]{1,0:T(8,128)(2,1)S(1)} %collective-permute-done.3.refs_5_) | copy-start | bytes 3145732
  69.0 56.1 %collective-permute-start.5 = (bf16[1024,256]{1,0:T(8,128)(2,1)S(1)}, bf16[1024,256]{1,0:T(8,128)(2,1)S(1)}, u32[]{:S(2)}, u32[]{:S(2)}) collective-permute-start(bf16[1024,256]{1,0:T(8,128)(2,1)S(1)} %slice.144), channel_id=1, source_target_pairs={{0,1},{1,2},{2,3},{3,0},{4,5},{5,6},{6,7},{7,4},{8,9},{9,10},{10,1... | collective-permute-start | bytes 1572872 | tf_op jit(solution)/shard_map/ppermute | solution.py:24
  91.4 26.4 %copy-start.7 = (bf16[2048,256]{1,0:T(8,128)(2,1)}, bf16[2048,256]{1,0:T(8,128)(2,1)S(1)}, u32[]{:S(2)}) copy-start(bf16[2048,256]{1,0:T(8,128)(2,1)S(1)} %collective-permute-done.2.refs_4_) | copy-start | bytes 3145732
  91.4 33.7 %collective-permute-start.6 = (bf16[1024,256]{1,0:T(8,128)(2,1)S(1)}, bf16[1024,256]{1,0:T(8,128)(2,1)S(1)}, u32[]{:S(2)}, u32[]{:S(2)}) collective-permute-start(bf16[1024,256]{1,0:T(8,128)(2,1)S(1)} %slice.145), channel_id=1, source_target_pairs={{0,3},{1,0},{2,1},{3,2},{4,7},{5,4},{6,5},{7,6},{8,11},{9,8},{10,9... | collective-permute-start | bytes 1572872 | tf_op jit(solution)/shard_map/ppermute | solution.py:24
  91.5 44.9 %copy-start.8 = (bf16[2048,256]{1,0:T(8,128)(2,1)}, bf16[2048,256]{1,0:T(8,128)(2,1)S(1)}, u32[]{:S(2)}) copy-start(bf16[2048,256]{1,0:T(8,128)(2,1)S(1)} %collective-permute-done.4.refs_6_) | copy-start | bytes 3145732
  91.5 44.9 %collective-permute-start.7 = (bf16[1024,256]{1,0:T(8,128)(2,1)S(1)}, bf16[1024,256]{1,0:T(8,128)(2,1)S(1)}, u32[]{:S(2)}, u32[]{:S(2)}) collective-permute-start(bf16[1024,256]{1,0:T(8,128)(2,1)S(1)} %slice.146), channel_id=1, source_target_pairs={{0,1},{1,2},{2,3},{3,0},{4,5},{5,6},{6,7},{7,4},{8,9},{9,10},{10,1... | collective-permute-start | bytes 1572872 | tf_op jit(solution)/shard_map/ppermute | solution.py:24
  113.9 22.5 %copy-start.9 = (bf16[256,2048]{1,0:T(8,128)(2,1)}, bf16[256,2048]{1,0:T(8,128)(2,1)S(1)}, u32[]{:S(2)}) copy-start(bf16[256,2048]{1,0:T(8,128)(2,1)S(1)} %collective-permute-done.9.refs_12_) | copy-start | bytes 3145732
  113.9 23.3 %collective-permute-start.8 = (bf16[1024,256]{1,0:T(8,128)(2,1)S(1)}, bf16[1024,256]{1,0:T(8,128)(2,1)}, u32[]{:S(2)}, u32[]{:S(2)}) collective-permute-start(bf16[1024,256]{1,0:T(8,128)(2,1)S(1)} %slice.147), channel_id=1, source_target_pairs={{0,3},{1,0},{2,1},{3,2},{4,7},{5,4},{6,5},{7,6},{8,11},{9,8},{10,9... | collective-permute-start | bytes 1572872 | tf_op jit(solution)/shard_map/ppermute | solution.py:24
  114.8 21.6 %copy-start.10 = (bf16[256,2048]{1,0:T(8,128)(2,1)}, bf16[256,2048]{1,0:T(8,128)(2,1)S(1)}, u32[]{:S(2)}) copy-start(bf16[256,2048]{1,0:T(8,128)(2,1)S(1)} %collective-permute-done.10.refs_13_) | copy-start | bytes 3145732
  114.8 32.9 %collective-permute-start.11 = (bf16[128,2048]{1,0:T(8,128)(2,1)}, bf16[128,2048]{1,0:T(8,128)(2,1)S(1)}, u32[]{:S(2)}, u32[]{:S(2)}) collective-permute-start(bf16[128,2048]{1,0:T(8,128)(2,1)} %slice.148), channel_id=1, source_target_pairs={{0,1},{1,2},{2,3},{3,0},{4,5},{5,6},{6,7},{7,4},{8,9},{9,10},{10,1... | collective-permute-start | bytes 1572872 | tf_op jit(solution)/shard_map/ppermute | solution.py:24
  125.2 11.2 %copy-start.12 = (bf16[1024,256]{1,0:T(8,128)(2,1)}, bf16[1024,256]{1,0:T(8,128)(2,1)S(1)}, u32[]{:S(2)}) copy-start(bf16[1024,256]{1,0:T(8,128)(2,1)S(1)} %collective-permute-done.5.refs_7_) | copy-start | bytes 1572868
  125.2 22.6 %collective-permute-start.12 = (bf16[128,2048]{1,0:T(8,128)(2,1)}, bf16[128,2048]{1,0:T(8,128)(2,1)S(1)}, u32[]{:S(2)}, u32[]{:S(2)}) collective-permute-start(bf16[128,2048]{1,0:T(8,128)(2,1)} %slice.149), channel_id=1, source_target_pairs={{0,3},{1,0},{2,1},{3,2},{4,7},{5,4},{6,5},{7,6},{8,11},{9,8},{10,9... | collective-permute-start | bytes 1572872 | tf_op jit(solution)/shard_map/ppermute | solution.py:24
  125.2 11.2 %copy-start.13 = (bf16[1024,256]{1,0:T(8,128)(2,1)}, bf16[1024,256]{1,0:T(8,128)(2,1)S(1)}, u32[]{:S(2)}) copy-start(bf16[1024,256]{1,0:T(8,128)(2,1)S(1)} %collective-permute-done.6.refs_8_) | copy-start | bytes 1572868
  136.4 0.8 copy-start.14
  137.2 1.3 copy-start.4
  149.9 61.7 %copy-start.1 = (f32[128,2048]{1,0:T(8,128)S(1)}, f32[128,2048]{1,0:T(8,128)}, u32[]{:S(2)}) copy-start(f32[128,2048]{1,0:T(8,128)} %get-tuple-element.11.stream_ref) | copy-start | bytes 3145732
  149.9 61.7 %all-to-all-start.2 = ((bf16[64,8,2048]{2,1,0:T(8,128)(2,1)}), bf16[64,8,2048]{2,1,0:T(8,128)(2,1)S(1)}, u32[]{:S(2)}, u32[]{:S(2)}) async-start(bf16[64,8,2048]{2,1,0:T(8,128)(2,1)} %bitcast.15), calls=%async_computation.2 | async-start | bytes 4194304 | tf_op jit(solution)/shard_map/all_to_all | solution.py:361

commit v8 on v7

--- a/solution.py
+++ b/solution.py
@@ -11,6 +11,7 @@
 RIM = 32
 LANES = 128
 BLOCK = 64
+RING = 8
 
 
 def passed_along(value, axis, steps):
@@ -24,10 +25,13 @@
     return lax.ppermute(value, axis, [(i, (i + steps) % count) for i in range(count)])
 
 
-def kernel(body, out, args, scratch=(), limit=16, far_in=(), far_out=()):
+def kernel(body, out, args, scratch=(), limit=16, far_in=(), far_out=(), scalar_in=()):
+    scalar = pl.BlockSpec(memory_space=pltpu.SMEM)
     whole, far = pl.BlockSpec(memory_space=pltpu.VMEM), pl.BlockSpec(memory_space=pltpu.HBM)
     args = [
-        pltpu.with_memory_space_constraint(a, pltpu.HBM if i in far_in else pltpu.VMEM)
+        a
+        if i in scalar_in
+        else pltpu.with_memory_space_constraint(a, pltpu.HBM if i in far_in else pltpu.VMEM)
         for i, a in enumerate(args)
     ]
     outs = out if isinstance(out, list) else [out]
@@ -36,7 +40,9 @@
         out_shape=[
             pltpu.HBM(*o) if i in far_out else jax.ShapeDtypeStruct(*o) for i, o in enumerate(outs)
         ],
-        in_specs=[far if i in far_in else whole for i in range(len(args))],
+        in_specs=[
+            scalar if i in scalar_in else far if i in far_in else whole for i in range(len(args))
+        ],
         out_specs=[far if i in far_out else whole for i in range(len(outs))],
         scratch_shapes=scratch,
         compiler_params=pltpu.CompilerParams(vmem_limit_bytes=limit << 20),
@@ -133,7 +139,7 @@
     return jnp.dot(a, b, preferred_element_type=jnp.float32)
 
 
-def places(routes, experts_n, capacity):
+def ranks(routes, experts_n):
     rows, top_count = routes.shape
     expert = lax.broadcasted_iota(jnp.int32, (rows, experts_n), 1)
     named = [jnp.where(expert == routes[:, m : m + 1], 1.0, 0.0) for m in range(top_count)]
@@ -142,12 +148,15 @@
     )
     earlier = jnp.where(earlier, 1.0, 0.0).astype(jnp.bfloat16)
     taken = dot(earlier, sum(named).astype(jnp.bfloat16))
-    number = lax.broadcasted_iota(jnp.int32, (rows, experts_n * capacity), 1)
-    found = []
-    for m in range(top_count):
-        rank = jnp.sum(named[m] * taken, axis=1, keepdims=True).astype(jnp.int32)
-        found.append(number == routes[:, m : m + 1] * capacity + rank)
-    return found
+    return [jnp.sum(n * taken, axis=1, keepdims=True).astype(jnp.int32) for n in named]
+
+
+def places(routes, experts_n, capacity, seen_as=lambda expert: expert):
+    number = lax.broadcasted_iota(jnp.int32, (routes.shape[0], experts_n * capacity), 1)
+    return [
+        number == seen_as(routes[:, m : m + 1]) * capacity + rank
+        for m, rank in enumerate(ranks(routes, experts_n))
+    ]
 
 
 def route_body(
@@ -180,24 +189,87 @@
         c.wait()
 
 
-def table_body(experts_n, routes_ref, weights_ref, high_ref, low_ref):
-    found = places(routes_ref[...], experts_n, high_ref.shape[1] // experts_n)
-    table = sum(jnp.where(hit, weights_ref[:, m : m + 1], 0.0) for m, hit in enumerate(found))
-    high = table.astype(jnp.bfloat16)
-    high_ref[...] = high
-    low_ref[...] = (table - high.astype(jnp.float32)).astype(jnp.bfloat16)
-
-
-def combine_body(stream_ref, high_ref, low_ref, back_ref, out, out_ref, sems):
-    stores, step = [], out_ref.shape[1] // 4
-    for i in range(4):
+def table_body(experts_n, me_ref, routes_ref, weights_ref, *out_refs):
+    me = me_ref[0]
+
+    def relative(expert):
+        along = (me // RING - expert // RING) % RING
+        across = (me // 2 % 4 - expert // 2 % 4) % 4
+        return along * RING + across * 2 + (me + expert) % 2
+
+    capacity = out_refs[0].shape[1] // experts_n
+    for i, seen_as in enumerate((lambda expert: expert, relative)):
+        found = places(routes_ref[...], experts_n, capacity, seen_as)
+        table = sum(jnp.where(hit, weights_ref[:, m : m + 1], 0.0) for m, hit in enumerate(found))
+        high = table.astype(jnp.bfloat16)
+        out_refs[2 * i][...] = high
+        out_refs[2 * i + 1][...] = (table - high.astype(jnp.float32)).astype(jnp.bfloat16)
+
+
+def side_body(stream_ref, high_ref, low_ref, *refs):
+    *parts, out_ref, back_ref, sems = refs
+    for c in fetch([(part, back_ref.at[i]) for i, part in enumerate(parts)], sems):
+        c.wait()
+    rows = back_ref[...].reshape(high_ref.shape[1], out_ref.shape[1])
+    mixed = dot(high_ref[...], rows) + dot(low_ref[...], rows)
+    cols = slice(stream_ref.shape[1] - out_ref.shape[1], stream_ref.shape[1])
+    out_ref[...] = (stream_ref[:, cols] + mixed).astype(jnp.bfloat16)
+
+
+def combine_body(stream_ref, high_ref, low_ref, back_ref, side_ref, out, out_ref, sems):
+    width = back_ref.shape[1]
+    stores, step = fetch([(side_ref, out.at[:, width:])], sems), width // 3
+    for i in range(3):
         cols = slice(i * step, (i + 1) * step)
         rows = back_ref[:, cols]
         mixed = dot(high_ref[...], rows) + dot(low_ref[...], rows)
         out_ref[:, cols] = (stream_ref[:, cols] + mixed).astype(jnp.bfloat16)
-        stores += fetch([(out_ref.at[:, cols], out.at[:, cols])], sems, i)
+        stores += fetch([(out_ref.at[:, cols], out.at[:, cols])], sems, 1 + i)
     for c in stores:
         c.wait()
+
+
+def across(value, step):
+    count = lax.axis_size("sp")
+
+    def to(i):
+        return i // RING * RING + (i // 2 + step // 2) % 4 * 2 + (i + step) % 2
+
+    return lax.ppermute(value, "sp", [(i, to(i)) for i in range(count)])
+
+
+def along(value, step):
+    count = lax.axis_size("sp")
+    return lax.ppermute(value, "sp", [(i, (i + step * RING) % count) for i in range(count)])
+
+
+def turn_body(me_ref, *refs):
+    parts, outs, (held, sems) = refs[:RING], refs[RING : 2 * RING], refs[2 * RING :]
+    z = me_ref[0] // RING
+    copies = [
+        (parts[j].at[(z + step) % RING], held.at[step, j]) for step in range(RING) for j in range(RING)
+    ]
+    for c in fetch(copies, sems):
+        c.wait()
+    for c in fetch([(held.at[step], outs[step]) for step in range(RING)], sems):
+        c.wait()
+
+
+def turned(me, parts):
+    shape = parts[0].shape
+    return kernel(
+        turn_body,
+        [(shape, jnp.bfloat16)] * RING,
+        (me, *parts),
+        scratch=[
+            pltpu.VMEM((RING, *shape), jnp.bfloat16),
+            pltpu.SemaphoreType.DMA((RING * RING,)),
+        ],
+        limit=8,
+        scalar_in=(0,),
+        far_in=range(1, 1 + RING),
+        far_out=range(RING),
+    )
 
 
 def hidden_body(counts, *refs):
@@ -257,30 +329,47 @@
     )
 
 
-def down_body(hidden_ref, sum_ref, *refs):
-    *pieces, out, out_ref, sems = refs
-    stores, step = [], out_ref.shape[1] // 4
-    for i in range(4):
-        cols = slice(i * step, (i + 1) * step)
+def down_body(me_ref, hidden_ref, sum_ref, *refs):
+    *pieces, out = refs[: -RING - 3]
+    side_outs, (out_ref, side_ref, sems) = refs[-RING - 3 : -3], refs[-3:]
+
+    def columns(cols):
         total, at = sum_ref[:, cols], 0
         for piece in pieces:
             total = total + dot(hidden_ref[:, at : at + piece.shape[0]], piece[:, cols])
             at += piece.shape[0]
-        out_ref[:, cols] = total.astype(jnp.bfloat16)
-        stores += fetch([(out_ref.at[:, cols], out.at[:, cols])], sems, i)
+        return total.astype(jnp.bfloat16)
+
+    width = out_ref.shape[1]
+    side_ref[...] = columns(slice(width, sum_ref.shape[1])).reshape(side_ref.shape)
+    me = me_ref[0]
+    stores = []
+    for step, side in enumerate(side_outs):
+        k = (me // 2 + step // 2) % 4 * 2 + (me + step) % 2
+        stores += fetch([(side_ref.at[:, k], side)], sems, step)
+    for i in range(3):
+        span = slice(i * width // 3, (i + 1) * width // 3)
+        out_ref[:, span] = columns(span)
+        stores += fetch([(out_ref.at[:, span], out.at[:, span])], sems, RING + i)
     for c in stores:
         c.wait()
 
 
-def down_rows(hidden, total, pieces):
-    n, width = total.shape
+def down_rows(me, hidden, total, pieces, width):
+    n, side = total.shape[0], total.shape[1] - width
+    capacity = n // RING // RING
     return kernel(
         down_body,
-        ((n, width), jnp.bfloat16),
-        (hidden, total, *pieces),
-        scratch=[pltpu.VMEM((n, width), jnp.bfloat16), pltpu.SemaphoreType.DMA((4,))],
+        [((n, width), jnp.bfloat16)] + [((RING, capacity, side), jnp.bfloat16)] * RING,
+        (me, hidden, total, *pieces),
+        scratch=[
+            pltpu.VMEM((n, width), jnp.bfloat16),
+            pltpu.VMEM((RING, RING, capacity, side), jnp.bfloat16),
+            pltpu.SemaphoreType.DMA((RING + 3,)),
+        ],
         limit=16,
-        far_out=(0,),
+        scalar_in=(0,),
+        far_out=range(1 + RING),
     )
 
 
@@ -357,20 +446,41 @@
         [([w_gate[0]], [w_up[0]])] + [(gates[side], ups[side]) for side in range(3)],
         [w_down[0], *downs[0], *downs[1]],
     )
-    out = down_rows(hidden, total, downs[2])
+    wide = model_width * 3 // 4
+    me = lax.axis_index("sp").astype(jnp.int32)[None]
+    out, *parts = down_rows(me, hidden, total, downs[2], wide)
     back = lax.all_to_all(
-        out.reshape(experts_n, capacity, model_width), "sp", 0, 0, tiled=True
-    ).reshape(slot_total, model_width)
-    high, low = kernel(
+        out.reshape(experts_n, capacity, wide), "sp", 0, 0, tiled=True
+    ).reshape(slot_total, wide)
+    parts = parts[:1] + [across(parts[step], step) for step in range(1, RING)]
+    parts = turned(me, parts)
+    came = [parts[0]] + [None] * (RING - 1)
+    for step in (4, 3, 5, 2, 6, 1, 7):
+        came[step] = along(parts[step], step)
+    high, low, side_high, side_low = kernel(
         functools.partial(table_body, experts_n),
-        [((rows_own, slot_total), jnp.bfloat16)] * 2,
-        (own_routes, own_weights),
+        [((rows_own, slot_total), jnp.bfloat16)] * 4,
+        (me, own_routes, own_weights),
+        scalar_in=(0,),
+    )
+    side = kernel(
+        side_body,
+        ((rows_own, model_width - wide), jnp.bfloat16),
+        (stream, side_high, side_low, *came),
+        scratch=[
+            pltpu.VMEM((RING, *came[0].shape), jnp.bfloat16),
+            pltpu.SemaphoreType.DMA((RING,)),
+        ],
+        far_in=range(3, 3 + RING),
     )
     return kernel(
         combine_body,
         ((rows_own, model_width), jnp.bfloat16),
-        (stream, high, low, back),
-        scratch=[pltpu.VMEM((rows_own, model_width), jnp.bfloat16), pltpu.SemaphoreType.DMA((4,))],
+        (stream, high, low, back, side),
+        scratch=[
+            pltpu.VMEM((rows_own, wide), jnp.bfloat16),
+            pltpu.SemaphoreType.DMA((4,)),
+        ],
         limit=24,
         far_out=(0,),
     )

time: 214 us -> 215 us (level)
  waiting for transfers between devices: 138 us -> 113 us
  starting transfers between devices: 42.5 us -> 64.4 us
  Pallas kernels: 25.2 us -> 29.2 us
    all_to_all x1, waiting for transfers between devices: 50 us -> 0.01 us  [shards(): lax.all_to_all(out.reshape(experts_n, capacity, wide), 'sp', 0, 0, tiled=...]
    ppermute x0 -> x14, waiting for transfers between devices: none -> 25 us  [the longest x7 16.1 us: along(): lax.ppermute(value, 'sp', [(i, (i + step * RING) % count) for i in range(...]
    ppermute x0 -> x14, starting transfers between devices: none -> 21.7 us  [the longest x7 13.7 us: along(): lax.ppermute(value, 'sp', [(i, (i + step * RING) % count) for i in range(...]
    pallas_call x6 -> x8, Pallas kernels: 23.8 us -> 27.8 us  [kernel(): pl.pallas_call(body, out_shape=[pltpu.HBM(*o) if i in far_out else jax.Sh...]
  transfers between devices with their start and end apart: 16 -> 30, of which waited for: 8 -> 18; matrix products, arithmetic and copies ran while one was open for 2% -> 2% of each run, Pallas kernels for 5% -> 6%
where the time goes in v8:
time: 215 us
  waiting for transfers between devices  113 us (53%)
  starting transfers between devices  64.4 us (30%)
  Pallas kernels  29.2 us (14%)
  local copies, waits for them, and re-layouts  5.81 us (3%)
    ppermute x12, waiting for transfers between devices, ring(): lax.ppermute(value, axis, [(i, (i + steps) % count) for i in range(count)])  79.5 us
    pallas_call x8, Pallas kernels, kernel(): pl.pallas_call(body, out_shape=[pltpu.HBM(*o) if i in far_out else jax.Sh...  27.8 us
    ppermute x7, waiting for transfers between devices, along(): lax.ppermute(value, 'sp', [(i, (i + step * RING) % count) for i in range(...  16.1 us
    ppermute x7, starting transfers between devices, along(): lax.ppermute(value, 'sp', [(i, (i + step * RING) % count) for i in range(...  13.7 us
    all_to_all x1, starting transfers between devices, shards(): lax.all_to_all(outgoing.reshape(experts_n, capacity, model_width), 'sp',...  13 us
    ppermute x12, starting transfers between devices, ring(): lax.ppermute(value, axis, [(i, (i + steps) % count) for i in range(count)])  12.9 us
    all_to_all x1, starting transfers between devices, shards(): lax.all_to_all(out.reshape(experts_n, capacity, wide), 'sp', 0, 0, tiled=...  10.4 us
    ppermute x7, waiting for transfers between devices, across(): return lax.ppermute(value, 'sp', [(i, to(i)) for i in range(count)])  8.87 us
  transfers between devices with their start and end apart: 30, of which 18 were waited for; matrix products, arithmetic and copies ran while one was open for 2% of the time, Pallas kernels for 6%

profile of v8, /device:TPU:2, one launch (start us, length us, event | category | flops | bytes accessed | tf_op | source)
XLA Modules:
  0.0 214.7 jit_solution(15724451114134378408)
XLA Ops:
  1.4 1.9 collective-permute-start
  3.3 1.9 convert_add_fusion
  6.8 6.3 %shard_map.136 = bf16[512,256]{1,0:T(8,128)(2,1)} custom-call(bf16[32,256]{1,0:T(8,128)(2,1)S(1)} %collective-permute-done.rim_ref, s32[512,128]{1,0:T(8,128)S(1)} %broadcast_in_dim.18.seen_ref, bf16[512,256]{1,0:T(8,128)(2,1)} %refs_0_.1, bf16[512,256]{1,0:T(8,128)(2,1)} %refs_1_.1, s32[4,128]{1,0:T(4,128)} %bitcast.27, f32[31,256]{1,0:T(8,128)} %refs_3_.1, ...), custom_call_target="tpu_custom_call" | custom-call | tf_op jit(solution)/shard_map/pallas_call | solution.py:38
  13.1 4.5 %all-to-all-start = ((bf16[4,128,256]{2,1,0:T(8,128)(2,1)}), bf16[4,128,256]{2,1,0:T(8,128)(2,1)S(1)}, u32[]{:S(2)}, u32[]{:S(2)}) async-start(bf16[4,128,256]{2,1,0:T(8,128)(2,1)} %bitcast.3), calls=%async_computation | async-start | bytes 524288 | tf_op jit(solution)/shard_map/all_to_all | solution.py:418
  17.7 6.9 %all-to-all-done.parts_ref = bf16[4,128,256]{2,1,0:T(8,128)(2,1)S(1)} async-done(((bf16[4,128,256]{2,1,0:T(8,128)(2,1)}), bf16[4,128,256]{2,1,0:T(8,128)(2,1)S(1)}, u32[]{:S(2)}, u32[]{:S(2)}) %all-to-all-start) | async-done | bytes 262176 | tf_op jit(solution)/shard_map/all_to_all | solution.py:418
  24.6 4.4 %shard_map.137 = (f32[128,2048]{1,0:T(8,128)}, bf16[512,2048]{1,0:T(8,128)(2,1)}) custom-call(bf16[4,128,256]{2,1,0:T(8,128)(2,1)S(1)} %all-to-all-done.parts_ref, bf16[128,2048]{1,0:T(8,128)(2,1)S(1)} %copy-done.2, f32[1,2048]{1,0:T(1,128)S(1)} %bitcast.14, s32[128,2]{1,0:T(8,128)S(1)} %copy.17.routes_ref, bf16[1024,2048]{1,0:T(8,128)(2,1)} %weight_ref.1), custom_call_target="tpu_custom_call" | custom-call | tf_op jit(solution)/shard_map/pallas_call | solution.py:38
  29.0 13.0 %all-to-all-start.1 = ((bf16[64,8,2048]{2,1,0:T(8,128)(2,1)}), bf16[64,8,2048]{2,1,0:T(8,128)(2,1)}, u32[]{:S(2)}, u32[]{:S(2)}) async-start(bf16[64,8,2048]{2,1,0:T(8,128)(2,1)} %bitcast.15), calls=%async_computation.1 | async-start | bytes 4194304 | tf_op jit(solution)/shard_map/all_to_all | solution.py:441
  42.7 2.7 %collective-permute-start.3 = (bf16[2048,256]{1,0:T(8,128)(2,1)S(1)}, bf16[2048,256]{1,0:T(8,128)(2,1)S(1)}, u32[]{:S(2)}, u32[]{:S(2)}) collective-permute-start(bf16[2048,256]{1,0:T(8,128)(2,1)S(1)} %bitcast.19), channel_id=1, source_target_pairs={{0,3},{1,0},{2,1},{3,2},{4,7},{5,4},{6,5},{7,6},{8,11},{9,8},{10,9... | collective-permute-start | bytes 3145736 | tf_op jit(solution)/shard_map/ppermute | solution.py:25
  45.4 3.2 %collective-permute-start.4 = (bf16[2048,256]{1,0:T(8,128)(2,1)S(1)}, bf16[2048,256]{1,0:T(8,128)(2,1)S(1)}, u32[]{:S(2)}, u32[]{:S(2)}) collective-permute-start(bf16[2048,256]{1,0:T(8,128)(2,1)S(1)} %bitcast.22), channel_id=1, source_target_pairs={{0,3},{1,0},{2,1},{3,2},{4,7},{5,4},{6,5},{7,6},{8,11},{9,8},{10,9... | collective-permute-start | bytes 3145736 | tf_op jit(solution)/shard_map/ppermute | solution.py:25
  48.6 20.8 %collective-permute-done.1.refs_3_ = bf16[2048,256]{1,0:T(8,128)(2,1)S(1)} collective-permute-done((bf16[2048,256]{1,0:T(8,128)(2,1)S(1)}, bf16[2048,256]{1,0:T(8,128)(2,1)S(1)}, u32[]{:S(2)}, u32[]{:S(2)}) %collective-permute-start.1) | collective-permute-done | bytes 1048608 | tf_op jit(solution)/shard_map/ppermute | solution.py:25
  69.4 2.1 collective-permute-start.5
  72.3 19.5 %collective-permute-done.2.refs_4_ = bf16[2048,256]{1,0:T(8,128)(2,1)S(1)} collective-permute-done((bf16[2048,256]{1,0:T(8,128)(2,1)S(1)}, bf16[2048,256]{1,0:T(8,128)(2,1)S(1)}, u32[]{:S(2)}, u32[]{:S(2)}) %collective-permute-start.2) | collective-permute-done | bytes 1048608 | tf_op jit(solution)/shard_map/ppermute | solution.py:25
  92.7 1.9 collective-permute-start.7
  94.7 19.6 %collective-permute-done.9.refs_12_ = bf16[256,2048]{1,0:T(8,128)(2,1)S(1)} collective-permute-done((bf16[256,2048]{1,0:T(8,128)(2,1)S(1)}, bf16[256,2048]{1,0:T(8,128)(2,1)S(1)}, u32[]{:S(2)}, u32[]{:S(2)}) %collective-permute-start.9) | collective-permute-done | bytes 1048608 | tf_op jit(solution)/shard_map/ppermute | solution.py:25
  114.4 2.3 %collective-permute-start.11 = (bf16[128,2048]{1,0:T(8,128)(2,1)S(1)}, bf16[128,2048]{1,0:T(8,128)(2,1)S(1)}, u32[]{:S(2)}, u32[]{:S(2)}) collective-permute-start(bf16[128,2048]{1,0:T(8,128)(2,1)S(1)} %slice.148), channel_id=1, source_target_pairs={{0,1},{1,2},{2,3},{3,0},{4,5},{5,6},{6,7},{7,4},{8,9},{9,10},{10,1... | collective-permute-start | bytes 1572872 | tf_op jit(solution)/shard_map/ppermute | solution.py:25
  116.7 8.8 %collective-permute-done.5.refs_7_ = bf16[1024,256]{1,0:T(8,128)(2,1)S(1)} collective-permute-done((bf16[1024,256]{1,0:T(8,128)(2,1)S(1)}, bf16[1024,256]{1,0:T(8,128)(2,1)S(1)}, u32[]{:S(2)}, u32[]{:S(2)}) %collective-permute-start.5) | collective-permute-done | bytes 524320 | tf_op jit(solution)/shard_map/ppermute | solution.py:25
  126.3 10.4 %collective-permute-done.7.refs_9_ = bf16[1024,256]{1,0:T(8,128)(2,1)S(1)} collective-permute-done((bf16[1024,256]{1,0:T(8,128)(2,1)}, bf16[1024,256]{1,0:T(8,128)(2,1)S(1)}, u32[]{:S(2)}, u32[]{:S(2)}) %collective-permute-start.7) | collective-permute-done | bytes 524320 | tf_op jit(solution)/shard_map/ppermute | solution.py:25
  137.6 9.2 %shard_map.139 = (bf16[512,256]{1,0:T(8,128)(2,1)S(1)}, f32[512,2048]{1,0:T(8,128)S(1)}) custom-call(bf16[512,2048]{1,0:T(8,128)(2,1)} %bitcast.7.refs_0_, bf16[2048,256]{1,0:T(8,128)(2,1)} %bitcast.17, bf16[2048,256]{1,0:T(8,128)(2,1)} %bitcast.20, bf16[2048,256]{1,0:T(8,128)(2,1)} %copy-done.4, bf16[2048,256]{1,0:T(8,128)(2,1)} %copy-done.6, ...), custom_call_target="tpu_custom_call" | custom-call | tf_op jit(solution)/shard_map/pallas_call | solution.py:38
  147.2 2.2 %shard_map.140 = (bf16[512,1536]{1,0:T(8,128)(2,1)}, bf16[8,8,512]{2,1,0:T(8,128)(2,1)}, bf16[8,8,512]{2,1,0:T(8,128)(2,1)}, bf16[8,8,512]{2,1,0:T(8,128)(2,1)},...) custom-call(s32[1]{0:T(128)} %bitcast.5.me_ref, ...), custom_call_target="tpu_custom_call" | custom-call | tf_op jit(solution)/shard_map/pallas_call | solution.py:38
  149.4 10.4 %all-to-all-start.2 = ((bf16[64,8,1536]{2,1,0:T(8,128)(2,1)}), bf16[64,8,1536]{2,1,0:T(8,128)(2,1)S(1)}, u32[]{:S(2)}, u32[]{:S(2)}) async-start(bf16[64,8,1536]{2,1,0:T(8,128)(2,1)} %bitcast.16), calls=%async_computation.2 | async-start | bytes 3145728 | tf_op jit(solution)/shard_map/all_to_all | solution.py:452
  163.9 1.8 collective-permute-start.17
  171.9 3.0 %collective-permute-done.18.refs_6_ = bf16[8,8,512]{2,1,0:T(8,128)(2,1)S(1)} collective-permute-done((bf16[8,8,512]{2,1,0:T(8,128)(2,1)S(1)}, bf16[8,8,512]{2,1,0:T(8,128)(2,1)S(1)}, u32[]{:S(2)}, u32[]{:S(2)}) %collective-permute-start.18) | collective-permute-done | bytes 65568 | tf_op jit(solution)/shard_map/ppermute | solution.py:238
  174.9 1.8 collective-permute-done.19.refs_7_
  177.4 2.4 %shard_map.141 = (bf16[8,8,512]{2,1,0:T(8,128)(2,1)}, bf16[8,8,512]{2,1,0:T(8,128)(2,1)}, bf16[8,8,512]{2,1,0:T(8,128)(2,1)}, bf16[8,8,512]{2,1,0:T(8,128)(2,1)}...) custom-call(s32[1]{0:T(128)} %bitcast.5.me_ref, ...), custom_call_target="tpu_custom_call" | custom-call | tf_op jit(solution)/shard_map/pallas_call | solution.py:38
  179.9 2.9 %collective-permute-start.21 = (bf16[8,8,512]{2,1,0:T(8,128)(2,1)}, bf16[8,8,512]{2,1,0:T(8,128)(2,1)S(1)}, u32[]{:S(2)}, u32[]{:S(2)}) collective-permute-start(bf16[8,8,512]{2,1,0:T(8,128)(2,1)} %get-tuple-element.49), channel_id=1, source_target_pairs={{0,64},{4,68},{8,72},{12,76},{16,80},{20,84},{24,88},{28,92},{32,9... | collective-permute-start | bytes 196616 | tf_op jit(solution)/shard_map/ppermute | solution.py:243
  182.9 3.1 %collective-permute-start.22 = (bf16[8,8,512]{2,1,0:T(8,128)(2,1)}, bf16[8,8,512]{2,1,0:T(8,128)(2,1)S(1)}, u32[]{:S(2)}, u32[]{:S(2)}) collective-permute-start(bf16[8,8,512]{2,1,0:T(8,128)(2,1)} %get-tuple-element.50), channel_id=1, source_target_pairs={{0,96},{4,100},{8,104},{12,108},{16,112},{20,116},{24,120},{28,124... | collective-permute-start | bytes 196616 | tf_op jit(solution)/shard_map/ppermute | solution.py:243
  186.0 3.3 %collective-permute-start.23 = (bf16[8,8,512]{2,1,0:T(8,128)(2,1)}, bf16[8,8,512]{2,1,0:T(8,128)(2,1)S(1)}, u32[]{:S(2)}, u32[]{:S(2)}) collective-permute-start(bf16[8,8,512]{2,1,0:T(8,128)(2,1)} %get-tuple-element.51), channel_id=1, source_target_pairs={{0,128},{4,132},{8,136},{12,140},{16,144},{20,148},{24,152},{28,15... | collective-permute-start | bytes 196616 | tf_op jit(solution)/shard_map/ppermute | solution.py:243
  190.9 8.4 %collective-permute-done.20.refs_1_ = bf16[8,8,512]{2,1,0:T(8,128)(2,1)S(1)} collective-permute-done((bf16[8,8,512]{2,1,0:T(8,128)(2,1)}, bf16[8,8,512]{2,1,0:T(8,128)(2,1)S(1)}, u32[]{:S(2)}, u32[]{:S(2)}) %collective-permute-start.20) | collective-permute-done | bytes 65568 | tf_op jit(solution)/shard_map/ppermute | solution.py:243
  199.3 2.4 %collective-permute-start.25 = (bf16[8,8,512]{2,1,0:T(8,128)(2,1)}, bf16[8,8,512]{2,1,0:T(8,128)(2,1)S(1)}, u32[]{:S(2)}, u32[]{:S(2)}) collective-permute-start(bf16[8,8,512]{2,1,0:T(8,128)(2,1)} %get-tuple-element.53), channel_id=1, source_target_pairs={{0,192},{4,196},{8,200},{12,204},{16,208},{20,212},{24,216},{28,22... | collective-permute-start | bytes 196616 | tf_op jit(solution)/shard_map/ppermute | solution.py:243
  201.7 2.2 %collective-permute-done.21.refs_2_ = bf16[8,8,512]{2,1,0:T(8,128)(2,1)S(1)} collective-permute-done((bf16[8,8,512]{2,1,0:T(8,128)(2,1)}, bf16[8,8,512]{2,1,0:T(8,128)(2,1)S(1)}, u32[]{:S(2)}, u32[]{:S(2)}) %collective-permute-start.21) | collective-permute-done | bytes 65568 | tf_op jit(solution)/shard_map/ppermute | solution.py:243
  205.5 2.0 collective-permute-done.22.refs_3_
  207.5 3.6 %collective-permute-done.23.refs_4_ = bf16[8,8,512]{2,1,0:T(8,128)(2,1)S(1)} collective-permute-done((bf16[8,8,512]{2,1,0:T(8,128)(2,1)}, bf16[8,8,512]{2,1,0:T(8,128)(2,1)S(1)}, u32[]{:S(2)}, u32[]{:S(2)}) %collective-permute-start.23) | collective-permute-done | bytes 65568 | tf_op jit(solution)/shard_map/ppermute | solution.py:243
  (121 shorter events, 25.2 us)
Async XLA Ops:
  1.4 5.3 %collective-permute-start = (bf16[32,256]{1,0:T(8,128)(2,1)}, bf16[32,256]{1,0:T(8,128)(2,1)S(1)}, u32[]{:S(2)}, u32[]{:S(2)}) collective-permute-start(bf16[32,256]{1,0:T(8,128)(2,1)} %rim_rows.1), channel_id=1, source_target_pairs={{0,4},{4,8},{8,12},{12,16},{16,20},{20,24},{24,28},{28,32},{32,36}... | collective-permute-start | bytes 49160 | tf_op jit(solution)/shard_map/ppermute | solution.py:20
  13.1 11.5 %all-to-all-start = ((bf16[4,128,256]{2,1,0:T(8,128)(2,1)}), bf16[4,128,256]{2,1,0:T(8,128)(2,1)S(1)}, u32[]{:S(2)}, u32[]{:S(2)}) async-start(bf16[4,128,256]{2,1,0:T(8,128)(2,1)} %bitcast.3), calls=%async_computation | async-start | bytes 524288 | tf_op jit(solution)/shard_map/all_to_all | solution.py:418
  29.0 107.8 %all-to-all-start.1 = ((bf16[64,8,2048]{2,1,0:T(8,128)(2,1)}), bf16[64,8,2048]{2,1,0:T(8,128)(2,1)}, u32[]{:S(2)}, u32[]{:S(2)}) async-start(bf16[64,8,2048]{2,1,0:T(8,128)(2,1)} %bitcast.15), calls=%async_computation.1 | async-start | bytes 4194304 | tf_op jit(solution)/shard_map/all_to_all | solution.py:441
  42.0 27.3 %collective-permute-start.1 = (bf16[2048,256]{1,0:T(8,128)(2,1)S(1)}, bf16[2048,256]{1,0:T(8,128)(2,1)S(1)}, u32[]{:S(2)}, u32[]{:S(2)}) collective-permute-start(bf16[2048,256]{1,0:T(8,128)(2,1)S(1)} %bitcast.18), channel_id=1, source_target_pairs={{0,1},{1,2},{2,3},{3,0},{4,5},{5,6},{6,7},{7,4},{8,9},{9,10},{10,1... | collective-permute-start | bytes 3145736 | tf_op jit(solution)/shard_map/ppermute | solution.py:25
  42.7 26.7 %collective-permute-start.3 = (bf16[2048,256]{1,0:T(8,128)(2,1)S(1)}, bf16[2048,256]{1,0:T(8,128)(2,1)S(1)}, u32[]{:S(2)}, u32[]{:S(2)}) collective-permute-start(bf16[2048,256]{1,0:T(8,128)(2,1)S(1)} %bitcast.19), channel_id=1, source_target_pairs={{0,3},{1,0},{2,1},{3,2},{4,7},{5,4},{6,5},{7,6},{8,11},{9,8},{10,9... | collective-permute-start | bytes 3145736 | tf_op jit(solution)/shard_map/ppermute | solution.py:25
  45.3 46.5 %collective-permute-start.2 = (bf16[2048,256]{1,0:T(8,128)(2,1)S(1)}, bf16[2048,256]{1,0:T(8,128)(2,1)S(1)}, u32[]{:S(2)}, u32[]{:S(2)}) collective-permute-start(bf16[2048,256]{1,0:T(8,128)(2,1)S(1)} %bitcast.21), channel_id=1, source_target_pairs={{0,1},{1,2},{2,3},{3,0},{4,5},{5,6},{6,7},{7,4},{8,9},{9,10},{10,1... | collective-permute-start | bytes 3145736 | tf_op jit(solution)/shard_map/ppermute | solution.py:25
  45.4 47.4 %collective-permute-start.4 = (bf16[2048,256]{1,0:T(8,128)(2,1)S(1)}, bf16[2048,256]{1,0:T(8,128)(2,1)S(1)}, u32[]{:S(2)}, u32[]{:S(2)}) collective-permute-start(bf16[2048,256]{1,0:T(8,128)(2,1)S(1)} %bitcast.22), channel_id=1, source_target_pairs={{0,3},{1,0},{2,1},{3,2},{4,7},{5,4},{6,5},{7,6},{8,11},{9,8},{10,9... | collective-permute-start | bytes 3145736 | tf_op jit(solution)/shard_map/ppermute | solution.py:25
  48.6 65.7 %collective-permute-start.9 = (bf16[256,2048]{1,0:T(8,128)(2,1)S(1)}, bf16[256,2048]{1,0:T(8,128)(2,1)S(1)}, u32[]{:S(2)}, u32[]{:S(2)}) collective-permute-start(bf16[256,2048]{1,0:T(8,128)(2,1)S(1)} %bitcast.24), channel_id=1, source_target_pairs={{0,1},{1,2},{2,3},{3,0},{4,5},{5,6},{6,7},{7,4},{8,9},{9,10},{10,1... | collective-permute-start | bytes 3145736 | tf_op jit(solution)/shard_map/ppermute | solution.py:25
  69.4 45.0 %collective-permute-start.10 = (bf16[256,2048]{1,0:T(8,128)(2,1)S(1)}, bf16[256,2048]{1,0:T(8,128)(2,1)S(1)}, u32[]{:S(2)}, u32[]{:S(2)}) collective-permute-start(bf16[256,2048]{1,0:T(8,128)(2,1)S(1)} %bitcast.25), channel_id=1, source_target_pairs={{0,3},{1,0},{2,1},{3,2},{4,7},{5,4},{6,5},{7,6},{8,11},{9,8},{10,9... | collective-permute-start | bytes 3145736 | tf_op jit(solution)/shard_map/ppermute | solution.py:25
  69.4 44.9 %copy-start.5 = (bf16[2048,256]{1,0:T(8,128)(2,1)}, bf16[2048,256]{1,0:T(8,128)(2,1)S(1)}, u32[]{:S(2)}) copy-start(bf16[2048,256]{1,0:T(8,128)(2,1)S(1)} %collective-permute-done.3.refs_5_) | copy-start | bytes 3145732
  69.4 56.1 %collective-permute-start.5 = (bf16[1024,256]{1,0:T(8,128)(2,1)S(1)}, bf16[1024,256]{1,0:T(8,128)(2,1)S(1)}, u32[]{:S(2)}, u32[]{:S(2)}) collective-permute-start(bf16[1024,256]{1,0:T(8,128)(2,1)S(1)} %slice.144), channel_id=1, source_target_pairs={{0,1},{1,2},{2,3},{3,0},{4,5},{5,6},{6,7},{7,4},{8,9},{9,10},{10,1... | collective-permute-start | bytes 1572872 | tf_op jit(solution)/shard_map/ppermute | solution.py:25
  91.8 34.5 %collective-permute-start.6 = (bf16[1024,256]{1,0:T(8,128)(2,1)}, bf16[1024,256]{1,0:T(8,128)(2,1)}, u32[]{:S(2)}, u32[]{:S(2)}) collective-permute-start(bf16[1024,256]{1,0:T(8,128)(2,1)} %slice.145), channel_id=1, source_target_pairs={{0,3},{1,0},{2,1},{3,2},{4,7},{5,4},{6,5},{7,6},{8,11},{9,8},{10,9... | collective-permute-start | bytes 1572872 | tf_op jit(solution)/shard_map/ppermute | solution.py:25
  92.7 44.0 %collective-permute-start.7 = (bf16[1024,256]{1,0:T(8,128)(2,1)}, bf16[1024,256]{1,0:T(8,128)(2,1)S(1)}, u32[]{:S(2)}, u32[]{:S(2)}) collective-permute-start(bf16[1024,256]{1,0:T(8,128)(2,1)} %slice.146), channel_id=1, source_target_pairs={{0,1},{1,2},{2,3},{3,0},{4,5},{5,6},{6,7},{7,4},{8,9},{9,10},{10,1... | collective-permute-start | bytes 1572872 | tf_op jit(solution)/shard_map/ppermute | solution.py:25
  114.3 22.5 %collective-permute-start.8 = (bf16[1024,256]{1,0:T(8,128)(2,1)S(1)}, bf16[1024,256]{1,0:T(8,128)(2,1)}, u32[]{:S(2)}, u32[]{:S(2)}) collective-permute-start(bf16[1024,256]{1,0:T(8,128)(2,1)S(1)} %slice.147), channel_id=1, source_target_pairs={{0,3},{1,0},{2,1},{3,2},{4,7},{5,4},{6,5},{7,6},{8,11},{9,8},{10,9... | collective-permute-start | bytes 1572872 | tf_op jit(solution)/shard_map/ppermute | solution.py:25
  114.4 32.8 %collective-permute-start.11 = (bf16[128,2048]{1,0:T(8,128)(2,1)S(1)}, bf16[128,2048]{1,0:T(8,128)(2,1)S(1)}, u32[]{:S(2)}, u32[]{:S(2)}) collective-permute-start(bf16[128,2048]{1,0:T(8,128)(2,1)S(1)} %slice.148), channel_id=1, source_target_pairs={{0,1},{1,2},{2,3},{3,0},{4,5},{5,6},{6,7},{7,4},{8,9},{9,10},{10,1... | collective-permute-start | bytes 1572872 | tf_op jit(solution)/shard_map/ppermute | solution.py:25
  126.3 20.8 %collective-permute-start.12 = (bf16[128,2048]{1,0:T(8,128)(2,1)S(1)}, bf16[128,2048]{1,0:T(8,128)(2,1)S(1)}, u32[]{:S(2)}, u32[]{:S(2)}) collective-permute-start(bf16[128,2048]{1,0:T(8,128)(2,1)S(1)} %slice.149), channel_id=1, source_target_pairs={{0,3},{1,0},{2,1},{3,2},{4,7},{5,4},{6,5},{7,6},{8,11},{9,8},{10,9... | collective-permute-start | bytes 1572872 | tf_op jit(solution)/shard_map/ppermute | solution.py:25
  149.4 62.4 %copy-start.1 = (f32[128,2048]{1,0:T(8,128)S(1)}, f32[128,2048]{1,0:T(8,128)}, u32[]{:S(2)}) copy-start(f32[128,2048]{1,0:T(8,128)} %get-tuple-element.30.stream_ref) | copy-start | bytes 3145732
  149.4 63.8 %all-to-all-start.2 = ((bf16[64,8,1536]{2,1,0:T(8,128)(2,1)}), bf16[64,8,1536]{2,1,0:T(8,128)(2,1)S(1)}, u32[]{:S(2)}, u32[]{:S(2)}) async-start(bf16[64,8,1536]{2,1,0:T(8,128)(2,1)} %bitcast.16), calls=%async_computation.2 | async-start | bytes 3145728 | tf_op jit(solution)/shard_map/all_to_all | solution.py:452
  159.9 5.8 %collective-permute-start.13 = (bf16[8,8,512]{2,1,0:T(8,128)(2,1)S(1)}, bf16[8,8,512]{2,1,0:T(8,128)(2,1)S(1)}, u32[]{:S(2)}, u32[]{:S(2)}) collective-permute-start(bf16[8,8,512]{2,1,0:T(8,128)(2,1)S(1)} %copy-done.35), channel_id=1, source_target_pairs={{0,4},{4,0},{8,12},{12,8},{16,20},{20,16},{24,28},{28,24},{32,36},... | collective-permute-start | bytes 196616 | tf_op jit(solution)/shard_map/ppermute | solution.py:238
  160.1 7.1 %collective-permute-start.14 = (bf16[8,8,512]{2,1,0:T(8,128)(2,1)S(1)}, bf16[8,8,512]{2,1,0:T(8,128)(2,1)S(1)}, u32[]{:S(2)}, u32[]{:S(2)}) collective-permute-start(bf16[8,8,512]{2,1,0:T(8,128)(2,1)S(1)} %copy-done.34), channel_id=1, source_target_pairs={{0,8},{4,12},{8,16},{12,20},{16,24},{20,28},{24,0},{28,4},{32,40},... | collective-permute-start | bytes 196616 | tf_op jit(solution)/shard_map/ppermute | solution.py:238
  161.5 7.7 %collective-permute-start.15 = (bf16[8,8,512]{2,1,0:T(8,128)(2,1)S(1)}, bf16[8,8,512]{2,1,0:T(8,128)(2,1)S(1)}, u32[]{:S(2)}, u32[]{:S(2)}) collective-permute-start(bf16[8,8,512]{2,1,0:T(8,128)(2,1)S(1)} %copy-done.33), channel_id=1, source_target_pairs={{0,12},{4,8},{8,20},{12,16},{16,28},{20,24},{24,4},{28,0},{32,44},... | collective-permute-start | bytes 196616 | tf_op jit(solution)/shard_map/ppermute | solution.py:238
  162.4 7.8 %collective-permute-start.16 = (bf16[8,8,512]{2,1,0:T(8,128)(2,1)S(1)}, bf16[8,8,512]{2,1,0:T(8,128)(2,1)S(1)}, u32[]{:S(2)}, u32[]{:S(2)}) collective-permute-start(bf16[8,8,512]{2,1,0:T(8,128)(2,1)S(1)} %copy-done.32), channel_id=1, source_target_pairs={{0,16},{4,20},{8,24},{12,28},{16,0},{20,4},{24,8},{28,12},{32,48},... | collective-permute-start | bytes 196616 | tf_op jit(solution)/shard_map/ppermute | solution.py:238
  163.9 8.0 %collective-permute-start.17 = (bf16[8,8,512]{2,1,0:T(8,128)(2,1)S(1)}, bf16[8,8,512]{2,1,0:T(8,128)(2,1)S(1)}, u32[]{:S(2)}, u32[]{:S(2)}) collective-permute-start(bf16[8,8,512]{2,1,0:T(8,128)(2,1)S(1)} %copy-done.31), channel_id=1, source_target_pairs={{0,20},{4,16},{8,28},{12,24},{16,4},{20,0},{24,12},{28,8},{32,52},... | collective-permute-start | bytes 196616 | tf_op jit(solution)/shard_map/ppermute | solution.py:238
  165.7 9.2 %collective-permute-start.18 = (bf16[8,8,512]{2,1,0:T(8,128)(2,1)S(1)}, bf16[8,8,512]{2,1,0:T(8,128)(2,1)S(1)}, u32[]{:S(2)}, u32[]{:S(2)}) collective-permute-start(bf16[8,8,512]{2,1,0:T(8,128)(2,1)S(1)} %copy-done.30), channel_id=1, source_target_pairs={{0,24},{4,28},{8,0},{12,4},{16,8},{20,12},{24,16},{28,20},{32,56},... | collective-permute-start | bytes 196616 | tf_op jit(solution)/shard_map/ppermute | solution.py:238
  167.2 9.6 %collective-permute-start.19 = (bf16[8,8,512]{2,1,0:T(8,128)(2,1)S(1)}, bf16[8,8,512]{2,1,0:T(8,128)(2,1)S(1)}, u32[]{:S(2)}, u32[]{:S(2)}) collective-permute-start(bf16[8,8,512]{2,1,0:T(8,128)(2,1)S(1)} %copy-done.29), channel_id=1, source_target_pairs={{0,28},{4,24},{8,4},{12,0},{16,12},{20,8},{24,20},{28,16},{32,60},... | collective-permute-start | bytes 196616 | tf_op jit(solution)/shard_map/ppermute | solution.py:238
  179.8 19.5 %collective-permute-start.20 = (bf16[8,8,512]{2,1,0:T(8,128)(2,1)}, bf16[8,8,512]{2,1,0:T(8,128)(2,1)S(1)}, u32[]{:S(2)}, u32[]{:S(2)}) collective-permute-start(bf16[8,8,512]{2,1,0:T(8,128)(2,1)} %get-tuple-element.48), channel_id=1, source_target_pairs={{0,32},{4,36},{8,40},{12,44},{16,48},{20,52},{24,56},{28,60},{32,6... | collective-permute-start | bytes 196616 | tf_op jit(solution)/shard_map/ppermute | solution.py:243
  179.9 24.0 %collective-permute-start.21 = (bf16[8,8,512]{2,1,0:T(8,128)(2,1)}, bf16[8,8,512]{2,1,0:T(8,128)(2,1)S(1)}, u32[]{:S(2)}, u32[]{:S(2)}) collective-permute-start(bf16[8,8,512]{2,1,0:T(8,128)(2,1)} %get-tuple-element.49), channel_id=1, source_target_pairs={{0,64},{4,68},{8,72},{12,76},{16,80},{20,84},{24,88},{28,92},{32,9... | collective-permute-start | bytes 196616 | tf_op jit(solution)/shard_map/ppermute | solution.py:243
  182.9 24.7 %collective-permute-start.22 = (bf16[8,8,512]{2,1,0:T(8,128)(2,1)}, bf16[8,8,512]{2,1,0:T(8,128)(2,1)S(1)}, u32[]{:S(2)}, u32[]{:S(2)}) collective-permute-start(bf16[8,8,512]{2,1,0:T(8,128)(2,1)} %get-tuple-element.50), channel_id=1, source_target_pairs={{0,96},{4,100},{8,104},{12,108},{16,112},{20,116},{24,120},{28,124... | collective-permute-start | bytes 196616 | tf_op jit(solution)/shard_map/ppermute | solution.py:243
  186.0 25.1 %collective-permute-start.23 = (bf16[8,8,512]{2,1,0:T(8,128)(2,1)}, bf16[8,8,512]{2,1,0:T(8,128)(2,1)S(1)}, u32[]{:S(2)}, u32[]{:S(2)}) collective-permute-start(bf16[8,8,512]{2,1,0:T(8,128)(2,1)} %get-tuple-element.51), channel_id=1, source_target_pairs={{0,128},{4,132},{8,136},{12,140},{16,144},{20,148},{24,152},{28,15... | collective-permute-start | bytes 196616 | tf_op jit(solution)/shard_map/ppermute | solution.py:243
  189.3 21.8 %collective-permute-start.24 = (bf16[8,8,512]{2,1,0:T(8,128)(2,1)}, bf16[8,8,512]{2,1,0:T(8,128)(2,1)S(1)}, u32[]{:S(2)}, u32[]{:S(2)}) collective-permute-start(bf16[8,8,512]{2,1,0:T(8,128)(2,1)} %get-tuple-element.52), channel_id=1, source_target_pairs={{0,160},{4,164},{8,168},{12,172},{16,176},{20,180},{24,184},{28,18... | collective-permute-start | bytes 196616 | tf_op jit(solution)/shard_map/ppermute | solution.py:243
  199.3 11.8 %collective-permute-start.25 = (bf16[8,8,512]{2,1,0:T(8,128)(2,1)}, bf16[8,8,512]{2,1,0:T(8,128)(2,1)S(1)}, u32[]{:S(2)}, u32[]{:S(2)}) collective-permute-start(bf16[8,8,512]{2,1,0:T(8,128)(2,1)} %get-tuple-element.53), channel_id=1, source_target_pairs={{0,192},{4,196},{8,200},{12,204},{16,208},{20,212},{24,216},{28,22... | collective-permute-start | bytes 196616 | tf_op jit(solution)/shard_map/ppermute | solution.py:243
  203.9 7.2 %collective-permute-start.26 = (bf16[8,8,512]{2,1,0:T(8,128)(2,1)}, bf16[8,8,512]{2,1,0:T(8,128)(2,1)S(1)}, u32[]{:S(2)}, u32[]{:S(2)}) collective-permute-start(bf16[8,8,512]{2,1,0:T(8,128)(2,1)} %get-tuple-element.54), channel_id=1, source_target_pairs={{0,224},{4,228},{8,232},{12,236},{16,240},{20,244},{24,248},{28,25... | collective-permute-start | bytes 196616 | tf_op jit(solution)/shard_map/ppermute | solution.py:243
  (34 other events, 385.4 us)

commit v9 on v8

--- a/solution.py
+++ b/solution.py
@@ -218,8 +218,8 @@
 
 def combine_body(stream_ref, high_ref, low_ref, back_ref, side_ref, out, out_ref, sems):
     width = back_ref.shape[1]
-    stores, step = fetch([(side_ref, out.at[:, width:])], sems), width // 3
-    for i in range(3):
+    stores, step = fetch([(side_ref, out.at[:, width:])], sems), width // 2
+    for i in range(2):
         cols = slice(i * step, (i + 1) * step)
         rows = back_ref[:, cols]
         mixed = dot(high_ref[...], rows) + dot(low_ref[...], rows)
@@ -347,8 +347,8 @@
     for step, side in enumerate(side_outs):
         k = (me // 2 + step // 2) % 4 * 2 + (me + step) % 2
         stores += fetch([(side_ref.at[:, k], side)], sems, step)
-    for i in range(3):
-        span = slice(i * width // 3, (i + 1) * width // 3)
+    for i in range(2):
+        span = slice(i * width // 2, (i + 1) * width // 2)
         out_ref[:, span] = columns(span)
         stores += fetch([(out_ref.at[:, span], out.at[:, span])], sems, RING + i)
     for c in stores:
@@ -365,7 +365,7 @@
         scratch=[
             pltpu.VMEM((n, width), jnp.bfloat16),
             pltpu.VMEM((RING, RING, capacity, side), jnp.bfloat16),
-            pltpu.SemaphoreType.DMA((RING + 3,)),
+            pltpu.SemaphoreType.DMA((RING + 2,)),
         ],
         limit=16,
         scalar_in=(0,),
@@ -446,7 +446,7 @@
         [([w_gate[0]], [w_up[0]])] + [(gates[side], ups[side]) for side in range(3)],
         [w_down[0], *downs[0], *downs[1]],
     )
-    wide = model_width * 3 // 4
+    wide = model_width * 7 // 8
     me = lax.axis_index("sp").astype(jnp.int32)[None]
     out, *parts = down_rows(me, hidden, total, downs[2], wide)
     back = lax.all_to_all(
@@ -479,7 +479,7 @@
         (stream, high, low, back, side),
         scratch=[
             pltpu.VMEM((rows_own, wide), jnp.bfloat16),
-            pltpu.SemaphoreType.DMA((4,)),
+            pltpu.SemaphoreType.DMA((3,)),
         ],
         limit=24,
         far_out=(0,),

time: 215 us -> 216 us (level)
  waiting for transfers between devices: 113 us -> 109 us
  starting transfers between devices: 64.4 us -> 68.2 us
    ppermute x7, waiting for transfers between devices: 8.87 us -> 3.24 us  [across(): return lax.ppermute(value, 'sp', [(i, to(i)) for i in range(count)])]
    ppermute x7, starting transfers between devices: 13.7 us -> 17 us  [along(): lax.ppermute(value, 'sp', [(i, (i + step * RING) % count) for i in range(...]
  transfers between devices with their start and end apart: 30 -> 30, of which waited for: 18 -> 15; matrix products, arithmetic and copies ran while one was open for 2% -> 2% of each run, Pallas kernels for 6% -> 6%
where the time goes in v9:
time: 216 us; the launch traced here: 215 us
  waiting for transfers between devices  109 us (50%)
  starting transfers between devices  68.2 us (32%)
  Pallas kernels  29.1 us (13%)
  local copies, waits for them, and re-layouts  5.76 us (3%)
    ppermute x12, waiting for transfers between devices, ring(): lax.ppermute(value, axis, [(i, (i + steps) % count) for i in range(count)])  79.5 us
    pallas_call x8, Pallas kernels, kernel(): pl.pallas_call(body, out_shape=[pltpu.HBM(*o) if i in far_out else jax.Sh...  27.6 us
    ppermute x7, waiting for transfers between devices, along(): lax.ppermute(value, 'sp', [(i, (i + step * RING) % count) for i in range(...  18.2 us
    ppermute x7, starting transfers between devices, along(): lax.ppermute(value, 'sp', [(i, (i + step * RING) % count) for i in range(...  17 us
    all_to_all x1, starting transfers between devices, shards(): lax.all_to_all(outgoing.reshape(experts_n, capacity, model_width), 'sp',...  13 us
    ppermute x12, starting transfers between devices, ring(): lax.ppermute(value, axis, [(i, (i + steps) % count) for i in range(count)])  12.9 us
    all_to_all x1, starting transfers between devices, shards(): lax.all_to_all(out.reshape(experts_n, capacity, wide), 'sp', 0, 0, tiled=...  10.4 us
    ppermute x7, starting transfers between devices, across(): return lax.ppermute(value, 'sp', [(i, to(i)) for i in range(count)])  8.52 us
  transfers between devices with their start and end apart: 30, of which 15 were waited for; matrix products, arithmetic and copies ran while one was open for 2% of the time, Pallas kernels for 6%

profile of v9, /device:TPU:2, one launch (start us, length us, event | category | flops | bytes accessed | tf_op | source)
XLA Modules:
  0.0 214.8 jit_solution(18320575770793827539)
XLA Ops:
  1.4 1.9 collective-permute-start
  3.3 1.9 convert_add_fusion
  6.8 6.3 %shard_map.136 = bf16[512,256]{1,0:T(8,128)(2,1)} custom-call(bf16[32,256]{1,0:T(8,128)(2,1)S(1)} %collective-permute-done.rim_ref, s32[512,128]{1,0:T(8,128)S(1)} %broadcast_in_dim.18.seen_ref, bf16[512,256]{1,0:T(8,128)(2,1)} %refs_0_.1, bf16[512,256]{1,0:T(8,128)(2,1)} %refs_1_.1, s32[4,128]{1,0:T(4,128)} %bitcast.27, f32[31,256]{1,0:T(8,128)} %refs_3_.1, ...), custom_call_target="tpu_custom_call" | custom-call | tf_op jit(solution)/shard_map/pallas_call | solution.py:38
  13.1 4.5 %all-to-all-start = ((bf16[4,128,256]{2,1,0:T(8,128)(2,1)}), bf16[4,128,256]{2,1,0:T(8,128)(2,1)S(1)}, u32[]{:S(2)}, u32[]{:S(2)}) async-start(bf16[4,128,256]{2,1,0:T(8,128)(2,1)} %bitcast.3), calls=%async_computation | async-start | bytes 524288 | tf_op jit(solution)/shard_map/all_to_all | solution.py:418
  17.7 6.9 %all-to-all-done.parts_ref = bf16[4,128,256]{2,1,0:T(8,128)(2,1)S(1)} async-done(((bf16[4,128,256]{2,1,0:T(8,128)(2,1)}), bf16[4,128,256]{2,1,0:T(8,128)(2,1)S(1)}, u32[]{:S(2)}, u32[]{:S(2)}) %all-to-all-start) | async-done | bytes 262176 | tf_op jit(solution)/shard_map/all_to_all | solution.py:418
  24.6 4.4 %shard_map.137 = (f32[128,2048]{1,0:T(8,128)}, bf16[512,2048]{1,0:T(8,128)(2,1)}) custom-call(bf16[4,128,256]{2,1,0:T(8,128)(2,1)S(1)} %all-to-all-done.parts_ref, bf16[128,2048]{1,0:T(8,128)(2,1)S(1)} %copy-done.2, f32[1,2048]{1,0:T(1,128)S(1)} %bitcast.14, s32[128,2]{1,0:T(8,128)S(1)} %copy.17.routes_ref, bf16[1024,2048]{1,0:T(8,128)(2,1)} %weight_ref.1), custom_call_target="tpu_custom_call" | custom-call | tf_op jit(solution)/shard_map/pallas_call | solution.py:38
  29.0 13.0 %all-to-all-start.1 = ((bf16[64,8,2048]{2,1,0:T(8,128)(2,1)}), bf16[64,8,2048]{2,1,0:T(8,128)(2,1)}, u32[]{:S(2)}, u32[]{:S(2)}) async-start(bf16[64,8,2048]{2,1,0:T(8,128)(2,1)} %bitcast.15), calls=%async_computation.1 | async-start | bytes 4194304 | tf_op jit(solution)/shard_map/all_to_all | solution.py:441
  42.7 2.7 %collective-permute-start.3 = (bf16[2048,256]{1,0:T(8,128)(2,1)S(1)}, bf16[2048,256]{1,0:T(8,128)(2,1)S(1)}, u32[]{:S(2)}, u32[]{:S(2)}) collective-permute-start(bf16[2048,256]{1,0:T(8,128)(2,1)S(1)} %bitcast.19), channel_id=1, source_target_pairs={{0,3},{1,0},{2,1},{3,2},{4,7},{5,4},{6,5},{7,6},{8,11},{9,8},{10,9... | collective-permute-start | bytes 3145736 | tf_op jit(solution)/shard_map/ppermute | solution.py:25
  45.4 3.2 %collective-permute-start.4 = (bf16[2048,256]{1,0:T(8,128)(2,1)S(1)}, bf16[2048,256]{1,0:T(8,128)(2,1)S(1)}, u32[]{:S(2)}, u32[]{:S(2)}) collective-permute-start(bf16[2048,256]{1,0:T(8,128)(2,1)S(1)} %bitcast.22), channel_id=1, source_target_pairs={{0,3},{1,0},{2,1},{3,2},{4,7},{5,4},{6,5},{7,6},{8,11},{9,8},{10,9... | collective-permute-start | bytes 3145736 | tf_op jit(solution)/shard_map/ppermute | solution.py:25
  48.6 20.8 %collective-permute-done.1.refs_3_ = bf16[2048,256]{1,0:T(8,128)(2,1)S(1)} collective-permute-done((bf16[2048,256]{1,0:T(8,128)(2,1)S(1)}, bf16[2048,256]{1,0:T(8,128)(2,1)S(1)}, u32[]{:S(2)}, u32[]{:S(2)}) %collective-permute-start.1) | collective-permute-done | bytes 1048608 | tf_op jit(solution)/shard_map/ppermute | solution.py:25
  69.4 2.1 collective-permute-start.5
  72.3 19.5 %collective-permute-done.2.refs_4_ = bf16[2048,256]{1,0:T(8,128)(2,1)S(1)} collective-permute-done((bf16[2048,256]{1,0:T(8,128)(2,1)S(1)}, bf16[2048,256]{1,0:T(8,128)(2,1)S(1)}, u32[]{:S(2)}, u32[]{:S(2)}) %collective-permute-start.2) | collective-permute-done | bytes 1048608 | tf_op jit(solution)/shard_map/ppermute | solution.py:25
  92.7 1.9 collective-permute-start.7
  94.7 19.6 %collective-permute-done.9.refs_12_ = bf16[256,2048]{1,0:T(8,128)(2,1)S(1)} collective-permute-done((bf16[256,2048]{1,0:T(8,128)(2,1)S(1)}, bf16[256,2048]{1,0:T(8,128)(2,1)S(1)}, u32[]{:S(2)}, u32[]{:S(2)}) %collective-permute-start.9) | collective-permute-done | bytes 1048608 | tf_op jit(solution)/shard_map/ppermute | solution.py:25
  114.4 2.3 %collective-permute-start.11 = (bf16[128,2048]{1,0:T(8,128)(2,1)S(1)}, bf16[128,2048]{1,0:T(8,128)(2,1)S(1)}, u32[]{:S(2)}, u32[]{:S(2)}) collective-permute-start(bf16[128,2048]{1,0:T(8,128)(2,1)S(1)} %slice.148), channel_id=1, source_target_pairs={{0,1},{1,2},{2,3},{3,0},{4,5},{5,6},{6,7},{7,4},{8,9},{9,10},{10,1... | collective-permute-start | bytes 1572872 | tf_op jit(solution)/shard_map/ppermute | solution.py:25
  116.7 8.8 %collective-permute-done.5.refs_7_ = bf16[1024,256]{1,0:T(8,128)(2,1)S(1)} collective-permute-done((bf16[1024,256]{1,0:T(8,128)(2,1)S(1)}, bf16[1024,256]{1,0:T(8,128)(2,1)S(1)}, u32[]{:S(2)}, u32[]{:S(2)}) %collective-permute-start.5) | collective-permute-done | bytes 524320 | tf_op jit(solution)/shard_map/ppermute | solution.py:25
  126.3 10.4 %collective-permute-done.7.refs_9_ = bf16[1024,256]{1,0:T(8,128)(2,1)S(1)} collective-permute-done((bf16[1024,256]{1,0:T(8,128)(2,1)}, bf16[1024,256]{1,0:T(8,128)(2,1)S(1)}, u32[]{:S(2)}, u32[]{:S(2)}) %collective-permute-start.7) | collective-permute-done | bytes 524320 | tf_op jit(solution)/shard_map/ppermute | solution.py:25
  137.6 9.2 %shard_map.139 = (bf16[512,256]{1,0:T(8,128)(2,1)S(1)}, f32[512,2048]{1,0:T(8,128)S(1)}) custom-call(bf16[512,2048]{1,0:T(8,128)(2,1)} %bitcast.7.refs_0_, bf16[2048,256]{1,0:T(8,128)(2,1)} %bitcast.17, bf16[2048,256]{1,0:T(8,128)(2,1)} %bitcast.20, bf16[2048,256]{1,0:T(8,128)(2,1)} %copy-done.4, bf16[2048,256]{1,0:T(8,128)(2,1)} %copy-done.6, ...), custom_call_target="tpu_custom_call" | custom-call | tf_op jit(solution)/shard_map/pallas_call | solution.py:38
  147.2 2.3 %shard_map.140 = (bf16[512,1792]{1,0:T(8,128)(2,1)}, bf16[8,8,256]{2,1,0:T(8,128)(2,1)}, bf16[8,8,256]{2,1,0:T(8,128)(2,1)}, bf16[8,8,256]{2,1,0:T(8,128)(2,1)},...) custom-call(s32[1]{0:T(128)} %bitcast.5.me_ref, ...), custom_call_target="tpu_custom_call" | custom-call | tf_op jit(solution)/shard_map/pallas_call | solution.py:38
  149.6 10.4 %all-to-all-start.2 = ((bf16[64,8,1792]{2,1,0:T(8,128)(2,1)}), bf16[64,8,1792]{2,1,0:T(8,128)(2,1)S(1)}, u32[]{:S(2)}, u32[]{:S(2)}) async-start(bf16[64,8,1792]{2,1,0:T(8,128)(2,1)} %bitcast.16), calls=%async_computation.2 | async-start | bytes 3670016 | tf_op jit(solution)/shard_map/all_to_all | solution.py:452
  160.2 1.5 collective-permute-start.14
  162.6 1.5 collective-permute-start.16
  164.1 1.8 collective-permute-start.17
  166.8 1.8 collective-permute-start.19
  168.6 1.7 collective-permute-done.17.refs_5_
  172.4 2.2 %shard_map.141 = (bf16[8,8,256]{2,1,0:T(8,128)(2,1)}, bf16[8,8,256]{2,1,0:T(8,128)(2,1)}, bf16[8,8,256]{2,1,0:T(8,128)(2,1)}, bf16[8,8,256]{2,1,0:T(8,128)(2,1)}...) custom-call(s32[1]{0:T(128)} %bitcast.5.me_ref, ...), custom_call_target="tpu_custom_call" | custom-call | tf_op jit(solution)/shard_map/pallas_call | solution.py:38
  175.9 2.5 %collective-permute-start.21 = (bf16[8,8,256]{2,1,0:T(8,128)(2,1)}, bf16[8,8,256]{2,1,0:T(8,128)(2,1)S(1)}, u32[]{:S(2)}, u32[]{:S(2)}) collective-permute-start(bf16[8,8,256]{2,1,0:T(8,128)(2,1)} %get-tuple-element.49), channel_id=1, source_target_pairs={{0,64},{4,68},{8,72},{12,76},{16,80},{20,84},{24,88},{28,92},{32,9... | collective-permute-start | bytes 98312 | tf_op jit(solution)/shard_map/ppermute | solution.py:243
  178.4 3.8 %collective-permute-start.22 = (bf16[8,8,256]{2,1,0:T(8,128)(2,1)}, bf16[8,8,256]{2,1,0:T(8,128)(2,1)S(1)}, u32[]{:S(2)}, u32[]{:S(2)}) collective-permute-start(bf16[8,8,256]{2,1,0:T(8,128)(2,1)} %get-tuple-element.50), channel_id=1, source_target_pairs={{0,96},{4,100},{8,104},{12,108},{16,112},{20,116},{24,120},{28,124... | collective-permute-start | bytes 98312 | tf_op jit(solution)/shard_map/ppermute | solution.py:243
  182.2 1.5 collective-permute-start.23
  183.7 4.1 %collective-permute-start.24 = (bf16[8,8,256]{2,1,0:T(8,128)(2,1)}, bf16[8,8,256]{2,1,0:T(8,128)(2,1)S(1)}, u32[]{:S(2)}, u32[]{:S(2)}) collective-permute-start(bf16[8,8,256]{2,1,0:T(8,128)(2,1)} %get-tuple-element.52), channel_id=1, source_target_pairs={{0,160},{4,164},{8,168},{12,172},{16,176},{20,180},{24,184},{28,18... | collective-permute-start | bytes 98312 | tf_op jit(solution)/shard_map/ppermute | solution.py:243
  187.9 16.0 %collective-permute-done.20.refs_1_ = bf16[8,8,256]{2,1,0:T(8,128)(2,1)S(1)} collective-permute-done((bf16[8,8,256]{2,1,0:T(8,128)(2,1)}, bf16[8,8,256]{2,1,0:T(8,128)(2,1)S(1)}, u32[]{:S(2)}, u32[]{:S(2)}) %collective-permute-start.20) | collective-permute-done | bytes 32800 | tf_op jit(solution)/shard_map/ppermute | solution.py:243
  203.8 2.6 %collective-permute-start.25 = (bf16[8,8,256]{2,1,0:T(8,128)(2,1)}, bf16[8,8,256]{2,1,0:T(8,128)(2,1)S(1)}, u32[]{:S(2)}, u32[]{:S(2)}) collective-permute-start(bf16[8,8,256]{2,1,0:T(8,128)(2,1)} %get-tuple-element.53), channel_id=1, source_target_pairs={{0,192},{4,196},{8,200},{12,204},{16,208},{20,212},{24,216},{28,22... | collective-permute-start | bytes 98312 | tf_op jit(solution)/shard_map/ppermute | solution.py:243
  (121 shorter events, 21.2 us)
Async XLA Ops:
  1.4 5.3 %collective-permute-start = (bf16[32,256]{1,0:T(8,128)(2,1)}, bf16[32,256]{1,0:T(8,128)(2,1)S(1)}, u32[]{:S(2)}, u32[]{:S(2)}) collective-permute-start(bf16[32,256]{1,0:T(8,128)(2,1)} %rim_rows.1), channel_id=1, source_target_pairs={{0,4},{4,8},{8,12},{12,16},{16,20},{20,24},{24,28},{28,32},{32,36}... | collective-permute-start | bytes 49160 | tf_op jit(solution)/shard_map/ppermute | solution.py:20
  13.1 11.5 %all-to-all-start = ((bf16[4,128,256]{2,1,0:T(8,128)(2,1)}), bf16[4,128,256]{2,1,0:T(8,128)(2,1)S(1)}, u32[]{:S(2)}, u32[]{:S(2)}) async-start(bf16[4,128,256]{2,1,0:T(8,128)(2,1)} %bitcast.3), calls=%async_computation | async-start | bytes 524288 | tf_op jit(solution)/shard_map/all_to_all | solution.py:418
  29.0 107.8 %all-to-all-start.1 = ((bf16[64,8,2048]{2,1,0:T(8,128)(2,1)}), bf16[64,8,2048]{2,1,0:T(8,128)(2,1)}, u32[]{:S(2)}, u32[]{:S(2)}) async-start(bf16[64,8,2048]{2,1,0:T(8,128)(2,1)} %bitcast.15), calls=%async_computation.1 | async-start | bytes 4194304 | tf_op jit(solution)/shard_map/all_to_all | solution.py:441
  42.0 27.3 %collective-permute-start.1 = (bf16[2048,256]{1,0:T(8,128)(2,1)S(1)}, bf16[2048,256]{1,0:T(8,128)(2,1)S(1)}, u32[]{:S(2)}, u32[]{:S(2)}) collective-permute-start(bf16[2048,256]{1,0:T(8,128)(2,1)S(1)} %bitcast.18), channel_id=1, source_target_pairs={{0,1},{1,2},{2,3},{3,0},{4,5},{5,6},{6,7},{7,4},{8,9},{9,10},{10,1... | collective-permute-start | bytes 3145736 | tf_op jit(solution)/shard_map/ppermute | solution.py:25
  42.7 26.7 %collective-permute-start.3 = (bf16[2048,256]{1,0:T(8,128)(2,1)S(1)}, bf16[2048,256]{1,0:T(8,128)(2,1)S(1)}, u32[]{:S(2)}, u32[]{:S(2)}) collective-permute-start(bf16[2048,256]{1,0:T(8,128)(2,1)S(1)} %bitcast.19), channel_id=1, source_target_pairs={{0,3},{1,0},{2,1},{3,2},{4,7},{5,4},{6,5},{7,6},{8,11},{9,8},{10,9... | collective-permute-start | bytes 3145736 | tf_op jit(solution)/shard_map/ppermute | solution.py:25
  45.3 46.5 %collective-permute-start.2 = (bf16[2048,256]{1,0:T(8,128)(2,1)S(1)}, bf16[2048,256]{1,0:T(8,128)(2,1)S(1)}, u32[]{:S(2)}, u32[]{:S(2)}) collective-permute-start(bf16[2048,256]{1,0:T(8,128)(2,1)S(1)} %bitcast.21), channel_id=1, source_target_pairs={{0,1},{1,2},{2,3},{3,0},{4,5},{5,6},{6,7},{7,4},{8,9},{9,10},{10,1... | collective-permute-start | bytes 3145736 | tf_op jit(solution)/shard_map/ppermute | solution.py:25
  45.4 47.4 %collective-permute-start.4 = (bf16[2048,256]{1,0:T(8,128)(2,1)S(1)}, bf16[2048,256]{1,0:T(8,128)(2,1)S(1)}, u32[]{:S(2)}, u32[]{:S(2)}) collective-permute-start(bf16[2048,256]{1,0:T(8,128)(2,1)S(1)} %bitcast.22), channel_id=1, source_target_pairs={{0,3},{1,0},{2,1},{3,2},{4,7},{5,4},{6,5},{7,6},{8,11},{9,8},{10,9... | collective-permute-start | bytes 3145736 | tf_op jit(solution)/shard_map/ppermute | solution.py:25
  48.6 65.7 %collective-permute-start.9 = (bf16[256,2048]{1,0:T(8,128)(2,1)S(1)}, bf16[256,2048]{1,0:T(8,128)(2,1)S(1)}, u32[]{:S(2)}, u32[]{:S(2)}) collective-permute-start(bf16[256,2048]{1,0:T(8,128)(2,1)S(1)} %bitcast.24), channel_id=1, source_target_pairs={{0,1},{1,2},{2,3},{3,0},{4,5},{5,6},{6,7},{7,4},{8,9},{9,10},{10,1... | collective-permute-start | bytes 3145736 | tf_op jit(solution)/shard_map/ppermute | solution.py:25
  69.4 45.0 %collective-permute-start.10 = (bf16[256,2048]{1,0:T(8,128)(2,1)S(1)}, bf16[256,2048]{1,0:T(8,128)(2,1)S(1)}, u32[]{:S(2)}, u32[]{:S(2)}) collective-permute-start(bf16[256,2048]{1,0:T(8,128)(2,1)S(1)} %bitcast.25), channel_id=1, source_target_pairs={{0,3},{1,0},{2,1},{3,2},{4,7},{5,4},{6,5},{7,6},{8,11},{9,8},{10,9... | collective-permute-start | bytes 3145736 | tf_op jit(solution)/shard_map/ppermute | solution.py:25
  69.4 44.9 %copy-start.5 = (bf16[2048,256]{1,0:T(8,128)(2,1)}, bf16[2048,256]{1,0:T(8,128)(2,1)S(1)}, u32[]{:S(2)}) copy-start(bf16[2048,256]{1,0:T(8,128)(2,1)S(1)} %collective-permute-done.3.refs_5_) | copy-start | bytes 3145732
  69.4 56.1 %collective-permute-start.5 = (bf16[1024,256]{1,0:T(8,128)(2,1)S(1)}, bf16[1024,256]{1,0:T(8,128)(2,1)S(1)}, u32[]{:S(2)}, u32[]{:S(2)}) collective-permute-start(bf16[1024,256]{1,0:T(8,128)(2,1)S(1)} %slice.144), channel_id=1, source_target_pairs={{0,1},{1,2},{2,3},{3,0},{4,5},{5,6},{6,7},{7,4},{8,9},{9,10},{10,1... | collective-permute-start | bytes 1572872 | tf_op jit(solution)/shard_map/ppermute | solution.py:25
  91.8 34.5 %collective-permute-start.6 = (bf16[1024,256]{1,0:T(8,128)(2,1)}, bf16[1024,256]{1,0:T(8,128)(2,1)}, u32[]{:S(2)}, u32[]{:S(2)}) collective-permute-start(bf16[1024,256]{1,0:T(8,128)(2,1)} %slice.145), channel_id=1, source_target_pairs={{0,3},{1,0},{2,1},{3,2},{4,7},{5,4},{6,5},{7,6},{8,11},{9,8},{10,9... | collective-permute-start | bytes 1572872 | tf_op jit(solution)/shard_map/ppermute | solution.py:25
  92.7 44.0 %collective-permute-start.7 = (bf16[1024,256]{1,0:T(8,128)(2,1)}, bf16[1024,256]{1,0:T(8,128)(2,1)S(1)}, u32[]{:S(2)}, u32[]{:S(2)}) collective-permute-start(bf16[1024,256]{1,0:T(8,128)(2,1)} %slice.146), channel_id=1, source_target_pairs={{0,1},{1,2},{2,3},{3,0},{4,5},{5,6},{6,7},{7,4},{8,9},{9,10},{10,1... | collective-permute-start | bytes 1572872 | tf_op jit(solution)/shard_map/ppermute | solution.py:25
  114.3 22.5 %collective-permute-start.8 = (bf16[1024,256]{1,0:T(8,128)(2,1)S(1)}, bf16[1024,256]{1,0:T(8,128)(2,1)}, u32[]{:S(2)}, u32[]{:S(2)}) collective-permute-start(bf16[1024,256]{1,0:T(8,128)(2,1)S(1)} %slice.147), channel_id=1, source_target_pairs={{0,3},{1,0},{2,1},{3,2},{4,7},{5,4},{6,5},{7,6},{8,11},{9,8},{10,9... | collective-permute-start | bytes 1572872 | tf_op jit(solution)/shard_map/ppermute | solution.py:25
  114.4 32.8 %collective-permute-start.11 = (bf16[128,2048]{1,0:T(8,128)(2,1)S(1)}, bf16[128,2048]{1,0:T(8,128)(2,1)S(1)}, u32[]{:S(2)}, u32[]{:S(2)}) collective-permute-start(bf16[128,2048]{1,0:T(8,128)(2,1)S(1)} %slice.148), channel_id=1, source_target_pairs={{0,1},{1,2},{2,3},{3,0},{4,5},{5,6},{6,7},{7,4},{8,9},{9,10},{10,1... | collective-permute-start | bytes 1572872 | tf_op jit(solution)/shard_map/ppermute | solution.py:25
  126.3 20.8 %collective-permute-start.12 = (bf16[128,2048]{1,0:T(8,128)(2,1)S(1)}, bf16[128,2048]{1,0:T(8,128)(2,1)S(1)}, u32[]{:S(2)}, u32[]{:S(2)}) collective-permute-start(bf16[128,2048]{1,0:T(8,128)(2,1)S(1)} %slice.149), channel_id=1, source_target_pairs={{0,3},{1,0},{2,1},{3,2},{4,7},{5,4},{6,5},{7,6},{8,11},{9,8},{10,9... | collective-permute-start | bytes 1572872 | tf_op jit(solution)/shard_map/ppermute | solution.py:25
  149.6 62.4 %copy-start.1 = (f32[128,2048]{1,0:T(8,128)S(1)}, f32[128,2048]{1,0:T(8,128)}, u32[]{:S(2)}) copy-start(f32[128,2048]{1,0:T(8,128)} %get-tuple-element.30.stream_ref) | copy-start | bytes 3145732
  149.6 63.6 %all-to-all-start.2 = ((bf16[64,8,1792]{2,1,0:T(8,128)(2,1)}), bf16[64,8,1792]{2,1,0:T(8,128)(2,1)S(1)}, u32[]{:S(2)}, u32[]{:S(2)}) async-start(bf16[64,8,1792]{2,1,0:T(8,128)(2,1)} %bitcast.16), calls=%async_computation.2 | async-start | bytes 3670016 | tf_op jit(solution)/shard_map/all_to_all | solution.py:452
  160.0 5.8 %collective-permute-start.13 = (bf16[8,8,256]{2,1,0:T(8,128)(2,1)S(1)}, bf16[8,8,256]{2,1,0:T(8,128)(2,1)S(1)}, u32[]{:S(2)}, u32[]{:S(2)}) collective-permute-start(bf16[8,8,256]{2,1,0:T(8,128)(2,1)S(1)} %copy-done.35), channel_id=1, source_target_pairs={{0,4},{4,0},{8,12},{12,8},{16,20},{20,16},{24,28},{28,24},{32,36},... | collective-permute-start | bytes 98312 | tf_op jit(solution)/shard_map/ppermute | solution.py:238
  160.2 6.6 %collective-permute-start.14 = (bf16[8,8,256]{2,1,0:T(8,128)(2,1)S(1)}, bf16[8,8,256]{2,1,0:T(8,128)(2,1)S(1)}, u32[]{:S(2)}, u32[]{:S(2)}) collective-permute-start(bf16[8,8,256]{2,1,0:T(8,128)(2,1)S(1)} %copy-done.34), channel_id=1, source_target_pairs={{0,8},{4,12},{8,16},{12,20},{16,24},{20,28},{24,0},{28,4},{32,40},... | collective-permute-start | bytes 98312 | tf_op jit(solution)/shard_map/ppermute | solution.py:238
  161.7 6.9 %collective-permute-start.15 = (bf16[8,8,256]{2,1,0:T(8,128)(2,1)S(1)}, bf16[8,8,256]{2,1,0:T(8,128)(2,1)S(1)}, u32[]{:S(2)}, u32[]{:S(2)}) collective-permute-start(bf16[8,8,256]{2,1,0:T(8,128)(2,1)S(1)} %copy-done.33), channel_id=1, source_target_pairs={{0,12},{4,8},{8,20},{12,16},{16,28},{20,24},{24,4},{28,0},{32,44},... | collective-permute-start | bytes 98312 | tf_op jit(solution)/shard_map/ppermute | solution.py:238
  162.6 6.0 %collective-permute-start.16 = (bf16[8,8,256]{2,1,0:T(8,128)(2,1)S(1)}, bf16[8,8,256]{2,1,0:T(8,128)(2,1)S(1)}, u32[]{:S(2)}, u32[]{:S(2)}) collective-permute-start(bf16[8,8,256]{2,1,0:T(8,128)(2,1)S(1)} %copy-done.32), channel_id=1, source_target_pairs={{0,16},{4,20},{8,24},{12,28},{16,0},{20,4},{24,8},{28,12},{32,48},... | collective-permute-start | bytes 98312 | tf_op jit(solution)/shard_map/ppermute | solution.py:238
  164.1 6.3 %collective-permute-start.17 = (bf16[8,8,256]{2,1,0:T(8,128)(2,1)S(1)}, bf16[8,8,256]{2,1,0:T(8,128)(2,1)S(1)}, u32[]{:S(2)}, u32[]{:S(2)}) collective-permute-start(bf16[8,8,256]{2,1,0:T(8,128)(2,1)S(1)} %copy-done.31), channel_id=1, source_target_pairs={{0,20},{4,16},{8,28},{12,24},{16,4},{20,0},{24,12},{28,8},{32,52},... | collective-permute-start | bytes 98312 | tf_op jit(solution)/shard_map/ppermute | solution.py:238
  165.9 5.3 %collective-permute-start.18 = (bf16[8,8,256]{2,1,0:T(8,128)(2,1)S(1)}, bf16[8,8,256]{2,1,0:T(8,128)(2,1)S(1)}, u32[]{:S(2)}, u32[]{:S(2)}) collective-permute-start(bf16[8,8,256]{2,1,0:T(8,128)(2,1)S(1)} %copy-done.30), channel_id=1, source_target_pairs={{0,24},{4,28},{8,0},{12,4},{16,8},{20,12},{24,16},{28,20},{32,56},... | collective-permute-start | bytes 98312 | tf_op jit(solution)/shard_map/ppermute | solution.py:238
  166.8 5.0 %collective-permute-start.19 = (bf16[8,8,256]{2,1,0:T(8,128)(2,1)S(1)}, bf16[8,8,256]{2,1,0:T(8,128)(2,1)S(1)}, u32[]{:S(2)}, u32[]{:S(2)}) collective-permute-start(bf16[8,8,256]{2,1,0:T(8,128)(2,1)S(1)} %copy-done.29), channel_id=1, source_target_pairs={{0,28},{4,24},{8,4},{12,0},{16,12},{20,8},{24,20},{28,16},{32,60},... | collective-permute-start | bytes 98312 | tf_op jit(solution)/shard_map/ppermute | solution.py:238
  174.7 29.1 %collective-permute-start.20 = (bf16[8,8,256]{2,1,0:T(8,128)(2,1)}, bf16[8,8,256]{2,1,0:T(8,128)(2,1)S(1)}, u32[]{:S(2)}, u32[]{:S(2)}) collective-permute-start(bf16[8,8,256]{2,1,0:T(8,128)(2,1)} %get-tuple-element.48), channel_id=1, source_target_pairs={{0,32},{4,36},{8,40},{12,44},{16,48},{20,52},{24,56},{28,60},{32,6... | collective-permute-start | bytes 98312 | tf_op jit(solution)/shard_map/ppermute | solution.py:243
  175.9 31.3 %collective-permute-start.21 = (bf16[8,8,256]{2,1,0:T(8,128)(2,1)}, bf16[8,8,256]{2,1,0:T(8,128)(2,1)S(1)}, u32[]{:S(2)}, u32[]{:S(2)}) collective-permute-start(bf16[8,8,256]{2,1,0:T(8,128)(2,1)} %get-tuple-element.49), channel_id=1, source_target_pairs={{0,64},{4,68},{8,72},{12,76},{16,80},{20,84},{24,88},{28,92},{32,9... | collective-permute-start | bytes 98312 | tf_op jit(solution)/shard_map/ppermute | solution.py:243
  178.4 31.5 %collective-permute-start.22 = (bf16[8,8,256]{2,1,0:T(8,128)(2,1)}, bf16[8,8,256]{2,1,0:T(8,128)(2,1)S(1)}, u32[]{:S(2)}, u32[]{:S(2)}) collective-permute-start(bf16[8,8,256]{2,1,0:T(8,128)(2,1)} %get-tuple-element.50), channel_id=1, source_target_pairs={{0,96},{4,100},{8,104},{12,108},{16,112},{20,116},{24,120},{28,124... | collective-permute-start | bytes 98312 | tf_op jit(solution)/shard_map/ppermute | solution.py:243
  182.2 29.0 %collective-permute-start.23 = (bf16[8,8,256]{2,1,0:T(8,128)(2,1)}, bf16[8,8,256]{2,1,0:T(8,128)(2,1)S(1)}, u32[]{:S(2)}, u32[]{:S(2)}) collective-permute-start(bf16[8,8,256]{2,1,0:T(8,128)(2,1)} %get-tuple-element.51), channel_id=1, source_target_pairs={{0,128},{4,132},{8,136},{12,140},{16,144},{20,148},{24,152},{28,15... | collective-permute-start | bytes 98312 | tf_op jit(solution)/shard_map/ppermute | solution.py:243
  183.7 27.5 %collective-permute-start.24 = (bf16[8,8,256]{2,1,0:T(8,128)(2,1)}, bf16[8,8,256]{2,1,0:T(8,128)(2,1)S(1)}, u32[]{:S(2)}, u32[]{:S(2)}) collective-permute-start(bf16[8,8,256]{2,1,0:T(8,128)(2,1)} %get-tuple-element.52), channel_id=1, source_target_pairs={{0,160},{4,164},{8,168},{12,172},{16,176},{20,180},{24,184},{28,18... | collective-permute-start | bytes 98312 | tf_op jit(solution)/shard_map/ppermute | solution.py:243
  203.8 7.4 %collective-permute-start.25 = (bf16[8,8,256]{2,1,0:T(8,128)(2,1)}, bf16[8,8,256]{2,1,0:T(8,128)(2,1)S(1)}, u32[]{:S(2)}, u32[]{:S(2)}) collective-permute-start(bf16[8,8,256]{2,1,0:T(8,128)(2,1)} %get-tuple-element.53), channel_id=1, source_target_pairs={{0,192},{4,196},{8,200},{12,204},{16,208},{20,212},{24,216},{28,22... | collective-permute-start | bytes 98312 | tf_op jit(solution)/shard_map/ppermute | solution.py:243
  207.2 4.1 %collective-permute-start.26 = (bf16[8,8,256]{2,1,0:T(8,128)(2,1)}, bf16[8,8,256]{2,1,0:T(8,128)(2,1)S(1)}, u32[]{:S(2)}, u32[]{:S(2)}) collective-permute-start(bf16[8,8,256]{2,1,0:T(8,128)(2,1)} %get-tuple-element.54), channel_id=1, source_target_pairs={{0,224},{4,228},{8,232},{12,236},{16,240},{20,244},{24,248},{28,25... | collective-permute-start | bytes 98312 | tf_op jit(solution)/shard_map/ppermute | solution.py:243
  (34 other events, 353.4 us)

commit v10 on v7

--- a/solution.py
+++ b/solution.py
@@ -216,8 +216,11 @@
             pieces = pieces[n:]
         loads.append(fetch(copies, sems, at))
         at += len(copies)
-    spans = [slice(q * width, (q + 1) * width) for q in range(len(pieces))]
-    downs = fetch([(piece, down_ref.at[rows]) for piece, rows in zip(pieces, spans)], sems, at)
+    copies, top = [], 0
+    for piece in pieces:
+        copies.append((piece, down_ref.at[top : top + piece.shape[0]]))
+        top += piece.shape[0]
+    downs = fetch(copies, sems, at)
     load.wait()
     for q, copies in enumerate(loads):
         for c in copies:
@@ -225,8 +228,8 @@
         act = dot(rows_ref[...], w_ref[q])
         gate = act[:, :width]
         hidden = (gate / (1.0 + jnp.exp(-gate)) * act[:, width:]).astype(jnp.bfloat16)
-        if q < len(spans):
-            hidden_ref[:, spans[q]] = hidden
+        if q < len(counts) - 1:
+            hidden_ref[:, q * width : (q + 1) * width] = hidden
         else:
             far_ref[...] = hidden
     for c in downs:
@@ -248,8 +251,8 @@
         scratch=[
             pltpu.VMEM((n, d), jnp.bfloat16),
             pltpu.VMEM((len(counts), d, 2 * width), jnp.bfloat16),
-            pltpu.VMEM((n, len(downs) * width), jnp.bfloat16),
-            pltpu.VMEM((len(downs) * width, out_width), jnp.bfloat16),
+            pltpu.VMEM((n, (len(counts) - 1) * width), jnp.bfloat16),
+            pltpu.VMEM(((len(counts) - 1) * width, out_width), jnp.bfloat16),
             pltpu.SemaphoreType.DMA((len(pieces) + 1,)),
         ],
         limit=26,
@@ -289,6 +292,15 @@
     half = shard.shape[0] // 2
     far = [ring(left[:half], "tp", 1), ring(right[half:], "tp", -1)]
     return [left], [right], far
+
+
+def gathered_halves(shard):
+    half = shard.shape[0] // 2
+    top, low = shard[:half], shard[half:]
+    left_top, right_low = ring(top, "tp", 1), ring(low, "tp", -1)
+    left_low, right_top = ring(low, "tp", 1), ring(top, "tp", -1)
+    far = [ring(left_top, "tp", 1), ring(right_low, "tp", -1)]
+    return [left_top, left_low], [right_top, right_low], far
 
 
 def shards(
@@ -312,7 +324,7 @@
     model_width = w_down.shape[2]
     gates = gathered(w_gate[0])
     ups = gathered(w_up[0])
-    downs = gathered(w_down[0])
+    downs = gathered_halves(w_down[0])
     lines = segments.reshape(tok_dev // LANES, LANES)
     rim = passed_along(rim_rows(conv_value, conv_gate, lines), "sp", 1)
     padded = jnp.pad(segments, (reach, 0), constant_values=-1)

time: 214 us -> 214 us (level)
    ppermute x12 -> x14, starting transfers between devices: 13 us -> 14.6 us  [ring(): lax.ppermute(value, axis, [(i, (i + steps) % count) for i in range(count)])]
    ppermute x12 -> x14, waiting for transfers between devices: 79.8 us -> 80 us  [ring(): lax.ppermute(value, axis, [(i, (i + steps) % count) for i in range(count)])]
  transfers between devices with their start and end apart: 16 -> 18, of which waited for: 8 -> 9; matrix products, arithmetic and copies ran while one was open for 2% -> 1% of each run, Pallas kernels for 5% -> 5%
where the time goes in v10:
time: 214 us; the launch traced here: 213 us
  waiting for transfers between devices  138 us (64%)
  starting transfers between devices  44.1 us (21%)
  Pallas kernels  25.3 us (12%)
  local copies, waits for them, and re-layouts  3.48 us (2%)
    ppermute x14, waiting for transfers between devices, ring(): lax.ppermute(value, axis, [(i, (i + steps) % count) for i in range(count)])  80 us
    all_to_all x1, waiting for transfers between devices, shards(): lax.all_to_all(out.reshape(experts_n, capacity, model_width), 'sp', 0, 0,...  50 us
    pallas_call x6, Pallas kernels, kernel(): pl.pallas_call(body, out_shape=[pltpu.HBM(*o) if i in far_out else jax.Sh...  23.9 us
    ppermute x14, starting transfers between devices, ring(): lax.ppermute(value, axis, [(i, (i + steps) % count) for i in range(count)])  14.6 us
    all_to_all x1, starting transfers between devices, shards(): lax.all_to_all(outgoing.reshape(experts_n, capacity, model_width), 'sp',...  12.7 us
    all_to_all x1, starting transfers between devices, shards(): lax.all_to_all(out.reshape(experts_n, capacity, model_width), 'sp', 0, 0,...  10.4 us
    all_to_all x1, waiting for transfers between devices, shards(): lax.all_to_all(conv_out.reshape(columns, rows_own, local_channels), 'tp',...  6.89 us
    all_to_all x1, starting transfers between devices, shards(): lax.all_to_all(conv_out.reshape(columns, rows_own, local_channels), 'tp',...  4.48 us
  transfers between devices with their start and end apart: 18, of which 9 were waited for; matrix products, arithmetic and copies ran while one was open for 1% of the time, Pallas kernels for 5%

profile of v10, /device:TPU:2, one launch (start us, length us, event | category | flops | bytes accessed | tf_op | source)
XLA Modules:
  0.0 213.5 jit_solution(14552453818356954002)
XLA Ops:
  0.0 1.4 rim_rows.1
  1.4 1.9 collective-permute-start
  3.3 1.9 convert_add_fusion
  5.3 1.4 collective-permute-done.rim_ref
  6.7 0.1 broadcast_in_dim.15.seen_ref
  6.8 6.3 %shard_map.136 = bf16[512,256]{1,0:T(8,128)(2,1)} custom-call(bf16[32,256]{1,0:T(8,128)(2,1)S(1)} %collective-permute-done.rim_ref, s32[512,128]{1,0:T(8,128)S(1)} %broadcast_in_dim.15.seen_ref, bf16[512,256]{1,0:T(8,128)(2,1)} %refs_0_.1, bf16[512,256]{1,0:T(8,128)(2,1)} %refs_1_.1, s32[4,128]{1,0:T(4,128)} %bitcast.29, f32[31,256]{1,0:T(8,128)} %refs_3_.1, ...), custom_call_target="tpu_custom_call" | custom-call | tf_op jit(solution)/shard_map/pallas_call | solution.py:34
  13.1 4.5 %all-to-all-start = ((bf16[4,128,256]{2,1,0:T(8,128)(2,1)}), bf16[4,128,256]{2,1,0:T(8,128)(2,1)S(1)}, u32[]{:S(2)}, u32[]{:S(2)}) async-start(bf16[4,128,256]{2,1,0:T(8,128)(2,1)} %bitcast.3), calls=%async_computation | async-start | bytes 524288 | tf_op jit(solution)/shard_map/all_to_all | solution.py:341
  17.6 0.1 copy.17.routes_ref
  17.7 6.9 %all-to-all-done.parts_ref = bf16[4,128,256]{2,1,0:T(8,128)(2,1)S(1)} async-done(((bf16[4,128,256]{2,1,0:T(8,128)(2,1)}), bf16[4,128,256]{2,1,0:T(8,128)(2,1)S(1)}, u32[]{:S(2)}, u32[]{:S(2)}) %all-to-all-start) | async-done | bytes 262176 | tf_op jit(solution)/shard_map/all_to_all | solution.py:341
  24.6 4.4 %shard_map.137 = (f32[128,2048]{1,0:T(8,128)}, bf16[512,2048]{1,0:T(8,128)(2,1)}) custom-call(bf16[4,128,256]{2,1,0:T(8,128)(2,1)S(1)} %all-to-all-done.parts_ref, bf16[128,2048]{1,0:T(8,128)(2,1)S(1)} %copy-done.2, f32[1,2048]{1,0:T(1,128)S(1)} %bitcast.17, s32[128,2]{1,0:T(8,128)S(1)} %copy.17.routes_ref, bf16[1024,2048]{1,0:T(8,128)(2,1)} %weight_ref.1), custom_call_target="tpu_custom_call" | custom-call | tf_op jit(solution)/shard_map/pallas_call | solution.py:34
  29.0 12.7 %all-to-all-start.1 = ((bf16[64,8,2048]{2,1,0:T(8,128)(2,1)}), bf16[64,8,2048]{2,1,0:T(8,128)(2,1)S(1)}, u32[]{:S(2)}, u32[]{:S(2)}) async-start(bf16[64,8,2048]{2,1,0:T(8,128)(2,1)} %bitcast.21), calls=%async_computation.1 | async-start | bytes 4194304 | tf_op jit(solution)/shard_map/all_to_all | solution.py:364
  41.7 0.6 collective-permute-start.1
  42.3 2.7 %collective-permute-start.3 = (bf16[2048,256]{1,0:T(8,128)(2,1)}, bf16[2048,256]{1,0:T(8,128)(2,1)S(1)}, u32[]{:S(2)}, u32[]{:S(2)}) collective-permute-start(bf16[2048,256]{1,0:T(8,128)(2,1)} %bitcast.23), channel_id=1, source_target_pairs={{0,3},{1,0},{2,1},{3,2},{4,7},{5,4},{6,5},{7,6},{8,11},{9,8},{10,9... | collective-permute-start | bytes 3145736 | tf_op jit(solution)/shard_map/ppermute | solution.py:24
  45.0 3.2 %collective-permute-start.4 = (bf16[2048,256]{1,0:T(8,128)(2,1)}, bf16[2048,256]{1,0:T(8,128)(2,1)S(1)}, u32[]{:S(2)}, u32[]{:S(2)}) collective-permute-start(bf16[2048,256]{1,0:T(8,128)(2,1)} %bitcast.26), channel_id=1, source_target_pairs={{0,3},{1,0},{2,1},{3,2},{4,7},{5,4},{6,5},{7,6},{8,11},{9,8},{10,9... | collective-permute-start | bytes 3145736 | tf_op jit(solution)/shard_map/ppermute | solution.py:24
  48.4 20.8 %collective-permute-done.1.refs_3_ = bf16[2048,256]{1,0:T(8,128)(2,1)S(1)} collective-permute-done((bf16[2048,256]{1,0:T(8,128)(2,1)}, bf16[2048,256]{1,0:T(8,128)(2,1)S(1)}, u32[]{:S(2)}, u32[]{:S(2)}) %collective-permute-start.1) | collective-permute-done | bytes 1048608 | tf_op jit(solution)/shard_map/ppermute | solution.py:24
  69.4 22.3 %collective-permute-done.2.refs_4_ = bf16[2048,256]{1,0:T(8,128)(2,1)S(1)} collective-permute-done((bf16[2048,256]{1,0:T(8,128)(2,1)}, bf16[2048,256]{1,0:T(8,128)(2,1)S(1)}, u32[]{:S(2)}, u32[]{:S(2)}) %collective-permute-start.2) | collective-permute-done | bytes 1048608 | tf_op jit(solution)/shard_map/ppermute | solution.py:24
  91.7 2.0 collective-permute-start.5
  93.9 8.6 %collective-permute-done.12.refs_15_ = bf16[128,2048]{1,0:T(8,128)(2,1)} collective-permute-done((bf16[128,2048]{1,0:T(8,128)(2,1)S(1)}, bf16[128,2048]{1,0:T(8,128)(2,1)}, u32[]{:S(2)}, u32[]{:S(2)}) %collective-permute-start.12) | collective-permute-done | bytes 524320 | tf_op jit(solution)/shard_map/ppermute | solution.py:24
  102.5 3.8 %collective-permute-start.6 = (bf16[1024,256]{1,0:T(8,128)(2,1)S(1)}, bf16[1024,256]{1,0:T(8,128)(2,1)S(1)}, u32[]{:S(2)}, u32[]{:S(2)}) collective-permute-start(bf16[1024,256]{1,0:T(8,128)(2,1)S(1)} %slice.153), channel_id=1, source_target_pairs={{0,3},{1,0},{2,1},{3,2},{4,7},{5,4},{6,5},{7,6},{8,11},{9,8},{10,9... | collective-permute-start | bytes 1572872 | tf_op jit(solution)/shard_map/ppermute | solution.py:24
  106.3 7.9 %collective-permute-done.10.refs_13_ = bf16[128,2048]{1,0:T(8,128)(2,1)S(1)} collective-permute-done((bf16[128,2048]{1,0:T(8,128)(2,1)S(1)}, bf16[128,2048]{1,0:T(8,128)(2,1)S(1)}, u32[]{:S(2)}, u32[]{:S(2)}) %collective-permute-start.10) | collective-permute-done | bytes 524320 | tf_op jit(solution)/shard_map/ppermute | solution.py:24
  114.2 2.0 collective-permute-start.13
  116.2 9.2 %collective-permute-done.5.refs_7_ = bf16[1024,256]{1,0:T(8,128)(2,1)S(1)} collective-permute-done((bf16[1024,256]{1,0:T(8,128)(2,1)S(1)}, bf16[1024,256]{1,0:T(8,128)(2,1)S(1)}, u32[]{:S(2)}, u32[]{:S(2)}) %collective-permute-start.5) | collective-permute-done | bytes 524320 | tf_op jit(solution)/shard_map/ppermute | solution.py:24
  125.4 11.2 %collective-permute-done.7.refs_9_ = bf16[1024,256]{1,0:T(8,128)(2,1)S(1)} collective-permute-done((bf16[1024,256]{1,0:T(8,128)(2,1)S(1)}, bf16[1024,256]{1,0:T(8,128)(2,1)S(1)}, u32[]{:S(2)}, u32[]{:S(2)}) %collective-permute-start.7) | collective-permute-done | bytes 524320 | tf_op jit(solution)/shard_map/ppermute | solution.py:24
  136.7 0.8 copy-done.14
  137.5 1.4 copy-done.4
  138.8 9.2 %shard_map.139 = (bf16[512,256]{1,0:T(8,128)(2,1)S(1)}, f32[512,2048]{1,0:T(8,128)S(1)}) custom-call(bf16[512,2048]{1,0:T(8,128)(2,1)} %bitcast.18, bf16[2048,256]{1,0:T(8,128)(2,1)} %bitcast.24, bf16[2048,256]{1,0:T(8,128)(2,1)} %bitcast.27, bf16[2048,256]{1,0:T(8,128)(2,1)} %copy-done.6, bf16[2048,256]{1,0:T(8,128)(2,1)} %copy-done.8, ...), custom_call_target="tpu_custom_call" | custom-call | tf_op jit(solution)/shard_map/pallas_call | solution.py:34
  148.1 2.1 shard_map.140
  150.2 10.4 %all-to-all-start.2 = ((bf16[64,8,2048]{2,1,0:T(8,128)(2,1)}), bf16[64,8,2048]{2,1,0:T(8,128)(2,1)S(1)}, u32[]{:S(2)}, u32[]{:S(2)}) async-start(bf16[64,8,2048]{2,1,0:T(8,128)(2,1)} %bitcast.19), calls=%async_computation.2 | async-start | bytes 4194304 | tf_op jit(solution)/shard_map/all_to_all | solution.py:373
  160.6 0.7 constant_dynamic-slice_fusion
  161.4 0.5 shard_map.138
  161.9 50.0 %all-to-all-done.2 = bf16[64,8,2048]{2,1,0:T(8,128)(2,1)S(1)} async-done(((bf16[64,8,2048]{2,1,0:T(8,128)(2,1)}), bf16[64,8,2048]{2,1,0:T(8,128)(2,1)S(1)}, u32[]{:S(2)}, u32[]{:S(2)}) %all-to-all-start.2) | async-done | bytes 2097184 | tf_op jit(solution)/shard_map/all_to_all | solution.py:373
  211.9 1.4 shard_map.141
  (52 shorter events, 0.6 us)
Async XLA Ops:
  0.0 17.6 %copy-start = (s32[512,2]{0,1:T(2,128)S(1)}, s32[512,2]{0,1:T(2,128)}, u32[]{:S(2)}) copy-start(s32[512,2]{0,1:T(2,128)} %param.23) | copy-start | bytes 12292
  0.0 24.6 %copy-start.3 = (f32[2048]{0:T(1024)S(1)}, f32[2048]{0:T(1024)}, u32[]{:S(2)}) copy-start(f32[2048]{0:T(1024)} %param.22) | copy-start | bytes 24580
  0.0 24.6 %copy-start.2 = (bf16[128,2048]{1,0:T(8,128)(2,1)S(1)}, bf16[128,2048]{1,0:T(8,128)(2,1)}, u32[]{:S(2)}) copy-start(bf16[128,2048]{1,0:T(8,128)(2,1)} %residual_ref.1) | copy-start | bytes 1572868
  1.4 5.3 %collective-permute-start = (bf16[32,256]{1,0:T(8,128)(2,1)}, bf16[32,256]{1,0:T(8,128)(2,1)S(1)}, u32[]{:S(2)}, u32[]{:S(2)}) collective-permute-start(bf16[32,256]{1,0:T(8,128)(2,1)} %rim_rows.1), channel_id=1, source_target_pairs={{0,4},{4,8},{8,12},{12,16},{16,20},{20,24},{24,28},{28,32},{32,36}... | collective-permute-start | bytes 49160 | tf_op jit(solution)/shard_map/ppermute | solution.py:19
  13.1 11.5 %all-to-all-start = ((bf16[4,128,256]{2,1,0:T(8,128)(2,1)}), bf16[4,128,256]{2,1,0:T(8,128)(2,1)S(1)}, u32[]{:S(2)}, u32[]{:S(2)}) async-start(bf16[4,128,256]{2,1,0:T(8,128)(2,1)} %bitcast.3), calls=%async_computation | async-start | bytes 524288 | tf_op jit(solution)/shard_map/all_to_all | solution.py:341
  29.0 19.3 %copy-start.5 = (bf16[1,256,2048]{2,1,0:T(8,128)(2,1)S(1)}, bf16[1,256,2048]{2,1,0:T(8,128)(2,1)}, u32[]{:S(2)}) copy-start(bf16[1,256,2048]{2,1,0:T(8,128)(2,1)} %param.27) | copy-start | bytes 3145732
  29.0 108.5 %all-to-all-start.1 = ((bf16[64,8,2048]{2,1,0:T(8,128)(2,1)}), bf16[64,8,2048]{2,1,0:T(8,128)(2,1)S(1)}, u32[]{:S(2)}, u32[]{:S(2)}) async-start(bf16[64,8,2048]{2,1,0:T(8,128)(2,1)} %bitcast.21), calls=%async_computation.1 | async-start | bytes 4194304 | tf_op jit(solution)/shard_map/all_to_all | solution.py:364
  41.7 27.5 %collective-permute-start.1 = (bf16[2048,256]{1,0:T(8,128)(2,1)}, bf16[2048,256]{1,0:T(8,128)(2,1)S(1)}, u32[]{:S(2)}, u32[]{:S(2)}) collective-permute-start(bf16[2048,256]{1,0:T(8,128)(2,1)} %bitcast.22), channel_id=1, source_target_pairs={{0,1},{1,2},{2,3},{3,0},{4,5},{5,6},{6,7},{7,4},{8,9},{9,10},{10,1... | collective-permute-start | bytes 3145736 | tf_op jit(solution)/shard_map/ppermute | solution.py:24
  42.3 26.9 %collective-permute-start.3 = (bf16[2048,256]{1,0:T(8,128)(2,1)}, bf16[2048,256]{1,0:T(8,128)(2,1)S(1)}, u32[]{:S(2)}, u32[]{:S(2)}) collective-permute-start(bf16[2048,256]{1,0:T(8,128)(2,1)} %bitcast.23), channel_id=1, source_target_pairs={{0,3},{1,0},{2,1},{3,2},{4,7},{5,4},{6,5},{7,6},{8,11},{9,8},{10,9... | collective-permute-start | bytes 3145736 | tf_op jit(solution)/shard_map/ppermute | solution.py:24
  45.0 46.7 %collective-permute-start.2 = (bf16[2048,256]{1,0:T(8,128)(2,1)}, bf16[2048,256]{1,0:T(8,128)(2,1)S(1)}, u32[]{:S(2)}, u32[]{:S(2)}) collective-permute-start(bf16[2048,256]{1,0:T(8,128)(2,1)} %bitcast.25), channel_id=1, source_target_pairs={{0,1},{1,2},{2,3},{3,0},{4,5},{5,6},{6,7},{7,4},{8,9},{9,10},{10,1... | collective-permute-start | bytes 3145736 | tf_op jit(solution)/shard_map/ppermute | solution.py:24
  45.0 46.7 %collective-permute-start.4 = (bf16[2048,256]{1,0:T(8,128)(2,1)}, bf16[2048,256]{1,0:T(8,128)(2,1)S(1)}, u32[]{:S(2)}, u32[]{:S(2)}) collective-permute-start(bf16[2048,256]{1,0:T(8,128)(2,1)} %bitcast.26), channel_id=1, source_target_pairs={{0,3},{1,0},{2,1},{3,2},{4,7},{5,4},{6,5},{7,6},{8,11},{9,8},{10,9... | collective-permute-start | bytes 3145736 | tf_op jit(solution)/shard_map/ppermute | solution.py:24
  48.4 54.1 %collective-permute-start.12 = (bf16[128,2048]{1,0:T(8,128)(2,1)S(1)}, bf16[128,2048]{1,0:T(8,128)(2,1)}, u32[]{:S(2)}, u32[]{:S(2)}) collective-permute-start(bf16[128,2048]{1,0:T(8,128)(2,1)S(1)} %get-tuple-element.17), channel_id=1, source_target_pairs={{0,3},{1,0},{2,1},{3,2},{4,7},{5,4},{6,5},{7,6},{8,11},{9,8},{10,9... | collective-permute-start | bytes 1572872 | tf_op jit(solution)/shard_map/ppermute | solution.py:24
  69.2 24.6 %copy-start.6 = (bf16[2048,256]{1,0:T(8,128)(2,1)}, bf16[2048,256]{1,0:T(8,128)(2,1)S(1)}, u32[]{:S(2)}) copy-start(bf16[2048,256]{1,0:T(8,128)(2,1)S(1)} %collective-permute-done.1.refs_3_) | copy-start | bytes 3145732
  69.2 37.0 %collective-permute-start.9 = (bf16[128,2048]{1,0:T(8,128)(2,1)S(1)}, bf16[128,2048]{1,0:T(8,128)(2,1)}, u32[]{:S(2)}, u32[]{:S(2)}) collective-permute-start(bf16[128,2048]{1,0:T(8,128)(2,1)S(1)} %get-tuple-element.18), channel_id=1, source_target_pairs={{0,1},{1,2},{2,3},{3,0},{4,5},{5,6},{6,7},{7,4},{8,9},{9,10},{10,1... | collective-permute-start | bytes 1572872 | tf_op jit(solution)/shard_map/ppermute | solution.py:24
  69.2 24.6 %copy-start.7 = (bf16[2048,256]{1,0:T(8,128)(2,1)}, bf16[2048,256]{1,0:T(8,128)(2,1)S(1)}, u32[]{:S(2)}) copy-start(bf16[2048,256]{1,0:T(8,128)(2,1)S(1)} %collective-permute-done.3.refs_5_) | copy-start | bytes 3145732
  69.2 44.9 %collective-permute-start.10 = (bf16[128,2048]{1,0:T(8,128)(2,1)S(1)}, bf16[128,2048]{1,0:T(8,128)(2,1)S(1)}, u32[]{:S(2)}, u32[]{:S(2)}) collective-permute-start(bf16[128,2048]{1,0:T(8,128)(2,1)S(1)} %get-tuple-element.17), channel_id=1, source_target_pairs={{0,1},{1,2},{2,3},{3,0},{4,5},{5,6},{6,7},{7,4},{8,9},{9,10},{10,1... | collective-permute-start | bytes 1572872 | tf_op jit(solution)/shard_map/ppermute | solution.py:24
  91.7 44.9 %copy-start.8 = (bf16[2048,256]{1,0:T(8,128)(2,1)}, bf16[2048,256]{1,0:T(8,128)(2,1)S(1)}, u32[]{:S(2)}) copy-start(bf16[2048,256]{1,0:T(8,128)(2,1)S(1)} %collective-permute-done.2.refs_4_) | copy-start | bytes 3145732
  91.7 22.5 %collective-permute-start.11 = (bf16[128,2048]{1,0:T(8,128)(2,1)S(1)}, bf16[128,2048]{1,0:T(8,128)(2,1)S(1)}, u32[]{:S(2)}, u32[]{:S(2)}) collective-permute-start(bf16[128,2048]{1,0:T(8,128)(2,1)S(1)} %get-tuple-element.18), channel_id=1, source_target_pairs={{0,3},{1,0},{2,1},{3,2},{4,7},{5,4},{6,5},{7,6},{8,11},{9,8},{10,9... | collective-permute-start | bytes 1572872 | tf_op jit(solution)/shard_map/ppermute | solution.py:24
  91.7 44.9 %copy-start.9 = (bf16[2048,256]{1,0:T(8,128)(2,1)}, bf16[2048,256]{1,0:T(8,128)(2,1)S(1)}, u32[]{:S(2)}) copy-start(bf16[2048,256]{1,0:T(8,128)(2,1)S(1)} %collective-permute-done.4.refs_6_) | copy-start | bytes 3145732
  91.7 33.7 %collective-permute-start.5 = (bf16[1024,256]{1,0:T(8,128)(2,1)S(1)}, bf16[1024,256]{1,0:T(8,128)(2,1)S(1)}, u32[]{:S(2)}, u32[]{:S(2)}) collective-permute-start(bf16[1024,256]{1,0:T(8,128)(2,1)S(1)} %slice.152), channel_id=1, source_target_pairs={{0,1},{1,2},{2,3},{3,0},{4,5},{5,6},{6,7},{7,4},{8,9},{9,10},{10,1... | collective-permute-start | bytes 1572872 | tf_op jit(solution)/shard_map/ppermute | solution.py:24
  102.5 22.9 %collective-permute-start.6 = (bf16[1024,256]{1,0:T(8,128)(2,1)S(1)}, bf16[1024,256]{1,0:T(8,128)(2,1)S(1)}, u32[]{:S(2)}, u32[]{:S(2)}) collective-permute-start(bf16[1024,256]{1,0:T(8,128)(2,1)S(1)} %slice.153), channel_id=1, source_target_pairs={{0,3},{1,0},{2,1},{3,2},{4,7},{5,4},{6,5},{7,6},{8,11},{9,8},{10,9... | collective-permute-start | bytes 1572872 | tf_op jit(solution)/shard_map/ppermute | solution.py:24
  106.3 30.4 %collective-permute-start.7 = (bf16[1024,256]{1,0:T(8,128)(2,1)S(1)}, bf16[1024,256]{1,0:T(8,128)(2,1)S(1)}, u32[]{:S(2)}, u32[]{:S(2)}) collective-permute-start(bf16[1024,256]{1,0:T(8,128)(2,1)S(1)} %slice.154), channel_id=1, source_target_pairs={{0,1},{1,2},{2,3},{3,0},{4,5},{5,6},{6,7},{7,4},{8,9},{9,10},{10,1... | collective-permute-start | bytes 1572872 | tf_op jit(solution)/shard_map/ppermute | solution.py:24
  114.2 22.5 %copy-start.10 = (bf16[128,2048]{1,0:T(8,128)(2,1)}, bf16[128,2048]{1,0:T(8,128)(2,1)S(1)}, u32[]{:S(2)}) copy-start(bf16[128,2048]{1,0:T(8,128)(2,1)S(1)} %collective-permute-done.10.refs_13_) | copy-start | bytes 1572868
  114.2 23.3 %collective-permute-start.8 = (bf16[1024,256]{1,0:T(8,128)(2,1)S(1)}, bf16[1024,256]{1,0:T(8,128)(2,1)}, u32[]{:S(2)}, u32[]{:S(2)}) collective-permute-start(bf16[1024,256]{1,0:T(8,128)(2,1)S(1)} %slice.155), channel_id=1, source_target_pairs={{0,3},{1,0},{2,1},{3,2},{4,7},{5,4},{6,5},{7,6},{8,11},{9,8},{10,9... | collective-permute-start | bytes 1572872 | tf_op jit(solution)/shard_map/ppermute | solution.py:24
  114.2 22.5 %copy-start.11 = (bf16[128,2048]{1,0:T(8,128)(2,1)}, bf16[128,2048]{1,0:T(8,128)(2,1)S(1)}, u32[]{:S(2)}) copy-start(bf16[128,2048]{1,0:T(8,128)(2,1)S(1)} %collective-permute-done.11.refs_14_) | copy-start | bytes 1572868
  114.2 33.9 %collective-permute-start.13 = (bf16[128,2048]{1,0:T(8,128)(2,1)}, bf16[128,2048]{1,0:T(8,128)(2,1)S(1)}, u32[]{:S(2)}, u32[]{:S(2)}) collective-permute-start(bf16[128,2048]{1,0:T(8,128)(2,1)} %collective-permute-done.9.refs_12_), channel_id=1, source_target_pairs={{0,1},{1,2},{2,3},{3,0},{4,5},{5,6},{6,7},{7,4},{8,9},{9,10},{10,1... | collective-permute-start | bytes 1572872 | tf_op jit(solution)/shard_map/ppermute | solution.py:24
  125.4 11.3 %copy-start.12 = (bf16[1024,256]{1,0:T(8,128)(2,1)}, bf16[1024,256]{1,0:T(8,128)(2,1)S(1)}, u32[]{:S(2)}) copy-start(bf16[1024,256]{1,0:T(8,128)(2,1)S(1)} %collective-permute-done.5.refs_7_) | copy-start | bytes 1572868
  125.4 22.7 %collective-permute-start.14 = (bf16[128,2048]{1,0:T(8,128)(2,1)}, bf16[128,2048]{1,0:T(8,128)(2,1)S(1)}, u32[]{:S(2)}, u32[]{:S(2)}) collective-permute-start(bf16[128,2048]{1,0:T(8,128)(2,1)} %collective-permute-done.12.refs_15_), channel_id=1, source_target_pairs={{0,3},{1,0},{2,1},{3,2},{4,7},{5,4},{6,5},{7,6},{8,11},{9,8},{10,9... | collective-permute-start | bytes 1572872 | tf_op jit(solution)/shard_map/ppermute | solution.py:24
  125.4 11.3 %copy-start.13 = (bf16[1024,256]{1,0:T(8,128)(2,1)}, bf16[1024,256]{1,0:T(8,128)(2,1)S(1)}, u32[]{:S(2)}) copy-start(bf16[1024,256]{1,0:T(8,128)(2,1)S(1)} %collective-permute-done.6.refs_8_) | copy-start | bytes 1572868
  137.5 1.4 copy-start.4
  150.2 61.7 %copy-start.1 = (f32[128,2048]{1,0:T(8,128)S(1)}, f32[128,2048]{1,0:T(8,128)}, u32[]{:S(2)}) copy-start(f32[128,2048]{1,0:T(8,128)} %get-tuple-element.11.stream_ref) | copy-start | bytes 3145732
  150.2 61.7 %all-to-all-start.2 = ((bf16[64,8,2048]{2,1,0:T(8,128)(2,1)}), bf16[64,8,2048]{2,1,0:T(8,128)(2,1)S(1)}, u32[]{:S(2)}, u32[]{:S(2)}) async-start(bf16[64,8,2048]{2,1,0:T(8,128)(2,1)} %bitcast.19), calls=%async_computation.2 | async-start | bytes 4194304 | tf_op jit(solution)/shard_map/all_to_all | solution.py:373
  (1 other events, 0.8 us)

commit v11 on v7

--- a/solution.py
+++ b/solution.py
@@ -201,10 +201,9 @@
 
 
 def hidden_body(counts, *refs):
-    rows_in, *pieces, far_ref, sum_ref, rows_ref, w_ref, hidden_ref, down_ref, sems = refs
+    rows_ref, *pieces, far_ref, sum_ref, w_ref, hidden_ref, down_ref, sems = refs
     width = pieces[0].shape[1]
-    (load,) = fetch([(rows_in, rows_ref)], sems)
-    loads, at = [], 1
+    loads, at = [], 0
     for q, kinds in enumerate(counts):
         copies = []
         for kind, n in enumerate(kinds):
@@ -218,7 +217,6 @@
         at += len(copies)
     spans = [slice(q * width, (q + 1) * width) for q in range(len(pieces))]
     downs = fetch([(piece, down_ref.at[rows]) for piece, rows in zip(pieces, spans)], sems, at)
-    load.wait()
     for q, copies in enumerate(loads):
         for c in copies:
             c.wait()
@@ -246,14 +244,13 @@
         [((n, width), jnp.bfloat16), ((n, out_width), jnp.float32)],
         (rows, *pieces),
         scratch=[
-            pltpu.VMEM((n, d), jnp.bfloat16),
             pltpu.VMEM((len(counts), d, 2 * width), jnp.bfloat16),
             pltpu.VMEM((n, len(downs) * width), jnp.bfloat16),
             pltpu.VMEM((len(downs) * width, out_width), jnp.bfloat16),
-            pltpu.SemaphoreType.DMA((len(pieces) + 1,)),
+            pltpu.SemaphoreType.DMA((len(pieces),)),
         ],
-        limit=26,
-        far_in=range(1 + len(pieces)),
+        limit=24,
+        far_in=range(1, 1 + len(pieces)),
     )
 
 

time: 214 us -> 213 us (level)
  transfers between devices with their start and end apart: 16 -> 16, of which waited for: 8 -> 9; matrix products, arithmetic and copies ran while one was open for 2% -> 2% of each run, Pallas kernels for 5% -> 4%
where the time goes in v11:
time: 213 us; the launch traced here: 212 us
  waiting for transfers between devices  139 us (65%)
  starting transfers between devices  42.5 us (20%)
  Pallas kernels  24.7 us (12%)
  local copies, waits for them, and re-layouts  3.73 us (2%)
    ppermute x12, waiting for transfers between devices, ring(): lax.ppermute(value, axis, [(i, (i + steps) % count) for i in range(count)])  80.7 us
    all_to_all x1, waiting for transfers between devices, shards(): lax.all_to_all(out.reshape(experts_n, capacity, model_width), 'sp', 0, 0,...  50 us
    pallas_call x6, Pallas kernels, kernel(): pl.pallas_call(body, out_shape=[pltpu.HBM(*o) if i in far_out else jax.Sh...  23.3 us
    ppermute x12, starting transfers between devices, ring(): lax.ppermute(value, axis, [(i, (i + steps) % count) for i in range(count)])  13 us
    all_to_all x1, starting transfers between devices, shards(): lax.all_to_all(outgoing.reshape(experts_n, capacity, model_width), 'sp',...  12.7 us
    all_to_all x1, starting transfers between devices, shards(): lax.all_to_all(out.reshape(experts_n, capacity, model_width), 'sp', 0, 0,...  10.4 us
    all_to_all x1, waiting for transfers between devices, shards(): lax.all_to_all(conv_out.reshape(columns, rows_own, local_channels), 'tp',...  6.89 us
    all_to_all x1, starting transfers between devices, shards(): lax.all_to_all(conv_out.reshape(columns, rows_own, local_channels), 'tp',...  4.48 us
  transfers between devices with their start and end apart: 16, of which 9 were waited for; matrix products, arithmetic and copies ran while one was open for 2% of the time, Pallas kernels for 4%

profile of v11, /device:TPU:2, one launch (start us, length us, event | category | flops | bytes accessed | tf_op | source)
XLA Modules:
  0.0 212.2 jit_solution(14090668991248351131)
XLA Ops:
  0.0 1.4 rim_rows.1
  1.4 1.9 collective-permute-start
  3.3 1.9 convert_add_fusion
  5.3 1.4 collective-permute-done.rim_ref
  6.7 0.1 broadcast_in_dim.15.seen_ref
  6.8 6.3 %shard_map.136 = bf16[512,256]{1,0:T(8,128)(2,1)} custom-call(bf16[32,256]{1,0:T(8,128)(2,1)S(1)} %collective-permute-done.rim_ref, s32[512,128]{1,0:T(8,128)S(1)} %broadcast_in_dim.15.seen_ref, bf16[512,256]{1,0:T(8,128)(2,1)} %refs_0_.1, bf16[512,256]{1,0:T(8,128)(2,1)} %refs_1_.1, s32[4,128]{1,0:T(4,128)} %bitcast.27, f32[31,256]{1,0:T(8,128)} %refs_3_.1, ...), custom_call_target="tpu_custom_call" | custom-call | tf_op jit(solution)/shard_map/pallas_call | solution.py:34
  13.1 4.5 %all-to-all-start = ((bf16[4,128,256]{2,1,0:T(8,128)(2,1)}), bf16[4,128,256]{2,1,0:T(8,128)(2,1)S(1)}, u32[]{:S(2)}, u32[]{:S(2)}) async-start(bf16[4,128,256]{2,1,0:T(8,128)(2,1)} %bitcast.3), calls=%async_computation | async-start | bytes 524288 | tf_op jit(solution)/shard_map/all_to_all | solution.py:326
  17.7 6.9 %all-to-all-done.parts_ref = bf16[4,128,256]{2,1,0:T(8,128)(2,1)S(1)} async-done(((bf16[4,128,256]{2,1,0:T(8,128)(2,1)}), bf16[4,128,256]{2,1,0:T(8,128)(2,1)S(1)}, u32[]{:S(2)}, u32[]{:S(2)}) %all-to-all-start) | async-done | bytes 262176 | tf_op jit(solution)/shard_map/all_to_all | solution.py:326
  24.6 4.4 %shard_map.137 = (f32[128,2048]{1,0:T(8,128)}, bf16[512,2048]{1,0:T(8,128)(2,1)}) custom-call(bf16[4,128,256]{2,1,0:T(8,128)(2,1)S(1)} %all-to-all-done.parts_ref, bf16[128,2048]{1,0:T(8,128)(2,1)S(1)} %copy-done.2, f32[1,2048]{1,0:T(1,128)S(1)} %bitcast.14, s32[128,2]{1,0:T(8,128)S(1)} %copy.17.routes_ref, bf16[1024,2048]{1,0:T(8,128)(2,1)} %weight_ref.1), custom_call_target="tpu_custom_call" | custom-call | tf_op jit(solution)/shard_map/pallas_call | solution.py:34
  29.0 12.7 %all-to-all-start.1 = ((bf16[64,8,2048]{2,1,0:T(8,128)(2,1)}), bf16[64,8,2048]{2,1,0:T(8,128)(2,1)S(1)}, u32[]{:S(2)}, u32[]{:S(2)}) async-start(bf16[64,8,2048]{2,1,0:T(8,128)(2,1)} %bitcast.16), calls=%async_computation.1 | async-start | bytes 4194304 | tf_op jit(solution)/shard_map/all_to_all | solution.py:349
  41.7 0.6 collective-permute-start.1
  42.3 2.7 %collective-permute-start.3 = (bf16[2048,256]{1,0:T(8,128)(2,1)S(1)}, bf16[2048,256]{1,0:T(8,128)(2,1)S(1)}, u32[]{:S(2)}, u32[]{:S(2)}) collective-permute-start(bf16[2048,256]{1,0:T(8,128)(2,1)S(1)} %bitcast.19), channel_id=1, source_target_pairs={{0,3},{1,0},{2,1},{3,2},{4,7},{5,4},{6,5},{7,6},{8,11},{9,8},{10,9... | collective-permute-start | bytes 3145736 | tf_op jit(solution)/shard_map/ppermute | solution.py:24
  45.0 3.2 %collective-permute-start.4 = (bf16[2048,256]{1,0:T(8,128)(2,1)}, bf16[2048,256]{1,0:T(8,128)(2,1)S(1)}, u32[]{:S(2)}, u32[]{:S(2)}) collective-permute-start(bf16[2048,256]{1,0:T(8,128)(2,1)} %bitcast.21), channel_id=1, source_target_pairs={{0,3},{1,0},{2,1},{3,2},{4,7},{5,4},{6,5},{7,6},{8,11},{9,8},{10,9... | collective-permute-start | bytes 3145736 | tf_op jit(solution)/shard_map/ppermute | solution.py:24
  48.2 20.8 %collective-permute-done.1.refs_3_ = bf16[2048,256]{1,0:T(8,128)(2,1)S(1)} collective-permute-done((bf16[2048,256]{1,0:T(8,128)(2,1)S(1)}, bf16[2048,256]{1,0:T(8,128)(2,1)S(1)}, u32[]{:S(2)}, u32[]{:S(2)}) %collective-permute-start.1) | collective-permute-done | bytes 1048608 | tf_op jit(solution)/shard_map/ppermute | solution.py:24
  69.1 2.1 collective-permute-start.5
  71.2 20.3 %collective-permute-done.2.refs_4_ = bf16[2048,256]{1,0:T(8,128)(2,1)S(1)} collective-permute-done((bf16[2048,256]{1,0:T(8,128)(2,1)}, bf16[2048,256]{1,0:T(8,128)(2,1)S(1)}, u32[]{:S(2)}, u32[]{:S(2)}) %collective-permute-start.2) | collective-permute-done | bytes 1048608 | tf_op jit(solution)/shard_map/ppermute | solution.py:24
  91.5 2.1 collective-permute-start.7
  93.7 20.3 %collective-permute-done.9.refs_12_ = bf16[256,2048]{1,0:T(8,128)(2,1)S(1)} collective-permute-done((bf16[256,2048]{1,0:T(8,128)(2,1)}, bf16[256,2048]{1,0:T(8,128)(2,1)S(1)}, u32[]{:S(2)}, u32[]{:S(2)}) %collective-permute-start.9) | collective-permute-done | bytes 1048608 | tf_op jit(solution)/shard_map/ppermute | solution.py:24
  113.9 0.9 slice.148
  114.8 2.2 %collective-permute-start.11 = (bf16[128,2048]{1,0:T(8,128)(2,1)}, bf16[128,2048]{1,0:T(8,128)(2,1)S(1)}, u32[]{:S(2)}, u32[]{:S(2)}) collective-permute-start(bf16[128,2048]{1,0:T(8,128)(2,1)} %slice.148), channel_id=1, source_target_pairs={{0,1},{1,2},{2,3},{3,0},{4,5},{5,6},{6,7},{7,4},{8,9},{9,10},{10,1... | collective-permute-start | bytes 1572872 | tf_op jit(solution)/shard_map/ppermute | solution.py:24
  117.0 0.8 slice.149
  117.9 7.3 %collective-permute-done.5.refs_7_ = bf16[1024,256]{1,0:T(8,128)(2,1)S(1)} collective-permute-done((bf16[1024,256]{1,0:T(8,128)(2,1)S(1)}, bf16[1024,256]{1,0:T(8,128)(2,1)S(1)}, u32[]{:S(2)}, u32[]{:S(2)}) %collective-permute-start.5) | collective-permute-done | bytes 524320 | tf_op jit(solution)/shard_map/ppermute | solution.py:24
  125.2 11.2 %collective-permute-done.7.refs_9_ = bf16[1024,256]{1,0:T(8,128)(2,1)S(1)} collective-permute-done((bf16[1024,256]{1,0:T(8,128)(2,1)S(1)}, bf16[1024,256]{1,0:T(8,128)(2,1)S(1)}, u32[]{:S(2)}, u32[]{:S(2)}) %collective-permute-start.7) | collective-permute-done | bytes 524320 | tf_op jit(solution)/shard_map/ppermute | solution.py:24
  136.4 0.8 copy-done.13
  137.2 8.6 %shard_map.139 = (bf16[512,256]{1,0:T(8,128)(2,1)S(1)}, f32[512,2048]{1,0:T(8,128)S(1)}) custom-call(bf16[512,2048]{1,0:T(8,128)(2,1)S(1)} %bitcast.13, bf16[2048,256]{1,0:T(8,128)(2,1)} %bitcast.17, bf16[2048,256]{1,0:T(8,128)(2,1)} %bitcast.22, bf16[2048,256]{1,0:T(8,128)(2,1)} %copy-done.4, bf16[2048,256]{1,0:T(8,128)(2,1)} %copy-done.6, ...), custom_call_target="tpu_custom_call" | custom-call | tf_op jit(solution)/shard_map/pallas_call | solution.py:34
  145.9 0.9 collective-permute-done.11.refs_0_
  146.8 2.1 %shard_map.140 = bf16[512,2048]{1,0:T(8,128)(2,1)} custom-call(bf16[512,256]{1,0:T(8,128)(2,1)S(1)} %get-tuple-element.15.hidden_ref, f32[512,2048]{1,0:T(8,128)S(1)} %get-tuple-element.16.sum_ref, bf16[128,2048]{1,0:T(8,128)(2,1)S(1)} %collective-permute-done.11.refs_0_, bf16[128,2048]{1,0:T(8,128)(2,1)S(1)} %collective-permute-done.12.refs_1_), custom_call_target="tpu_custom_call" | custom-call | tf_op jit(solution)/shard_map/pallas_call | solution.py:34
  148.9 10.4 %all-to-all-start.2 = ((bf16[64,8,2048]{2,1,0:T(8,128)(2,1)}), bf16[64,8,2048]{2,1,0:T(8,128)(2,1)S(1)}, u32[]{:S(2)}, u32[]{:S(2)}) async-start(bf16[64,8,2048]{2,1,0:T(8,128)(2,1)} %bitcast.15), calls=%async_computation.2 | async-start | bytes 4194304 | tf_op jit(solution)/shard_map/all_to_all | solution.py:358
  159.4 0.7 constant_dynamic-slice_fusion
  160.2 0.5 shard_map.138
  160.7 50.0 %all-to-all-done.2 = bf16[64,8,2048]{2,1,0:T(8,128)(2,1)S(1)} async-done(((bf16[64,8,2048]{2,1,0:T(8,128)(2,1)}), bf16[64,8,2048]{2,1,0:T(8,128)(2,1)S(1)}, u32[]{:S(2)}, u32[]{:S(2)}) %all-to-all-start.2) | async-done | bytes 2097184 | tf_op jit(solution)/shard_map/all_to_all | solution.py:358
  210.6 1.4 shard_map.141
  (47 shorter events, 0.5 us)
Async XLA Ops:
  0.0 17.6 %copy-start = (s32[512,2]{0,1:T(2,128)S(1)}, s32[512,2]{0,1:T(2,128)}, u32[]{:S(2)}) copy-start(s32[512,2]{0,1:T(2,128)} %param.23) | copy-start | bytes 12292
  0.0 24.6 %copy-start.3 = (f32[2048]{0:T(1024)S(1)}, f32[2048]{0:T(1024)}, u32[]{:S(2)}) copy-start(f32[2048]{0:T(1024)} %param.22) | copy-start | bytes 24580
  0.0 24.6 %copy-start.2 = (bf16[128,2048]{1,0:T(8,128)(2,1)S(1)}, bf16[128,2048]{1,0:T(8,128)(2,1)}, u32[]{:S(2)}) copy-start(bf16[128,2048]{1,0:T(8,128)(2,1)} %residual_ref.1) | copy-start | bytes 1572868
  1.4 5.3 %collective-permute-start = (bf16[32,256]{1,0:T(8,128)(2,1)}, bf16[32,256]{1,0:T(8,128)(2,1)S(1)}, u32[]{:S(2)}, u32[]{:S(2)}) collective-permute-start(bf16[32,256]{1,0:T(8,128)(2,1)} %rim_rows.1), channel_id=1, source_target_pairs={{0,4},{4,8},{8,12},{12,16},{16,20},{20,24},{24,28},{28,32},{32,36}... | collective-permute-start | bytes 49160 | tf_op jit(solution)/shard_map/ppermute | solution.py:19
  13.1 11.5 %all-to-all-start = ((bf16[4,128,256]{2,1,0:T(8,128)(2,1)}), bf16[4,128,256]{2,1,0:T(8,128)(2,1)S(1)}, u32[]{:S(2)}, u32[]{:S(2)}) async-start(bf16[4,128,256]{2,1,0:T(8,128)(2,1)} %bitcast.3), calls=%async_computation | async-start | bytes 524288 | tf_op jit(solution)/shard_map/all_to_all | solution.py:326
  29.0 12.7 %copy-start.10 = (bf16[1,2048,256]{2,1,0:T(8,128)(2,1)S(1)}, bf16[1,2048,256]{2,1,0:T(8,128)(2,1)}, u32[]{:S(2)}) copy-start(bf16[1,2048,256]{2,1,0:T(8,128)(2,1)} %param.25) | copy-start | bytes 3145732
  29.0 108.3 %all-to-all-start.1 = ((bf16[64,8,2048]{2,1,0:T(8,128)(2,1)}), bf16[64,8,2048]{2,1,0:T(8,128)(2,1)S(1)}, u32[]{:S(2)}, u32[]{:S(2)}) async-start(bf16[64,8,2048]{2,1,0:T(8,128)(2,1)} %bitcast.16), calls=%async_computation.1 | async-start | bytes 4194304 | tf_op jit(solution)/shard_map/all_to_all | solution.py:349
  41.7 27.3 %collective-permute-start.1 = (bf16[2048,256]{1,0:T(8,128)(2,1)S(1)}, bf16[2048,256]{1,0:T(8,128)(2,1)S(1)}, u32[]{:S(2)}, u32[]{:S(2)}) collective-permute-start(bf16[2048,256]{1,0:T(8,128)(2,1)S(1)} %bitcast.18), channel_id=1, source_target_pairs={{0,1},{1,2},{2,3},{3,0},{4,5},{5,6},{6,7},{7,4},{8,9},{9,10},{10,1... | collective-permute-start | bytes 3145736 | tf_op jit(solution)/shard_map/ppermute | solution.py:24
  42.3 26.7 %collective-permute-start.3 = (bf16[2048,256]{1,0:T(8,128)(2,1)S(1)}, bf16[2048,256]{1,0:T(8,128)(2,1)S(1)}, u32[]{:S(2)}, u32[]{:S(2)}) collective-permute-start(bf16[2048,256]{1,0:T(8,128)(2,1)S(1)} %bitcast.19), channel_id=1, source_target_pairs={{0,3},{1,0},{2,1},{3,2},{4,7},{5,4},{6,5},{7,6},{8,11},{9,8},{10,9... | collective-permute-start | bytes 3145736 | tf_op jit(solution)/shard_map/ppermute | solution.py:24
  45.0 46.5 %collective-permute-start.2 = (bf16[2048,256]{1,0:T(8,128)(2,1)}, bf16[2048,256]{1,0:T(8,128)(2,1)S(1)}, u32[]{:S(2)}, u32[]{:S(2)}) collective-permute-start(bf16[2048,256]{1,0:T(8,128)(2,1)} %bitcast.20), channel_id=1, source_target_pairs={{0,1},{1,2},{2,3},{3,0},{4,5},{5,6},{6,7},{7,4},{8,9},{9,10},{10,1... | collective-permute-start | bytes 3145736 | tf_op jit(solution)/shard_map/ppermute | solution.py:24
  45.0 46.5 %collective-permute-start.4 = (bf16[2048,256]{1,0:T(8,128)(2,1)}, bf16[2048,256]{1,0:T(8,128)(2,1)S(1)}, u32[]{:S(2)}, u32[]{:S(2)}) collective-permute-start(bf16[2048,256]{1,0:T(8,128)(2,1)} %bitcast.21), channel_id=1, source_target_pairs={{0,3},{1,0},{2,1},{3,2},{4,7},{5,4},{6,5},{7,6},{8,11},{9,8},{10,9... | collective-permute-start | bytes 3145736 | tf_op jit(solution)/shard_map/ppermute | solution.py:24
  48.2 65.7 %collective-permute-start.9 = (bf16[256,2048]{1,0:T(8,128)(2,1)}, bf16[256,2048]{1,0:T(8,128)(2,1)S(1)}, u32[]{:S(2)}, u32[]{:S(2)}) collective-permute-start(bf16[256,2048]{1,0:T(8,128)(2,1)} %bitcast.23), channel_id=1, source_target_pairs={{0,1},{1,2},{2,3},{3,0},{4,5},{5,6},{6,7},{7,4},{8,9},{9,10},{10,1... | collective-permute-start | bytes 3145736 | tf_op jit(solution)/shard_map/ppermute | solution.py:24
  69.0 24.7 %copy-start.4 = (bf16[2048,256]{1,0:T(8,128)(2,1)}, bf16[2048,256]{1,0:T(8,128)(2,1)S(1)}, u32[]{:S(2)}) copy-start(bf16[2048,256]{1,0:T(8,128)(2,1)S(1)} %collective-permute-done.1.refs_3_) | copy-start | bytes 3145732
  69.0 45.8 %collective-permute-start.10 = (bf16[256,2048]{1,0:T(8,128)(2,1)}, bf16[256,2048]{1,0:T(8,128)(2,1)S(1)}, u32[]{:S(2)}, u32[]{:S(2)}) collective-permute-start(bf16[256,2048]{1,0:T(8,128)(2,1)} %bitcast.24), channel_id=1, source_target_pairs={{0,3},{1,0},{2,1},{3,2},{4,7},{5,4},{6,5},{7,6},{8,11},{9,8},{10,9... | collective-permute-start | bytes 3145736 | tf_op jit(solution)/shard_map/ppermute | solution.py:24
  69.0 45.8 %copy-start.5 = (bf16[2048,256]{1,0:T(8,128)(2,1)}, bf16[2048,256]{1,0:T(8,128)(2,1)S(1)}, u32[]{:S(2)}) copy-start(bf16[2048,256]{1,0:T(8,128)(2,1)S(1)} %collective-permute-done.3.refs_5_) | copy-start | bytes 3145732
  69.1 56.1 %collective-permute-start.5 = (bf16[1024,256]{1,0:T(8,128)(2,1)S(1)}, bf16[1024,256]{1,0:T(8,128)(2,1)S(1)}, u32[]{:S(2)}, u32[]{:S(2)}) collective-permute-start(bf16[1024,256]{1,0:T(8,128)(2,1)S(1)} %slice.144), channel_id=1, source_target_pairs={{0,1},{1,2},{2,3},{3,0},{4,5},{5,6},{6,7},{7,4},{8,9},{9,10},{10,1... | collective-permute-start | bytes 1572872 | tf_op jit(solution)/shard_map/ppermute | solution.py:24
  91.5 26.4 %copy-start.6 = (bf16[2048,256]{1,0:T(8,128)(2,1)}, bf16[2048,256]{1,0:T(8,128)(2,1)S(1)}, u32[]{:S(2)}) copy-start(bf16[2048,256]{1,0:T(8,128)(2,1)S(1)} %collective-permute-done.2.refs_4_) | copy-start | bytes 3145732
  91.5 33.7 %collective-permute-start.6 = (bf16[1024,256]{1,0:T(8,128)(2,1)S(1)}, bf16[1024,256]{1,0:T(8,128)(2,1)S(1)}, u32[]{:S(2)}, u32[]{:S(2)}) collective-permute-start(bf16[1024,256]{1,0:T(8,128)(2,1)S(1)} %slice.145), channel_id=1, source_target_pairs={{0,3},{1,0},{2,1},{3,2},{4,7},{5,4},{6,5},{7,6},{8,11},{9,8},{10,9... | collective-permute-start | bytes 1572872 | tf_op jit(solution)/shard_map/ppermute | solution.py:24
  91.5 44.9 %copy-start.7 = (bf16[2048,256]{1,0:T(8,128)(2,1)}, bf16[2048,256]{1,0:T(8,128)(2,1)S(1)}, u32[]{:S(2)}) copy-start(bf16[2048,256]{1,0:T(8,128)(2,1)S(1)} %collective-permute-done.4.refs_6_) | copy-start | bytes 3145732
  91.5 44.9 %collective-permute-start.7 = (bf16[1024,256]{1,0:T(8,128)(2,1)S(1)}, bf16[1024,256]{1,0:T(8,128)(2,1)S(1)}, u32[]{:S(2)}, u32[]{:S(2)}) collective-permute-start(bf16[1024,256]{1,0:T(8,128)(2,1)S(1)} %slice.146), channel_id=1, source_target_pairs={{0,1},{1,2},{2,3},{3,0},{4,5},{5,6},{6,7},{7,4},{8,9},{9,10},{10,1... | collective-permute-start | bytes 1572872 | tf_op jit(solution)/shard_map/ppermute | solution.py:24
  113.9 22.5 %copy-start.8 = (bf16[256,2048]{1,0:T(8,128)(2,1)}, bf16[256,2048]{1,0:T(8,128)(2,1)S(1)}, u32[]{:S(2)}) copy-start(bf16[256,2048]{1,0:T(8,128)(2,1)S(1)} %collective-permute-done.9.refs_12_) | copy-start | bytes 3145732
  113.9 23.3 %collective-permute-start.8 = (bf16[1024,256]{1,0:T(8,128)(2,1)S(1)}, bf16[1024,256]{1,0:T(8,128)(2,1)}, u32[]{:S(2)}, u32[]{:S(2)}) collective-permute-start(bf16[1024,256]{1,0:T(8,128)(2,1)S(1)} %slice.147), channel_id=1, source_target_pairs={{0,3},{1,0},{2,1},{3,2},{4,7},{5,4},{6,5},{7,6},{8,11},{9,8},{10,9... | collective-permute-start | bytes 1572872 | tf_op jit(solution)/shard_map/ppermute | solution.py:24
  114.8 21.6 %copy-start.9 = (bf16[256,2048]{1,0:T(8,128)(2,1)}, bf16[256,2048]{1,0:T(8,128)(2,1)S(1)}, u32[]{:S(2)}) copy-start(bf16[256,2048]{1,0:T(8,128)(2,1)S(1)} %collective-permute-done.10.refs_13_) | copy-start | bytes 3145732
  114.8 32.0 %collective-permute-start.11 = (bf16[128,2048]{1,0:T(8,128)(2,1)}, bf16[128,2048]{1,0:T(8,128)(2,1)S(1)}, u32[]{:S(2)}, u32[]{:S(2)}) collective-permute-start(bf16[128,2048]{1,0:T(8,128)(2,1)} %slice.148), channel_id=1, source_target_pairs={{0,1},{1,2},{2,3},{3,0},{4,5},{5,6},{6,7},{7,4},{8,9},{9,10},{10,1... | collective-permute-start | bytes 1572872 | tf_op jit(solution)/shard_map/ppermute | solution.py:24
  125.2 11.2 %copy-start.11 = (bf16[1024,256]{1,0:T(8,128)(2,1)}, bf16[1024,256]{1,0:T(8,128)(2,1)S(1)}, u32[]{:S(2)}) copy-start(bf16[1024,256]{1,0:T(8,128)(2,1)S(1)} %collective-permute-done.5.refs_7_) | copy-start | bytes 1572868
  125.2 21.6 %collective-permute-start.12 = (bf16[128,2048]{1,0:T(8,128)(2,1)}, bf16[128,2048]{1,0:T(8,128)(2,1)S(1)}, u32[]{:S(2)}, u32[]{:S(2)}) collective-permute-start(bf16[128,2048]{1,0:T(8,128)(2,1)} %slice.149), channel_id=1, source_target_pairs={{0,3},{1,0},{2,1},{3,2},{4,7},{5,4},{6,5},{7,6},{8,11},{9,8},{10,9... | collective-permute-start | bytes 1572872 | tf_op jit(solution)/shard_map/ppermute | solution.py:24
  125.2 11.2 %copy-start.12 = (bf16[1024,256]{1,0:T(8,128)(2,1)}, bf16[1024,256]{1,0:T(8,128)(2,1)S(1)}, u32[]{:S(2)}) copy-start(bf16[1024,256]{1,0:T(8,128)(2,1)S(1)} %collective-permute-done.6.refs_8_) | copy-start | bytes 1572868
  136.4 0.8 copy-start.13
  148.9 61.7 %copy-start.1 = (f32[128,2048]{1,0:T(8,128)S(1)}, f32[128,2048]{1,0:T(8,128)}, u32[]{:S(2)}) copy-start(f32[128,2048]{1,0:T(8,128)} %get-tuple-element.11.stream_ref) | copy-start | bytes 3145732
  148.9 61.7 %all-to-all-start.2 = ((bf16[64,8,2048]{2,1,0:T(8,128)(2,1)}), bf16[64,8,2048]{2,1,0:T(8,128)(2,1)S(1)}, u32[]{:S(2)}, u32[]{:S(2)}) async-start(bf16[64,8,2048]{2,1,0:T(8,128)(2,1)} %bitcast.15), calls=%async_computation.2 | async-start | bytes 4194304 | tf_op jit(solution)/shard_map/all_to_all | solution.py:358

commit v12 on v11

--- a/solution.py
+++ b/solution.py
@@ -202,7 +202,7 @@
 
 def hidden_body(counts, *refs):
     rows_ref, *pieces, far_ref, sum_ref, w_ref, hidden_ref, down_ref, sems = refs
-    width = pieces[0].shape[1]
+    deep, width = pieces[0].shape
     loads, at = [], 0
     for q, kinds in enumerate(counts):
         copies = []
@@ -213,14 +213,24 @@
                 copies.append((piece, w_ref.at[q, top:end, kind * width : (kind + 1) * width]))
                 top = end
             pieces = pieces[n:]
+        if q == 0:
+            copies = [
+                (src.at[rows], dst.at[rows])
+                for rows in (slice(0, deep // 2), slice(deep // 2, deep))
+                for src, dst in copies
+            ]
         loads.append(fetch(copies, sems, at))
         at += len(copies)
     spans = [slice(q * width, (q + 1) * width) for q in range(len(pieces))]
     downs = fetch([(piece, down_ref.at[rows]) for piece, rows in zip(pieces, spans)], sems, at)
     for q, copies in enumerate(loads):
-        for c in copies:
-            c.wait()
-        act = dot(rows_ref[...], w_ref[q])
+        act, parts = None, 2 if q == 0 else 1
+        for part in range(parts):
+            for c in copies[part * len(copies) // parts : (part + 1) * len(copies) // parts]:
+                c.wait()
+            rows = slice(part * deep // parts, (part + 1) * deep // parts)
+            found = dot(rows_ref[:, rows], w_ref[q, rows])
+            act = found if act is None else act + found
         gate = act[:, :width]
         hidden = (gate / (1.0 + jnp.exp(-gate)) * act[:, width:]).astype(jnp.bfloat16)
         if q < len(spans):
@@ -247,7 +257,7 @@
             pltpu.VMEM((len(counts), d, 2 * width), jnp.bfloat16),
             pltpu.VMEM((n, len(downs) * width), jnp.bfloat16),
             pltpu.VMEM((len(downs) * width, out_width), jnp.bfloat16),
-            pltpu.SemaphoreType.DMA((len(pieces),)),
+            pltpu.SemaphoreType.DMA((len(pieces) + 2,)),
         ],
         limit=24,
         far_in=range(1, 1 + len(pieces)),

time: 213 us -> 213 us (level)
  no operation moved by 1% of the time
where the time goes in v12:
time: 213 us; the launch traced here: 212 us
  waiting for transfers between devices  139 us (65%)
  starting transfers between devices  42.5 us (20%)
  Pallas kernels  24.7 us (12%)
  local copies, waits for them, and re-layouts  3.73 us (2%)
    ppermute x12, waiting for transfers between devices, ring(): lax.ppermute(value, axis, [(i, (i + steps) % count) for i in range(count)])  80.7 us
    all_to_all x1, waiting for transfers between devices, shards(): lax.all_to_all(out.reshape(experts_n, capacity, model_width), 'sp', 0, 0,...  50 us
    pallas_call x6, Pallas kernels, kernel(): pl.pallas_call(body, out_shape=[pltpu.HBM(*o) if i in far_out else jax.Sh...  23.3 us
    ppermute x12, starting transfers between devices, ring(): lax.ppermute(value, axis, [(i, (i + steps) % count) for i in range(count)])  13 us
    all_to_all x1, starting transfers between devices, shards(): lax.all_to_all(outgoing.reshape(experts_n, capacity, model_width), 'sp',...  12.7 us
    all_to_all x1, starting transfers between devices, shards(): lax.all_to_all(out.reshape(experts_n, capacity, model_width), 'sp', 0, 0,...  10.4 us
    all_to_all x1, waiting for transfers between devices, shards(): lax.all_to_all(conv_out.reshape(columns, rows_own, local_channels), 'tp',...  6.89 us
    all_to_all x1, starting transfers between devices, shards(): lax.all_to_all(conv_out.reshape(columns, rows_own, local_channels), 'tp',...  4.48 us
  transfers between devices with their start and end apart: 16, of which 9 were waited for; matrix products, arithmetic and copies ran while one was open for 2% of the time, Pallas kernels for 4%

profile of v12, /device:TPU:2, one launch (start us, length us, event | category | flops | bytes accessed | tf_op | source)
XLA Modules:
  0.0 212.2 jit_solution(8515483512661344125)
XLA Ops:
  0.0 1.4 rim_rows.1
  1.4 1.9 collective-permute-start
  3.3 1.9 convert_add_fusion
  5.3 1.4 collective-permute-done.rim_ref
  6.7 0.1 broadcast_in_dim.15.seen_ref
  6.8 6.3 %shard_map.136 = bf16[512,256]{1,0:T(8,128)(2,1)} custom-call(bf16[32,256]{1,0:T(8,128)(2,1)S(1)} %collective-permute-done.rim_ref, s32[512,128]{1,0:T(8,128)S(1)} %broadcast_in_dim.15.seen_ref, bf16[512,256]{1,0:T(8,128)(2,1)} %refs_0_.1, bf16[512,256]{1,0:T(8,128)(2,1)} %refs_1_.1, s32[4,128]{1,0:T(4,128)} %bitcast.27, f32[31,256]{1,0:T(8,128)} %refs_3_.1, ...), custom_call_target="tpu_custom_call" | custom-call | tf_op jit(solution)/shard_map/pallas_call | solution.py:34
  13.1 4.5 %all-to-all-start = ((bf16[4,128,256]{2,1,0:T(8,128)(2,1)}), bf16[4,128,256]{2,1,0:T(8,128)(2,1)S(1)}, u32[]{:S(2)}, u32[]{:S(2)}) async-start(bf16[4,128,256]{2,1,0:T(8,128)(2,1)} %bitcast.3), calls=%async_computation | async-start | bytes 524288 | tf_op jit(solution)/shard_map/all_to_all | solution.py:336
  17.7 6.9 %all-to-all-done.parts_ref = bf16[4,128,256]{2,1,0:T(8,128)(2,1)S(1)} async-done(((bf16[4,128,256]{2,1,0:T(8,128)(2,1)}), bf16[4,128,256]{2,1,0:T(8,128)(2,1)S(1)}, u32[]{:S(2)}, u32[]{:S(2)}) %all-to-all-start) | async-done | bytes 262176 | tf_op jit(solution)/shard_map/all_to_all | solution.py:336
  24.6 4.4 %shard_map.137 = (f32[128,2048]{1,0:T(8,128)}, bf16[512,2048]{1,0:T(8,128)(2,1)}) custom-call(bf16[4,128,256]{2,1,0:T(8,128)(2,1)S(1)} %all-to-all-done.parts_ref, bf16[128,2048]{1,0:T(8,128)(2,1)S(1)} %copy-done.2, f32[1,2048]{1,0:T(1,128)S(1)} %bitcast.14, s32[128,2]{1,0:T(8,128)S(1)} %copy.17.routes_ref, bf16[1024,2048]{1,0:T(8,128)(2,1)} %weight_ref.1), custom_call_target="tpu_custom_call" | custom-call | tf_op jit(solution)/shard_map/pallas_call | solution.py:34
  29.0 12.7 %all-to-all-start.1 = ((bf16[64,8,2048]{2,1,0:T(8,128)(2,1)}), bf16[64,8,2048]{2,1,0:T(8,128)(2,1)S(1)}, u32[]{:S(2)}, u32[]{:S(2)}) async-start(bf16[64,8,2048]{2,1,0:T(8,128)(2,1)} %bitcast.16), calls=%async_computation.1 | async-start | bytes 4194304 | tf_op jit(solution)/shard_map/all_to_all | solution.py:359
  41.7 0.6 collective-permute-start.1
  42.3 2.7 %collective-permute-start.3 = (bf16[2048,256]{1,0:T(8,128)(2,1)S(1)}, bf16[2048,256]{1,0:T(8,128)(2,1)S(1)}, u32[]{:S(2)}, u32[]{:S(2)}) collective-permute-start(bf16[2048,256]{1,0:T(8,128)(2,1)S(1)} %bitcast.19), channel_id=1, source_target_pairs={{0,3},{1,0},{2,1},{3,2},{4,7},{5,4},{6,5},{7,6},{8,11},{9,8},{10,9... | collective-permute-start | bytes 3145736 | tf_op jit(solution)/shard_map/ppermute | solution.py:24
  45.0 3.2 %collective-permute-start.4 = (bf16[2048,256]{1,0:T(8,128)(2,1)}, bf16[2048,256]{1,0:T(8,128)(2,1)S(1)}, u32[]{:S(2)}, u32[]{:S(2)}) collective-permute-start(bf16[2048,256]{1,0:T(8,128)(2,1)} %bitcast.21), channel_id=1, source_target_pairs={{0,3},{1,0},{2,1},{3,2},{4,7},{5,4},{6,5},{7,6},{8,11},{9,8},{10,9... | collective-permute-start | bytes 3145736 | tf_op jit(solution)/shard_map/ppermute | solution.py:24
  48.2 20.8 %collective-permute-done.1.refs_3_ = bf16[2048,256]{1,0:T(8,128)(2,1)S(1)} collective-permute-done((bf16[2048,256]{1,0:T(8,128)(2,1)S(1)}, bf16[2048,256]{1,0:T(8,128)(2,1)S(1)}, u32[]{:S(2)}, u32[]{:S(2)}) %collective-permute-start.1) | collective-permute-done | bytes 1048608 | tf_op jit(solution)/shard_map/ppermute | solution.py:24
  69.1 2.1 collective-permute-start.5
  71.2 20.3 %collective-permute-done.2.refs_4_ = bf16[2048,256]{1,0:T(8,128)(2,1)S(1)} collective-permute-done((bf16[2048,256]{1,0:T(8,128)(2,1)}, bf16[2048,256]{1,0:T(8,128)(2,1)S(1)}, u32[]{:S(2)}, u32[]{:S(2)}) %collective-permute-start.2) | collective-permute-done | bytes 1048608 | tf_op jit(solution)/shard_map/ppermute | solution.py:24
  91.5 2.1 collective-permute-start.7
  93.7 20.3 %collective-permute-done.9.refs_12_ = bf16[256,2048]{1,0:T(8,128)(2,1)S(1)} collective-permute-done((bf16[256,2048]{1,0:T(8,128)(2,1)}, bf16[256,2048]{1,0:T(8,128)(2,1)S(1)}, u32[]{:S(2)}, u32[]{:S(2)}) %collective-permute-start.9) | collective-permute-done | bytes 1048608 | tf_op jit(solution)/shard_map/ppermute | solution.py:24
  113.9 0.9 slice.148
  114.8 2.2 %collective-permute-start.11 = (bf16[128,2048]{1,0:T(8,128)(2,1)}, bf16[128,2048]{1,0:T(8,128)(2,1)S(1)}, u32[]{:S(2)}, u32[]{:S(2)}) collective-permute-start(bf16[128,2048]{1,0:T(8,128)(2,1)} %slice.148), channel_id=1, source_target_pairs={{0,1},{1,2},{2,3},{3,0},{4,5},{5,6},{6,7},{7,4},{8,9},{9,10},{10,1... | collective-permute-start | bytes 1572872 | tf_op jit(solution)/shard_map/ppermute | solution.py:24
  117.0 0.8 slice.149
  117.9 7.3 %collective-permute-done.5.refs_7_ = bf16[1024,256]{1,0:T(8,128)(2,1)S(1)} collective-permute-done((bf16[1024,256]{1,0:T(8,128)(2,1)S(1)}, bf16[1024,256]{1,0:T(8,128)(2,1)S(1)}, u32[]{:S(2)}, u32[]{:S(2)}) %collective-permute-start.5) | collective-permute-done | bytes 524320 | tf_op jit(solution)/shard_map/ppermute | solution.py:24
  125.2 11.2 %collective-permute-done.7.refs_9_ = bf16[1024,256]{1,0:T(8,128)(2,1)S(1)} collective-permute-done((bf16[1024,256]{1,0:T(8,128)(2,1)S(1)}, bf16[1024,256]{1,0:T(8,128)(2,1)S(1)}, u32[]{:S(2)}, u32[]{:S(2)}) %collective-permute-start.7) | collective-permute-done | bytes 524320 | tf_op jit(solution)/shard_map/ppermute | solution.py:24
  136.4 0.8 copy-done.13
  137.2 8.6 %shard_map.139 = (bf16[512,256]{1,0:T(8,128)(2,1)S(1)}, f32[512,2048]{1,0:T(8,128)S(1)}) custom-call(bf16[512,2048]{1,0:T(8,128)(2,1)S(1)} %bitcast.13, bf16[2048,256]{1,0:T(8,128)(2,1)} %bitcast.17, bf16[2048,256]{1,0:T(8,128)(2,1)} %bitcast.22, bf16[2048,256]{1,0:T(8,128)(2,1)} %copy-done.4, bf16[2048,256]{1,0:T(8,128)(2,1)} %copy-done.6, ...), custom_call_target="tpu_custom_call" | custom-call | tf_op jit(solution)/shard_map/pallas_call | solution.py:34
  145.8 0.9 collective-permute-done.11.refs_0_
  146.8 2.1 %shard_map.140 = bf16[512,2048]{1,0:T(8,128)(2,1)} custom-call(bf16[512,256]{1,0:T(8,128)(2,1)S(1)} %get-tuple-element.15.hidden_ref, f32[512,2048]{1,0:T(8,128)S(1)} %get-tuple-element.16.sum_ref, bf16[128,2048]{1,0:T(8,128)(2,1)S(1)} %collective-permute-done.11.refs_0_, bf16[128,2048]{1,0:T(8,128)(2,1)S(1)} %collective-permute-done.12.refs_1_), custom_call_target="tpu_custom_call" | custom-call | tf_op jit(solution)/shard_map/pallas_call | solution.py:34
  148.9 10.4 %all-to-all-start.2 = ((bf16[64,8,2048]{2,1,0:T(8,128)(2,1)}), bf16[64,8,2048]{2,1,0:T(8,128)(2,1)S(1)}, u32[]{:S(2)}, u32[]{:S(2)}) async-start(bf16[64,8,2048]{2,1,0:T(8,128)(2,1)} %bitcast.15), calls=%async_computation.2 | async-start | bytes 4194304 | tf_op jit(solution)/shard_map/all_to_all | solution.py:368
  159.4 0.7 constant_dynamic-slice_fusion
  160.2 0.5 shard_map.138
  160.7 50.0 %all-to-all-done.2 = bf16[64,8,2048]{2,1,0:T(8,128)(2,1)S(1)} async-done(((bf16[64,8,2048]{2,1,0:T(8,128)(2,1)}), bf16[64,8,2048]{2,1,0:T(8,128)(2,1)S(1)}, u32[]{:S(2)}, u32[]{:S(2)}) %all-to-all-start.2) | async-done | bytes 2097184 | tf_op jit(solution)/shard_map/all_to_all | solution.py:368
  210.6 1.4 shard_map.141
  (47 shorter events, 0.5 us)
Async XLA Ops:
  0.0 17.6 %copy-start = (s32[512,2]{0,1:T(2,128)S(1)}, s32[512,2]{0,1:T(2,128)}, u32[]{:S(2)}) copy-start(s32[512,2]{0,1:T(2,128)} %param.23) | copy-start | bytes 12292
  0.0 24.6 %copy-start.3 = (f32[2048]{0:T(1024)S(1)}, f32[2048]{0:T(1024)}, u32[]{:S(2)}) copy-start(f32[2048]{0:T(1024)} %param.22) | copy-start | bytes 24580
  0.0 24.6 %copy-start.2 = (bf16[128,2048]{1,0:T(8,128)(2,1)S(1)}, bf16[128,2048]{1,0:T(8,128)(2,1)}, u32[]{:S(2)}) copy-start(bf16[128,2048]{1,0:T(8,128)(2,1)} %residual_ref.1) | copy-start | bytes 1572868
  1.4 5.3 %collective-permute-start = (bf16[32,256]{1,0:T(8,128)(2,1)}, bf16[32,256]{1,0:T(8,128)(2,1)S(1)}, u32[]{:S(2)}, u32[]{:S(2)}) collective-permute-start(bf16[32,256]{1,0:T(8,128)(2,1)} %rim_rows.1), channel_id=1, source_target_pairs={{0,4},{4,8},{8,12},{12,16},{16,20},{20,24},{24,28},{28,32},{32,36}... | collective-permute-start | bytes 49160 | tf_op jit(solution)/shard_map/ppermute | solution.py:19
  13.1 11.5 %all-to-all-start = ((bf16[4,128,256]{2,1,0:T(8,128)(2,1)}), bf16[4,128,256]{2,1,0:T(8,128)(2,1)S(1)}, u32[]{:S(2)}, u32[]{:S(2)}) async-start(bf16[4,128,256]{2,1,0:T(8,128)(2,1)} %bitcast.3), calls=%async_computation | async-start | bytes 524288 | tf_op jit(solution)/shard_map/all_to_all | solution.py:336
  29.0 12.7 %copy-start.10 = (bf16[1,2048,256]{2,1,0:T(8,128)(2,1)S(1)}, bf16[1,2048,256]{2,1,0:T(8,128)(2,1)}, u32[]{:S(2)}) copy-start(bf16[1,2048,256]{2,1,0:T(8,128)(2,1)} %param.25) | copy-start | bytes 3145732
  29.0 108.3 %all-to-all-start.1 = ((bf16[64,8,2048]{2,1,0:T(8,128)(2,1)}), bf16[64,8,2048]{2,1,0:T(8,128)(2,1)S(1)}, u32[]{:S(2)}, u32[]{:S(2)}) async-start(bf16[64,8,2048]{2,1,0:T(8,128)(2,1)} %bitcast.16), calls=%async_computation.1 | async-start | bytes 4194304 | tf_op jit(solution)/shard_map/all_to_all | solution.py:359
  41.7 27.3 %collective-permute-start.1 = (bf16[2048,256]{1,0:T(8,128)(2,1)S(1)}, bf16[2048,256]{1,0:T(8,128)(2,1)S(1)}, u32[]{:S(2)}, u32[]{:S(2)}) collective-permute-start(bf16[2048,256]{1,0:T(8,128)(2,1)S(1)} %bitcast.18), channel_id=1, source_target_pairs={{0,1},{1,2},{2,3},{3,0},{4,5},{5,6},{6,7},{7,4},{8,9},{9,10},{10,1... | collective-permute-start | bytes 3145736 | tf_op jit(solution)/shard_map/ppermute | solution.py:24
  42.3 26.7 %collective-permute-start.3 = (bf16[2048,256]{1,0:T(8,128)(2,1)S(1)}, bf16[2048,256]{1,0:T(8,128)(2,1)S(1)}, u32[]{:S(2)}, u32[]{:S(2)}) collective-permute-start(bf16[2048,256]{1,0:T(8,128)(2,1)S(1)} %bitcast.19), channel_id=1, source_target_pairs={{0,3},{1,0},{2,1},{3,2},{4,7},{5,4},{6,5},{7,6},{8,11},{9,8},{10,9... | collective-permute-start | bytes 3145736 | tf_op jit(solution)/shard_map/ppermute | solution.py:24
  45.0 46.5 %collective-permute-start.2 = (bf16[2048,256]{1,0:T(8,128)(2,1)}, bf16[2048,256]{1,0:T(8,128)(2,1)S(1)}, u32[]{:S(2)}, u32[]{:S(2)}) collective-permute-start(bf16[2048,256]{1,0:T(8,128)(2,1)} %bitcast.20), channel_id=1, source_target_pairs={{0,1},{1,2},{2,3},{3,0},{4,5},{5,6},{6,7},{7,4},{8,9},{9,10},{10,1... | collective-permute-start | bytes 3145736 | tf_op jit(solution)/shard_map/ppermute | solution.py:24
  45.0 46.5 %collective-permute-start.4 = (bf16[2048,256]{1,0:T(8,128)(2,1)}, bf16[2048,256]{1,0:T(8,128)(2,1)S(1)}, u32[]{:S(2)}, u32[]{:S(2)}) collective-permute-start(bf16[2048,256]{1,0:T(8,128)(2,1)} %bitcast.21), channel_id=1, source_target_pairs={{0,3},{1,0},{2,1},{3,2},{4,7},{5,4},{6,5},{7,6},{8,11},{9,8},{10,9... | collective-permute-start | bytes 3145736 | tf_op jit(solution)/shard_map/ppermute | solution.py:24
  48.2 65.7 %collective-permute-start.9 = (bf16[256,2048]{1,0:T(8,128)(2,1)}, bf16[256,2048]{1,0:T(8,128)(2,1)S(1)}, u32[]{:S(2)}, u32[]{:S(2)}) collective-permute-start(bf16[256,2048]{1,0:T(8,128)(2,1)} %bitcast.23), channel_id=1, source_target_pairs={{0,1},{1,2},{2,3},{3,0},{4,5},{5,6},{6,7},{7,4},{8,9},{9,10},{10,1... | collective-permute-start | bytes 3145736 | tf_op jit(solution)/shard_map/ppermute | solution.py:24
  69.0 24.7 %copy-start.4 = (bf16[2048,256]{1,0:T(8,128)(2,1)}, bf16[2048,256]{1,0:T(8,128)(2,1)S(1)}, u32[]{:S(2)}) copy-start(bf16[2048,256]{1,0:T(8,128)(2,1)S(1)} %collective-permute-done.1.refs_3_) | copy-start | bytes 3145732
  69.0 45.8 %collective-permute-start.10 = (bf16[256,2048]{1,0:T(8,128)(2,1)}, bf16[256,2048]{1,0:T(8,128)(2,1)S(1)}, u32[]{:S(2)}, u32[]{:S(2)}) collective-permute-start(bf16[256,2048]{1,0:T(8,128)(2,1)} %bitcast.24), channel_id=1, source_target_pairs={{0,3},{1,0},{2,1},{3,2},{4,7},{5,4},{6,5},{7,6},{8,11},{9,8},{10,9... | collective-permute-start | bytes 3145736 | tf_op jit(solution)/shard_map/ppermute | solution.py:24
  69.0 45.8 %copy-start.5 = (bf16[2048,256]{1,0:T(8,128)(2,1)}, bf16[2048,256]{1,0:T(8,128)(2,1)S(1)}, u32[]{:S(2)}) copy-start(bf16[2048,256]{1,0:T(8,128)(2,1)S(1)} %collective-permute-done.3.refs_5_) | copy-start | bytes 3145732
  69.1 56.1 %collective-permute-start.5 = (bf16[1024,256]{1,0:T(8,128)(2,1)S(1)}, bf16[1024,256]{1,0:T(8,128)(2,1)S(1)}, u32[]{:S(2)}, u32[]{:S(2)}) collective-permute-start(bf16[1024,256]{1,0:T(8,128)(2,1)S(1)} %slice.144), channel_id=1, source_target_pairs={{0,1},{1,2},{2,3},{3,0},{4,5},{5,6},{6,7},{7,4},{8,9},{9,10},{10,1... | collective-permute-start | bytes 1572872 | tf_op jit(solution)/shard_map/ppermute | solution.py:24
  91.5 26.4 %copy-start.6 = (bf16[2048,256]{1,0:T(8,128)(2,1)}, bf16[2048,256]{1,0:T(8,128)(2,1)S(1)}, u32[]{:S(2)}) copy-start(bf16[2048,256]{1,0:T(8,128)(2,1)S(1)} %collective-permute-done.2.refs_4_) | copy-start | bytes 3145732
  91.5 33.7 %collective-permute-start.6 = (bf16[1024,256]{1,0:T(8,128)(2,1)S(1)}, bf16[1024,256]{1,0:T(8,128)(2,1)S(1)}, u32[]{:S(2)}, u32[]{:S(2)}) collective-permute-start(bf16[1024,256]{1,0:T(8,128)(2,1)S(1)} %slice.145), channel_id=1, source_target_pairs={{0,3},{1,0},{2,1},{3,2},{4,7},{5,4},{6,5},{7,6},{8,11},{9,8},{10,9... | collective-permute-start | bytes 1572872 | tf_op jit(solution)/shard_map/ppermute | solution.py:24
  91.5 44.9 %copy-start.7 = (bf16[2048,256]{1,0:T(8,128)(2,1)}, bf16[2048,256]{1,0:T(8,128)(2,1)S(1)}, u32[]{:S(2)}) copy-start(bf16[2048,256]{1,0:T(8,128)(2,1)S(1)} %collective-permute-done.4.refs_6_) | copy-start | bytes 3145732
  91.5 44.9 %collective-permute-start.7 = (bf16[1024,256]{1,0:T(8,128)(2,1)S(1)}, bf16[1024,256]{1,0:T(8,128)(2,1)S(1)}, u32[]{:S(2)}, u32[]{:S(2)}) collective-permute-start(bf16[1024,256]{1,0:T(8,128)(2,1)S(1)} %slice.146), channel_id=1, source_target_pairs={{0,1},{1,2},{2,3},{3,0},{4,5},{5,6},{6,7},{7,4},{8,9},{9,10},{10,1... | collective-permute-start | bytes 1572872 | tf_op jit(solution)/shard_map/ppermute | solution.py:24
  113.9 22.5 %copy-start.8 = (bf16[256,2048]{1,0:T(8,128)(2,1)}, bf16[256,2048]{1,0:T(8,128)(2,1)S(1)}, u32[]{:S(2)}) copy-start(bf16[256,2048]{1,0:T(8,128)(2,1)S(1)} %collective-permute-done.9.refs_12_) | copy-start | bytes 3145732
  113.9 23.3 %collective-permute-start.8 = (bf16[1024,256]{1,0:T(8,128)(2,1)S(1)}, bf16[1024,256]{1,0:T(8,128)(2,1)}, u32[]{:S(2)}, u32[]{:S(2)}) collective-permute-start(bf16[1024,256]{1,0:T(8,128)(2,1)S(1)} %slice.147), channel_id=1, source_target_pairs={{0,3},{1,0},{2,1},{3,2},{4,7},{5,4},{6,5},{7,6},{8,11},{9,8},{10,9... | collective-permute-start | bytes 1572872 | tf_op jit(solution)/shard_map/ppermute | solution.py:24
  114.8 21.6 %copy-start.9 = (bf16[256,2048]{1,0:T(8,128)(2,1)}, bf16[256,2048]{1,0:T(8,128)(2,1)S(1)}, u32[]{:S(2)}) copy-start(bf16[256,2048]{1,0:T(8,128)(2,1)S(1)} %collective-permute-done.10.refs_13_) | copy-start | bytes 3145732
  114.8 32.0 %collective-permute-start.11 = (bf16[128,2048]{1,0:T(8,128)(2,1)}, bf16[128,2048]{1,0:T(8,128)(2,1)S(1)}, u32[]{:S(2)}, u32[]{:S(2)}) collective-permute-start(bf16[128,2048]{1,0:T(8,128)(2,1)} %slice.148), channel_id=1, source_target_pairs={{0,1},{1,2},{2,3},{3,0},{4,5},{5,6},{6,7},{7,4},{8,9},{9,10},{10,1... | collective-permute-start | bytes 1572872 | tf_op jit(solution)/shard_map/ppermute | solution.py:24
  125.2 11.2 %copy-start.11 = (bf16[1024,256]{1,0:T(8,128)(2,1)}, bf16[1024,256]{1,0:T(8,128)(2,1)S(1)}, u32[]{:S(2)}) copy-start(bf16[1024,256]{1,0:T(8,128)(2,1)S(1)} %collective-permute-done.5.refs_7_) | copy-start | bytes 1572868
  125.2 21.6 %collective-permute-start.12 = (bf16[128,2048]{1,0:T(8,128)(2,1)}, bf16[128,2048]{1,0:T(8,128)(2,1)S(1)}, u32[]{:S(2)}, u32[]{:S(2)}) collective-permute-start(bf16[128,2048]{1,0:T(8,128)(2,1)} %slice.149), channel_id=1, source_target_pairs={{0,3},{1,0},{2,1},{3,2},{4,7},{5,4},{6,5},{7,6},{8,11},{9,8},{10,9... | collective-permute-start | bytes 1572872 | tf_op jit(solution)/shard_map/ppermute | solution.py:24
  125.2 11.2 %copy-start.12 = (bf16[1024,256]{1,0:T(8,128)(2,1)}, bf16[1024,256]{1,0:T(8,128)(2,1)S(1)}, u32[]{:S(2)}) copy-start(bf16[1024,256]{1,0:T(8,128)(2,1)S(1)} %collective-permute-done.6.refs_8_) | copy-start | bytes 1572868
  136.4 0.8 copy-start.13
  148.9 61.7 %copy-start.1 = (f32[128,2048]{1,0:T(8,128)S(1)}, f32[128,2048]{1,0:T(8,128)}, u32[]{:S(2)}) copy-start(f32[128,2048]{1,0:T(8,128)} %get-tuple-element.11.stream_ref) | copy-start | bytes 3145732
  148.9 61.7 %all-to-all-start.2 = ((bf16[64,8,2048]{2,1,0:T(8,128)(2,1)}), bf16[64,8,2048]{2,1,0:T(8,128)(2,1)S(1)}, u32[]{:S(2)}, u32[]{:S(2)}) async-start(bf16[64,8,2048]{2,1,0:T(8,128)(2,1)} %bitcast.15), calls=%async_computation.2 | async-start | bytes 4194304 | tf_op jit(solution)/shard_map/all_to_all | solution.py:368
